TPU v7x, 32 devices: a whole 2x2x4 slice. The times are simulated.
32 devices in a mesh: sp: 16 (over z, y, x), tp: 2 (over core).
Axes of the slice: x: 2, y: 2, z: 4, core: 2. Of those that a mesh axis runs over, the one named last changes fastest.
Arguments:
- query: bfloat16 [2048, 2048], P('sp', 'tp'), may hold values from -6 to 6
- forget_logit: bfloat16 [2048, 2048], P('sp', 'tp'), may hold values from -7.5 to 7.5
- value: bfloat16 [2048, 2048], P('sp', 'tp'), may hold values from -6 to 6
- out_gate: bfloat16 [2048, 2048], P('sp', 'tp'), may hold values from -6 to 6
- lower_bound: float32 [2048], P('tp'), may hold values from 0.9 to 1, as said below
- head_gain: float32 [2048], P('tp'), may hold values from 0.1 to 1.9
- residual_in: bfloat16 [2048, 2048], P(('sp', 'tp')), may hold values from -6 to 6
- w_out: bfloat16 [2048, 2048], replicated, may hold values from -0.125 to 0.125
- ffn_gain: float32 [2048], replicated, may hold values from 0.1 to 1.9
- routing: int32 [2048, 2], P(('sp', 'tp')), may hold values from 0 to 15, all different within a row; in each aligned block of 64 rows (0 to 63, 64 to 127, ...) at most 16 rows name the same one
- route_weight: float32 [2048, 2], P(('sp', 'tp')), may hold values from 0.25 to 1
- expert_gate: bfloat16 [16, 2048, 1024], P('sp', None, 'tp'), may hold values from -0.125 to 0.125
- expert_up: bfloat16 [16, 2048, 1024], P('sp', None, 'tp'), may hold values from -0.125 to 0.125
- expert_down: bfloat16 [16, 1024, 2048], P('sp', 'tp'), may hold values from -0.1875 to 0.1875
Outputs:
- layer_out: bfloat16 [2048, 2048], P(('sp', 'tp'))
Inputs may be any that keep to these rules, and one draw needn't show every extreme that they name: `routing`: each row names 2 different experts. In each aligned block of 64 rows (the rows of one device) no expert is named by more than 16 rows, a bound that some blocks reach. 1 - lower_bound is at least 1 / 4096.
All inputs are finite; a program needn't handle non-finite values.
Results may differ from a plain program's by a relative error of at most 0.012.
Values may be sent and summed in bfloat16 or wider, within the bound.
No kernel may reach another device: no remote copies, remote signals or barrier semaphores. Data moves between devices by JAX's collectives and lax.ppermute only.
A program may use at most 128 MiB of HBM per device.

v0:
```python
import jax
import jax.numpy as jnp
from jax import lax
from jax.sharding import PartitionSpec as P

HEAD_DIM = 128
BLOCK = 16


epsilon = 1e-06
highest = lax.Precision.HIGHEST


def carried_in(part, axis, combine, identity):
    place = lax.axis_index(axis)
    gathered = lax.all_gather(part, axis)
    state = jnp.zeros_like(part) + jnp.asarray(identity, part.dtype)

    def one(hop, state):
        return combine(state, lax.dynamic_index_in_dim(gathered, hop, 0, False))

    return lax.fori_loop(0, place, one, state)


def combine_pair(former, latter):
    return (former[0] * latter[0], latter[0][..., None] * former[1] + latter[1])


def combine_packed(former, latter):
    former_decay = former[..., -1]
    latter_decay = latter[..., -1]
    state_part = latter_decay[..., None] * former[..., :-1] + latter[..., :-1]
    return jnp.concatenate([state_part, (former_decay * latter_decay)[..., None]], axis=-1)


def body(
    query,
    forget_logit,
    value,
    out_gate,
    lower_bound,
    head_gain,
    residual_in,
    w_out,
    ffn_gain,
    routing,
    route_weight,
    expert_gate,
    expert_up,
    expert_down,
):
    length = query.shape[0]
    local_heads = query.shape[1] // HEAD_DIM
    blocks = length // BLOCK
    grid = (blocks, BLOCK, local_heads, HEAD_DIM)
    floor_gate = lower_bound.reshape(local_heads, HEAD_DIM)
    logits = forget_logit.astype(jnp.float32).reshape(grid)
    log_forget = jnp.logaddexp(
        jnp.log(floor_gate), jnp.log1p(-floor_gate) + jax.nn.log_sigmoid(logits)
    )
    key_gate = (1.0 - floor_gate) * jax.nn.sigmoid(-logits)
    queries = query.astype(jnp.float32).reshape(grid)
    values = value.astype(jnp.float32).reshape(grid)
    cumulative = jnp.cumsum(log_forget, axis=1)
    causal = jnp.arange(BLOCK)[:, None] >= jnp.arange(BLOCK)[None, :]
    log_gaps = cumulative[:, :, None] - cumulative[:, None, :]
    decays = jnp.exp(jnp.where(causal[None, :, :, None, None], log_gaps, -jnp.inf))
    scores = jnp.einsum("ntjd,nsjd,ntsjd->njts", queries, key_gate, decays, precision=highest)
    within = jnp.einsum("njts,nsjv->ntjv", scores, values, precision=highest)
    last_log = cumulative[:, -1]
    weighted = key_gate * jnp.exp(last_log[:, None] - cumulative)
    block_states = jnp.einsum("nsjd,nsjv->njdv", weighted, values, precision=highest)
    running_decay, running_state = lax.associative_scan(
        combine_pair, (jnp.exp(last_log), block_states), axis=0
    )
    identity = (
        jnp.ones(floor_gate.shape, jnp.float32),
        jnp.zeros(block_states.shape[1:], jnp.float32),
    )
    packed_total = jnp.concatenate([running_state[-1], running_decay[-1][..., None]], axis=-1)
    packed_identity = jnp.concatenate([identity[1], identity[0][..., None]], axis=-1)
    carried = carried_in(packed_total, "sp", combine_packed, packed_identity)
    carried_state = carried[..., :-1]
    prior_decay = jnp.concatenate([identity[0][None], running_decay[:-1]], axis=0)
    prior_state = jnp.concatenate([identity[1][None], running_state[:-1]], axis=0)
    start_state = prior_state + prior_decay[..., None] * carried_state[None]
    head_out = within + jnp.einsum(
        "ntjd,njdv->ntjv", queries * jnp.exp(cumulative), start_state, precision=highest
    )
    normed_heads = head_out * lax.rsqrt(
        jnp.mean(head_out * head_out, axis=-1, keepdims=True) + epsilon
    )
    gates = jax.nn.silu(out_gate.astype(jnp.float32).reshape(grid))
    mixed = (
        (normed_heads * head_gain.reshape(local_heads, HEAD_DIM) * gates)
        .astype(jnp.bfloat16)
        .reshape(length, -1)
    )
    regrouped = lax.all_to_all(mixed, "tp", split_axis=0, concat_axis=1, tiled=True)
    projected = jnp.dot(regrouped, w_out, preferred_element_type=jnp.float32)
    updated_f = (
        (residual_in.astype(jnp.float32) + projected).astype(jnp.bfloat16).astype(jnp.float32)
    )
    normed = (
        updated_f
        * lax.rsqrt(jnp.mean(updated_f * updated_f, axis=-1, keepdims=True) + epsilon)
        * ffn_gain
    ).astype(jnp.bfloat16)
    half_rows = normed.shape[0]
    top_count = routing.shape[1]
    width = normed.shape[1]
    experts = lax.axis_size("sp")
    capacity = 2 * half_rows * top_count // experts
    flat_routes = routing.reshape(-1)
    one_hot = (flat_routes[:, None] == jnp.arange(experts, dtype=jnp.int32)[None, :]).astype(
        jnp.int32
    )
    slot_rank = jnp.sum(one_hot * (jnp.cumsum(one_hot, axis=0) - 1), axis=1)
    slot_index = flat_routes * capacity + slot_rank
    outbox = (
        jnp.zeros((experts * capacity, width), jnp.bfloat16)
        .at[slot_index]
        .set(jnp.repeat(normed, top_count, axis=0))
    )
    arrived = lax.all_to_all(
        outbox.reshape(experts, capacity, width), "sp", split_axis=0, concat_axis=0, tiled=True
    )
    arrived_rows = arrived.reshape(experts * capacity, width)
    stacked = jnp.stack([expert_gate, expert_up], axis=0)
    piece = lax.all_gather(stacked, "tp", axis=3, tiled=True)
    gate_part = jnp.dot(arrived_rows, piece[0, 0], preferred_element_type=jnp.float32)
    up_part = jnp.dot(arrived_rows, piece[1, 0], preferred_element_type=jnp.float32)
    hidden = (jax.nn.silu(gate_part) * up_part).astype(jnp.bfloat16)
    result = jnp.dot(
        hidden,
        lax.all_gather(expert_down, "tp", axis=1, tiled=True)[0],
        preferred_element_type=jnp.float32,
    )
    expert_out = result.astype(jnp.bfloat16).reshape(experts, capacity, width)
    returned = lax.all_to_all(expert_out, "sp", split_axis=0, concat_axis=0, tiled=True)
    picked = (
        returned.reshape(experts * capacity, width)[slot_index]
        .reshape(half_rows, top_count, width)
        .astype(jnp.float32)
    )
    expert_sum = jnp.sum(picked * route_weight[:, :, None], axis=1)
    return (updated_f + expert_sum).astype(jnp.bfloat16)


def solution(mesh):
    placed = (
        P("sp", "tp"),
        P("sp", "tp"),
        P("sp", "tp"),
        P("sp", "tp"),
        P("tp"),
        P("tp"),
        P(("sp", "tp"), None),
        P(),
        P(),
        P(("sp", "tp"), None),
        P(("sp", "tp"), None),
        P("sp", None, "tp"),
        P("sp", None, "tp"),
        P("sp", "tp", None),
    )
    return jax.shard_map(
        body, mesh=mesh, in_specs=placed, out_specs=P(("sp", "tp"), None), check_vma=False
    )
```

profile of v0, /device:TPU:8, one launch (start us, length us, event | category | flops | bytes accessed | tf_op | source)
XLA Modules:
  0.0 305.3 jit_solution(16403134711104120234)
XLA Ops:
  6.5 0.7 subtract_bitcast_fusion
  7.3 1.1 fusion.28
  8.5 0.8 fusion.44
  9.5 1.0 convert_bitcast_fusion
  10.7 1.2 exponential_multiply_fusion
  11.9 1.9 fusion.39
  13.8 0.6 slice_add_fusion.2
  14.5 1.3 copy-done
  16.2 6.4 %pad.43 = f32[4,8,128,128]{2,3,1,0:T(8,128)} pad(f32[2,8,128,128]{2,3,1,0:T(8,128)S(1)} %pad_maximum_fusion.3, f32[]{:T(128)} %constant.19.clone.1), padding=0_1_1x0_0_0x0_0_0x0_0_0 | pad | bytes 3145732 | tf_op jit(solution)/shard_map/pad | solution.py:73
  22.5 6.5 %pad.44 = f32[4,8,128,128]{2,3,1,0:T(8,128)} pad(f32[2,8,128,128]{2,3,1,0:T(8,128)S(1)} %pad_add_fusion, f32[]{:T(128)} %constant.19.clone.1), padding=1_0_1x0_0_0x0_0_0x0_0_0 | pad | bytes 3145732 | tf_op jit(solution)/shard_map/pad | solution.py:73
  29.1 2.5 add.174
  31.6 11.9 %pad.114 = f32[7,8,128,128]{2,3,1,0:T(8,128)} pad(f32[4,8,128,128]{2,3,1,0:T(8,128)S(1)} %add.174, f32[]{:T(128)} %constant.19.clone.1), padding=0_0_1x0_0_0x0_0_0x0_0_0 | pad | bytes 5767172
  43.5 1.1 add_bitcast_fusion
  44.6 0.9 copy.69
  45.6 4.6 %pad_maximum_fusion.1 = bf16[2,1,2048,512]{3,2,1,0:T(8,128)(2,1)} fusion(bf16[1,1,2048,512]{3,2,1,0:T(8,128)(2,1)} %bitcast.144, bf16[1,1,2048,512]{3,2,1,0:T(8,128)(2,1)} %bitcast.145), kind=kLoop, calls=%fused_computation.14 | loop fusion | flops 2097152 | bytes 8388608 | tf_op jit(solution)/shard_map/stack | solution.py:129
  50.2 0.2 all-gather.7.cloned.1.call-start
  50.4 0.5 all-gather.7.cloned.1.call-update
  51.0 12.1 %pad.46 = f32[8,8,128,128]{2,3,1,0:T(8,128)} pad(f32[4,8,128,128]{2,3,1,0:T(8,128)S(1)} %add.174, f32[]{:T(128)} %constant.19.clone.1), padding=1_0_1x0_0_0x0_0_0x0_0_0 | pad | bytes 6291460 | tf_op jit(solution)/shard_map/pad | solution.py:73
  63.2 1.0 convert_bitcast_fusion.1
  64.2 0.9 copy.97
  65.1 1.3 exponential_bitcast_fusion
  66.7 5.6 %fusion = f32[8,8,16,16]{2,3,1,0:T(8,128)S(1)} fusion(f32[8,8,16,16,128]{4,1,3,2,0:T(8,128)S(1)} %exponential_bitcast_fusion, f32[8,8,128,16]{2,3,1,0:T(8,128)S(1)} %copy.64, f32[8,8,128,16]{2,3,1,0:T(8,128)S(1)} %copy.63), kind=kLoop, calls=%fused_computation.8 | loop fusion | flops 6275072 | bytes 9502720 | tf_op jit(solution)/shard_map/ntjd,nsjd,ntsjd->njts/dot_general | solution.py:68
  72.4 0.6 convolution_bitcast_fusion
  73.0 0.5 fusion.16
  73.7 12.1 %pad.45 = f32[8,8,128,128]{2,3,1,0:T(8,128)} pad(f32[4,8,128,128]{2,3,1,0:T(8,128)S(1)} %pad_maximum_fusion.2, f32[]{:T(128)} %constant.19.clone.1), padding=0_1_1x0_0_0x0_0_0x0_0_0 | pad | bytes 6291460 | tf_op jit(solution)/shard_map/pad | solution.py:73
  86.7 5.9 %slice_add_fusion.1 = f32[7,8,128,128]{2,3,1,0:T(8,128)} fusion(f32[8,8,128,128]{2,3,1,0:T(8,128)} %pad.46, f32[8,8,128,128]{2,3,1,0:T(8,128)} %pad.45), kind=kLoop, calls=%fused_computation.21 | loop fusion | flops 917504 | bytes 11010048 | tf_op jit(solution)/shard_map/add | solution.py:73
  92.7 86.4 %all-gather.9.cloned.1.call-done = f32[128,128,129]{1,0,2:T(8,128)} async-done(((f32[8,128,129]{1,0,2:T(8,128)}), f32[128,128,129]{1,0,2:T(8,128)}) %all-gather.9.cloned.1.call-update) | async-done | bytes 8454160 | tf_op jit(solution)/shard_map/all_gather | solution.py:16
  179.3 5.3 %while.10 = (s32[]{:T(128)}, f32[8,128,129]{1,0,2:T(8,128)S(1)}, s32[]{:T(128)}, f32[16,8,128,129]{2,1,0,3:T(8,128)}, s32[]{:T(128)}, /*index=5*/s32[]{:T(128)}, s32[]{:T(128)}) while((s32[]{:T(128)}, f32[8,128,129]{1,0,2:T(8,128)S(1)}, s32[]{:T(128)}, f32[16,8,128,129]{2,1,0,3:T(8,128)}, s32[]{:T(128)}, /*index=5*/s32[]{:T(128)}, ...), condition=%wide.region_2.3_spmd, body=%wide.region_1.2_spmd.sunk | while | flops 395269 | bytes 3707003 | solution.py:22
  179.3 1.1 dynamic-slice_bitcast_fusion.2
  180.6 1.1 dynamic-slice_bitcast_fusion.2
  181.9 1.1 dynamic-slice_bitcast_fusion.2
  183.1 1.1 dynamic-slice_bitcast_fusion.2
  184.8 8.9 %multiply_reduce_fusion.2 = (f32[8,16,8]{1,2,0:T(8,128)S(1)}, f32[8,16,8,128]{3,1,2,0:T(8,128)S(1)}) fusion(f32[8,16,8,128]{3,1,2,0:T(8,128)S(1)} %convolution_bitcast_fusion, f32[8,16,8,128]{3,2,1,0:T(8,128)S(1)} %copy-done.4, f32[7,8,128,128]{2,3,1,0:T(8,128)} %slice_add_fusion.1, f32[8,128,128]{1,2,0:T(8,128)S(1)} %copy.71, f32[8,8,128]{2,1,0:T(8,128)S(1)} %concatenate.34), kind=kOutput, calls=%fused_computation.78 | convolution fusion | flops 203815936 | bytes 5804032 | tf_op jit(solution)/shard_map/ntjd,njdv->ntjv/dot_general | solution.py:87
  193.7 0.2 multiply_convert_fusion.1
  194.2 4.1 %all_to_all.29 = bf16[2,64,1024]{2,1,0:T(8,128)(2,1)S(1)} all-to-all(bf16[2,64,1024]{2,1,0:T(8,128)(2,1)S(1)} %all_to_all.20), channel_id=1, replica_groups=mesh['sp'=16,'tp'=2] {'tp'}, dimensions={0} | all-to-all | bytes 524288 | tf_op jit(solution)/shard_map/all_to_all | solution.py:99
  198.4 5.1 %multiply_reduce_fusion.1 = (f32[64]{0:T(128)S(1)}, f32[64,2048]{1,0:T(8,128)S(1)}) fusion(bf16[64,2048]{1,0:T(8,128)(2,1)S(1)} %bitcast.146, bf16[2048,2048]{1,0:T(8,128)(2,1)} %param.23, bf16[64,2048]{1,0:T(8,128)(2,1)S(1)} %copy-done.7), kind=kOutput, calls=%fused_computation.74 | convolution fusion | flops 537657280 | bytes 9437440 | tf_op jit(solution)/shard_map/dot_general | solution.py:100
  203.6 0.3 broadcast_in_dim.22
  204.1 2.5 scatter_custom_fusion
  206.6 22.6 %all-to-all-start.1 = ((bf16[16,16,2048]{2,1,0:T(8,128)(2,1)}), bf16[16,16,2048]{2,1,0:T(8,128)(2,1)S(1)}, u32[]{:S(2)}, u32[]{:S(2)}) async-start(bf16[16,16,2048]{2,1,0:T(8,128)(2,1)} %bitcast.23), calls=%async_computation.1 | async-start | bytes 2097152 | tf_op jit(solution)/shard_map/all_to_all | solution.py:125
  229.2 25.7 %all-to-all-done.1 = bf16[16,16,2048]{2,1,0:T(8,128)(2,1)S(1)} async-done(((bf16[16,16,2048]{2,1,0:T(8,128)(2,1)}), bf16[16,16,2048]{2,1,0:T(8,128)(2,1)S(1)}, u32[]{:S(2)}, u32[]{:S(2)}) %all-to-all-start.1) | async-done | bytes 1048608 | tf_op jit(solution)/shard_map/all_to_all | solution.py:125
  254.9 3.4 %fusion.2 = f32[256,1024]{1,0:T(8,128)S(1)} fusion(bf16[256,2048]{1,0:T(8,128)(2,1)S(1)} %bitcast.147, bf16[2,1,2048,1024]{3,2,1,0:T(8,128)(2,1)} %all-gather.5.cloned.1.call-done), kind=kOutput, calls=%fused_computation.13 | convolution fusion | flops 1073741824 | bytes 6291456 | tf_op jit(solution)/shard_map/dot_general | solution.py:131
  258.4 7.0 %fusion.9 = bf16[256,2048]{1,0:T(8,128)(2,1)} fusion(bf16[1,1024,2048]{2,1,0:T(8,128)(2,1)} %all-gather.7.cloned.1.call-done, bf16[256,2048]{1,0:T(8,128)(2,1)S(1)} %bitcast.148, bf16[2,1,2048,1024]{3,2,1,0:T(8,128)(2,1)} %all-gather.5.cloned.1.call-done, f32[256,1024]{1,0:T(8,128)S(1)} %fusion.2), kind=kOutput, calls=%fused_computation.22 | convolution fusion | flops 2149580800 | bytes 11534336 | tf_op jit(solution)/shard_map/dot_general | solution.py:134
  265.4 5.0 %all-to-all-start.2 = ((bf16[16,16,2048]{2,1,0:T(8,128)(2,1)}), bf16[16,16,2048]{2,1,0:T(8,128)(2,1)S(1)}, u32[]{:S(2)}, u32[]{:S(2)}) async-start(bf16[16,16,2048]{2,1,0:T(8,128)(2,1)} %bitcast.30), calls=%async_computation.2 | async-start | bytes 2097152 | tf_op jit(solution)/shard_map/all_to_all | solution.py:140
  270.6 24.3 %all-to-all-done.2 = bf16[16,16,2048]{2,1,0:T(8,128)(2,1)S(1)} async-done(((bf16[16,16,2048]{2,1,0:T(8,128)(2,1)}), bf16[16,16,2048]{2,1,0:T(8,128)(2,1)S(1)}, u32[]{:S(2)}, u32[]{:S(2)}) %all-to-all-start.2) | async-done | bytes 1048608 | tf_op jit(solution)/shard_map/all_to_all | solution.py:140
  294.9 0.9 gather_fusion
  295.8 0.7 reshape.156
  296.5 1.5 multiply_reduce_fusion
  298.0 0.8 add_convert_fusion
  (106 shorter events, 4.0 us)
Async XLA Ops:
  6.5 4.1 %copy-start.8 = (bf16[128,1024]{1,0:T(8,128)(2,1)S(1)}, bf16[128,1024]{1,0:T(8,128)(2,1)}, u32[]{:S(2)}) copy-start(bf16[128,1024]{1,0:T(8,128)(2,1)} %param.18) | copy-start | bytes 786436
  6.5 172.6 %all-gather.9.cloned.1.call-start = ((), (), s32[]{:S(2)}) async-start(), calls=%async_computation.5 | async-start | bytes 8982528 | tf_op jit(solution)/shard_map/all_gather | solution.py:16
  9.4 53.7 %copy-start.9 = (f32[8,8,128]{2,1,0:T(8,128)}, f32[8,8,128]{2,1,0:T(8,128)S(1)}, u32[]{:S(2)}) copy-start(f32[8,8,128]{2,1,0:T(8,128)S(1)} %fusion.69) | copy-start | bytes 98308
  13.8 2.0 copy-start
  45.5 183.7 %all-gather.5.cloned.1.call-start = ((), (), s32[]{:S(2)}) async-start(), calls=%async_computation.3 | async-start | bytes 12582912 | tf_op jit(solution)/shard_map/all_gather | solution.py:130
  50.2 208.2 %all-gather.7.cloned.1.call-start = ((), (), s32[]{:S(2)}) async-start(), calls=%async_computation.4 | async-start | bytes 6291456 | tf_op jit(solution)/shard_map/all_gather | solution.py:136
  50.9 12.2 %copy-start.12 = (s32[64,2]{0,1:T(2,128)S(1)}, s32[64,2]{0,1:T(2,128)}, u32[]{:S(2)}) copy-start(s32[64,2]{0,1:T(2,128)} %param.25) | copy-start | bytes 1540
  65.1 1.5 copy-start.5
  66.7 6.3 %copy-start.1 = (f32[8,8,128,128]{2,3,1,0:T(8,128)S(1)}, f32[8,8,128,128]{2,3,1,0:T(8,128)}, u32[]{:S(2)}) copy-start(f32[8,8,128,128]{2,3,1,0:T(8,128)} %copy-done) | copy-start | bytes 12582916
  66.7 6.3 %copy-start.2 = (f32[4,8,128,128]{2,3,1,0:T(8,128)S(1)}, f32[4,8,128,128]{2,3,1,0:T(8,128)}, u32[]{:S(2)}) copy-start(f32[4,8,128,128]{2,3,1,0:T(8,128)} %pad.43) | copy-start | bytes 6291460
  66.7 6.3 %copy-start.3 = (f32[4,8,128,128]{2,3,1,0:T(8,128)S(1)}, f32[4,8,128,128]{2,3,1,0:T(8,128)}, u32[]{:S(2)}) copy-start(f32[4,8,128,128]{2,3,1,0:T(8,128)} %pad.44) | copy-start | bytes 6291460
  72.4 1.2 slice-start
  73.7 12.1 %slice-start.1 = ((f32[8,8,128]{2,1,0:T(8,128)}), f32[1,8,128]{2,1,0:T(8,128)S(1)}, s32[]{:S(2)}) async-start(f32[8,8,128]{2,1,0:T(8,128)} %copy-done.9), calls=%async_computation.7 | async-start | bytes 8192 | tf_op jit(solution)/shard_map/slice | solution.py:73
  179.3 5.5 %copy-start.4 = (f32[8,16,8,128]{3,2,1,0:T(8,128)S(1)}, f32[8,16,8,128]{3,2,1,0:T(8,128)}, u32[]{:S(2)}) copy-start(f32[8,16,8,128]{3,2,1,0:T(8,128)} %get-tuple-element.61) | copy-start | bytes 1572868
  184.6 9.1 %copy-start.6 = (f32[16,8,8,128]{3,2,1,0:T(8,128)S(1)}, f32[16,8,8,128]{3,2,1,0:T(8,128)}, u32[]{:S(2)}) copy-start(f32[16,8,8,128]{3,2,1,0:T(8,128)} %copy.97) | copy-start | bytes 1572868
  184.6 9.1 %copy-start.11 = (f32[1024]{0:T(1024)S(1)}, f32[1024]{0:T(1024)}, u32[]{:S(2)}) copy-start(f32[1024]{0:T(1024)} %param.21) | copy-start | bytes 12292
  184.8 13.6 %copy-start.7 = (bf16[64,2048]{1,0:T(8,128)(2,1)S(1)}, bf16[64,2048]{1,0:T(8,128)(2,1)}, u32[]{:S(2)}) copy-start(bf16[64,2048]{1,0:T(8,128)(2,1)} %param.22) | copy-start | bytes 786436
  198.4 5.1 %copy-start.10 = (f32[2048]{0:T(1024)S(1)}, f32[2048]{0:T(1024)}, u32[]{:S(2)}) copy-start(f32[2048]{0:T(1024)} %param.24) | copy-start | bytes 24580
  206.6 48.3 %all-to-all-start.1 = ((bf16[16,16,2048]{2,1,0:T(8,128)(2,1)}), bf16[16,16,2048]{2,1,0:T(8,128)(2,1)S(1)}, u32[]{:S(2)}, u32[]{:S(2)}) async-start(bf16[16,16,2048]{2,1,0:T(8,128)(2,1)} %bitcast.23), calls=%async_computation.1 | async-start | bytes 2097152 | tf_op jit(solution)/shard_map/all_to_all | solution.py:125
  258.4 12.1 %copy-start.13 = (f32[64,2]{0,1:T(2,128)S(1)}, f32[64,2]{0,1:T(2,128)}, u32[]{:S(2)}) copy-start(f32[64,2]{0,1:T(2,128)} %param.26) | copy-start | bytes 1540
  265.4 29.5 %all-to-all-start.2 = ((bf16[16,16,2048]{2,1,0:T(8,128)(2,1)}), bf16[16,16,2048]{2,1,0:T(8,128)(2,1)S(1)}, u32[]{:S(2)}, u32[]{:S(2)}) async-start(bf16[16,16,2048]{2,1,0:T(8,128)(2,1)} %bitcast.30), calls=%async_computation.2 | async-start | bytes 2097152 | tf_op jit(solution)/shard_map/all_to_all | solution.py:140
Sparse Core Ops, SparseCore 0:
  45.6 133.4 all-gather.8
  180.7 21.4 all-gather.4
  203.7 14.6 all-gather.6
where the time goes:
time: 307 us; the launch traced here: 305 us
  waiting for transfers between devices  137 us (45%)
  local copies, waits for them, and re-layouts  62.8 us (20%)
  other arithmetic  32.4 us (11%)
  starting transfers between devices  27.9 us (9%)
  matrix products  26.9 us (9%)
  between operations  13.8 us (4%)
  blocking collectives  4.14 us (1%)
    all_gather x1, waiting for transfers between devices, carried_in(): gathered = lax.all_gather(part, axis)  86.4 us
    pad x8, local copies, waits for them, and re-layouts, body(): lax.associative_scan(combine_pair, (jnp.exp(last_log), block_states), axi...  37.1 us
    all_to_all x1, waiting for transfers between devices, body(): lax.all_to_all(outbox.reshape(experts, capacity, width), 'sp', split_axis...  25.7 us
    all_to_all x1, waiting for transfers between devices, body(): lax.all_to_all(expert_out, 'sp', split_axis=0, concat_axis=0, tiled=True)  24.3 us
    all_to_all x1, starting transfers between devices, body(): lax.all_to_all(outbox.reshape(experts, capacity, width), 'sp', split_axis...  22.6 us
    unnamed x37, local copies, waits for them, and re-layouts  14.6 us
    dot_general x1, matrix products, body(): jnp.einsum('ntjd,njdv->ntjv', queries * jnp.exp(cumulative), start_state,...  8.89 us
    add x6, other arithmetic, body(): lax.associative_scan(combine_pair, (jnp.exp(last_log), block_states), axi...  8.53 us
  transfers between devices with their start and end apart: 5, of which 3 were waited for; matrix products, arithmetic and copies ran while one was open for 24% of the time, Pallas kernels for 0%

commit v1 on v0

v1 whole, which is shorter than its diff:
```python
import functools

import jax
import jax.numpy as jnp
from jax import lax
from jax.experimental import pallas as pl
from jax.experimental.pallas import tpu as pltpu
from jax.sharding import PartitionSpec as P

HEAD_DIM = 128
TAIL = 8
epsilon = 1e-06
f32 = jnp.float32
bf16 = jnp.bfloat16

NN = (((1,), (0,)), ((), ()))
NT = (((1,), (1,)), ((), ()))
TN = (((0,), (0,)), ((), ()))


def dot(a, b, dims=NN):
    return lax.dot_general(a, b, dims, preferred_element_type=f32)


def split(x):
    hi = x.astype(bf16)
    return hi, (x - hi.astype(f32)).astype(bf16)


def sigmoid(x):
    return 1.0 / (1.0 + jnp.exp(-x))


def local_kernel(q_ref, f_ref, v_ref, low_ref, intra_ref, qe_ref, out_ref, *, heads, rows):
    length = q_ref.shape[0]
    per = HEAD_DIM // rows
    t = lax.broadcasted_iota(jnp.int32, (length, length), 0)
    s = lax.broadcasted_iota(jnp.int32, (length, length), 1)
    causal = t >= s
    tri = jnp.where(causal, 1.0, 0.0).astype(bf16)
    gap = 1.0 - low_ref[...]
    key_gate = gap * sigmoid(-f_ref[...].astype(f32))
    hi, lo = split(jnp.log1p(-key_gate))
    total = dot(tri, hi) + dot(tri, lo)
    middle = total[length // 2 - 1 : length // 2]
    last = total[length - 1 : length]
    query = q_ref[...].astype(f32)
    scaled_query = (query * jnp.exp(total - middle)).astype(bf16)
    scaled_key = (key_gate * jnp.exp(middle - total)).astype(bf16)
    weighted = (key_gate * jnp.exp(last - total)).astype(bf16)
    qe_ref[...] = (query * jnp.exp(total)).astype(bf16)
    last_hi, last_lo = split(last)
    place = lax.broadcasted_iota(jnp.int32, (TAIL, HEAD_DIM), 0)
    for h in range(heads):
        lanes = slice(h * HEAD_DIM, (h + 1) * HEAD_DIM)
        value = v_ref[:, lanes]
        scores = dot(scaled_query[:, lanes], scaled_key[:, lanes], NT)
        scores = jnp.where(causal, scores, 0.0).astype(bf16)
        intra_ref[:, lanes] = dot(scores, value)
        state = dot(value, weighted[:, lanes], TN).astype(bf16)
        tail = jnp.where(
            place == 0,
            last_hi[:, lanes].astype(f32),
            jnp.where(place == 1, last_lo[:, lanes].astype(f32), 0.0),
        ).astype(bf16)
        for j in range(per):
            out_ref[h * per + j, :rows] = state[j * rows : (j + 1) * rows]
            out_ref[h * per + j, rows:] = tail


def scan_kernel(in_ref, out_ref, *, rows):
    state = jnp.zeros((rows, HEAD_DIM), f32)
    for i in range(in_ref.shape[0]):
        out_ref[i] = state.astype(bf16)
        tail = in_ref[i, rows:].astype(f32)
        decay = jnp.exp(tail[0:1] + tail[1:2])
        state = state * decay + in_ref[i, :rows].astype(f32)


def mix_kernel(tp_ref, intra_ref, qe_ref, state_ref, gate_ref, gain_ref, mine_ref, send_ref, *, heads):
    half = mine_ref.shape[0]
    own = tp_ref[0]
    for ref, side in ((send_ref, 1 - own), (mine_ref, own)):
        at = pl.ds(pl.multiple_of(side * half, half), half)
        for h in range(heads):
            lanes = slice(h * HEAD_DIM, (h + 1) * HEAD_DIM)
            out = intra_ref[at, lanes] + dot(qe_ref[at, lanes], state_ref[h], NT)
            scale = lax.rsqrt(jnp.mean(out * out, axis=-1, keepdims=True) + epsilon)
            gate = gate_ref[at, lanes].astype(f32)
            ref[:, lanes] = (out * scale * gain_ref[:, lanes] * (gate * sigmoid(gate))).astype(bf16)


def slots_of(routing, capacity):
    count, top = routing.shape
    t = lax.broadcasted_iota(jnp.int32, (count, count), 0)
    s = lax.broadcasted_iota(jnp.int32, (count, count), 1)
    before = jnp.where(t > s, 1.0, 0.0).astype(bf16)
    lane = lax.broadcasted_iota(jnp.int32, (count, 128), 1)
    taken = jnp.zeros((1, 128), f32)
    slots = []
    for k in range(top):
        expert = routing[:, k : k + 1]
        named = jnp.where(lane == expert, 1.0, 0.0)
        rank = dot(before, named.astype(bf16)) + taken
        rank = jnp.sum(named * rank, axis=1, keepdims=True)
        slots.append(expert * capacity + rank.astype(jnp.int32))
        taken = taken + jnp.sum(named, axis=0, keepdims=True)
    return slots


def project_kernel(
    tp_ref, mine_ref, recv_ref, w_ref, res_ref, gain_ref, route_ref, upd_ref, box_ref, acc_ref, *, capacity
):
    step = pl.program_id(0)
    steps = pl.num_programs(0)

    @pl.when(step == 0)
    def _():
        acc_ref[...] = dot(mine_ref[...], w_ref[...])

    @pl.when((step > 0) & (step < steps // 2))
    def _():
        acc_ref[...] += dot(mine_ref[...], w_ref[...])

    @pl.when(step >= steps // 2)
    def _():
        acc_ref[...] += dot(recv_ref[...], w_ref[...])

    @pl.when(step == steps - 1)
    def _():
        updated = (res_ref[...].astype(f32) + acc_ref[...]).astype(bf16)
        upd_ref[...] = updated
        updated = updated.astype(f32)
        scale = lax.rsqrt(jnp.mean(updated * updated, axis=-1, keepdims=True) + epsilon)
        normed = (updated * scale * gain_ref[...]).astype(bf16)
        lane = lax.broadcasted_iota(jnp.int32, (normed.shape[0], box_ref.shape[0]), 1)
        chosen = jnp.zeros(lane.shape, f32)
        for slot in slots_of(route_ref[...], capacity):
            chosen = chosen + jnp.where(lane == slot, 1.0, 0.0)
        box_ref[...] = dot(chosen.astype(bf16), normed, TN).astype(bf16)


def expert_kernel(x_ref, g0_ref, u0_ref, d0_ref, g1_ref, u1_ref, d1_ref, out_ref, acc_ref):
    step = pl.program_id(0)
    steps = pl.num_programs(0)

    def part(g_ref, u_ref, d_ref):
        x = x_ref[...]
        gate = dot(x, g_ref[...])
        hidden = (gate * sigmoid(gate) * dot(x, u_ref[...])).astype(bf16)
        return dot(hidden, d_ref[...])

    @pl.when(step == 0)
    def _():
        acc_ref[...] = part(g0_ref, u0_ref, d0_ref)

    @pl.when((step > 0) & (step < steps // 2))
    def _():
        acc_ref[...] += part(g0_ref, u0_ref, d0_ref)

    @pl.when(step >= steps // 2)
    def _():
        acc_ref[...] += part(g1_ref, u1_ref, d1_ref)

    @pl.when(step == steps - 1)
    def _():
        out_ref[...] = acc_ref[...].astype(bf16)


def combine_kernel(route_ref, weight_ref, back_ref, upd_ref, out_ref, *, capacity):
    lane = lax.broadcasted_iota(jnp.int32, (upd_ref.shape[0], back_ref.shape[0]), 1)
    chosen = jnp.zeros(lane.shape, f32)
    for k, slot in enumerate(slots_of(route_ref[...], capacity)):
        chosen = chosen + jnp.where(lane == slot, weight_ref[:, k : k + 1], 0.0)
    hi, lo = split(chosen)
    back = back_ref[...]
    out_ref[...] = (upd_ref[...].astype(f32) + (dot(hi, back) + dot(lo, back))).astype(bf16)


def params(mib, dims=1):
    return pltpu.CompilerParams(
        dimension_semantics=("arbitrary",) * dims, vmem_limit_bytes=mib * 1024 * 1024
    )


def body(
    query,
    forget_logit,
    value,
    out_gate,
    lower_bound,
    head_gain,
    residual_in,
    w_out,
    ffn_gain,
    routing,
    route_weight,
    expert_gate,
    expert_up,
    expert_down,
):
    ranks = lax.axis_size("sp")
    sides = lax.axis_size("tp")
    length, channels = query.shape
    heads = channels // HEAD_DIM
    rows = channels // ranks
    half = length // sides
    width = w_out.shape[1]
    top = routing.shape[1]
    capacity = 2 * half * top // ranks
    slots = ranks * capacity
    units = expert_gate.shape[2]
    tp = lax.axis_index("tp").reshape(1)
    swap = [(i, i ^ 1) for i in range(sides)]

    weights = (expert_gate[0], expert_up[0], expert_down[0])
    others = tuple(lax.ppermute(w, "tp", swap) for w in weights)

    group = 2
    intra, qe, packed = pl.pallas_call(
        functools.partial(local_kernel, heads=group, rows=rows),
        grid=(heads // group,),
        in_specs=[
            pl.BlockSpec((length, group * HEAD_DIM), lambda i: (0, i)),
            pl.BlockSpec((length, group * HEAD_DIM), lambda i: (0, i)),
            pl.BlockSpec((length, group * HEAD_DIM), lambda i: (0, i)),
            pl.BlockSpec((1, group * HEAD_DIM), lambda i: (0, i)),
        ],
        out_specs=[
            pl.BlockSpec((length, group * HEAD_DIM), lambda i: (0, i)),
            pl.BlockSpec((length, group * HEAD_DIM), lambda i: (0, i)),
            pl.BlockSpec((group * HEAD_DIM // rows, rows + TAIL, HEAD_DIM), lambda i: (i, 0, 0)),
        ],
        out_shape=[
            jax.ShapeDtypeStruct((length, channels), f32),
            jax.ShapeDtypeStruct((length, channels), bf16),
            jax.ShapeDtypeStruct((ranks, rows + TAIL, HEAD_DIM), bf16),
        ],
        compiler_params=params(16),
        name="local",
    )(query, forget_logit, value, lower_bound.reshape(1, -1))

    gathered = lax.all_to_all(packed, "sp", split_axis=0, concat_axis=0, tiled=True)
    prior = pl.pallas_call(
        functools.partial(scan_kernel, rows=rows),
        out_shape=jax.ShapeDtypeStruct((ranks, rows, HEAD_DIM), bf16),
        compiler_params=params(16, 0),
        name="scan",
    )(gathered)
    carried = lax.all_to_all(prior, "sp", split_axis=0, concat_axis=0, tiled=True)

    mine, send = pl.pallas_call(
        functools.partial(mix_kernel, heads=heads),
        grid_spec=pltpu.PrefetchScalarGridSpec(
            num_scalar_prefetch=1,
            grid=(1,),
            in_specs=[
                pl.BlockSpec((length, channels), lambda i, t: (0, 0)),
                pl.BlockSpec((length, channels), lambda i, t: (0, 0)),
                pl.BlockSpec((heads, HEAD_DIM, HEAD_DIM), lambda i, t: (0, 0, 0)),
                pl.BlockSpec((length, channels), lambda i, t: (0, 0)),
                pl.BlockSpec((1, channels), lambda i, t: (0, 0)),
            ],
            out_specs=[pl.BlockSpec((half, channels), lambda i, t: (0, 0))] * 2,
        ),
        out_shape=[jax.ShapeDtypeStruct((half, channels), bf16)] * 2,
        compiler_params=params(16),
        name="mix",
    )(tp, intra, qe, carried.reshape(heads, HEAD_DIM, HEAD_DIM), out_gate, head_gain.reshape(1, -1))
    recv = lax.ppermute(send, "tp", swap)

    block = 256
    per = channels // block
    updated, outbox = pl.pallas_call(
        functools.partial(project_kernel, capacity=capacity),
        grid_spec=pltpu.PrefetchScalarGridSpec(
            num_scalar_prefetch=1,
            grid=(sides * per,),
            in_specs=[
                pl.BlockSpec((half, block), lambda i, t: (0, jnp.minimum(i, per - 1))),
                pl.BlockSpec((half, block), lambda i, t: (0, jnp.maximum(i - per, 0))),
                pl.BlockSpec((block, width), lambda i, t: ((t[0] ^ (i // per)) * per + i % per, 0)),
                pl.BlockSpec((half, width), lambda i, t: (0, 0)),
                pl.BlockSpec((1, width), lambda i, t: (0, 0)),
                pl.BlockSpec((half, top), lambda i, t: (0, 0)),
            ],
            out_specs=[
                pl.BlockSpec((half, width), lambda i, t: (0, 0)),
                pl.BlockSpec((slots, width), lambda i, t: (0, 0)),
            ],
            scratch_shapes=[pltpu.VMEM((half, width), f32)],
        ),
        out_shape=[
            jax.ShapeDtypeStruct((half, width), bf16),
            jax.ShapeDtypeStruct((slots, width), bf16),
        ],
        compiler_params=params(24),
        name="project",
    )(tp, mine, recv, w_out, residual_in, ffn_gain.reshape(1, -1), routing)

    arrived = lax.all_to_all(
        outbox.reshape(ranks, capacity, width), "sp", split_axis=0, concat_axis=0, tiled=True
    )

    unit = 256
    parts = units // unit

    def first(i):
        return jnp.minimum(i, parts - 1)

    def second(i):
        return jnp.maximum(i - parts, 0)

    expert_out = pl.pallas_call(
        expert_kernel,
        grid=(2 * parts,),
        in_specs=[
            pl.BlockSpec((slots, width), lambda i: (0, 0)),
            pl.BlockSpec((width, unit), lambda i: (0, first(i))),
            pl.BlockSpec((width, unit), lambda i: (0, first(i))),
            pl.BlockSpec((unit, width), lambda i: (first(i), 0)),
            pl.BlockSpec((width, unit), lambda i: (0, second(i))),
            pl.BlockSpec((width, unit), lambda i: (0, second(i))),
            pl.BlockSpec((unit, width), lambda i: (second(i), 0)),
        ],
        out_specs=pl.BlockSpec((slots, width), lambda i: (0, 0)),
        out_shape=jax.ShapeDtypeStruct((slots, width), bf16),
        scratch_shapes=[pltpu.VMEM((slots, width), f32)],
        compiler_params=params(32),
        name="experts",
    )(arrived.reshape(slots, width), *weights, *others)

    returned = lax.all_to_all(
        expert_out.reshape(ranks, capacity, width), "sp", split_axis=0, concat_axis=0, tiled=True
    )
    columns = width // 4
    return pl.pallas_call(
        functools.partial(combine_kernel, capacity=capacity),
        grid=(width // columns,),
        in_specs=[
            pl.BlockSpec((half, top), lambda i: (0, 0)),
            pl.BlockSpec((half, top), lambda i: (0, 0)),
            pl.BlockSpec((slots, columns), lambda i: (0, i)),
            pl.BlockSpec((half, columns), lambda i: (0, i)),
        ],
        out_specs=pl.BlockSpec((half, columns), lambda i: (0, i)),
        out_shape=jax.ShapeDtypeStruct((half, width), bf16),
        compiler_params=params(16),
        name="combine",
    )(routing, route_weight, returned.reshape(slots, width), updated)


def solution(mesh):
    placed = (
        P("sp", "tp"),
        P("sp", "tp"),
        P("sp", "tp"),
        P("sp", "tp"),
        P("tp"),
        P("tp"),
        P(("sp", "tp"), None),
        P(),
        P(),
        P(("sp", "tp"), None),
        P(("sp", "tp"), None),
        P("sp", None, "tp"),
        P("sp", None, "tp"),
        P("sp", "tp", None),
    )
    return jax.shard_map(
        body, mesh=mesh, in_specs=placed, out_specs=P(("sp", "tp"), None), check_vma=False
    )
```

time: 307 us -> 126 us (0.41)
  waiting for transfers between devices: 137 us -> 59.5 us
  local copies, waits for them, and re-layouts: 62.8 us -> 13.9 us
  other arithmetic: 32.4 us -> 0 us
  matrix products: 26.9 us -> 0 us
  Pallas kernels: 0 us -> 19.6 us
  between operations: 13.8 us -> 0.08 us
  blocking collectives: 4.14 us -> 16.7 us
  starting transfers between devices: 27.9 us -> 15.4 us
    all_gather x3 -> x0, waiting for transfers between devices: 86.5 us -> none  [the longest x1 86.4 us: carried_in(): gathered = lax.all_gather(part, axis)]
    pad x8 -> x0, local copies, waits for them, and re-layouts: 37.1 us -> none  [body(): lax.associative_scan(combine_pair, (jnp.exp(last_log), block_states), axi...]
    dot_general x6 -> x0, matrix products: 26.9 us -> none  [the longest x1 8.89 us: body(): jnp.einsum('ntjd,njdv->ntjv', queries * jnp.exp(cumulative), start_state,...]
    pallas_call x0 -> x6, Pallas kernels: none -> 19.6 us  [the longest x1 8.3 us: body(): pl.pallas_call(expert_kernel, grid=(2 * parts,), in_specs=[pl.BlockSpec((...]
    all_to_all x2 -> x3, starting transfers between devices: 27.6 us -> 14.4 us  [the longest x1 5.56 us: body(): lax.all_to_all(expert_out.reshape(ranks, capacity, width), 'sp', split_ax...]
    all_to_all x1, blocking collectives: 4.14 us -> 16.7 us  [body(): lax.all_to_all(packed, 'sp', split_axis=0, concat_axis=0, tiled=True)]
    add x13 -> x0, other arithmetic: 10.1 us -> none  [the longest x6 8.53 us: body(): lax.associative_scan(combine_pair, (jnp.exp(last_log), block_states), axi...]
    all_to_all x2 -> x3, waiting for transfers between devices: 50.1 us -> 59.1 us  [the longest x1 26.1 us: body(): lax.all_to_all(outbox.reshape(ranks, capacity, width), 'sp', split_axis=0...]
  transfers between devices with their start and end apart: 5 -> 7, of which waited for: 3 -> 4; matrix products, arithmetic and copies ran while one was open for 24% -> 0% of each run, Pallas kernels for 0% -> 3%
where the time goes in v1:
time: 126 us; the launch traced here: 125 us
  waiting for transfers between devices  59.5 us (47%)
  Pallas kernels  19.6 us (16%)
  blocking collectives  16.7 us (13%)
  starting transfers between devices  15.4 us (12%)
  local copies, waits for them, and re-layouts  13.9 us (11%)
    all_to_all x1, waiting for transfers between devices, body(): lax.all_to_all(outbox.reshape(ranks, capacity, width), 'sp', split_axis=0...  26.1 us
    all_to_all x1, waiting for transfers between devices, body(): lax.all_to_all(expert_out.reshape(ranks, capacity, width), 'sp', split_ax...  24.6 us
    all_to_all x1, blocking collectives, body(): lax.all_to_all(packed, 'sp', split_axis=0, concat_axis=0, tiled=True)  16.7 us
    unnamed x36, local copies, waits for them, and re-layouts  13.9 us
    all_to_all x1, waiting for transfers between devices, body(): lax.all_to_all(prior, 'sp', split_axis=0, concat_axis=0, tiled=True)  8.39 us
    pallas_call x1, Pallas kernels, body(): pl.pallas_call(expert_kernel, grid=(2 * parts,), in_specs=[pl.BlockSpec((...  8.3 us
    all_to_all x1, starting transfers between devices, body(): lax.all_to_all(expert_out.reshape(ranks, capacity, width), 'sp', split_ax...  5.56 us
    all_to_all x1, starting transfers between devices, body(): lax.all_to_all(prior, 'sp', split_axis=0, concat_axis=0, tiled=True)  4.41 us
  transfers between devices with their start and end apart: 7, of which 4 were waited for; matrix products, arithmetic and copies ran while one was open for 0% of the time, Pallas kernels for 3%

profile of v1, /device:TPU:8, one launch (start us, length us, event | category | flops | bytes accessed | tf_op | source)
XLA Modules:
  0.0 125.3 jit_solution(10670166445881795532)
XLA Ops:
  0.0 0.0 copy-start.5
  0.0 1.1 copy-done.5
  1.1 0.0 copy-start.6
  1.1 0.9 copy-done.6
  2.1 0.0 copy-start.7
  2.1 0.9 copy-done.7
  3.0 0.0 copy-start.13
  3.0 0.7 copy-done.13
  3.7 0.0 copy-start.8
  3.7 0.0 copy-start.14
  3.7 0.0 copy-start.15
  3.7 2.8 %local.1 = (f32[128,1024]{1,0:T(8,128)S(1)}, bf16[128,1024]{1,0:T(8,128)(2,1)S(1)}, bf16[16,72,128]{2,1,0:T(8,128)(2,1)S(1)}) custom-call(bf16[128,1024]{1,0:T(8,128)(2,1)S(1)} %copy-done.5, bf16[128,1024]{1,0:T(8,128)(2,1)S(1)} %copy-done.6, bf16[128,1024]{1,0:T(8,128)(2,1)S(1)} %copy-done.7, f32[1,1024]{1,0:T(1,128)S(1)} %bitcast.23), custom_call_target="tpu_custom_call" | custom-call | tf_op jit(solution)/shard_map/local/pallas_call | solution.py:220
  6.5 16.7 %all_to_all.20.in_ref = bf16[16,72,128]{2,1,0:T(8,128)(2,1)S(1)} all-to-all(bf16[16,72,128]{2,1,0:T(8,128)(2,1)S(1)} %get-tuple-element.14), channel_id=1, replica_groups=mesh['sp'=16,'tp'=2] {'sp'}, dimensions={0} | all-to-all | bytes 589824 | tf_op jit(solution)/shard_map/all_to_all | solution.py:243
  23.2 0.8 scan.1
  24.0 4.4 %all-to-all-start.1 = ((bf16[16,64,128]{2,1,0:T(8,128)(2,1)}), bf16[16,64,128]{2,1,0:T(8,128)(2,1)S(1)}, u32[]{:S(2)}, u32[]{:S(2)}) async-start(bf16[16,64,128]{2,1,0:T(8,128)(2,1)} %scan.1), calls=%async_computation.1 | async-start | bytes 524288 | tf_op jit(solution)/shard_map/all_to_all | solution.py:250
  28.4 8.4 %all-to-all-done.1 = bf16[16,64,128]{2,1,0:T(8,128)(2,1)S(1)} async-done(((bf16[16,64,128]{2,1,0:T(8,128)(2,1)}), bf16[16,64,128]{2,1,0:T(8,128)(2,1)S(1)}, u32[]{:S(2)}, u32[]{:S(2)}) %all-to-all-start.1) | async-done | bytes 262176 | tf_op jit(solution)/shard_map/all_to_all | solution.py:250
  36.8 0.0 copy-done.8
  36.8 0.0 copy-done.14
  36.8 1.1 mix.1
  37.9 0.6 copy-done.10
  38.6 0.0 collective-permute-start
  38.6 0.0 copy-done.1
  38.6 0.5 collective-permute-start.1
  39.1 0.0 collective-permute-start.2
  39.1 0.5 collective-permute-start.3
  39.6 0.0 copy-done.15
  39.6 0.1 copy.16.route_ref
  39.7 0.4 collective-permute-done.recv_ref
  40.1 0.0 copy-done.12
  40.1 3.4 %copy-done = bf16[2048,2048]{1,0:T(8,128)(2,1)S(1)} copy-done((bf16[2048,2048]{1,0:T(8,128)(2,1)S(1)}, bf16[2048,2048]{1,0:T(8,128)(2,1)}, u32[]{:S(2)}) %copy-start) | copy-done | bytes 8388632
  43.5 0.9 copy-done.9
  44.5 0.9 copy-done.11
  45.4 3.6 %project.1 = (bf16[64,2048]{1,0:T(8,128)(2,1)S(1)}, bf16[256,2048]{1,0:T(8,128)(2,1)S(1)}) custom-call(s32[1]{0:T(128)} %bitcast.tp_ref, bf16[64,1024]{1,0:T(8,128)(2,1)S(1)} %copy-done.11, bf16[64,1024]{1,0:T(8,128)(2,1)S(1)} %collective-permute-done.recv_ref, bf16[2048,2048]{1,0:T(8,128)(2,1)S(1)} %copy-done, bf16[64,2048]{1,0:T(8,128)(2,1)S(1)} %copy-done.9, ...), custom_call_target="tpu_custom_call" | custom-call | tf_op jit(solution)/shard_map/project/pallas_call | solution.py:274
  48.9 0.0 copy-start.4
  49.0 0.9 copy-done.4
  49.9 4.4 %all-to-all-start.2 = ((bf16[16,16,2048]{2,1,0:T(8,128)(2,1)}), bf16[16,16,2048]{2,1,0:T(8,128)(2,1)S(1)}, u32[]{:S(2)}, u32[]{:S(2)}) async-start(bf16[16,16,2048]{2,1,0:T(8,128)(2,1)} %bitcast.21), calls=%async_computation.2 | async-start | bytes 2097152 | tf_op jit(solution)/shard_map/all_to_all | solution.py:301
  54.3 0.0 collective-permute-done.1.g1_ref
  54.3 0.0 collective-permute-done.2.u1_ref
  54.3 0.0 collective-permute-done.3.d1_ref
  54.3 26.1 %all-to-all-done.2 = bf16[16,16,2048]{2,1,0:T(8,128)(2,1)S(1)} async-done(((bf16[16,16,2048]{2,1,0:T(8,128)(2,1)}), bf16[16,16,2048]{2,1,0:T(8,128)(2,1)S(1)}, u32[]{:S(2)}, u32[]{:S(2)}) %all-to-all-start.2) | async-done | bytes 1048608 | tf_op jit(solution)/shard_map/all_to_all | solution.py:301
  80.4 1.6 %copy-done.2 = bf16[1,2048,512]{2,1,0:T(8,128)(2,1)S(1)} copy-done((bf16[1,2048,512]{2,1,0:T(8,128)(2,1)S(1)}, bf16[1,2048,512]{2,1,0:T(8,128)(2,1)}, u32[]{:S(2)}) %copy-start.2) | copy-done | bytes 2097176
  82.0 1.6 %copy-done.3 = bf16[1,512,2048]{2,1,0:T(8,128)(2,1)S(1)} copy-done((bf16[1,512,2048]{2,1,0:T(8,128)(2,1)S(1)}, bf16[1,512,2048]{2,1,0:T(8,128)(2,1)}, u32[]{:S(2)}) %copy-start.3) | copy-done | bytes 2097176
  83.6 8.3 %experts.1 = bf16[256,2048]{1,0:T(8,128)(2,1)} custom-call(bf16[256,2048]{1,0:T(8,128)(2,1)S(1)} %bitcast.12, bf16[2048,512]{1,0:T(8,128)(2,1)S(1)} %bitcast.15, bf16[2048,512]{1,0:T(8,128)(2,1)S(1)} %bitcast.17, bf16[512,2048]{1,0:T(8,128)(2,1)S(1)} %bitcast.19, bf16[2048,512]{1,0:T(8,128)(2,1)} %collective-permute-done.1.g1_ref, ...), custom_call_target="tpu_custom_call" | custom-call | tf_op jit(solution)/shard_map/experts/pallas_call | solution.py:314
  91.9 5.6 %all-to-all-start.3 = ((bf16[16,16,2048]{2,1,0:T(8,128)(2,1)}), bf16[16,16,2048]{2,1,0:T(8,128)(2,1)S(1)}, u32[]{:S(2)}, u32[]{:S(2)}) async-start(bf16[16,16,2048]{2,1,0:T(8,128)(2,1)} %bitcast.10), calls=%async_computation.3 | async-start | bytes 2097152 | tf_op jit(solution)/shard_map/all_to_all | solution.py:333
  97.4 0.0 copy-done.16
  97.4 0.1 copy.17.weight_ref
  97.5 24.6 %all-to-all-done.3 = bf16[16,16,2048]{2,1,0:T(8,128)(2,1)S(1)} async-done(((bf16[16,16,2048]{2,1,0:T(8,128)(2,1)}), bf16[16,16,2048]{2,1,0:T(8,128)(2,1)S(1)}, u32[]{:S(2)}, u32[]{:S(2)}) %all-to-all-start.3) | async-done | bytes 1048608 | tf_op jit(solution)/shard_map/all_to_all | solution.py:333
  122.1 3.1 %combine.1 = bf16[64,2048]{1,0:T(8,128)(2,1)} custom-call(s32[64,2]{1,0:T(8,128)S(1)} %copy.16.route_ref, f32[64,2]{1,0:T(8,128)S(1)} %copy.17.weight_ref, bf16[256,2048]{1,0:T(8,128)(2,1)S(1)} %bitcast.13, bf16[64,2048]{1,0:T(8,128)(2,1)S(1)} %get-tuple-element.18.upd_ref), custom_call_target="tpu_custom_call" | custom-call | tf_op jit(solution)/shard_map/combine/pallas_call | solution.py:337
  (9 shorter events, 0.0 us)
Async XLA Ops:
  0.0 38.6 %copy-start.1 = (bf16[1,2048,512]{2,1,0:T(8,128)(2,1)S(1)}, bf16[1,2048,512]{2,1,0:T(8,128)(2,1)}, u32[]{:S(2)}) copy-start(bf16[1,2048,512]{2,1,0:T(8,128)(2,1)} %param.25) | copy-start | bytes 6291460
  0.0 1.1 copy-start.5
  1.1 0.9 copy-start.6
  2.1 0.9 copy-start.7
  3.0 0.7 copy-start.13
  3.7 33.1 %copy-start.8 = (bf16[128,1024]{1,0:T(8,128)(2,1)S(1)}, bf16[128,1024]{1,0:T(8,128)(2,1)}, u32[]{:S(2)}) copy-start(bf16[128,1024]{1,0:T(8,128)(2,1)} %gate_ref.1) | copy-start | bytes 786436
  3.7 33.1 %copy-start.14 = (f32[1024]{0:T(1024)S(1)}, f32[1024]{0:T(1024)}, u32[]{:S(2)}) copy-start(f32[1024]{0:T(1024)} %param.19) | copy-start | bytes 12292
  3.7 35.9 %copy-start.15 = (s32[64,2]{0,1:T(2,128)S(1)}, s32[64,2]{0,1:T(2,128)}, u32[]{:S(2)}) copy-start(s32[64,2]{0,1:T(2,128)} %param.23) | copy-start | bytes 1540
  3.7 36.4 %copy-start.12 = (f32[2048]{0:T(1024)S(1)}, f32[2048]{0:T(1024)}, u32[]{:S(2)}) copy-start(f32[2048]{0:T(1024)} %param.22) | copy-start | bytes 24580
  24.0 12.8 %all-to-all-start.1 = ((bf16[16,64,128]{2,1,0:T(8,128)(2,1)}), bf16[16,64,128]{2,1,0:T(8,128)(2,1)S(1)}, u32[]{:S(2)}, u32[]{:S(2)}) async-start(bf16[16,64,128]{2,1,0:T(8,128)(2,1)} %scan.1), calls=%async_computation.1 | async-start | bytes 524288 | tf_op jit(solution)/shard_map/all_to_all | solution.py:250
  37.9 0.7 copy-start.10
  38.6 1.6 %collective-permute-start = (bf16[64,1024]{1,0:T(8,128)(2,1)}, bf16[64,1024]{1,0:T(8,128)(2,1)S(1)}, u32[]{:S(2)}, u32[]{:S(2)}) collective-permute-start(bf16[64,1024]{1,0:T(8,128)(2,1)} %get-tuple-element.16), channel_id=1, source_target_pairs={{0,1},{1,0},{2,3},{3,2},{4,5},{5,4},{6,7},{7,6},{8,9},{9,8},{10,11... | collective-permute-start | bytes 393224 | tf_op jit(solution)/shard_map/ppermute | solution.py:270
  38.6 15.8 %collective-permute-start.1 = (bf16[2048,512]{1,0:T(8,128)(2,1)S(1)}, bf16[2048,512]{1,0:T(8,128)(2,1)}, u32[]{:S(2)}, u32[]{:S(2)}) collective-permute-start(bf16[2048,512]{1,0:T(8,128)(2,1)S(1)} %bitcast.14), channel_id=1, source_target_pairs={{0,1},{1,0},{2,3},{3,2},{4,5},{5,4},{6,7},{7,6},{8,9},{9,8},{10,11... | collective-permute-start | bytes 6291464 | tf_op jit(solution)/shard_map/ppermute | solution.py:217
  39.1 15.2 %collective-permute-start.2 = (bf16[2048,512]{1,0:T(8,128)(2,1)}, bf16[2048,512]{1,0:T(8,128)(2,1)}, u32[]{:S(2)}, u32[]{:S(2)}) collective-permute-start(bf16[2048,512]{1,0:T(8,128)(2,1)} %bitcast.16), channel_id=1, source_target_pairs={{0,1},{1,0},{2,3},{3,2},{4,5},{5,4},{6,7},{7,6},{8,9},{9,8},{10,11... | collective-permute-start | bytes 6291464 | tf_op jit(solution)/shard_map/ppermute | solution.py:217
  39.1 15.3 %collective-permute-start.3 = (bf16[512,2048]{1,0:T(8,128)(2,1)}, bf16[512,2048]{1,0:T(8,128)(2,1)}, u32[]{:S(2)}, u32[]{:S(2)}) collective-permute-start(bf16[512,2048]{1,0:T(8,128)(2,1)} %bitcast.18), channel_id=1, source_target_pairs={{0,1},{1,0},{2,3},{3,2},{4,5},{5,4},{6,7},{7,6},{8,9},{9,8},{10,11... | collective-permute-start | bytes 6291464 | tf_op jit(solution)/shard_map/ppermute | solution.py:217
  40.1 3.4 %copy-start = (bf16[2048,2048]{1,0:T(8,128)(2,1)S(1)}, bf16[2048,2048]{1,0:T(8,128)(2,1)}, u32[]{:S(2)}) copy-start(bf16[2048,2048]{1,0:T(8,128)(2,1)} %w_ref.1) | copy-start | bytes 25165828
  43.5 0.9 copy-start.9
  44.4 0.9 copy-start.11
  48.9 1.0 copy-start.4
  49.9 30.5 %all-to-all-start.2 = ((bf16[16,16,2048]{2,1,0:T(8,128)(2,1)}), bf16[16,16,2048]{2,1,0:T(8,128)(2,1)S(1)}, u32[]{:S(2)}, u32[]{:S(2)}) async-start(bf16[16,16,2048]{2,1,0:T(8,128)(2,1)} %bitcast.21), calls=%async_computation.2 | async-start | bytes 2097152 | tf_op jit(solution)/shard_map/all_to_all | solution.py:301
  80.4 1.6 %copy-start.2 = (bf16[1,2048,512]{2,1,0:T(8,128)(2,1)S(1)}, bf16[1,2048,512]{2,1,0:T(8,128)(2,1)}, u32[]{:S(2)}) copy-start(bf16[1,2048,512]{2,1,0:T(8,128)(2,1)} %param.26) | copy-start | bytes 6291460
  82.0 1.6 %copy-start.3 = (bf16[1,512,2048]{2,1,0:T(8,128)(2,1)S(1)}, bf16[1,512,2048]{2,1,0:T(8,128)(2,1)}, u32[]{:S(2)}) copy-start(bf16[1,512,2048]{2,1,0:T(8,128)(2,1)} %param.27) | copy-start | bytes 6291460
  91.9 5.6 %copy-start.16 = (f32[64,2]{0,1:T(2,128)S(1)}, f32[64,2]{0,1:T(2,128)}, u32[]{:S(2)}) copy-start(f32[64,2]{0,1:T(2,128)} %param.24) | copy-start | bytes 1540
  91.9 30.3 %all-to-all-start.3 = ((bf16[16,16,2048]{2,1,0:T(8,128)(2,1)}), bf16[16,16,2048]{2,1,0:T(8,128)(2,1)S(1)}, u32[]{:S(2)}, u32[]{:S(2)}) async-start(bf16[16,16,2048]{2,1,0:T(8,128)(2,1)} %bitcast.10), calls=%async_computation.3 | async-start | bytes 2097152 | tf_op jit(solution)/shard_map/all_to_all | solution.py:333

commit v2 on v1

v2 whole, which is shorter than its diff:
```python
import functools

import jax
import jax.numpy as jnp
from jax import lax
from jax.experimental import pallas as pl
from jax.experimental.pallas import tpu as pltpu
from jax.sharding import PartitionSpec as P

HEAD_DIM = 128
TAIL = 8
GROUPS = 4
COLUMNS = 4
epsilon = 1e-06
f32 = jnp.float32
bf16 = jnp.bfloat16

NN = (((1,), (0,)), ((), ()))
NT = (((1,), (1,)), ((), ()))
TN = (((0,), (0,)), ((), ()))


def dot(a, b, dims=NN):
    return lax.dot_general(a, b, dims, preferred_element_type=f32)


def split(x):
    hi = x.astype(bf16)
    return hi, (x - hi.astype(f32)).astype(bf16)


def sigmoid(x):
    return 1.0 / (1.0 + jnp.exp(-x))


def fetch(copies):
    for copy in copies:
        copy.start()
    return copies


def local_kernel(
    q_hbm, f_hbm, v_hbm, low_hbm, intra_ref, qe_ref, out_ref, q_ref, f_ref, v_ref, low_ref, sem, *, rows
):
    length, channels = q_ref.shape
    per = HEAD_DIM // rows
    block = channels // GROUPS
    low = pltpu.make_async_copy(low_hbm, low_ref, sem.at[3 * GROUPS])
    low.start()
    copies = []
    for g in range(GROUPS):
        lanes = slice(g * block, (g + 1) * block)
        copies.append(
            fetch(
                [
                    pltpu.make_async_copy(hbm.at[:, lanes], ref.at[:, lanes], sem.at[3 * g + i])
                    for i, (hbm, ref) in enumerate(((f_hbm, f_ref), (q_hbm, q_ref), (v_hbm, v_ref)))
                ]
            )
        )
    t = lax.broadcasted_iota(jnp.int32, (length, length), 0)
    s = lax.broadcasted_iota(jnp.int32, (length, length), 1)
    causal = t >= s
    tri = jnp.where(causal, 1.0, 0.0).astype(bf16)
    place = lax.broadcasted_iota(jnp.int32, (TAIL, HEAD_DIM), 0)
    low.wait()
    for g in range(GROUPS):
        group = slice(g * block, (g + 1) * block)
        for copy in copies[g]:
            copy.wait()
        gap = 1.0 - low_ref[:, group]
        key_gate = gap * sigmoid(-f_ref[:, group].astype(f32))
        hi, lo = split(jnp.log1p(-key_gate))
        total = dot(tri, hi) + dot(tri, lo)
        middle = total[length // 2 - 1 : length // 2]
        last = total[length - 1 : length]
        query = q_ref[:, group].astype(f32)
        scaled_query = (query * jnp.exp(total - middle)).astype(bf16)
        scaled_key = (key_gate * jnp.exp(middle - total)).astype(bf16)
        weighted = (key_gate * jnp.exp(last - total)).astype(bf16)
        qe_ref[:, group] = (query * jnp.exp(total)).astype(bf16)
        last_hi, last_lo = split(last)
        for i in range(block // HEAD_DIM):
            h = g * (block // HEAD_DIM) + i
            inner = slice(i * HEAD_DIM, (i + 1) * HEAD_DIM)
            lanes = slice(h * HEAD_DIM, (h + 1) * HEAD_DIM)
            value = v_ref[:, lanes]
            state = dot(value, weighted[:, inner], TN).astype(bf16)
            scores = dot(scaled_query[:, inner], scaled_key[:, inner], NT)
            scores = jnp.where(causal, scores, 0.0).astype(bf16)
            intra_ref[:, lanes] = dot(scores, value)
            tail = jnp.where(
                place == 0,
                last_hi[:, inner].astype(f32),
                jnp.where(place == 1, last_lo[:, inner].astype(f32), 0.0),
            ).astype(bf16)
            for j in range(per):
                out_ref[h * per + j, :rows] = state[j * rows : (j + 1) * rows]
                out_ref[h * per + j, rows:] = tail


def scan_kernel(in_ref, out_ref, *, rows):
    state = jnp.zeros((rows, HEAD_DIM), f32)
    for i in range(in_ref.shape[0]):
        out_ref[i] = state.astype(bf16)
        tail = in_ref[i, rows:].astype(f32)
        decay = jnp.exp(tail[0:1] + tail[1:2])
        state = state * decay + in_ref[i, :rows].astype(f32)


def mixed_head(h, at, intra_ref, qe_ref, state_ref, gate_ref, gain_ref):
    lanes = slice(h * HEAD_DIM, (h + 1) * HEAD_DIM)
    out = intra_ref[at, lanes] + dot(qe_ref[at, lanes], state_ref[h], NT)
    scale = lax.rsqrt(jnp.mean(out * out, axis=-1, keepdims=True) + epsilon)
    gate = gate_ref[:, lanes].astype(f32)
    return (out * scale * gain_ref[:, lanes] * (gate * sigmoid(gate))).astype(bf16)


def send_kernel(tp_ref, intra_ref, qe_ref, state_ref, gate_hbm, gain_hbm, send_ref, gate_ref, gain_ref, sem):
    half = send_ref.shape[0]
    at = pl.ds(pl.multiple_of((1 - tp_ref[0]) * half, half), half)
    copies = fetch(
        [
            pltpu.make_async_copy(gate_hbm.at[at], gate_ref, sem.at[0]),
            pltpu.make_async_copy(gain_hbm, gain_ref, sem.at[1]),
        ]
    )
    for copy in copies:
        copy.wait()
    for h in range(state_ref.shape[0]):
        lanes = slice(h * HEAD_DIM, (h + 1) * HEAD_DIM)
        send_ref[:, lanes] = mixed_head(h, at, intra_ref, qe_ref, state_ref, gate_ref, gain_ref)


def keep_kernel(
    tp_ref, intra_ref, qe_ref, state_ref, gate_hbm, gain_hbm, w_hbm, acc_ref, gate_ref, gain_ref, mix_ref, w_ref, sem
):
    half, width = acc_ref.shape
    channels = mix_ref.shape[1]
    own = tp_ref[0]
    at = pl.ds(pl.multiple_of(own * half, half), half)
    copies = fetch(
        [
            pltpu.make_async_copy(gate_hbm.at[at], gate_ref, sem.at[0]),
            pltpu.make_async_copy(gain_hbm, gain_ref, sem.at[1]),
        ]
    )
    block = width // COLUMNS
    from_row = pl.ds(pl.multiple_of(own * channels, channels), channels)
    weights = fetch(
        [
            pltpu.make_async_copy(
                w_hbm.at[from_row, n * block : (n + 1) * block],
                w_ref.at[:, n * block : (n + 1) * block],
                sem.at[2 + n],
            )
            for n in range(COLUMNS)
        ]
    )
    for copy in copies:
        copy.wait()
    for h in range(state_ref.shape[0]):
        lanes = slice(h * HEAD_DIM, (h + 1) * HEAD_DIM)
        mix_ref[:, lanes] = mixed_head(h, at, intra_ref, qe_ref, state_ref, gate_ref, gain_ref)
    for n in range(COLUMNS):
        weights[n].wait()
        lanes = slice(n * block, (n + 1) * block)
        acc_ref[:, lanes] = dot(mix_ref[...], w_ref[:, lanes])


def slots_of(routing, capacity):
    count, top = routing.shape
    t = lax.broadcasted_iota(jnp.int32, (count, count), 0)
    s = lax.broadcasted_iota(jnp.int32, (count, count), 1)
    before = jnp.where(t > s, 1.0, 0.0).astype(bf16)
    lane = lax.broadcasted_iota(jnp.int32, (count, 128), 1)
    taken = jnp.zeros((1, 128), f32)
    slots = []
    for k in range(top):
        expert = routing[:, k : k + 1]
        named = jnp.where(lane == expert, 1.0, 0.0)
        rank = dot(before, named.astype(bf16)) + taken
        rank = jnp.sum(named * rank, axis=1, keepdims=True)
        slots.append(expert * capacity + rank.astype(jnp.int32))
        taken = taken + jnp.sum(named, axis=0, keepdims=True)
    return slots


def project_kernel(
    tp_ref, recv_ref, acc_ref, route_ref, w_hbm, res_hbm, gain_hbm, upd_ref, box_hbm,
    w_ref, res_ref, gain_ref, box_ref, sem, *, capacity,
):
    half, width = acc_ref.shape
    channels = recv_ref.shape[1]
    other = 1 - tp_ref[0]
    block = width // COLUMNS
    from_row = pl.ds(pl.multiple_of(other * channels, channels), channels)
    weights = fetch(
        [
            pltpu.make_async_copy(
                w_hbm.at[from_row, n * block : (n + 1) * block],
                w_ref.at[:, n * block : (n + 1) * block],
                sem.at[2 + n],
            )
            for n in range(COLUMNS)
        ]
    )
    copies = fetch(
        [
            pltpu.make_async_copy(res_hbm, res_ref, sem.at[0]),
            pltpu.make_async_copy(gain_hbm, gain_ref, sem.at[1]),
        ]
    )
    lane = lax.broadcasted_iota(jnp.int32, (half, box_ref.shape[0]), 1)
    chosen = jnp.zeros(lane.shape, f32)
    for slot in slots_of(route_ref[...], capacity):
        chosen = chosen + jnp.where(lane == slot, 1.0, 0.0)
    chosen = chosen.astype(bf16)
    square = jnp.zeros((half, 1), f32)
    recv = recv_ref[...]
    for n in range(COLUMNS):
        lanes = slice(n * block, (n + 1) * block)
        weights[n].wait()
        if n == 0:
            for copy in copies:
                copy.wait()
        updated = (res_ref[:, lanes].astype(f32) + (acc_ref[:, lanes] + dot(recv, w_ref[:, lanes]))).astype(bf16)
        upd_ref[:, lanes] = updated
        updated = updated.astype(f32)
        square = square + jnp.sum(updated * updated, axis=-1, keepdims=True)
    scale = lax.rsqrt(square * (1.0 / width) + epsilon)
    stores = []
    for n in range(COLUMNS):
        lanes = slice(n * block, (n + 1) * block)
        normed = (upd_ref[:, lanes].astype(f32) * scale * gain_ref[:, lanes]).astype(bf16)
        box_ref[:, lanes] = dot(chosen, normed, TN).astype(bf16)
        stores.append(
            pltpu.make_async_copy(box_ref.at[:, lanes], box_hbm.at[:, lanes], sem.at[2 + COLUMNS + n])
        )
        stores[n].start()
    for copy in stores:
        copy.wait()


def expert_kernel(
    x_ref, g0_hbm, u0_hbm, d0_hbm, g1_hbm, u1_hbm, d1_hbm, out_hbm, g_ref, u_ref, d_ref, hid_ref, out_ref, sem
):
    units = g0_hbm.shape[1]
    width = d0_hbm.shape[1]
    block = 256
    parts = units // block
    ups = []
    for side, (g_hbm, u_hbm) in enumerate(((g0_hbm, u0_hbm), (g1_hbm, u1_hbm))):
        for j in range(parts):
            i = side * parts + j
            here = slice(j * block, (j + 1) * block)
            there = slice(i * block, (i + 1) * block)
            ups.append(
                fetch(
                    [
                        pltpu.make_async_copy(g_hbm.at[:, here], g_ref.at[:, there], sem.at[2 * i]),
                        pltpu.make_async_copy(u_hbm.at[:, here], u_ref.at[:, there], sem.at[2 * i + 1]),
                    ]
                )
            )
    base = 4 * parts
    downs = fetch(
        [
            pltpu.make_async_copy(d0_hbm, d_ref.at[:units], sem.at[base]),
            pltpu.make_async_copy(d1_hbm, d_ref.at[units:], sem.at[base + 1]),
        ]
    )
    x = x_ref[...]
    for i in range(2 * parts):
        lanes = slice(i * block, (i + 1) * block)
        for copy in ups[i]:
            copy.wait()
        gate = dot(x, g_ref[:, lanes])
        hid_ref[:, lanes] = (gate * sigmoid(gate) * dot(x, u_ref[:, lanes])).astype(bf16)
    for copy in downs:
        copy.wait()
    block = width // COLUMNS
    stores = []
    for n in range(COLUMNS):
        lanes = slice(n * block, (n + 1) * block)
        out_ref[:, lanes] = dot(hid_ref[...], d_ref[:, lanes]).astype(bf16)
        stores.append(pltpu.make_async_copy(out_ref.at[:, lanes], out_hbm.at[:, lanes], sem.at[base + 2 + n]))
        stores[n].start()
    for copy in stores:
        copy.wait()


def combine_kernel(route_ref, weight_ref, back_ref, upd_ref, out_ref, *, capacity):
    lane = lax.broadcasted_iota(jnp.int32, (upd_ref.shape[0], back_ref.shape[0]), 1)
    chosen = jnp.zeros(lane.shape, f32)
    for k, slot in enumerate(slots_of(route_ref[...], capacity)):
        chosen = chosen + jnp.where(lane == slot, weight_ref[:, k : k + 1], 0.0)
    hi, lo = split(chosen)
    back = back_ref[...]
    out_ref[...] = (upd_ref[...].astype(f32) + (dot(hi, back) + dot(lo, back))).astype(bf16)


HBM = pl.BlockSpec(memory_space=pltpu.HBM)
SMEM = pl.BlockSpec(memory_space=pltpu.SMEM)
VMEM = pl.BlockSpec(memory_space=pltpu.VMEM)


def call(kernel, name, ins, outs, scratch=(), mib=16):
    run = pl.pallas_call(
        kernel,
        in_specs=ins,
        out_specs=[spec for spec, _ in outs],
        out_shape=[
            pltpu.HBM(shape.shape, shape.dtype) if spec is HBM else shape for spec, shape in outs
        ],
        scratch_shapes=list(scratch),
        compiler_params=pltpu.CompilerParams(vmem_limit_bytes=mib * 1024 * 1024),
        name=name,
    )

    def placed(*args):
        return run(
            *(
                pltpu.with_memory_space_constraint(arg, pltpu.HBM) if spec is HBM else arg
                for spec, arg in zip(ins, args)
            )
        )

    return placed


def body(
    query,
    forget_logit,
    value,
    out_gate,
    lower_bound,
    head_gain,
    residual_in,
    w_out,
    ffn_gain,
    routing,
    route_weight,
    expert_gate,
    expert_up,
    expert_down,
):
    shape = jax.ShapeDtypeStruct
    dma = pltpu.SemaphoreType.DMA
    ranks = lax.axis_size("sp")
    sides = lax.axis_size("tp")
    length, channels = query.shape
    heads = channels // HEAD_DIM
    rows = channels // ranks
    half = length // sides
    width = w_out.shape[1]
    top = routing.shape[1]
    capacity = 2 * half * top // ranks
    slots = ranks * capacity
    units = expert_gate.shape[2]
    tp = lax.axis_index("tp").reshape(1)
    swap = [(i, i ^ 1) for i in range(sides)]

    weights = (expert_gate[0], expert_up[0], expert_down[0])
    others = tuple(lax.ppermute(w, "tp", swap) for w in weights)

    intra, qe, packed = call(
        functools.partial(local_kernel, rows=rows),
        "local",
        [HBM] * 4,
        [
            (VMEM, shape((length, channels), f32)),
            (VMEM, shape((length, channels), bf16)),
            (VMEM, shape((ranks, rows + TAIL, HEAD_DIM), bf16)),
        ],
        [pltpu.VMEM((length, channels), bf16)] * 3
        + [pltpu.VMEM((1, channels), f32), dma((3 * GROUPS + 1,))],
    )(query, forget_logit, value, lower_bound.reshape(1, -1))

    gathered = lax.all_to_all(packed, "sp", split_axis=0, concat_axis=0, tiled=True)
    (prior,) = call(
        functools.partial(scan_kernel, rows=rows),
        "scan",
        [VMEM],
        [(VMEM, shape((ranks, rows, HEAD_DIM), bf16))],
    )(gathered)
    carried = lax.all_to_all(prior, "sp", split_axis=0, concat_axis=0, tiled=True)

    mix_args = (
        tp,
        intra,
        qe,
        carried.reshape(heads, HEAD_DIM, HEAD_DIM),
        out_gate,
        head_gain.reshape(1, -1),
    )
    mix_specs = [SMEM, VMEM, VMEM, VMEM, HBM, HBM]
    mix_scratch = [pltpu.VMEM((half, channels), bf16), pltpu.VMEM((1, channels), f32)]
    (send,) = call(
        send_kernel,
        "send",
        mix_specs,
        [(VMEM, shape((half, channels), bf16))],
        mix_scratch + [dma((2,))],
    )(*mix_args)
    recv = lax.ppermute(send, "tp", swap)
    (partial,) = call(
        keep_kernel,
        "keep",
        mix_specs + [HBM],
        [(VMEM, shape((half, width), f32))],
        mix_scratch
        + [pltpu.VMEM((half, channels), bf16), pltpu.VMEM((channels, width), bf16), dma((2 + COLUMNS,))],
    )(*mix_args, w_out)
    updated, outbox = call(
        functools.partial(project_kernel, capacity=capacity),
        "project",
        [SMEM, VMEM, VMEM, VMEM, HBM, HBM, HBM],
        [(VMEM, shape((half, width), bf16)), (HBM, shape((slots, width), bf16))],
        [
            pltpu.VMEM((channels, width), bf16),
            pltpu.VMEM((half, width), bf16),
            pltpu.VMEM((1, width), f32),
            pltpu.VMEM((slots, width), bf16),
            dma((2 + 2 * COLUMNS,)),
        ],
    )(tp, recv, partial, routing, w_out, residual_in, ffn_gain.reshape(1, -1))

    arrived = lax.all_to_all(
        outbox.reshape(ranks, capacity, width), "sp", split_axis=0, concat_axis=0, tiled=True
    )
    (expert_out,) = call(
        expert_kernel,
        "experts",
        [VMEM] + [HBM] * 6,
        [(HBM, shape((slots, width), bf16))],
        [pltpu.VMEM((width, 2 * units), bf16)] * 2
        + [
            pltpu.VMEM((2 * units, width), bf16),
            pltpu.VMEM((slots, 2 * units), bf16),
            pltpu.VMEM((slots, width), bf16),
            dma((4 * (units // 256) + 2 + COLUMNS,)),
        ],
        32,
    )(arrived.reshape(slots, width), *weights, *others)

    returned = lax.all_to_all(
        expert_out.reshape(ranks, capacity, width), "sp", split_axis=0, concat_axis=0, tiled=True
    )
    (layer_out,) = call(
        functools.partial(combine_kernel, capacity=capacity),
        "combine",
        [VMEM] * 4,
        [(VMEM, shape((half, width), bf16))],
    )(routing, route_weight, returned.reshape(slots, width), updated)
    return layer_out


def solution(mesh):
    placed = (
        P("sp", "tp"),
        P("sp", "tp"),
        P("sp", "tp"),
        P("sp", "tp"),
        P("tp"),
        P("tp"),
        P(("sp", "tp"), None),
        P(),
        P(),
        P(("sp", "tp"), None),
        P(("sp", "tp"), None),
        P("sp", None, "tp"),
        P("sp", None, "tp"),
        P("sp", "tp", None),
    )
    return jax.shard_map(
        body, mesh=mesh, in_specs=placed, out_specs=P(("sp", "tp"), None), check_vma=False
    )
```

time: 126 us -> 115 us (0.913)
  local copies, waits for them, and re-layouts: 13.9 us -> 0.2 us
  Pallas kernels: 19.6 us -> 22.4 us
    unnamed x36 -> x6, local copies, waits for them, and re-layouts: 13.9 us -> 0.2 us
    pallas_call x6 -> x7, Pallas kernels: 19.6 us -> 22.4 us  [placed(): run(*(pltpu.with_memory_space_constraint(arg, pltpu.HBM) if spec is HBM e...]
  transfers between devices with their start and end apart: 7 -> 7, of which waited for: 4 -> 3; matrix products, arithmetic and copies ran while one was open for 0% -> 0% of each run, Pallas kernels for 3% -> 7%
where the time goes in v2:
time: 115 us; the launch traced here: 114 us
  waiting for transfers between devices  60 us (52%)
  Pallas kernels  22.4 us (19%)
  blocking collectives  16.7 us (15%)
  starting transfers between devices  14.8 us (13%)
    all_to_all x1, waiting for transfers between devices, body(): lax.all_to_all(outbox.reshape(ranks, capacity, width), 'sp', split_axis=0...  26.5 us
    all_to_all x1, waiting for transfers between devices, body(): lax.all_to_all(expert_out.reshape(ranks, capacity, width), 'sp', split_ax...  25.1 us
    pallas_call x7, Pallas kernels, placed(): run(*(pltpu.with_memory_space_constraint(arg, pltpu.HBM) if spec is HBM e...  22.4 us
    all_to_all x1, blocking collectives, body(): lax.all_to_all(packed, 'sp', split_axis=0, concat_axis=0, tiled=True)  16.7 us
    all_to_all x1, waiting for transfers between devices, body(): lax.all_to_all(prior, 'sp', split_axis=0, concat_axis=0, tiled=True)  8.37 us
    all_to_all x1, starting transfers between devices, body(): lax.all_to_all(expert_out.reshape(ranks, capacity, width), 'sp', split_ax...  5.34 us
    all_to_all x1, starting transfers between devices, body(): lax.all_to_all(outbox.reshape(ranks, capacity, width), 'sp', split_axis=0...  4.41 us
    all_to_all x1, starting transfers between devices, body(): lax.all_to_all(prior, 'sp', split_axis=0, concat_axis=0, tiled=True)  4.41 us
  transfers between devices with their start and end apart: 7, of which 3 were waited for; matrix products, arithmetic and copies ran while one was open for 0% of the time, Pallas kernels for 7%

profile of v2, /device:TPU:8, one launch (start us, length us, event | category | flops | bytes accessed | tf_op | source)
XLA Modules:
  0.0 114.3 jit_solution(1564009299993678137)
XLA Ops:
  0.0 0.0 copy-start
  0.0 4.2 %local.1 = (f32[128,1024]{1,0:T(8,128)S(1)}, bf16[128,1024]{1,0:T(8,128)(2,1)S(1)}, bf16[16,72,128]{2,1,0:T(8,128)(2,1)S(1)}) custom-call(bf16[128,1024]{1,0:T(8,128)(2,1)} %q_hbm.1, bf16[128,1024]{1,0:T(8,128)(2,1)} %f_hbm.1, bf16[128,1024]{1,0:T(8,128)(2,1)} %v_hbm.1, f32[1,1024]{1,0:T(1,128)} %bitcast.21), custom_call_target="tpu_custom_call" | custom-call | tf_op jit(solution)/shard_map/local/pallas_call | solution.py:322
  4.2 16.7 %all_to_all.20.in_ref = bf16[16,72,128]{2,1,0:T(8,128)(2,1)S(1)} all-to-all(bf16[16,72,128]{2,1,0:T(8,128)(2,1)S(1)} %get-tuple-element.12), channel_id=1, replica_groups=mesh['sp'=16,'tp'=2] {'sp'}, dimensions={0} | all-to-all | bytes 589824 | tf_op jit(solution)/shard_map/all_to_all | solution.py:380
  21.0 0.8 scan.1
  21.8 4.4 %all-to-all-start.1 = ((bf16[16,64,128]{2,1,0:T(8,128)(2,1)}), bf16[16,64,128]{2,1,0:T(8,128)(2,1)S(1)}, u32[]{:S(2)}, u32[]{:S(2)}) async-start(bf16[16,64,128]{2,1,0:T(8,128)(2,1)} %scan.1), calls=%async_computation.1 | async-start | bytes 524288 | tf_op jit(solution)/shard_map/all_to_all | solution.py:387
  26.2 0.0 collective-permute-start.1
  26.2 8.4 %all-to-all-done.1 = bf16[16,64,128]{2,1,0:T(8,128)(2,1)S(1)} async-done(((bf16[16,64,128]{2,1,0:T(8,128)(2,1)}), bf16[16,64,128]{2,1,0:T(8,128)(2,1)S(1)}, u32[]{:S(2)}, u32[]{:S(2)}) %all-to-all-start.1) | async-done | bytes 262176 | tf_op jit(solution)/shard_map/all_to_all | solution.py:387
  34.6 1.3 %send.1 = bf16[64,1024]{1,0:T(8,128)(2,1)S(1)} custom-call(s32[1]{0:T(128)} %bitcast.tp_ref, f32[128,1024]{1,0:T(8,128)S(1)} %get-tuple-element.10.intra_ref, bf16[128,1024]{1,0:T(8,128)(2,1)S(1)} %get-tuple-element.11.qe_ref, bf16[8,128,128]{2,1,0:T(8,128)(2,1)S(1)} %bitcast.14, bf16[128,1024]{1,0:T(8,128)(2,1)} %gate_hbm.3, f32[1,1024]{1,0:T(1,128)} %bitcast.18), custom_call_target="tpu_custom_call" | custom-call | tf_op jit(solution)/shard_map/send/pallas_call | solution.py:322
  35.9 0.1 collective-permute-start
  35.9 0.5 collective-permute-start.2
  36.4 0.1 collective-permute-start.3
  36.5 0.0 copy-done
  36.5 0.1 copy.16.route_ref
  36.6 2.6 %keep.1.acc_ref = f32[64,2048]{1,0:T(8,128)S(1)} custom-call(s32[1]{0:T(128)} %bitcast.tp_ref, f32[128,1024]{1,0:T(8,128)S(1)} %get-tuple-element.10.intra_ref, bf16[128,1024]{1,0:T(8,128)(2,1)S(1)} %get-tuple-element.11.qe_ref, bf16[8,128,128]{2,1,0:T(8,128)(2,1)S(1)} %bitcast.15, bf16[128,1024]{1,0:T(8,128)(2,1)} %gate_hbm.3, f32[1,1024]{1,0:T(1,128)} %bitcast.19, ...), custom_call_target="tpu_custom_call" | custom-call | tf_op jit(solution)/shard_map/keep/pallas_call | solution.py:322
  39.3 0.0 collective-permute-done.recv_ref
  39.3 5.1 %project.1 = (bf16[64,2048]{1,0:T(8,128)(2,1)S(1)}, bf16[256,2048]{1,0:T(8,128)(2,1)}) custom-call(s32[1]{0:T(128)} %bitcast.tp_ref, bf16[64,1024]{1,0:T(8,128)(2,1)S(1)} %collective-permute-done.recv_ref, f32[64,2048]{1,0:T(8,128)S(1)} %keep.1.acc_ref, s32[64,2]{1,0:T(8,128)S(1)} %copy.16.route_ref, bf16[2048,2048]{1,0:T(8,128)(2,1)} %w_hbm.3, ...), custom_call_target="tpu_custom_call" | custom-call | tf_op jit(solution)/shard_map/project/pallas_call | solution.py:322
  44.4 4.4 %all-to-all-start.2 = ((bf16[16,16,2048]{2,1,0:T(8,128)(2,1)}), bf16[16,16,2048]{2,1,0:T(8,128)(2,1)S(1)}, u32[]{:S(2)}, u32[]{:S(2)}) async-start(bf16[16,16,2048]{2,1,0:T(8,128)(2,1)} %bitcast.17), calls=%async_computation.2 | async-start | bytes 2097152 | tf_op jit(solution)/shard_map/all_to_all | solution.py:429
  48.8 0.0 collective-permute-done.1.g1_hbm
  48.8 0.0 collective-permute-done.2.u1_hbm
  48.8 0.0 collective-permute-done.3.d1_hbm
  48.8 26.5 %all-to-all-done.2 = bf16[16,16,2048]{2,1,0:T(8,128)(2,1)S(1)} async-done(((bf16[16,16,2048]{2,1,0:T(8,128)(2,1)}), bf16[16,16,2048]{2,1,0:T(8,128)(2,1)S(1)}, u32[]{:S(2)}, u32[]{:S(2)}) %all-to-all-start.2) | async-done | bytes 1048608 | tf_op jit(solution)/shard_map/all_to_all | solution.py:429
  75.4 6.8 %experts.1 = bf16[256,2048]{1,0:T(8,128)(2,1)} custom-call(bf16[256,2048]{1,0:T(8,128)(2,1)S(1)} %bitcast.12, bf16[2048,512]{1,0:T(8,128)(2,1)} %bitcast.7.g0_hbm, bf16[2048,512]{1,0:T(8,128)(2,1)} %bitcast.8.u0_hbm, bf16[512,2048]{1,0:T(8,128)(2,1)} %bitcast.9.d0_hbm, bf16[2048,512]{1,0:T(8,128)(2,1)} %collective-permute-done.1.g1_hbm, ...), custom_call_target="tpu_custom_call" | custom-call | tf_op jit(solution)/shard_map/experts/pallas_call | solution.py:322
  82.2 0.0 copy-start.1
  82.2 5.3 %all-to-all-start.3 = ((bf16[16,16,2048]{2,1,0:T(8,128)(2,1)}), bf16[16,16,2048]{2,1,0:T(8,128)(2,1)S(1)}, u32[]{:S(2)}, u32[]{:S(2)}) async-start(bf16[16,16,2048]{2,1,0:T(8,128)(2,1)} %bitcast.16), calls=%async_computation.3 | async-start | bytes 2097152 | tf_op jit(solution)/shard_map/all_to_all | solution.py:447
  87.5 0.0 copy-done.1
  87.5 0.1 copy.17.weight_ref
  87.6 25.1 %all-to-all-done.3 = bf16[16,16,2048]{2,1,0:T(8,128)(2,1)S(1)} async-done(((bf16[16,16,2048]{2,1,0:T(8,128)(2,1)}), bf16[16,16,2048]{2,1,0:T(8,128)(2,1)S(1)}, u32[]{:S(2)}, u32[]{:S(2)}) %all-to-all-start.3) | async-done | bytes 1048608 | tf_op jit(solution)/shard_map/all_to_all | solution.py:447
  112.8 1.6 %combine.1 = bf16[64,2048]{1,0:T(8,128)(2,1)} custom-call(s32[64,2]{1,0:T(8,128)S(1)} %copy.16.route_ref, f32[64,2]{1,0:T(8,128)S(1)} %copy.17.weight_ref, bf16[256,2048]{1,0:T(8,128)(2,1)S(1)} %bitcast.13, bf16[64,2048]{1,0:T(8,128)(2,1)S(1)} %get-tuple-element.14.upd_ref), custom_call_target="tpu_custom_call" | custom-call | tf_op jit(solution)/shard_map/combine/pallas_call | solution.py:322
Async XLA Ops:
  0.0 36.5 %copy-start = (s32[64,2]{0,1:T(2,128)S(1)}, s32[64,2]{0,1:T(2,128)}, u32[]{:S(2)}) copy-start(s32[64,2]{0,1:T(2,128)} %param.23) | copy-start | bytes 1540
  21.8 12.8 %all-to-all-start.1 = ((bf16[16,64,128]{2,1,0:T(8,128)(2,1)}), bf16[16,64,128]{2,1,0:T(8,128)(2,1)S(1)}, u32[]{:S(2)}, u32[]{:S(2)}) async-start(bf16[16,64,128]{2,1,0:T(8,128)(2,1)} %scan.1), calls=%async_computation.1 | async-start | bytes 524288 | tf_op jit(solution)/shard_map/all_to_all | solution.py:387
  26.2 22.6 %collective-permute-start.1 = (bf16[2048,512]{1,0:T(8,128)(2,1)}, bf16[2048,512]{1,0:T(8,128)(2,1)}, u32[]{:S(2)}, u32[]{:S(2)}) collective-permute-start(bf16[2048,512]{1,0:T(8,128)(2,1)} %bitcast.7.g0_hbm), channel_id=1, source_target_pairs={{0,1},{1,0},{2,3},{3,2},{4,5},{5,4},{6,7},{7,6},{8,9},{9,8},{10,11... | collective-permute-start | bytes 6291464 | tf_op jit(solution)/shard_map/ppermute | solution.py:365
  35.9 3.4 %collective-permute-start = (bf16[64,1024]{1,0:T(8,128)(2,1)S(1)}, bf16[64,1024]{1,0:T(8,128)(2,1)S(1)}, u32[]{:S(2)}, u32[]{:S(2)}) collective-permute-start(bf16[64,1024]{1,0:T(8,128)(2,1)S(1)} %send.1), channel_id=1, source_target_pairs={{0,1},{1,0},{2,3},{3,2},{4,5},{5,4},{6,7},{7,6},{8,9},{9,8},{10,11... | collective-permute-start | bytes 393224 | tf_op jit(solution)/shard_map/ppermute | solution.py:406
  35.9 12.9 %collective-permute-start.2 = (bf16[2048,512]{1,0:T(8,128)(2,1)}, bf16[2048,512]{1,0:T(8,128)(2,1)}, u32[]{:S(2)}, u32[]{:S(2)}) collective-permute-start(bf16[2048,512]{1,0:T(8,128)(2,1)} %bitcast.8.u0_hbm), channel_id=1, source_target_pairs={{0,1},{1,0},{2,3},{3,2},{4,5},{5,4},{6,7},{7,6},{8,9},{9,8},{10,11... | collective-permute-start | bytes 6291464 | tf_op jit(solution)/shard_map/ppermute | solution.py:365
  36.4 12.4 %collective-permute-start.3 = (bf16[512,2048]{1,0:T(8,128)(2,1)}, bf16[512,2048]{1,0:T(8,128)(2,1)}, u32[]{:S(2)}, u32[]{:S(2)}) collective-permute-start(bf16[512,2048]{1,0:T(8,128)(2,1)} %bitcast.9.d0_hbm), channel_id=1, source_target_pairs={{0,1},{1,0},{2,3},{3,2},{4,5},{5,4},{6,7},{7,6},{8,9},{9,8},{10,11... | collective-permute-start | bytes 6291464 | tf_op jit(solution)/shard_map/ppermute | solution.py:365
  44.4 31.0 %all-to-all-start.2 = ((bf16[16,16,2048]{2,1,0:T(8,128)(2,1)}), bf16[16,16,2048]{2,1,0:T(8,128)(2,1)S(1)}, u32[]{:S(2)}, u32[]{:S(2)}) async-start(bf16[16,16,2048]{2,1,0:T(8,128)(2,1)} %bitcast.17), calls=%async_computation.2 | async-start | bytes 2097152 | tf_op jit(solution)/shard_map/all_to_all | solution.py:429
  82.2 5.4 %copy-start.1 = (f32[64,2]{0,1:T(2,128)S(1)}, f32[64,2]{0,1:T(2,128)}, u32[]{:S(2)}) copy-start(f32[64,2]{0,1:T(2,128)} %param.24) | copy-start | bytes 1540
  82.2 30.6 %all-to-all-start.3 = ((bf16[16,16,2048]{2,1,0:T(8,128)(2,1)}), bf16[16,16,2048]{2,1,0:T(8,128)(2,1)S(1)}, u32[]{:S(2)}, u32[]{:S(2)}) async-start(bf16[16,16,2048]{2,1,0:T(8,128)(2,1)} %bitcast.16), calls=%async_computation.3 | async-start | bytes 2097152 | tf_op jit(solution)/shard_map/all_to_all | solution.py:447

commit v3 on v2

v3 whole, which is shorter than its diff:
```python
import functools

import jax
import jax.numpy as jnp
from jax import lax
from jax.experimental import pallas as pl
from jax.experimental.pallas import tpu as pltpu
from jax.sharding import PartitionSpec as P


HEAD_DIM = 128
TAIL = 8
GROUPS = 4
COLUMNS = 4
epsilon = 1e-06
f32 = jnp.float32
bf16 = jnp.bfloat16

NN = (((1,), (0,)), ((), ()))
NT = (((1,), (1,)), ((), ()))
TN = (((0,), (0,)), ((), ()))


def dot(a, b, dims=NN):
    return lax.dot_general(a, b, dims, preferred_element_type=f32)


def split(x):
    hi = x.astype(bf16)
    return hi, (x - hi.astype(f32)).astype(bf16)


def sigmoid(x):
    return 1.0 / (1.0 + jnp.exp(-x))


def fetch(copies):
    for copy in copies:
        copy.start()
    return copies


def local_kernel(
    q_hbm, f_hbm, v_hbm, low_hbm, w_hbm, intra_ref, qe_ref, out_ref, w_ref, q_ref, f_ref, v_ref, low_ref, sem, *, rows
):
    length, channels = q_ref.shape
    per = HEAD_DIM // rows
    block = channels // GROUPS
    low = pltpu.make_async_copy(low_hbm, low_ref, sem.at[3 * GROUPS])
    low.start()
    copies = []
    for g in range(GROUPS):
        lanes = slice(g * block, (g + 1) * block)
        copies.append(
            fetch(
                [
                    pltpu.make_async_copy(hbm.at[:, lanes], ref.at[:, lanes], sem.at[3 * g + i])
                    for i, (hbm, ref) in enumerate(((f_hbm, f_ref), (q_hbm, q_ref), (v_hbm, v_ref)))
                ]
            )
        )
    ahead = pltpu.make_async_copy(w_hbm, w_ref, sem.at[3 * GROUPS + 1])
    ahead.start()
    t = lax.broadcasted_iota(jnp.int32, (length, length), 0)
    s = lax.broadcasted_iota(jnp.int32, (length, length), 1)
    causal = t >= s
    tri = jnp.where(causal, 1.0, 0.0).astype(bf16)
    place = lax.broadcasted_iota(jnp.int32, (TAIL, HEAD_DIM), 0)
    low.wait()
    for g in range(GROUPS):
        group = slice(g * block, (g + 1) * block)
        for copy in copies[g]:
            copy.wait()
        gap = 1.0 - low_ref[:, group]
        key_gate = gap * sigmoid(-f_ref[:, group].astype(f32))
        hi, lo = split(jnp.log1p(-key_gate))
        total = dot(tri, hi) + dot(tri, lo)
        middle = total[length // 2 - 1 : length // 2]
        last = total[length - 1 : length]
        query = q_ref[:, group].astype(f32)
        scaled_query = (query * jnp.exp(total - middle)).astype(bf16)
        scaled_key = (key_gate * jnp.exp(middle - total)).astype(bf16)
        weighted = (key_gate * jnp.exp(last - total)).astype(bf16)
        qe_ref[:, group] = (query * jnp.exp(total)).astype(bf16)
        last_hi, last_lo = split(last)
        for i in range(block // HEAD_DIM):
            h = g * (block // HEAD_DIM) + i
            inner = slice(i * HEAD_DIM, (i + 1) * HEAD_DIM)
            lanes = slice(h * HEAD_DIM, (h + 1) * HEAD_DIM)
            value = v_ref[:, lanes]
            state = dot(value, weighted[:, inner], TN).astype(bf16)
            scores = dot(scaled_query[:, inner], scaled_key[:, inner], NT)
            scores = jnp.where(causal, scores, 0.0).astype(bf16)
            intra_ref[:, lanes] = dot(scores, value)
            tail = jnp.where(
                place == 0,
                last_hi[:, inner].astype(f32),
                jnp.where(place == 1, last_lo[:, inner].astype(f32), 0.0),
            ).astype(bf16)
            for j in range(per):
                out_ref[h * per + j, :rows] = state[j * rows : (j + 1) * rows]
                out_ref[h * per + j, rows:] = tail
    ahead.wait()


def scan_kernel(in_ref, out_ref, *, rows):
    state = jnp.zeros((rows, HEAD_DIM), f32)
    for i in range(in_ref.shape[0]):
        out_ref[i] = state.astype(bf16)
        tail = in_ref[i, rows:].astype(f32)
        decay = jnp.exp(tail[0:1] + tail[1:2])
        state = state * decay + in_ref[i, :rows].astype(f32)


def mixed_head(h, at, intra_ref, qe_ref, state_ref, gate_ref, gain_ref):
    lanes = slice(h * HEAD_DIM, (h + 1) * HEAD_DIM)
    out = intra_ref[at, lanes] + dot(qe_ref[at, lanes], state_ref[h], NT)
    scale = lax.rsqrt(jnp.mean(out * out, axis=-1, keepdims=True) + epsilon)
    gate = gate_ref[:, lanes].astype(f32)
    return (out * scale * gain_ref[:, lanes] * (gate * sigmoid(gate))).astype(bf16)


def send_kernel(tp_ref, intra_ref, qe_ref, state_ref, gate_hbm, gain_hbm, send_ref, gate_ref, gain_ref, sem):
    half = send_ref.shape[0]
    at = pl.ds(pl.multiple_of((1 - tp_ref[0]) * half, half), half)
    copies = fetch(
        [
            pltpu.make_async_copy(gate_hbm.at[at], gate_ref, sem.at[0]),
            pltpu.make_async_copy(gain_hbm, gain_ref, sem.at[1]),
        ]
    )
    for copy in copies:
        copy.wait()
    for h in range(state_ref.shape[0]):
        lanes = slice(h * HEAD_DIM, (h + 1) * HEAD_DIM)
        send_ref[:, lanes] = mixed_head(h, at, intra_ref, qe_ref, state_ref, gate_ref, gain_ref)


def keep_kernel(
    tp_ref, intra_ref, qe_ref, state_ref, gate_hbm, gain_hbm, w_ref, g_hbm, u_hbm, acc_ref, g_ref, u_ref,
    gate_ref, gain_ref, mix_ref, sem,
):
    channels = mix_ref.shape[1]
    half = mix_ref.shape[0]
    own = tp_ref[0]
    at = pl.ds(pl.multiple_of(own * half, half), half)
    copies = fetch(
        [
            pltpu.make_async_copy(gate_hbm.at[at], gate_ref, sem.at[0]),
            pltpu.make_async_copy(gain_hbm, gain_ref, sem.at[1]),
        ]
    )
    ahead = fetch(
        [
            pltpu.make_async_copy(g_hbm, g_ref, sem.at[2]),
            pltpu.make_async_copy(u_hbm, u_ref, sem.at[3]),
        ]
    )
    for copy in copies:
        copy.wait()
    for h in range(state_ref.shape[0]):
        lanes = slice(h * HEAD_DIM, (h + 1) * HEAD_DIM)
        mix_ref[:, lanes] = mixed_head(h, at, intra_ref, qe_ref, state_ref, gate_ref, gain_ref)
    acc_ref[...] = dot(mix_ref[...], w_ref[pl.ds(pl.multiple_of(own * channels, channels), channels)])
    for copy in ahead:
        copy.wait()


def slots_of(routing, capacity):
    top, count = routing.shape
    s = lax.broadcasted_iota(jnp.int32, (count, count), 0)
    t = lax.broadcasted_iota(jnp.int32, (count, count), 1)
    before = jnp.where(s < t, 1.0, 0.0).astype(bf16)
    place = lax.broadcasted_iota(jnp.int32, (128, count), 0)
    taken = jnp.zeros((128, 1), f32)
    slots = []
    for k in range(top):
        expert = routing[k : k + 1]
        named = jnp.where(place == expert, 1.0, 0.0)
        rank = dot(named.astype(bf16), before) + taken
        rank = jnp.sum(named * rank, axis=0, keepdims=True)
        slots.append(expert * capacity + rank.astype(jnp.int32))
        taken = taken + jnp.sum(named, axis=1, keepdims=True)
    return slots


def project_kernel(
    tp_ref, recv_ref, acc_ref, route_ref, weight_ref, w_ref, res_hbm, gain_hbm, d0_hbm, u1_hbm, d1_hbm,
    upd_ref, hi_ref, lo_ref, box_hbm, d0_ref, u1_ref, d1_ref,
    res_ref, gain_ref, box_ref, sem, *, capacity,
):
    half, width = acc_ref.shape
    channels = recv_ref.shape[1]
    other = 1 - tp_ref[0]
    block = width // COLUMNS
    copies = fetch(
        [
            pltpu.make_async_copy(res_hbm, res_ref, sem.at[0]),
            pltpu.make_async_copy(gain_hbm, gain_ref, sem.at[1]),
        ]
    )
    ahead = fetch(
        [
            pltpu.make_async_copy(hbm, ref, sem.at[2 + COLUMNS + i])
            for i, (hbm, ref) in enumerate(((d0_hbm, d0_ref), (u1_hbm, u1_ref), (d1_hbm, d1_ref)))
        ]
    )
    place = lax.broadcasted_iota(jnp.int32, (box_ref.shape[0], half), 0)
    chosen = jnp.zeros(place.shape, f32)
    weighted = jnp.zeros(place.shape, f32)
    for k, slot in enumerate(slots_of(route_ref[...], capacity)):
        chosen = chosen + jnp.where(place == slot, 1.0, 0.0)
        weighted = weighted + jnp.where(place == slot, weight_ref[k : k + 1], 0.0)
    chosen = chosen.astype(bf16)
    hi_ref[...], lo_ref[...] = split(weighted)
    partial = dot(recv_ref[...], w_ref[pl.ds(pl.multiple_of(other * channels, channels), channels)])
    for copy in copies:
        copy.wait()
    updated = (res_ref[...].astype(f32) + (acc_ref[...] + partial)).astype(bf16)
    upd_ref[...] = updated
    updated = updated.astype(f32)
    scale = lax.rsqrt(jnp.mean(updated * updated, axis=-1, keepdims=True) + epsilon)
    stores = []
    for n in range(COLUMNS):
        lanes = slice(n * block, (n + 1) * block)
        normed = (upd_ref[:, lanes].astype(f32) * scale * gain_ref[:, lanes]).astype(bf16)
        box_ref[:, lanes] = dot(chosen, normed).astype(bf16)
        stores.append(
            pltpu.make_async_copy(box_ref.at[:, lanes], box_hbm.at[:, lanes], sem.at[2 + n])
        )
        stores[n].start()
    for copy in stores:
        copy.wait()
    for copy in ahead:
        copy.wait()


def expert_kernel(x_ref, g0_ref, u0_ref, d0_ref, g1_ref, u1_ref, d1_ref, out_hbm, hid_ref, out_ref, sem):
    units = g0_ref.shape[1]
    width = d0_ref.shape[1]
    block = 256
    x = x_ref[...]
    for side, (g_ref, u_ref) in enumerate(((g0_ref, u0_ref), (g1_ref, u1_ref))):
        for j in range(units // block):
            lanes = slice(j * block, (j + 1) * block)
            gate = dot(x, g_ref[:, lanes])
            hidden = (gate * sigmoid(gate) * dot(x, u_ref[:, lanes])).astype(bf16)
            hid_ref[:, side * units + j * block : side * units + (j + 1) * block] = hidden
    block = width // COLUMNS
    stores = []
    for n in range(COLUMNS):
        lanes = slice(n * block, (n + 1) * block)
        out = dot(hid_ref[:, :units], d0_ref[:, lanes]) + dot(hid_ref[:, units:], d1_ref[:, lanes])
        out_ref[:, lanes] = out.astype(bf16)
        stores.append(pltpu.make_async_copy(out_ref.at[:, lanes], out_hbm.at[:, lanes], sem.at[n]))
        stores[n].start()
    for copy in stores:
        copy.wait()


def combine_kernel(hi_ref, lo_ref, back_ref, upd_ref, out_ref):
    back = back_ref[...]
    out_ref[...] = (
        upd_ref[...].astype(f32) + (dot(hi_ref[...], back, TN) + dot(lo_ref[...], back, TN))
    ).astype(bf16)


HBM = pl.BlockSpec(memory_space=pltpu.HBM)
SMEM = pl.BlockSpec(memory_space=pltpu.SMEM)
VMEM = pl.BlockSpec(memory_space=pltpu.VMEM)
KEPT = pl.BlockSpec(memory_space=pltpu.VMEM)
FIXED = ((HBM, pltpu.HBM), (KEPT, pltpu.VMEM))


def call(kernel, ins, outs, scratch=(), mib=16):
    def fixed(spec):
        return next((space for known, space in FIXED if known is spec), None)

    run = pl.pallas_call(
        kernel,
        in_specs=ins,
        out_specs=[spec for spec, _ in outs],
        out_shape=[
            fixed(spec)(shape.shape, shape.dtype) if fixed(spec) else shape for spec, shape in outs
        ],
        scratch_shapes=list(scratch),
        compiler_params=pltpu.CompilerParams(vmem_limit_bytes=mib * 1024 * 1024),
    )

    def placed(*args):
        return run(
            *(
                pltpu.with_memory_space_constraint(arg, fixed(spec)) if fixed(spec) else arg
                for spec, arg in zip(ins, args)
            )
        )

    return placed


def body(
    query,
    forget_logit,
    value,
    out_gate,
    lower_bound,
    head_gain,
    residual_in,
    w_out,
    ffn_gain,
    routing,
    route_weight,
    expert_gate,
    expert_up,
    expert_down,
):
    shape = jax.ShapeDtypeStruct
    dma = pltpu.SemaphoreType.DMA
    ranks = lax.axis_size("sp")
    sides = lax.axis_size("tp")
    length, channels = query.shape
    heads = channels // HEAD_DIM
    rows = channels // ranks
    half = length // sides
    width = w_out.shape[1]
    top = routing.shape[1]
    capacity = 2 * half * top // ranks
    slots = ranks * capacity
    units = expert_gate.shape[2]
    tp = lax.axis_index("tp").reshape(1)
    swap = [(i, i ^ 1) for i in range(sides)]

    weights = (expert_gate[0], expert_up[0], expert_down[0])
    others = tuple(lax.ppermute(w, "tp", swap) for w in weights)

    intra, qe, packed, w_kept = call(
        functools.partial(local_kernel, rows=rows),
        [HBM] * 5,
        [
            (VMEM, shape((length, channels), f32)),
            (VMEM, shape((length, channels), bf16)),
            (VMEM, shape((ranks, rows + TAIL, HEAD_DIM), bf16)),
            (KEPT, shape(w_out.shape, bf16)),
        ],
        [pltpu.VMEM((length, channels), bf16)] * 3
        + [pltpu.VMEM((1, channels), f32), dma((3 * GROUPS + 2,))],
    )(query, forget_logit, value, lower_bound.reshape(1, -1), w_out)

    packed, tp = lax.optimization_barrier((packed, tp))
    gathered = lax.all_to_all(packed, "sp", split_axis=0, concat_axis=0, tiled=True)
    gathered, others = lax.optimization_barrier((gathered, others))
    (prior,) = call(
        functools.partial(scan_kernel, rows=rows),
        [VMEM],
        [(VMEM, shape((ranks, rows, HEAD_DIM), bf16))],
    )(gathered)
    carried = lax.all_to_all(prior, "sp", split_axis=0, concat_axis=0, tiled=True)

    mix_args = (
        tp,
        intra,
        qe,
        carried.reshape(heads, HEAD_DIM, HEAD_DIM),
        out_gate,
        head_gain.reshape(1, -1),
    )
    mix_specs = [SMEM, VMEM, VMEM, VMEM, HBM, HBM]
    mix_scratch = [pltpu.VMEM((half, channels), bf16), pltpu.VMEM((1, channels), f32)]
    (send,) = call(
        send_kernel, mix_specs, [(VMEM, shape((half, channels), bf16))], mix_scratch + [dma((2,))]
    )(*mix_args)
    recv = lax.ppermute(send, "tp", swap)
    partial, gate_kept, up_kept = call(
        keep_kernel,
        mix_specs + [KEPT, HBM, HBM],
        [(VMEM, shape((half, width), f32))] + [(KEPT, shape((width, units), bf16))] * 2,
        mix_scratch + [pltpu.VMEM((half, channels), bf16), dma((4,))],
    )(*mix_args, w_kept, *weights[:2])
    updated, hi, lo, outbox, *downs = call(
        functools.partial(project_kernel, capacity=capacity),
        [SMEM, VMEM, VMEM, VMEM, VMEM, KEPT] + [HBM] * 5,
        [
            (VMEM, shape((half, width), bf16)),
            (VMEM, shape((slots, half), bf16)),
            (VMEM, shape((slots, half), bf16)),
            (HBM, shape((slots, width), bf16)),
            (KEPT, shape((units, width), bf16)),
            (KEPT, shape((width, units), bf16)),
            (KEPT, shape((units, width), bf16)),
        ],
        [
            pltpu.VMEM((half, width), bf16),
            pltpu.VMEM((1, width), f32),
            pltpu.VMEM((slots, width), bf16),
            dma((5 + COLUMNS,)),
        ],
    )(
        tp,
        recv,
        partial,
        routing.T,
        route_weight.T,
        w_kept,
        residual_in,
        ffn_gain.reshape(1, -1),
        weights[2],
        *others[1:],
    )
    down_kept, other_up, other_down = downs

    arrived = lax.all_to_all(
        outbox.reshape(ranks, capacity, width), "sp", split_axis=0, concat_axis=0, tiled=True
    )
    (expert_out,) = call(
        expert_kernel,
        [VMEM] + [KEPT] * 6,
        [(HBM, shape((slots, width), bf16))],
        [
            pltpu.VMEM((slots, 2 * units), bf16),
            pltpu.VMEM((slots, width), bf16),
            dma((COLUMNS,)),
        ],
    )(arrived.reshape(slots, width), gate_kept, up_kept, down_kept, others[0], other_up, other_down)

    returned = lax.all_to_all(
        expert_out.reshape(ranks, capacity, width), "sp", split_axis=0, concat_axis=0, tiled=True
    )
    (layer_out,) = call(
        combine_kernel, [VMEM] * 4, [(VMEM, shape((half, width), bf16))]
    )(hi, lo, returned.reshape(slots, width), updated)
    return layer_out


def solution(mesh):
    placed = (
        P("sp", "tp"),
        P("sp", "tp"),
        P("sp", "tp"),
        P("sp", "tp"),
        P("tp"),
        P("tp"),
        P(("sp", "tp"), None),
        P(),
        P(),
        P(("sp", "tp"), None),
        P(("sp", "tp"), None),
        P("sp", None, "tp"),
        P("sp", None, "tp"),
        P("sp", "tp", None),
    )

    return jax.shard_map(
        body, mesh=mesh, in_specs=placed, out_specs=P(("sp", "tp"), None), check_vma=False
    )
```

time: 115 us -> 112 us (0.974); the launches traced: 114 us -> 110 us
  blocking collectives: 16.7 us -> 91.1 us
  waiting for transfers between devices: 60 us -> 0.01 us
  starting transfers between devices: 14.8 us -> 0.58 us
  Pallas kernels: 22.4 us -> 17.7 us
    all_to_all x0 -> x3, blocking collectives: none -> 73.7 us  [the longest x1 31.1 us: body(): lax.all_to_all(outbox.reshape(ranks, capacity, width), 'sp', split_axis=0...]
    all_to_all x3 -> x0, waiting for transfers between devices: 60 us -> none  [the longest x1 26.5 us: body(): lax.all_to_all(outbox.reshape(ranks, capacity, width), 'sp', split_axis=0...]
    all_to_all x3 -> x0, starting transfers between devices: 14.2 us -> none  [the longest x1 5.34 us: body(): lax.all_to_all(expert_out.reshape(ranks, capacity, width), 'sp', split_ax...]
    pallas_call x7, Pallas kernels: 22.4 us -> 17.7 us  [placed(): run(*(pltpu.with_memory_space_constraint(arg, fixed(spec)) if fixed(spec)...]
  transfers between devices with their start and end apart: 7 -> 4, of which waited for: 3 -> 0; matrix products, arithmetic and copies ran while one was open for 0% -> 0% of each run, Pallas kernels for 7% -> 6%
where the time goes in v3:
time: 112 us; the launch traced here: 110 us
  blocking collectives  91.1 us (81%)
  Pallas kernels  17.7 us (16%)
    all_to_all x1, blocking collectives, body(): lax.all_to_all(outbox.reshape(ranks, capacity, width), 'sp', split_axis=0...  31.1 us
    all_to_all x1, blocking collectives, body(): lax.all_to_all(expert_out.reshape(ranks, capacity, width), 'sp', split_ax...  29.8 us
    pallas_call x7, Pallas kernels, placed(): run(*(pltpu.with_memory_space_constraint(arg, fixed(spec)) if fixed(spec)...  17.7 us
    all_to_all x1, blocking collectives, body(): lax.all_to_all(packed, 'sp', split_axis=0, concat_axis=0, tiled=True)  17.4 us
    all_to_all x1, blocking collectives, body(): lax.all_to_all(prior, 'sp', split_axis=0, concat_axis=0, tiled=True)  12.8 us
  transfers between devices with their start and end apart: 4, of which 0 were waited for; matrix products, arithmetic and copies ran while one was open for 0% of the time, Pallas kernels for 6%

profile of v3, /device:TPU:8, one launch (start us, length us, event | category | flops | bytes accessed | tf_op | source)
XLA Modules:
  0.0 109.5 jit_solution(7586735295448736424)
XLA Ops:
  0.0 0.0 collective-permute-start
  0.0 0.5 collective-permute-start.1
  0.5 0.0 collective-permute-start.2
  0.5 4.2 %shard_map.136 = (f32[128,1024]{1,0:T(8,128)S(1)}, bf16[128,1024]{1,0:T(8,128)(2,1)S(1)}, bf16[16,72,128]{2,1,0:T(8,128)(2,1)S(1)}, bf16[2048,2048]{1,0:T(8,128)(2,1)S(1)}) custom-call(bf16[128,1024]{1,0:T(8,128)(2,1)} %q_hbm.1, bf16[128,1024]{1,0:T(8,128)(2,1)} %f_hbm.1, bf16[128,1024]{1,0:T(8,128)(2,1)} %v_hbm.1, f32[1,1024]{1,0:T(1,128)} %bitcast.31, ...), custom_call_target="tpu_custom_call" | custom-call | tf_op jit(solution)/shard_map/pallas_call | solution.py:291
  4.8 17.4 %all_to_all.20.in_ref = bf16[16,72,128]{2,1,0:T(8,128)(2,1)S(1)} all-to-all(bf16[16,72,128]{2,1,0:T(8,128)(2,1)S(1)} %get-tuple-element.29), channel_id=1, replica_groups=mesh['sp'=16,'tp'=2] {'sp'}, dimensions={0} | all-to-all | bytes 589824 | tf_op jit(solution)/shard_map/all_to_all | solution.py:350
  22.2 0.0 collective-permute-done.g1_ref
  22.2 0.0 collective-permute-done.1.u1_hbm
  22.2 0.0 collective-permute-done.2.d1_hbm
  22.2 0.1 shard_map.137
  22.3 12.8 %all_to_all.21 = bf16[16,64,128]{2,1,0:T(8,128)(2,1)S(1)} all-to-all(bf16[16,64,128]{2,1,0:T(8,128)(2,1)S(1)} %shard_map.137), channel_id=1, replica_groups=mesh['sp'=16,'tp'=2] {'sp'}, dimensions={0} | all-to-all | bytes 524288 | tf_op jit(solution)/shard_map/all_to_all | solution.py:357
  35.1 1.3 %shard_map.138 = bf16[64,1024]{1,0:T(8,128)(2,1)S(1)} custom-call(s32[1]{0:T(128)} %bitcast.1.tp_ref, f32[128,1024]{1,0:T(8,128)S(1)} %get-tuple-element.27.intra_ref, bf16[128,1024]{1,0:T(8,128)(2,1)S(1)} %get-tuple-element.28.qe_ref, bf16[8,128,128]{2,1,0:T(8,128)(2,1)S(1)} %bitcast.16, bf16[128,1024]{1,0:T(8,128)(2,1)} %gate_hbm.3, f32[1,1024]{1,0:T(1,128)} %bitcast.28), custom_call_target="tpu_custom_call" | custom-call | tf_op jit(solution)/shard_map/pallas_call | solution.py:291
  36.4 0.1 collective-permute-start.3
  36.5 0.0 copy-start
  36.5 0.0 copy-start.1
  36.5 2.4 %shard_map.139 = (f32[64,2048]{1,0:T(8,128)S(1)}, bf16[2048,512]{1,0:T(8,128)(2,1)S(1)}, bf16[2048,512]{1,0:T(8,128)(2,1)S(1)}) custom-call(s32[1]{0:T(128)} %bitcast.1.tp_ref, f32[128,1024]{1,0:T(8,128)S(1)} %get-tuple-element.27.intra_ref, bf16[128,1024]{1,0:T(8,128)(2,1)S(1)} %get-tuple-element.28.qe_ref, bf16[8,128,128]{2,1,0:T(8,128)(2,1)S(1)} %bitcast.17, ...), custom_call_target="tpu_custom_call" | custom-call | tf_op jit(solution)/shard_map/pallas_call | solution.py:291
  38.9 0.0 collective-permute-done.3.recv_ref
  38.9 0.0 copy-done
  38.9 0.0 copy-done.1
  38.9 4.2 %shard_map.140 = (bf16[64,2048]{1,0:T(8,128)(2,1)S(1)}, bf16[256,64]{1,0:T(8,128)(2,1)S(1)}, bf16[256,64]{1,0:T(8,128)(2,1)S(1)}, bf16[256,2048]{1,0:T(8,128)(2,...) custom-call(s32[1]{0:T(128)} %bitcast.1.tp_ref, ...), custom_call_target="tpu_custom_call" | custom-call | tf_op jit(solution)/shard_map/pallas_call | solution.py:291
  43.1 31.1 %all_to_all.22 = bf16[16,16,2048]{2,1,0:T(8,128)(2,1)S(1)} all-to-all(bf16[16,16,2048]{2,1,0:T(8,128)(2,1)} %bitcast.27), channel_id=1, replica_groups=mesh['sp'=16,'tp'=2] {'sp'}, dimensions={0} | all-to-all | bytes 2097152 | tf_op jit(solution)/shard_map/all_to_all | solution.py:411
  74.2 4.3 %shard_map.141 = bf16[256,2048]{1,0:T(8,128)(2,1)} custom-call(bf16[256,2048]{1,0:T(8,128)(2,1)S(1)} %bitcast.14, bf16[2048,512]{1,0:T(8,128)(2,1)S(1)} %get-tuple-element.38.g0_ref, bf16[2048,512]{1,0:T(8,128)(2,1)S(1)} %get-tuple-element.39.u0_ref, bf16[512,2048]{1,0:T(8,128)(2,1)S(1)} %get-tuple-element.40.d0_ref, ...), custom_call_target="tpu_custom_call" | custom-call | tf_op jit(solution)/shard_map/pallas_call | solution.py:291
  78.5 29.8 %all_to_all.23 = bf16[16,16,2048]{2,1,0:T(8,128)(2,1)S(1)} all-to-all(bf16[16,16,2048]{2,1,0:T(8,128)(2,1)} %bitcast.20), channel_id=1, replica_groups=mesh['sp'=16,'tp'=2] {'sp'}, dimensions={0} | all-to-all | bytes 2097152 | tf_op jit(solution)/shard_map/all_to_all | solution.py:425
  108.3 1.2 %shard_map.142 = bf16[64,2048]{1,0:T(8,128)(2,1)} custom-call(bf16[256,64]{1,0:T(8,128)(2,1)S(1)} %get-tuple-element.35.hi_ref, bf16[256,64]{1,0:T(8,128)(2,1)S(1)} %get-tuple-element.36.lo_ref, bf16[256,2048]{1,0:T(8,128)(2,1)S(1)} %bitcast.15, bf16[64,2048]{1,0:T(8,128)(2,1)S(1)} %get-tuple-element.44.upd_ref), custom_call_target="tpu_custom_call" | custom-call | tf_op jit(solution)/shard_map/pallas_call | solution.py:291
Async XLA Ops:
  0.0 22.2 %collective-permute-start = (bf16[2048,512]{1,0:T(8,128)(2,1)}, bf16[2048,512]{1,0:T(8,128)(2,1)S(1)}, u32[]{:S(2)}, u32[]{:S(2)}) collective-permute-start(bf16[2048,512]{1,0:T(8,128)(2,1)} %bitcast.21), channel_id=1, source_target_pairs={{0,1},{1,0},{2,3},{3,2},{4,5},{5,4},{6,7},{7,6},{8,9},{9,8},{10,11... | collective-permute-start | bytes 6291464 | tf_op jit(solution)/shard_map/ppermute | solution.py:334
  0.0 22.2 %collective-permute-start.1 = (bf16[2048,512]{1,0:T(8,128)(2,1)}, bf16[2048,512]{1,0:T(8,128)(2,1)}, u32[]{:S(2)}, u32[]{:S(2)}) collective-permute-start(bf16[2048,512]{1,0:T(8,128)(2,1)} %bitcast.23), channel_id=1, source_target_pairs={{0,1},{1,0},{2,3},{3,2},{4,5},{5,4},{6,7},{7,6},{8,9},{9,8},{10,11... | collective-permute-start | bytes 6291464 | tf_op jit(solution)/shard_map/ppermute | solution.py:334
  0.5 21.7 %collective-permute-start.2 = (bf16[512,2048]{1,0:T(8,128)(2,1)}, bf16[512,2048]{1,0:T(8,128)(2,1)}, u32[]{:S(2)}, u32[]{:S(2)}) collective-permute-start(bf16[512,2048]{1,0:T(8,128)(2,1)} %bitcast.25), channel_id=1, source_target_pairs={{0,1},{1,0},{2,3},{3,2},{4,5},{5,4},{6,7},{7,6},{8,9},{9,8},{10,11... | collective-permute-start | bytes 6291464 | tf_op jit(solution)/shard_map/ppermute | solution.py:334
  36.4 2.5 %collective-permute-start.3 = (bf16[64,1024]{1,0:T(8,128)(2,1)S(1)}, bf16[64,1024]{1,0:T(8,128)(2,1)S(1)}, u32[]{:S(2)}, u32[]{:S(2)}) collective-permute-start(bf16[64,1024]{1,0:T(8,128)(2,1)S(1)} %shard_map.138), channel_id=1, source_target_pairs={{0,1},{1,0},{2,3},{3,2},{4,5},{5,4},{6,7},{7,6},{8,9},{9,8},{10,11... | collective-permute-start | bytes 393224 | tf_op jit(solution)/shard_map/ppermute | solution.py:372
  36.5 2.4 %copy-start = (s32[64,2]{0,1:T(2,128)S(1)}, s32[64,2]{0,1:T(2,128)}, u32[]{:S(2)}) copy-start(s32[64,2]{0,1:T(2,128)} %param.23) | copy-start | bytes 1540
  36.5 2.4 %copy-start.1 = (f32[64,2]{0,1:T(2,128)S(1)}, f32[64,2]{0,1:T(2,128)}, u32[]{:S(2)}) copy-start(f32[64,2]{0,1:T(2,128)} %param.24) | copy-start | bytes 1540

commit v4 on v3

v4 whole, which is shorter than its diff:
```python
import functools

import jax
import jax.numpy as jnp
from jax import lax
from jax.experimental import pallas as pl
from jax.experimental.pallas import tpu as pltpu
from jax.sharding import PartitionSpec as P


HEAD_DIM = 128
TAIL = 8
GROUP = 4
COLUMNS = 4
epsilon = 1e-06
f32 = jnp.float32
bf16 = jnp.bfloat16

NN = (((1,), (0,)), ((), ()))
NT = (((1,), (1,)), ((), ()))
TN = (((0,), (0,)), ((), ()))


def dot(a, b, dims=NN):
    return lax.dot_general(a, b, dims, preferred_element_type=f32)


def split(x):
    hi = x.astype(bf16)
    return hi, (x - hi.astype(f32)).astype(bf16)


def sigmoid(x):
    return 1.0 / (1.0 + jnp.exp(-x))


def fetch(copies):
    for copy in copies:
        copy.start()
    return copies


def side_of(place_ref):
    return place_ref[0] & 1


def member_of(place_ref):
    return (place_ref[0] >> 1) & (GROUP - 1)


def group_of(place_ref):
    return (place_ref[0] >> 1) // GROUP


def decay_tail(log_decay):
    hi, lo = split(log_decay)
    place = lax.broadcasted_iota(jnp.int32, (TAIL, HEAD_DIM), 0)
    rows = jnp.where(place == 0, hi.astype(f32), jnp.where(place == 1, lo.astype(f32), 0.0))
    return rows.astype(bf16)


def log_decay_of(ref, at, h, heads):
    start = heads * HEAD_DIM + h * TAIL
    rows = ref[at, start : start + TAIL].astype(f32)
    return rows[0:1] + rows[1:2]


def first_kernel(place_ref, f_hbm, v_hbm, low_hbm, *refs):
    outs, (total_ref, key_ref, f_ref, v_ref, low_ref, sem) = refs[:GROUP], refs[GROUP:]
    length, block = f_ref.shape[1:]
    heads = block // HEAD_DIM
    member = member_of(place_ref)
    copies = []
    for k in range(GROUP):
        lanes = pl.ds(pl.multiple_of((member ^ k) * block, block), block)
        copies.append(
            fetch(
                [
                    pltpu.make_async_copy(hbm.at[:, lanes], ref.at[k], sem.at[3 * k + i])
                    for i, (hbm, ref) in enumerate(((f_hbm, f_ref), (low_hbm, low_ref), (v_hbm, v_ref)))
                ]
            )
        )
    t = lax.broadcasted_iota(jnp.int32, (length, length), 0)
    s = lax.broadcasted_iota(jnp.int32, (length, length), 1)
    tri = jnp.where(t >= s, 1.0, 0.0).astype(bf16)
    for k in range(GROUP):
        for copy in copies[k]:
            copy.wait()
        key_gate = (1.0 - low_ref[k]) * sigmoid(-f_ref[k].astype(f32))
        hi, lo = split(jnp.log1p(-key_gate))
        total = dot(tri, hi) + dot(tri, lo)
        last = total[length - 1 : length]
        weighted = (key_gate * jnp.exp(last - total)).astype(bf16)
        total_ref[k] = total
        key_ref[k] = key_gate
        for h in range(heads):
            lanes = slice(h * HEAD_DIM, (h + 1) * HEAD_DIM)
            outs[k][lanes] = dot(v_ref[k, :, lanes], weighted[:, lanes], TN).astype(bf16)
            start = heads * HEAD_DIM + h * TAIL
            outs[k][start : start + TAIL] = decay_tail(last[:, lanes])


def intra_kernel(
    place_ref, total_ref, key_ref, q_hbm, v_hbm, gate_hbm, gain_hbm, w_hbm, intra_ref, qe_ref, gated_ref, w_ref,
    q_ref, v_ref, gate_ref, gain_ref, sem,
):
    length, block = q_ref.shape[1:]
    member = member_of(place_ref)
    copies = []
    for k in range(GROUP):
        lanes = pl.ds(pl.multiple_of((member ^ k) * block, block), block)
        pairs = ((q_hbm, q_ref), (v_hbm, v_ref), (gate_hbm, gate_ref), (gain_hbm, gain_ref))
        copies.append(
            fetch(
                [
                    pltpu.make_async_copy(hbm.at[:, lanes], ref.at[k], sem.at[4 * k + i])
                    for i, (hbm, ref) in enumerate(pairs)
                ]
            )
        )
    ahead = pltpu.make_async_copy(w_hbm, w_ref, sem.at[4 * GROUP])
    ahead.start()
    t = lax.broadcasted_iota(jnp.int32, (length, length), 0)
    s = lax.broadcasted_iota(jnp.int32, (length, length), 1)
    for k in range(GROUP):
        for copy in copies[k]:
            copy.wait()
        total = total_ref[k]
        middle = total[length // 2 - 1 : length // 2]
        query = q_ref[k].astype(f32)
        scaled_query = (query * jnp.exp(total - middle)).astype(bf16)
        scaled_key = (key_ref[k] * jnp.exp(middle - total)).astype(bf16)
        qe_ref[k] = (query * jnp.exp(total)).astype(bf16)
        gate = gate_ref[k].astype(f32)
        gated_ref[k] = gain_ref[k] * (gate * sigmoid(gate))
        for h in range(block // HEAD_DIM):
            lanes = slice(h * HEAD_DIM, (h + 1) * HEAD_DIM)
            scores = dot(scaled_query[:, lanes], scaled_key[:, lanes], NT)
            scores = jnp.where(t >= s, scores, 0.0).astype(bf16)
            intra_ref[k, :, lanes] = dot(scores, v_ref[k, :, lanes])
    ahead.wait()


def total_kernel(place_ref, *refs):
    parts, (out_ref, part_ref) = refs[:GROUP], refs[GROUP:]
    heads = out_ref.shape[0] // (HEAD_DIM + TAIL)
    member = member_of(place_ref)
    for k in range(GROUP):
        part_ref[member ^ k] = parts[k][...]
    for h in range(heads):
        rows = slice(h * HEAD_DIM, (h + 1) * HEAD_DIM)
        state = part_ref[0, rows].astype(f32)
        log_decay = log_decay_of(part_ref, 0, h, heads)
        for j in range(1, GROUP):
            more = log_decay_of(part_ref, j, h, heads)
            state = state * jnp.exp(more) + part_ref[j, rows].astype(f32)
            log_decay = log_decay + more
        out_ref[rows] = state.astype(bf16)
        start = heads * HEAD_DIM + h * TAIL
        out_ref[start : start + TAIL] = decay_tail(log_decay)


def carry_kernel(place_ref, *refs, groups):
    parts, totals = refs[:GROUP], refs[GROUP : GROUP + groups]
    outs, (part_ref, total_ref, state_ref) = refs[GROUP + groups : 2 * GROUP + groups], refs[-3:]
    heads = outs[0].shape[0] // HEAD_DIM
    member = member_of(place_ref)
    group = group_of(place_ref)
    for k in range(GROUP):
        part_ref[member ^ k] = parts[k][...]
    for k in range(groups):
        total_ref[group ^ k] = totals[k][...]
    for h in range(heads):
        rows = slice(h * HEAD_DIM, (h + 1) * HEAD_DIM)

        def one(g, state):
            return state * jnp.exp(log_decay_of(total_ref, g, h, heads)) + total_ref[g, rows].astype(f32)

        state = lax.fori_loop(0, group, one, jnp.zeros((HEAD_DIM, HEAD_DIM), f32))
        for j in range(GROUP):
            state_ref[j, rows] = state.astype(bf16)
            if j + 1 < GROUP:
                state = state * jnp.exp(log_decay_of(part_ref, j, h, heads)) + part_ref[j, rows].astype(f32)
    for k in range(GROUP):
        outs[k][...] = state_ref[member ^ k]


def mixed_rows(out_ref, side, member, intra_ref, qe_ref, gated_ref, states):
    half = out_ref.shape[0]
    block = intra_ref.shape[2]
    at = pl.ds(pl.multiple_of(side * half, half), half)
    for k in range(GROUP):
        mixed = []
        for h in range(block // HEAD_DIM):
            lanes = slice(h * HEAD_DIM, (h + 1) * HEAD_DIM)
            out = intra_ref[k, at, lanes] + dot(qe_ref[k, at, lanes], states[k][lanes], NT)
            scale = lax.rsqrt(jnp.mean(out * out, axis=-1, keepdims=True) + epsilon)
            mixed.append((out * scale * gated_ref[k, at, lanes]).astype(bf16))
        where = pl.ds(pl.multiple_of((member ^ k) * block, block), block)
        out_ref[:, where] = jnp.concatenate(mixed, axis=1)


def send_kernel(place_ref, intra_ref, qe_ref, gated_ref, *refs):
    mixed_rows(refs[GROUP], 1 - side_of(place_ref), member_of(place_ref), intra_ref, qe_ref, gated_ref, refs[:GROUP])


def keep_kernel(place_ref, intra_ref, qe_ref, gated_ref, *refs):
    states, (w_ref, g_hbm, u_hbm, acc_ref, g_ref, u_ref, mix_ref, sem) = refs[:GROUP], refs[GROUP:]
    channels = mix_ref.shape[1]
    own = side_of(place_ref)
    ahead = fetch(
        [
            pltpu.make_async_copy(g_hbm, g_ref, sem.at[0]),
            pltpu.make_async_copy(u_hbm, u_ref, sem.at[1]),
        ]
    )
    mixed_rows(mix_ref, own, member_of(place_ref), intra_ref, qe_ref, gated_ref, states)
    acc_ref[...] = dot(mix_ref[...], w_ref[pl.ds(pl.multiple_of(own * channels, channels), channels)])
    for copy in ahead:
        copy.wait()


def slots_of(routing, capacity):
    top, count = routing.shape
    s = lax.broadcasted_iota(jnp.int32, (count, count), 0)
    t = lax.broadcasted_iota(jnp.int32, (count, count), 1)
    before = jnp.where(s < t, 1.0, 0.0).astype(bf16)
    place = lax.broadcasted_iota(jnp.int32, (128, count), 0)
    taken = jnp.zeros((128, 1), f32)
    slots = []
    for k in range(top):
        expert = routing[k : k + 1]
        named = jnp.where(place == expert, 1.0, 0.0)
        rank = dot(named.astype(bf16), before) + taken
        rank = jnp.sum(named * rank, axis=0, keepdims=True)
        slots.append(expert * capacity + rank.astype(jnp.int32))
        taken = taken + jnp.sum(named, axis=1, keepdims=True)
    return slots


def project_kernel(
    place_ref, recv_ref, acc_ref, route_ref, weight_ref, w_ref, res_hbm, gain_hbm, d0_hbm, u1_hbm, d1_hbm,
    upd_ref, hi_ref, lo_ref, box_ref, d0_ref, u1_ref, d1_ref,
    res_ref, gain_ref, sem, *, capacity,
):
    half, _ = acc_ref.shape
    channels = recv_ref.shape[1]
    other = 1 - side_of(place_ref)
    copies = fetch(
        [
            pltpu.make_async_copy(res_hbm, res_ref, sem.at[0]),
            pltpu.make_async_copy(gain_hbm, gain_ref, sem.at[1]),
        ]
    )
    ahead = fetch(
        [
            pltpu.make_async_copy(hbm, ref, sem.at[2 + i])
            for i, (hbm, ref) in enumerate(((d0_hbm, d0_ref), (u1_hbm, u1_ref), (d1_hbm, d1_ref)))
        ]
    )
    place = lax.broadcasted_iota(jnp.int32, (box_ref.shape[0], half), 0)
    chosen = jnp.zeros(place.shape, f32)
    weighted = jnp.zeros(place.shape, f32)
    for k, slot in enumerate(slots_of(route_ref[...], capacity)):
        chosen = chosen + jnp.where(place == slot, 1.0, 0.0)
        weighted = weighted + jnp.where(place == slot, weight_ref[k : k + 1], 0.0)
    chosen = chosen.astype(bf16)
    hi_ref[...], lo_ref[...] = split(weighted)
    partial = dot(recv_ref[...], w_ref[pl.ds(pl.multiple_of(other * channels, channels), channels)])
    for copy in copies:
        copy.wait()
    updated = (res_ref[...].astype(f32) + (acc_ref[...] + partial)).astype(bf16)
    upd_ref[...] = updated
    updated = updated.astype(f32)
    scale = lax.rsqrt(jnp.mean(updated * updated, axis=-1, keepdims=True) + epsilon)
    normed = (updated * scale * gain_ref[...]).astype(bf16)
    box_ref[...] = dot(chosen, normed).astype(bf16)
    for copy in ahead:
        copy.wait()


def expert_kernel(x_ref, g0_ref, u0_ref, d0_ref, g1_ref, u1_ref, d1_ref, out_ref, hid_ref):
    units = g0_ref.shape[1]
    width = d0_ref.shape[1]
    block = 256
    x = x_ref[...]
    for side, (g_ref, u_ref) in enumerate(((g0_ref, u0_ref), (g1_ref, u1_ref))):
        for j in range(units // block):
            lanes = slice(j * block, (j + 1) * block)
            gate = dot(x, g_ref[:, lanes])
            hidden = (gate * sigmoid(gate) * dot(x, u_ref[:, lanes])).astype(bf16)
            hid_ref[:, side * units + j * block : side * units + (j + 1) * block] = hidden
    block = width // COLUMNS
    for n in range(COLUMNS):
        lanes = slice(n * block, (n + 1) * block)
        out = dot(hid_ref[:, :units], d0_ref[:, lanes]) + dot(hid_ref[:, units:], d1_ref[:, lanes])
        out_ref[:, lanes] = out.astype(bf16)


def combine_kernel(hi_ref, lo_ref, back_ref, upd_ref, out_ref):
    back = back_ref[...]
    out_ref[...] = (
        upd_ref[...].astype(f32) + (dot(hi_ref[...], back, TN) + dot(lo_ref[...], back, TN))
    ).astype(bf16)


HBM = pl.BlockSpec(memory_space=pltpu.HBM)
SMEM = pl.BlockSpec(memory_space=pltpu.SMEM)
VMEM = pl.BlockSpec(memory_space=pltpu.VMEM)
KEPT = pl.BlockSpec(memory_space=pltpu.VMEM)
FIXED = ((HBM, pltpu.HBM), (KEPT, pltpu.VMEM))


def call(kernel, ins, outs, scratch=(), mib=16):
    def fixed(spec):
        return next((space for known, space in FIXED if known is spec), None)

    run = pl.pallas_call(
        kernel,
        in_specs=ins,
        out_specs=[spec for spec, _ in outs],
        out_shape=[
            fixed(spec)(shape.shape, shape.dtype) if fixed(spec) else shape for spec, shape in outs
        ],
        scratch_shapes=list(scratch),
        compiler_params=pltpu.CompilerParams(vmem_limit_bytes=mib * 1024 * 1024),
    )

    def placed(*args):
        return run(
            *(
                pltpu.with_memory_space_constraint(arg, fixed(spec)) if fixed(spec) else arg
                for spec, arg in zip(ins, args)
            )
        )

    return placed


def body(
    query,
    forget_logit,
    value,
    out_gate,
    lower_bound,
    head_gain,
    residual_in,
    w_out,
    ffn_gain,
    routing,
    route_weight,
    expert_gate,
    expert_up,
    expert_down,
):
    shape = jax.ShapeDtypeStruct
    dma = pltpu.SemaphoreType.DMA
    ranks = lax.axis_size("sp")
    sides = lax.axis_size("tp")
    length, channels = query.shape
    part = channels // GROUP
    carried = part + part // HEAD_DIM * TAIL
    groups = ranks // GROUP
    half = length // sides
    width = w_out.shape[1]
    top = routing.shape[1]
    capacity = 2 * half * top // ranks
    slots = ranks * capacity
    units = expert_gate.shape[2]
    rank = lax.axis_index("sp")
    place = (rank * 2 + lax.axis_index("tp")).reshape(1)
    swap = [(i, i ^ 1) for i in range(sides)]

    def away(x, k):
        return lax.ppermute(x, "sp", [(i, i ^ k) for i in range(ranks)])

    weights = (expert_gate[0], expert_up[0], expert_down[0])
    others = tuple(lax.ppermute(w, "tp", swap) for w in weights)

    *states, total, key_gate = call(
        first_kernel,
        [SMEM] + [HBM] * 3,
        [(VMEM, shape((carried, HEAD_DIM), bf16))] * GROUP
        + [(VMEM, shape((GROUP, length, part), f32))] * 2,
        [pltpu.VMEM((GROUP, length, part), bf16)] * 2
        + [pltpu.VMEM((GROUP, 1, part), f32), dma((3 * GROUP,))],
    )(place, forget_logit, value, lower_bound.reshape(1, -1))
    states = states[:1] + [away(states[k], k) for k in range(1, GROUP)]
    intra, qe, gated, w_kept = call(
        intra_kernel,
        [SMEM] + [VMEM] * 2 + [HBM] * 5,
        [
            (VMEM, shape((GROUP, length, part), f32)),
            (VMEM, shape((GROUP, length, part), bf16)),
            (VMEM, shape((GROUP, length, part), f32)),
            (KEPT, shape(w_out.shape, bf16)),
        ],
        [pltpu.VMEM((GROUP, length, part), bf16)] * 3
        + [pltpu.VMEM((GROUP, 1, part), f32), dma((4 * GROUP + 1,))],
    )(place, total, key_gate, query, value, out_gate, head_gain.reshape(1, -1), w_out)
    (totals,) = call(
        total_kernel,
        [SMEM] + [VMEM] * GROUP,
        [(VMEM, shape((carried, HEAD_DIM), bf16))],
        [pltpu.VMEM((GROUP, carried, HEAD_DIM), bf16)],
    )(place, *states)
    totals = [totals] + [away(totals, GROUP * k) for k in range(1, groups)]
    priors = call(
        functools.partial(carry_kernel, groups=groups),
        [SMEM] + [VMEM] * (GROUP + groups),
        [(VMEM, shape((part, HEAD_DIM), bf16))] * GROUP,
        [
            pltpu.VMEM((GROUP, carried, HEAD_DIM), bf16),
            pltpu.VMEM((groups, carried, HEAD_DIM), bf16),
            pltpu.VMEM((GROUP, part, HEAD_DIM), bf16),
        ],
    )(place, *states, *totals)
    priors = list(priors[:1]) + [away(priors[k], k) for k in range(1, GROUP)]

    mix_args = (place, intra, qe, gated, *priors)
    mix_specs = [SMEM] + [VMEM] * (3 + GROUP)
    (send,) = call(send_kernel, mix_specs, [(VMEM, shape((half, channels), bf16))])(*mix_args)
    recv = lax.ppermute(send, "tp", swap)
    partial, gate_kept, up_kept = call(
        keep_kernel,
        mix_specs + [KEPT, HBM, HBM],
        [(VMEM, shape((half, width), f32))] + [(KEPT, shape((width, units), bf16))] * 2,
        [pltpu.VMEM((half, channels), bf16), dma((2,))],
    )(*mix_args, w_kept, *weights[:2])
    recv, others = lax.optimization_barrier((recv, others))
    updated, hi, lo, outbox, down_kept, other_up, other_down = call(
        functools.partial(project_kernel, capacity=capacity),
        [SMEM] + [VMEM] * 4 + [KEPT] + [HBM] * 5,
        [
            (VMEM, shape((half, width), bf16)),
            (VMEM, shape((slots, half), bf16)),
            (VMEM, shape((slots, half), bf16)),
            (VMEM, shape((slots, width), bf16)),
            (KEPT, shape((units, width), bf16)),
            (KEPT, shape((width, units), bf16)),
            (KEPT, shape((units, width), bf16)),
        ],
        [pltpu.VMEM((half, width), bf16), pltpu.VMEM((1, width), f32), dma((5,))],
    )(
        place,
        recv,
        partial,
        routing.T,
        route_weight.T,
        w_kept,
        residual_in,
        ffn_gain.reshape(1, -1),
        weights[2],
        *others[1:],
    )

    arrived = lax.all_to_all(
        outbox.reshape(ranks, capacity, width), "sp", split_axis=0, concat_axis=0, tiled=True
    )
    (expert_out,) = call(
        expert_kernel,
        [VMEM] + [KEPT] * 6,
        [(VMEM, shape((slots, width), bf16))],
        [pltpu.VMEM((slots, 2 * units), bf16)],
    )(arrived.reshape(slots, width), gate_kept, up_kept, down_kept, others[0], other_up, other_down)

    returned = lax.all_to_all(
        expert_out.reshape(ranks, capacity, width), "sp", split_axis=0, concat_axis=0, tiled=True
    )
    (layer_out,) = call(
        combine_kernel, [VMEM] * 4, [(VMEM, shape((half, width), bf16))]
    )(hi, lo, returned.reshape(slots, width), updated)
    return layer_out


def solution(mesh):
    placed = (
        P("sp", "tp"),
        P("sp", "tp"),
        P("sp", "tp"),
        P("sp", "tp"),
        P("tp"),
        P("tp"),
        P(("sp", "tp"), None),
        P(),
        P(),
        P(("sp", "tp"), None),
        P(("sp", "tp"), None),
        P("sp", None, "tp"),
        P("sp", None, "tp"),
        P("sp", "tp", None),
    )

    return jax.shard_map(
        body, mesh=mesh, in_specs=placed, out_specs=P(("sp", "tp"), None), check_vma=False
    )
```

time: 112 us -> 110 us (0.982)
  blocking collectives: 91.1 us -> 61.8 us
  waiting for transfers between devices: 0.01 us -> 15.1 us
  starting transfers between devices: 0.58 us -> 12.5 us
    all_to_all x2 -> x0, blocking collectives: 30.2 us -> none  [the longest x1 17.4 us: body(): lax.all_to_all(packed, 'sp', split_axis=0, concat_axis=0, tiled=True)]
    ppermute x0 -> x9, waiting for transfers between devices: none -> 15.1 us  [away(): return lax.ppermute(x, 'sp', [(i, i ^ k) for i in range(ranks)])]
    ppermute x0 -> x9, starting transfers between devices: none -> 11.9 us  [away(): return lax.ppermute(x, 'sp', [(i, i ^ k) for i in range(ranks)])]
    all_to_all x1, blocking collectives: 31.1 us -> 32.4 us  [body(): lax.all_to_all(outbox.reshape(ranks, capacity, width), 'sp', split_axis=0...]
    pallas_call x7 -> x9, Pallas kernels: 17.7 us -> 18.5 us  [placed(): run(*(pltpu.with_memory_space_constraint(arg, fixed(spec)) if fixed(spec)...]
  transfers between devices with their start and end apart: 4 -> 13, of which waited for: 0 -> 5; matrix products, arithmetic and copies ran while one was open for 0% -> 0% of each run, Pallas kernels for 6% -> 9%
where the time goes in v4:
time: 110 us; the launch traced here: 108 us
  blocking collectives  61.8 us (56%)
  Pallas kernels  18.5 us (17%)
  waiting for transfers between devices  15.1 us (14%)
  starting transfers between devices  12.5 us (11%)
    all_to_all x1, blocking collectives, body(): lax.all_to_all(outbox.reshape(ranks, capacity, width), 'sp', split_axis=0...  32.4 us
    all_to_all x1, blocking collectives, body(): lax.all_to_all(expert_out.reshape(ranks, capacity, width), 'sp', split_ax...  29.4 us
    pallas_call x9, Pallas kernels, placed(): run(*(pltpu.with_memory_space_constraint(arg, fixed(spec)) if fixed(spec)...  18.5 us
    ppermute x9, waiting for transfers between devices, away(): return lax.ppermute(x, 'sp', [(i, i ^ k) for i in range(ranks)])  15.1 us
    ppermute x9, starting transfers between devices, away(): return lax.ppermute(x, 'sp', [(i, i ^ k) for i in range(ranks)])  11.9 us
  transfers between devices with their start and end apart: 13, of which 5 were waited for; matrix products, arithmetic and copies ran while one was open for 0% of the time, Pallas kernels for 9%

profile of v4, /device:TPU:8, one launch (start us, length us, event | category | flops | bytes accessed | tf_op | source)
XLA Modules:
  0.0 108.0 jit_solution(11685058931758946827)
XLA Ops:
  0.0 0.0 collective-permute-start.10
  0.0 0.5 collective-permute-start.11
  0.5 0.0 collective-permute-start.12
  0.5 2.8 %shard_map.136 = (bf16[272,128]{1,0:T(8,128)(2,1)S(1)}, bf16[272,128]{1,0:T(8,128)(2,1)S(1)}, bf16[272,128]{1,0:T(8,128)(2,1)S(1)}, bf16[272,128]{1,0:T(8,128)(2...) custom-call(s32[1]{0:T(128)} %bitcast.place_ref, bf16[128,1024]{1,0:T(8,128)(2,1)} %f_hbm.1, ...), custom_call_target="tpu_custom_call" | custom-call | tf_op jit(solution)/shard_map/pallas_call | solution.py:331
  3.4 1.6 %collective-permute-start = (bf16[272,128]{1,0:T(8,128)(2,1)S(1)}, bf16[272,128]{1,0:T(8,128)(2,1)S(1)}, u32[]{:S(2)}, u32[]{:S(2)}) collective-permute-start(bf16[272,128]{1,0:T(8,128)(2,1)S(1)} %get-tuple-element.39), channel_id=1, source_target_pairs={{0,2},{2,0},{4,6},{6,4},{8,10},{10,8},{12,14},{14,12},{16,18},{18,... | collective-permute-start | bytes 208904 | tf_op jit(solution)/shard_map/ppermute | solution.py:376
  4.9 1.5 %collective-permute-start.1 = (bf16[272,128]{1,0:T(8,128)(2,1)S(1)}, bf16[272,128]{1,0:T(8,128)(2,1)S(1)}, u32[]{:S(2)}, u32[]{:S(2)}) collective-permute-start(bf16[272,128]{1,0:T(8,128)(2,1)S(1)} %get-tuple-element.40), channel_id=1, source_target_pairs={{0,4},{2,6},{4,0},{6,2},{8,12},{10,14},{12,8},{14,10},{16,20},{18,... | collective-permute-start | bytes 208904 | tf_op jit(solution)/shard_map/ppermute | solution.py:376
  6.5 1.6 %collective-permute-done.refs_1_ = bf16[272,128]{1,0:T(8,128)(2,1)S(1)} collective-permute-done((bf16[272,128]{1,0:T(8,128)(2,1)S(1)}, bf16[272,128]{1,0:T(8,128)(2,1)S(1)}, u32[]{:S(2)}, u32[]{:S(2)}) %collective-permute-start) | collective-permute-done | bytes 69664 | tf_op jit(solution)/shard_map/ppermute | solution.py:376
  8.0 2.4 %collective-permute-start.2 = (bf16[272,128]{1,0:T(8,128)(2,1)S(1)}, bf16[272,128]{1,0:T(8,128)(2,1)S(1)}, u32[]{:S(2)}, u32[]{:S(2)}) collective-permute-start(bf16[272,128]{1,0:T(8,128)(2,1)S(1)} %get-tuple-element.41), channel_id=1, source_target_pairs={{0,6},{2,4},{4,2},{6,0},{8,14},{10,12},{12,10},{14,8},{16,22},{18,... | collective-permute-start | bytes 208904 | tf_op jit(solution)/shard_map/ppermute | solution.py:376
  10.5 0.0 collective-permute-done.1.refs_2_
  10.5 2.8 %collective-permute-done.2.refs_3_ = bf16[272,128]{1,0:T(8,128)(2,1)S(1)} collective-permute-done((bf16[272,128]{1,0:T(8,128)(2,1)S(1)}, bf16[272,128]{1,0:T(8,128)(2,1)S(1)}, u32[]{:S(2)}, u32[]{:S(2)}) %collective-permute-start.2) | collective-permute-done | bytes 69664 | tf_op jit(solution)/shard_map/ppermute | solution.py:376
  13.2 0.1 shard_map.138.refs_4_
  13.3 1.6 %collective-permute-start.5 = (bf16[272,128]{1,0:T(8,128)(2,1)S(1)}, bf16[272,128]{1,0:T(8,128)(2,1)S(1)}, u32[]{:S(2)}, u32[]{:S(2)}) collective-permute-start(bf16[272,128]{1,0:T(8,128)(2,1)S(1)} %shard_map.138.refs_4_), channel_id=1, source_target_pairs={{0,24},{2,26},{4,28},{6,30},{8,16},{10,18},{12,20},{14,22},{16,8},... | collective-permute-start | bytes 208904 | tf_op jit(solution)/shard_map/ppermute | solution.py:376
  15.0 1.1 %collective-permute-start.4 = (bf16[272,128]{1,0:T(8,128)(2,1)S(1)}, bf16[272,128]{1,0:T(8,128)(2,1)S(1)}, u32[]{:S(2)}, u32[]{:S(2)}) collective-permute-start(bf16[272,128]{1,0:T(8,128)(2,1)S(1)} %shard_map.138.refs_4_), channel_id=1, source_target_pairs={{0,16},{2,18},{4,20},{6,22},{8,24},{10,26},{12,28},{14,30},{16,0},... | collective-permute-start | bytes 208904 | tf_op jit(solution)/shard_map/ppermute | solution.py:376
  16.1 4.3 %collective-permute-done.5.refs_7_ = bf16[272,128]{1,0:T(8,128)(2,1)S(1)} collective-permute-done((bf16[272,128]{1,0:T(8,128)(2,1)S(1)}, bf16[272,128]{1,0:T(8,128)(2,1)S(1)}, u32[]{:S(2)}, u32[]{:S(2)}) %collective-permute-start.5) | collective-permute-done | bytes 69664 | tf_op jit(solution)/shard_map/ppermute | solution.py:376
  20.3 0.0 collective-permute-start.3
  20.3 0.0 collective-permute-done.4.refs_6_
  20.3 4.3 %collective-permute-done.3.refs_5_ = bf16[272,128]{1,0:T(8,128)(2,1)S(1)} collective-permute-done((bf16[272,128]{1,0:T(8,128)(2,1)S(1)}, bf16[272,128]{1,0:T(8,128)(2,1)S(1)}, u32[]{:S(2)}, u32[]{:S(2)}) %collective-permute-start.3) | collective-permute-done | bytes 69664 | tf_op jit(solution)/shard_map/ppermute | solution.py:376
  24.6 0.2 shard_map.139
  24.8 0.6 collective-permute-start.6
  25.4 1.5 %collective-permute-start.7 = (bf16[256,128]{1,0:T(8,128)(2,1)S(1)}, bf16[256,128]{1,0:T(8,128)(2,1)S(1)}, u32[]{:S(2)}, u32[]{:S(2)}) collective-permute-start(bf16[256,128]{1,0:T(8,128)(2,1)S(1)} %get-tuple-element.44), channel_id=1, source_target_pairs={{0,4},{2,6},{4,0},{6,2},{8,12},{10,14},{12,8},{14,10},{16,20},{18,... | collective-permute-start | bytes 196616 | tf_op jit(solution)/shard_map/ppermute | solution.py:376
  26.9 2.2 %collective-permute-done.6.refs_1_ = bf16[256,128]{1,0:T(8,128)(2,1)S(1)} collective-permute-done((bf16[256,128]{1,0:T(8,128)(2,1)S(1)}, bf16[256,128]{1,0:T(8,128)(2,1)S(1)}, u32[]{:S(2)}, u32[]{:S(2)}) %collective-permute-start.6) | collective-permute-done | bytes 65568 | tf_op jit(solution)/shard_map/ppermute | solution.py:376
  29.1 1.5 %collective-permute-start.8 = (bf16[256,128]{1,0:T(8,128)(2,1)S(1)}, bf16[256,128]{1,0:T(8,128)(2,1)S(1)}, u32[]{:S(2)}, u32[]{:S(2)}) collective-permute-start(bf16[256,128]{1,0:T(8,128)(2,1)S(1)} %get-tuple-element.45), channel_id=1, source_target_pairs={{0,6},{2,4},{4,2},{6,0},{8,14},{10,12},{12,10},{14,8},{16,22},{18,... | collective-permute-start | bytes 196616 | tf_op jit(solution)/shard_map/ppermute | solution.py:376
  30.7 4.0 %shard_map.137 = (f32[4,128,256]{2,1,0:T(8,128)S(1)}, bf16[4,128,256]{2,1,0:T(8,128)(2,1)S(1)}, f32[4,128,256]{2,1,0:T(8,128)S(1)}, bf16[2048,2048]{1,0:T(8,128)(2,1)S(1)}) custom-call(s32[1]{0:T(128)} %bitcast.place_ref, f32[4,128,256]{2,1,0:T(8,128)S(1)} %get-tuple-element.33.total_ref, f32[4,128,256]{2,1,0:T(8,128)S(1)} %get-tuple-element.34.key_ref, ...), custom_call_target="tpu_custom_call" | custom-call | tf_op jit(solution)/shard_map/pallas_call | solution.py:331
  34.6 0.0 collective-permute-done.7.refs_2_
  34.6 0.0 collective-permute-done.8.refs_3_
  34.6 0.4 shard_map.140
  35.0 0.1 collective-permute-start.9
  35.1 0.0 copy-start
  35.1 0.0 copy-start.1
  35.1 2.5 %shard_map.141 = (f32[64,2048]{1,0:T(8,128)S(1)}, bf16[2048,512]{1,0:T(8,128)(2,1)S(1)}, bf16[2048,512]{1,0:T(8,128)(2,1)S(1)}) custom-call(s32[1]{0:T(128)} %bitcast.place_ref, f32[4,128,256]{2,1,0:T(8,128)S(1)} %get-tuple-element.35.intra_ref, bf16[4,128,256]{2,1,0:T(8,128)(2,1)S(1)} %get-tuple-element.36.qe_ref, ...), custom_call_target="tpu_custom_call" | custom-call | tf_op jit(solution)/shard_map/pallas_call | solution.py:331
  37.7 0.0 collective-permute-done.9.recv_ref
  37.7 0.0 collective-permute-done.10.g1_ref
  37.7 0.0 collective-permute-done.11.u1_hbm
  37.7 0.0 collective-permute-done.12.d1_hbm
  37.7 0.0 copy-done
  37.7 0.0 copy-done.1
  37.7 3.8 %shard_map.142 = (bf16[64,2048]{1,0:T(8,128)(2,1)S(1)}, bf16[256,64]{1,0:T(8,128)(2,1)S(1)}, bf16[256,64]{1,0:T(8,128)(2,1)S(1)}, bf16[256,2048]{1,0:T(8,128)(2,...) custom-call(s32[1]{0:T(128)} %bitcast.place_ref, ...), custom_call_target="tpu_custom_call" | custom-call | tf_op jit(solution)/shard_map/pallas_call | solution.py:331
  41.6 32.4 %all_to_all.10 = bf16[16,16,2048]{2,1,0:T(8,128)(2,1)S(1)} all-to-all(bf16[16,16,2048]{2,1,0:T(8,128)(2,1)S(1)} %bitcast.16), channel_id=1, replica_groups=mesh['sp'=16,'tp'=2] {'sp'}, dimensions={0} | all-to-all | bytes 2097152 | tf_op jit(solution)/shard_map/all_to_all | solution.py:458
  74.0 3.5 %shard_map.143 = bf16[256,2048]{1,0:T(8,128)(2,1)S(1)} custom-call(bf16[256,2048]{1,0:T(8,128)(2,1)S(1)} %bitcast.13, bf16[2048,512]{1,0:T(8,128)(2,1)S(1)} %get-tuple-element.54.g0_ref, bf16[2048,512]{1,0:T(8,128)(2,1)S(1)} %get-tuple-element.55.u0_ref, bf16[512,2048]{1,0:T(8,128)(2,1)S(1)} %get-tuple-element.56.d0_ref, ...), custom_call_target="tpu_custom_call" | custom-call | tf_op jit(solution)/shard_map/pallas_call | solution.py:331
  77.4 29.4 %all_to_all.11 = bf16[16,16,2048]{2,1,0:T(8,128)(2,1)S(1)} all-to-all(bf16[16,16,2048]{2,1,0:T(8,128)(2,1)S(1)} %bitcast.14), channel_id=1, replica_groups=mesh['sp'=16,'tp'=2] {'sp'}, dimensions={0} | all-to-all | bytes 2097152 | tf_op jit(solution)/shard_map/all_to_all | solution.py:468
  106.8 1.2 %shard_map.144 = bf16[64,2048]{1,0:T(8,128)(2,1)} custom-call(bf16[256,64]{1,0:T(8,128)(2,1)S(1)} %get-tuple-element.51.hi_ref, bf16[256,64]{1,0:T(8,128)(2,1)S(1)} %get-tuple-element.52.lo_ref, bf16[256,2048]{1,0:T(8,128)(2,1)S(1)} %bitcast.15, bf16[64,2048]{1,0:T(8,128)(2,1)S(1)} %get-tuple-element.60.upd_ref), custom_call_target="tpu_custom_call" | custom-call | tf_op jit(solution)/shard_map/pallas_call | solution.py:331
Async XLA Ops:
  0.0 37.7 %collective-permute-start.10 = (bf16[2048,512]{1,0:T(8,128)(2,1)}, bf16[2048,512]{1,0:T(8,128)(2,1)S(1)}, u32[]{:S(2)}, u32[]{:S(2)}) collective-permute-start(bf16[2048,512]{1,0:T(8,128)(2,1)} %bitcast.21), channel_id=1, source_target_pairs={{0,1},{1,0},{2,3},{3,2},{4,5},{5,4},{6,7},{7,6},{8,9},{9,8},{10,11... | collective-permute-start | bytes 6291464 | tf_op jit(solution)/shard_map/ppermute | solution.py:379
  0.0 37.7 %collective-permute-start.11 = (bf16[2048,512]{1,0:T(8,128)(2,1)}, bf16[2048,512]{1,0:T(8,128)(2,1)}, u32[]{:S(2)}, u32[]{:S(2)}) collective-permute-start(bf16[2048,512]{1,0:T(8,128)(2,1)} %bitcast.23), channel_id=1, source_target_pairs={{0,1},{1,0},{2,3},{3,2},{4,5},{5,4},{6,7},{7,6},{8,9},{9,8},{10,11... | collective-permute-start | bytes 6291464 | tf_op jit(solution)/shard_map/ppermute | solution.py:379
  0.5 37.2 %collective-permute-start.12 = (bf16[512,2048]{1,0:T(8,128)(2,1)}, bf16[512,2048]{1,0:T(8,128)(2,1)}, u32[]{:S(2)}, u32[]{:S(2)}) collective-permute-start(bf16[512,2048]{1,0:T(8,128)(2,1)} %bitcast.19), channel_id=1, source_target_pairs={{0,1},{1,0},{2,3},{3,2},{4,5},{5,4},{6,7},{7,6},{8,9},{9,8},{10,11... | collective-permute-start | bytes 6291464 | tf_op jit(solution)/shard_map/ppermute | solution.py:379
  3.4 4.7 %collective-permute-start = (bf16[272,128]{1,0:T(8,128)(2,1)S(1)}, bf16[272,128]{1,0:T(8,128)(2,1)S(1)}, u32[]{:S(2)}, u32[]{:S(2)}) collective-permute-start(bf16[272,128]{1,0:T(8,128)(2,1)S(1)} %get-tuple-element.39), channel_id=1, source_target_pairs={{0,2},{2,0},{4,6},{6,4},{8,10},{10,8},{12,14},{14,12},{16,18},{18,... | collective-permute-start | bytes 208904 | tf_op jit(solution)/shard_map/ppermute | solution.py:376
  4.9 5.5 %collective-permute-start.1 = (bf16[272,128]{1,0:T(8,128)(2,1)S(1)}, bf16[272,128]{1,0:T(8,128)(2,1)S(1)}, u32[]{:S(2)}, u32[]{:S(2)}) collective-permute-start(bf16[272,128]{1,0:T(8,128)(2,1)S(1)} %get-tuple-element.40), channel_id=1, source_target_pairs={{0,4},{2,6},{4,0},{6,2},{8,12},{10,14},{12,8},{14,10},{16,20},{18,... | collective-permute-start | bytes 208904 | tf_op jit(solution)/shard_map/ppermute | solution.py:376
  8.0 5.2 %collective-permute-start.2 = (bf16[272,128]{1,0:T(8,128)(2,1)S(1)}, bf16[272,128]{1,0:T(8,128)(2,1)S(1)}, u32[]{:S(2)}, u32[]{:S(2)}) collective-permute-start(bf16[272,128]{1,0:T(8,128)(2,1)S(1)} %get-tuple-element.41), channel_id=1, source_target_pairs={{0,6},{2,4},{4,2},{6,0},{8,14},{10,12},{12,10},{14,8},{16,22},{18,... | collective-permute-start | bytes 208904 | tf_op jit(solution)/shard_map/ppermute | solution.py:376
  13.3 7.0 %collective-permute-start.5 = (bf16[272,128]{1,0:T(8,128)(2,1)S(1)}, bf16[272,128]{1,0:T(8,128)(2,1)S(1)}, u32[]{:S(2)}, u32[]{:S(2)}) collective-permute-start(bf16[272,128]{1,0:T(8,128)(2,1)S(1)} %shard_map.138.refs_4_), channel_id=1, source_target_pairs={{0,24},{2,26},{4,28},{6,30},{8,16},{10,18},{12,20},{14,22},{16,8},... | collective-permute-start | bytes 208904 | tf_op jit(solution)/shard_map/ppermute | solution.py:376
  15.0 5.4 %collective-permute-start.4 = (bf16[272,128]{1,0:T(8,128)(2,1)S(1)}, bf16[272,128]{1,0:T(8,128)(2,1)S(1)}, u32[]{:S(2)}, u32[]{:S(2)}) collective-permute-start(bf16[272,128]{1,0:T(8,128)(2,1)S(1)} %shard_map.138.refs_4_), channel_id=1, source_target_pairs={{0,16},{2,18},{4,20},{6,22},{8,24},{10,26},{12,28},{14,30},{16,0},... | collective-permute-start | bytes 208904 | tf_op jit(solution)/shard_map/ppermute | solution.py:376
  20.3 4.3 %collective-permute-start.3 = (bf16[272,128]{1,0:T(8,128)(2,1)S(1)}, bf16[272,128]{1,0:T(8,128)(2,1)S(1)}, u32[]{:S(2)}, u32[]{:S(2)}) collective-permute-start(bf16[272,128]{1,0:T(8,128)(2,1)S(1)} %shard_map.138.refs_4_), channel_id=1, source_target_pairs={{0,8},{2,10},{4,12},{6,14},{8,0},{10,2},{12,4},{14,6},{16,24},{18,... | collective-permute-start | bytes 208904 | tf_op jit(solution)/shard_map/ppermute | solution.py:376
  24.8 4.3 %collective-permute-start.6 = (bf16[256,128]{1,0:T(8,128)(2,1)S(1)}, bf16[256,128]{1,0:T(8,128)(2,1)S(1)}, u32[]{:S(2)}, u32[]{:S(2)}) collective-permute-start(bf16[256,128]{1,0:T(8,128)(2,1)S(1)} %get-tuple-element.43), channel_id=1, source_target_pairs={{0,2},{2,0},{4,6},{6,4},{8,10},{10,8},{12,14},{14,12},{16,18},{18,... | collective-permute-start | bytes 196616 | tf_op jit(solution)/shard_map/ppermute | solution.py:376
  25.4 9.2 %collective-permute-start.7 = (bf16[256,128]{1,0:T(8,128)(2,1)S(1)}, bf16[256,128]{1,0:T(8,128)(2,1)S(1)}, u32[]{:S(2)}, u32[]{:S(2)}) collective-permute-start(bf16[256,128]{1,0:T(8,128)(2,1)S(1)} %get-tuple-element.44), channel_id=1, source_target_pairs={{0,4},{2,6},{4,0},{6,2},{8,12},{10,14},{12,8},{14,10},{16,20},{18,... | collective-permute-start | bytes 196616 | tf_op jit(solution)/shard_map/ppermute | solution.py:376
  29.1 5.5 %collective-permute-start.8 = (bf16[256,128]{1,0:T(8,128)(2,1)S(1)}, bf16[256,128]{1,0:T(8,128)(2,1)S(1)}, u32[]{:S(2)}, u32[]{:S(2)}) collective-permute-start(bf16[256,128]{1,0:T(8,128)(2,1)S(1)} %get-tuple-element.45), channel_id=1, source_target_pairs={{0,6},{2,4},{4,2},{6,0},{8,14},{10,12},{12,10},{14,8},{16,22},{18,... | collective-permute-start | bytes 196616 | tf_op jit(solution)/shard_map/ppermute | solution.py:376
  35.0 2.6 %collective-permute-start.9 = (bf16[64,1024]{1,0:T(8,128)(2,1)S(1)}, bf16[64,1024]{1,0:T(8,128)(2,1)S(1)}, u32[]{:S(2)}, u32[]{:S(2)}) collective-permute-start(bf16[64,1024]{1,0:T(8,128)(2,1)S(1)} %shard_map.140), channel_id=1, source_target_pairs={{0,1},{1,0},{2,3},{3,2},{4,5},{5,4},{6,7},{7,6},{8,9},{9,8},{10,11... | collective-permute-start | bytes 393224 | tf_op jit(solution)/shard_map/ppermute | solution.py:424
  35.1 2.6 %copy-start = (s32[64,2]{0,1:T(2,128)S(1)}, s32[64,2]{0,1:T(2,128)}, u32[]{:S(2)}) copy-start(s32[64,2]{0,1:T(2,128)} %param.23) | copy-start | bytes 1540
  35.1 2.6 %copy-start.1 = (f32[64,2]{0,1:T(2,128)S(1)}, f32[64,2]{0,1:T(2,128)}, u32[]{:S(2)}) copy-start(f32[64,2]{0,1:T(2,128)} %param.24) | copy-start | bytes 1540

commit v5 on v4

--- a/solution.py
+++ b/solution.py
@@ -102,25 +102,22 @@
 
 
 def intra_kernel(
-    place_ref, total_ref, key_ref, q_hbm, v_hbm, gate_hbm, gain_hbm, w_hbm, intra_ref, qe_ref, gated_ref, w_ref,
-    q_ref, v_ref, gate_ref, gain_ref, sem,
+    place_ref, total_ref, key_ref, q_hbm, v_hbm, w_hbm, intra_ref, qe_ref, w_ref, q_ref, v_ref, sem
 ):
     length, block = q_ref.shape[1:]
     member = member_of(place_ref)
     copies = []
     for k in range(GROUP):
         lanes = pl.ds(pl.multiple_of((member ^ k) * block, block), block)
-        pairs = ((q_hbm, q_ref), (v_hbm, v_ref), (gate_hbm, gate_ref), (gain_hbm, gain_ref))
         copies.append(
             fetch(
                 [
-                    pltpu.make_async_copy(hbm.at[:, lanes], ref.at[k], sem.at[4 * k + i])
-                    for i, (hbm, ref) in enumerate(pairs)
+                    pltpu.make_async_copy(hbm.at[:, lanes], ref.at[k], sem.at[2 * k + i])
+                    for i, (hbm, ref) in enumerate(((q_hbm, q_ref), (v_hbm, v_ref)))
                 ]
             )
         )
-    ahead = pltpu.make_async_copy(w_hbm, w_ref, sem.at[4 * GROUP])
-    ahead.start()
+    ahead = side_rows(w_hbm, w_ref, side_of(place_ref), sem.at[2 * GROUP])
     t = lax.broadcasted_iota(jnp.int32, (length, length), 0)
     s = lax.broadcasted_iota(jnp.int32, (length, length), 1)
     for k in range(GROUP):
@@ -132,14 +129,51 @@
         scaled_query = (query * jnp.exp(total - middle)).astype(bf16)
         scaled_key = (key_ref[k] * jnp.exp(middle - total)).astype(bf16)
         qe_ref[k] = (query * jnp.exp(total)).astype(bf16)
-        gate = gate_ref[k].astype(f32)
-        gated_ref[k] = gain_ref[k] * (gate * sigmoid(gate))
         for h in range(block // HEAD_DIM):
             lanes = slice(h * HEAD_DIM, (h + 1) * HEAD_DIM)
             scores = dot(scaled_query[:, lanes], scaled_key[:, lanes], NT)
             scores = jnp.where(t >= s, scores, 0.0).astype(bf16)
             intra_ref[k, :, lanes] = dot(scores, v_ref[k, :, lanes])
     ahead.wait()
+
+
+def side_rows(hbm, ref, side, sem):
+    rows = ref.shape[0]
+    copy = pltpu.make_async_copy(hbm.at[pl.ds(pl.multiple_of(side * rows, rows), rows)], ref, sem)
+    copy.start()
+    return copy
+
+
+def gate_kernel(place_ref, gate_hbm, gain_hbm, w_hbm, gated_ref, w_ref, gate_ref, gain_ref, sem):
+    block = gate_ref.shape[2]
+    copies = []
+    for k in range(GROUP):
+        lanes = pl.ds(pl.multiple_of((member_of(place_ref) ^ k) * block, block), block)
+        copies.append(
+            fetch(
+                [
+                    pltpu.make_async_copy(hbm.at[:, lanes], ref.at[k], sem.at[2 * k + i])
+                    for i, (hbm, ref) in enumerate(((gate_hbm, gate_ref), (gain_hbm, gain_ref)))
+                ]
+            )
+        )
+    ahead = side_rows(w_hbm, w_ref, 1 - side_of(place_ref), sem.at[2 * GROUP])
+    for k in range(GROUP):
+        for copy in copies[k]:
+            copy.wait()
+        gate = gate_ref[k].astype(f32)
+        gated_ref[k] = gain_ref[k] * (gate * sigmoid(gate))
+    ahead.wait()
+
+
+def bring_kernel(*refs):
+    count = len(refs) // 2
+    sem = refs[-1]
+    copies = fetch(
+        [pltpu.make_async_copy(refs[i], refs[count + i], sem.at[i]) for i in range(count)]
+    )
+    for copy in copies:
+        copy.wait()
 
 
 def total_kernel(place_ref, *refs):
@@ -206,19 +240,10 @@
 
 
 def keep_kernel(place_ref, intra_ref, qe_ref, gated_ref, *refs):
-    states, (w_ref, g_hbm, u_hbm, acc_ref, g_ref, u_ref, mix_ref, sem) = refs[:GROUP], refs[GROUP:]
-    channels = mix_ref.shape[1]
-    own = side_of(place_ref)
-    ahead = fetch(
-        [
-            pltpu.make_async_copy(g_hbm, g_ref, sem.at[0]),
-            pltpu.make_async_copy(u_hbm, u_ref, sem.at[1]),
-        ]
-    )
-    mixed_rows(mix_ref, own, member_of(place_ref), intra_ref, qe_ref, gated_ref, states)
-    acc_ref[...] = dot(mix_ref[...], w_ref[pl.ds(pl.multiple_of(own * channels, channels), channels)])
-    for copy in ahead:
-        copy.wait()
+    states, (w_ref, acc_ref, mix_ref) = refs[:GROUP], refs[GROUP:]
+    side, member = side_of(place_ref), member_of(place_ref)
+    mixed_rows(mix_ref, side, member, intra_ref, qe_ref, gated_ref, states)
+    acc_ref[...] = dot(mix_ref[...], w_ref[...])
 
 
 def slots_of(routing, capacity):
@@ -240,34 +265,27 @@
 
 
 def project_kernel(
-    place_ref, recv_ref, acc_ref, route_ref, weight_ref, w_ref, res_hbm, gain_hbm, d0_hbm, u1_hbm, d1_hbm,
-    upd_ref, hi_ref, lo_ref, box_ref, d0_ref, u1_ref, d1_ref,
-    res_ref, gain_ref, sem, *, capacity,
+    place_ref, recv_ref, acc_ref, route_ref, weight_ref, w_ref, res_hbm, gain_hbm, d_hbm,
+    upd_ref, hi_ref, lo_ref, d_ref, *refs, capacity,
 ):
-    half, _ = acc_ref.shape
-    channels = recv_ref.shape[1]
-    other = 1 - side_of(place_ref)
+    boxes, (res_ref, gain_ref, sem) = refs[:-3], refs[-3:]
     copies = fetch(
         [
             pltpu.make_async_copy(res_hbm, res_ref, sem.at[0]),
             pltpu.make_async_copy(gain_hbm, gain_ref, sem.at[1]),
         ]
     )
-    ahead = fetch(
-        [
-            pltpu.make_async_copy(hbm, ref, sem.at[2 + i])
-            for i, (hbm, ref) in enumerate(((d0_hbm, d0_ref), (u1_hbm, u1_ref), (d1_hbm, d1_ref)))
-        ]
-    )
-    place = lax.broadcasted_iota(jnp.int32, (box_ref.shape[0], half), 0)
+    ahead = pltpu.make_async_copy(d_hbm, d_ref, sem.at[2])
+    ahead.start()
+    place = lax.broadcasted_iota(jnp.int32, hi_ref.shape, 0)
     chosen = jnp.zeros(place.shape, f32)
     weighted = jnp.zeros(place.shape, f32)
-    for k, slot in enumerate(slots_of(route_ref[...], capacity)):
+    for k, slot in enumerate(slots_of(route_ref[...] ^ (place_ref[0] >> 1), capacity)):
         chosen = chosen + jnp.where(place == slot, 1.0, 0.0)
         weighted = weighted + jnp.where(place == slot, weight_ref[k : k + 1], 0.0)
     chosen = chosen.astype(bf16)
     hi_ref[...], lo_ref[...] = split(weighted)
-    partial = dot(recv_ref[...], w_ref[pl.ds(pl.multiple_of(other * channels, channels), channels)])
+    partial = dot(recv_ref[...], w_ref[...])
     for copy in copies:
         copy.wait()
     updated = (res_ref[...].astype(f32) + (acc_ref[...] + partial)).astype(bf16)
@@ -275,12 +293,20 @@
     updated = updated.astype(f32)
     scale = lax.rsqrt(jnp.mean(updated * updated, axis=-1, keepdims=True) + epsilon)
     normed = (updated * scale * gain_ref[...]).astype(bf16)
-    box_ref[...] = dot(chosen, normed).astype(bf16)
-    for copy in ahead:
-        copy.wait()
-
-
-def expert_kernel(x_ref, g0_ref, u0_ref, d0_ref, g1_ref, u1_ref, d1_ref, out_ref, hid_ref):
+    box = dot(chosen, normed).astype(bf16)
+    rows = box.shape[0] // len(boxes)
+    for i, ref in enumerate(boxes):
+        ref[...] = box[i * rows : (i + 1) * rows]
+    ahead.wait()
+
+
+def expert_kernel(*refs):
+    blocks = (len(refs) - 8) // 2
+    weights, (x_ref, hid_ref) = refs[blocks : blocks + 6], refs[-2:]
+    g0_ref, u0_ref, d0_ref, g1_ref, u1_ref, d1_ref = weights
+    rows = refs[0].shape[0]
+    for i in range(blocks):
+        x_ref[i * rows : (i + 1) * rows] = refs[i][...]
     units = g0_ref.shape[1]
     width = d0_ref.shape[1]
     block = 256
@@ -295,14 +321,20 @@
     for n in range(COLUMNS):
         lanes = slice(n * block, (n + 1) * block)
         out = dot(hid_ref[:, :units], d0_ref[:, lanes]) + dot(hid_ref[:, units:], d1_ref[:, lanes])
-        out_ref[:, lanes] = out.astype(bf16)
-
-
-def combine_kernel(hi_ref, lo_ref, back_ref, upd_ref, out_ref):
+        out = out.astype(bf16)
+        for i in range(blocks):
+            refs[blocks + 6 + i][:, lanes] = out[i * rows : (i + 1) * rows]
+
+
+def combine_kernel(base_ref, hi_ref, lo_ref, *refs, start):
+    blocks, (out_ref, back_ref) = refs[:-2], refs[-2:]
+    rows = blocks[0].shape[0]
+    for i, ref in enumerate(blocks):
+        back_ref[i * rows : (i + 1) * rows] = ref[...]
+    here = slice(start, start + back_ref.shape[0])
     back = back_ref[...]
-    out_ref[...] = (
-        upd_ref[...].astype(f32) + (dot(hi_ref[...], back, TN) + dot(lo_ref[...], back, TN))
-    ).astype(bf16)
+    total = dot(hi_ref[here], back, TN) + dot(lo_ref[here], back, TN)
+    out_ref[...] = (base_ref[...].astype(f32) + total).astype(out_ref.dtype)
 
 
 HBM = pl.BlockSpec(memory_space=pltpu.HBM)
@@ -376,8 +408,6 @@
         return lax.ppermute(x, "sp", [(i, i ^ k) for i in range(ranks)])
 
     weights = (expert_gate[0], expert_up[0], expert_down[0])
-    others = tuple(lax.ppermute(w, "tp", swap) for w in weights)
-
     *states, total, key_gate = call(
         first_kernel,
         [SMEM] + [HBM] * 3,
@@ -387,18 +417,17 @@
         + [pltpu.VMEM((GROUP, 1, part), f32), dma((3 * GROUP,))],
     )(place, forget_logit, value, lower_bound.reshape(1, -1))
     states = states[:1] + [away(states[k], k) for k in range(1, GROUP)]
-    intra, qe, gated, w_kept = call(
+    others = tuple(lax.ppermute(w, "tp", swap) for w in weights)
+    intra, qe, w_own = call(
         intra_kernel,
-        [SMEM] + [VMEM] * 2 + [HBM] * 5,
+        [SMEM] + [VMEM] * 2 + [HBM] * 3,
         [
             (VMEM, shape((GROUP, length, part), f32)),
             (VMEM, shape((GROUP, length, part), bf16)),
-            (VMEM, shape((GROUP, length, part), f32)),
-            (KEPT, shape(w_out.shape, bf16)),
+            (KEPT, shape((channels, width), bf16)),
         ],
-        [pltpu.VMEM((GROUP, length, part), bf16)] * 3
-        + [pltpu.VMEM((GROUP, 1, part), f32), dma((4 * GROUP + 1,))],
-    )(place, total, key_gate, query, value, out_gate, head_gain.reshape(1, -1), w_out)
+        [pltpu.VMEM((GROUP, length, part), bf16)] * 2 + [dma((2 * GROUP + 1,))],
+    )(place, total, key_gate, query, value, w_out)
     (totals,) = call(
         total_kernel,
         [SMEM] + [VMEM] * GROUP,
@@ -406,6 +435,16 @@
         [pltpu.VMEM((GROUP, carried, HEAD_DIM), bf16)],
     )(place, *states)
     totals = [totals] + [away(totals, GROUP * k) for k in range(1, groups)]
+    gated, w_other = call(
+        gate_kernel,
+        [SMEM] + [HBM] * 3,
+        [(VMEM, shape((GROUP, length, part), f32)), (KEPT, shape((channels, width), bf16))],
+        [
+            pltpu.VMEM((GROUP, length, part), bf16),
+            pltpu.VMEM((GROUP, 1, part), f32),
+            dma((2 * GROUP + 1,)),
+        ],
+    )(place, out_gate, head_gain.reshape(1, -1), w_out)
     priors = call(
         functools.partial(carry_kernel, groups=groups),
         [SMEM] + [VMEM] * (GROUP + groups),
@@ -418,60 +457,94 @@
     )(place, *states, *totals)
     priors = list(priors[:1]) + [away(priors[k], k) for k in range(1, GROUP)]
 
+    gate_kept, up_kept = call(
+        bring_kernel, [HBM] * 2, [(KEPT, shape((width, units), bf16))] * 2, [dma((2,))]
+    )(*weights[:2])
+
     mix_args = (place, intra, qe, gated, *priors)
     mix_specs = [SMEM] + [VMEM] * (3 + GROUP)
     (send,) = call(send_kernel, mix_specs, [(VMEM, shape((half, channels), bf16))])(*mix_args)
     recv = lax.ppermute(send, "tp", swap)
-    partial, gate_kept, up_kept = call(
+    (partial,) = call(
         keep_kernel,
-        mix_specs + [KEPT, HBM, HBM],
-        [(VMEM, shape((half, width), f32))] + [(KEPT, shape((width, units), bf16))] * 2,
-        [pltpu.VMEM((half, channels), bf16), dma((2,))],
-    )(*mix_args, w_kept, *weights[:2])
+        mix_specs + [KEPT],
+        [(VMEM, shape((half, width), f32))],
+        [pltpu.VMEM((half, channels), bf16)],
+    )(*mix_args, w_own)
     recv, others = lax.optimization_barrier((recv, others))
-    updated, hi, lo, outbox, down_kept, other_up, other_down = call(
+    direct = capacity % 16 == 0
+    blocks = ranks if direct else 1
+    block = shape((slots // blocks, width), bf16)
+    updated, hi, lo, down_kept, *boxes = call(
         functools.partial(project_kernel, capacity=capacity),
-        [SMEM] + [VMEM] * 4 + [KEPT] + [HBM] * 5,
+        [SMEM] + [VMEM] * 4 + [KEPT] + [HBM] * 3,
         [
             (VMEM, shape((half, width), bf16)),
             (VMEM, shape((slots, half), bf16)),
             (VMEM, shape((slots, half), bf16)),
-            (VMEM, shape((slots, width), bf16)),
             (KEPT, shape((units, width), bf16)),
-            (KEPT, shape((width, units), bf16)),
-            (KEPT, shape((units, width), bf16)),
-        ],
-        [pltpu.VMEM((half, width), bf16), pltpu.VMEM((1, width), f32), dma((5,))],
+        ]
+        + [(VMEM, block)] * blocks,
+        [pltpu.VMEM((half, width), bf16), pltpu.VMEM((1, width), f32), dma((3,))],
     )(
         place,
         recv,
         partial,
         routing.T,
         route_weight.T,
-        w_kept,
+        w_other,
         residual_in,
         ffn_gain.reshape(1, -1),
         weights[2],
-        *others[1:],
     )
-
-    arrived = lax.all_to_all(
-        outbox.reshape(ranks, capacity, width), "sp", split_axis=0, concat_axis=0, tiled=True
-    )
-    (expert_out,) = call(
-        expert_kernel,
-        [VMEM] + [KEPT] * 6,
-        [(VMEM, shape((slots, width), bf16))],
-        [pltpu.VMEM((slots, 2 * units), bf16)],
-    )(arrived.reshape(slots, width), gate_kept, up_kept, down_kept, others[0], other_up, other_down)
-
-    returned = lax.all_to_all(
-        expert_out.reshape(ranks, capacity, width), "sp", split_axis=0, concat_axis=0, tiled=True
-    )
-    (layer_out,) = call(
-        combine_kernel, [VMEM] * 4, [(VMEM, shape((half, width), bf16))]
-    )(hi, lo, returned.reshape(slots, width), updated)
-    return layer_out
+    kept = (gate_kept, up_kept, down_kept, *others)
+
+    def experts(arrays):
+        rows = sum(x.shape[0] for x in arrays)
+        return call(
+            expert_kernel,
+            [VMEM] * len(arrays) + [KEPT] * 6,
+            [(VMEM, shape(x.shape, bf16)) for x in arrays],
+            [pltpu.VMEM((rows, width), bf16), pltpu.VMEM((rows, 2 * units), bf16)],
+        )(*arrays, *kept)
+
+    def combine(base, arrays, start, kind):
+        rows = sum(x.shape[0] for x in arrays)
+        (out,) = call(
+            functools.partial(combine_kernel, start=start),
+            [VMEM] * (3 + len(arrays)),
+            [(VMEM, shape((half, width), kind))],
+            [pltpu.VMEM((rows, width), bf16)],
+        )(base, hi, lo, *arrays)
+        return out
+
+    if not direct:
+
+        def exchange(x):
+            order = jnp.arange(ranks, dtype=jnp.int32) ^ rank
+            x = jnp.take(x.reshape(ranks, capacity, width), order, axis=0)
+            x = lax.all_to_all(x, "sp", split_axis=0, concat_axis=0, tiled=True)
+            return jnp.take(x, order, axis=0).reshape(slots, width)
+
+        (result,) = experts([exchange(boxes[0])])
+        return combine(updated, [exchange(result)], 0, bf16)
+
+    def moved(arrays, ks):
+        out = []
+        for k, x in zip(ks, arrays):
+            out.append(away(x, k) if k else x)
+        return out
+
+    middle = ranks // 2
+    near, far = range(middle), range(middle, ranks)
+    near_in = moved(boxes[:middle], near)
+    far_in = moved(boxes[middle:], far)
+    near_out = experts(near_in)
+    near_back = moved(near_out, near)
+    far_out = experts(far_in)
+    far_back = moved(far_out, far)
+    base = combine(updated, near_back, 0, f32)
+    return combine(base, far_back, middle * capacity, bf16)
 
 
 def solution(mesh):

time: 110 us -> 118 us (1.073)
  the two profiles are of different devices: /device:TPU:8 before, /device:TPU:0 now
where the time goes in v5:
time: 118 us; the launch traced here: 117 us
  starting transfers between devices  74.1 us (63%)
  Pallas kernels  24.3 us (21%)
  waiting for transfers between devices  18.7 us (16%)
    ppermute x39, starting transfers between devices, away(): return lax.ppermute(x, 'sp', [(i, i ^ k) for i in range(ranks)])  73 us
    pallas_call x13, Pallas kernels, placed(): run(*(pltpu.with_memory_space_constraint(arg, fixed(spec)) if fixed(spec)...  24.3 us
    ppermute x39, waiting for transfers between devices, away(): return lax.ppermute(x, 'sp', [(i, i ^ k) for i in range(ranks)])  18.6 us
  transfers between devices with their start and end apart: 43, of which 11 were waited for; matrix products, arithmetic and copies ran while one was open for 0% of the time, Pallas kernels for 18%

profile of v5, /device:TPU:0, one launch (start us, length us, event | category | flops | bytes accessed | tf_op | source)
XLA Modules:
  0.0 117.3 jit_solution(13449279154547080003)
XLA Ops:
  1.0 2.8 %shard_map.136 = (bf16[272,128]{1,0:T(8,128)(2,1)S(1)}, bf16[272,128]{1,0:T(8,128)(2,1)S(1)}, bf16[272,128]{1,0:T(8,128)(2,1)S(1)}, bf16[272,128]{1,0:T(8,128)(2...) custom-call(s32[1]{0:T(128)} %bitcast.place_ref, bf16[128,1024]{1,0:T(8,128)(2,1)} %f_hbm.1, ...), custom_call_target="tpu_custom_call" | custom-call | tf_op jit(solution)/shard_map/pallas_call | solution.py:363
  3.9 2.5 %collective-permute-start = (bf16[272,128]{1,0:T(8,128)(2,1)S(1)}, bf16[272,128]{1,0:T(8,128)(2,1)S(1)}, u32[]{:S(2)}, u32[]{:S(2)}) collective-permute-start(bf16[272,128]{1,0:T(8,128)(2,1)S(1)} %get-tuple-element.68), channel_id=1, source_target_pairs={{0,2},{2,0},{4,6},{6,4},{8,10},{10,8},{12,14},{14,12},{16,18},{18,... | collective-permute-start | bytes 208904 | tf_op jit(solution)/shard_map/ppermute | solution.py:408
  6.4 1.5 %collective-permute-start.1 = (bf16[272,128]{1,0:T(8,128)(2,1)S(1)}, bf16[272,128]{1,0:T(8,128)(2,1)S(1)}, u32[]{:S(2)}, u32[]{:S(2)}) collective-permute-start(bf16[272,128]{1,0:T(8,128)(2,1)S(1)} %get-tuple-element.69), channel_id=1, source_target_pairs={{0,4},{2,6},{4,0},{6,2},{8,12},{10,14},{12,8},{14,10},{16,20},{18,... | collective-permute-start | bytes 208904 | tf_op jit(solution)/shard_map/ppermute | solution.py:408
  7.9 1.3 %collective-permute-done.refs_1_ = bf16[272,128]{1,0:T(8,128)(2,1)S(1)} collective-permute-done((bf16[272,128]{1,0:T(8,128)(2,1)S(1)}, bf16[272,128]{1,0:T(8,128)(2,1)S(1)}, u32[]{:S(2)}, u32[]{:S(2)}) %collective-permute-start) | collective-permute-done | bytes 69664 | tf_op jit(solution)/shard_map/ppermute | solution.py:408
  9.3 2.7 %collective-permute-start.2 = (bf16[272,128]{1,0:T(8,128)(2,1)S(1)}, bf16[272,128]{1,0:T(8,128)(2,1)S(1)}, u32[]{:S(2)}, u32[]{:S(2)}) collective-permute-start(bf16[272,128]{1,0:T(8,128)(2,1)S(1)} %get-tuple-element.70), channel_id=1, source_target_pairs={{0,6},{2,4},{4,2},{6,0},{8,14},{10,12},{12,10},{14,8},{16,22},{18,... | collective-permute-start | bytes 208904 | tf_op jit(solution)/shard_map/ppermute | solution.py:408
  12.0 2.5 %collective-permute-done.2.refs_3_ = bf16[272,128]{1,0:T(8,128)(2,1)S(1)} collective-permute-done((bf16[272,128]{1,0:T(8,128)(2,1)S(1)}, bf16[272,128]{1,0:T(8,128)(2,1)S(1)}, u32[]{:S(2)}, u32[]{:S(2)}) %collective-permute-start.2) | collective-permute-done | bytes 69664 | tf_op jit(solution)/shard_map/ppermute | solution.py:408
  14.5 1.9 %collective-permute-start.3 = (bf16[272,128]{1,0:T(8,128)(2,1)S(1)}, bf16[272,128]{1,0:T(8,128)(2,1)S(1)}, u32[]{:S(2)}, u32[]{:S(2)}) collective-permute-start(bf16[272,128]{1,0:T(8,128)(2,1)S(1)} %shard_map.139.refs_4_), channel_id=1, source_target_pairs={{0,8},{2,10},{4,12},{6,14},{8,0},{10,2},{12,4},{14,6},{16,24},{18,... | collective-permute-start | bytes 208904 | tf_op jit(solution)/shard_map/ppermute | solution.py:408
  16.4 2.6 %collective-permute-start.4 = (bf16[272,128]{1,0:T(8,128)(2,1)S(1)}, bf16[272,128]{1,0:T(8,128)(2,1)S(1)}, u32[]{:S(2)}, u32[]{:S(2)}) collective-permute-start(bf16[272,128]{1,0:T(8,128)(2,1)S(1)} %shard_map.139.refs_4_), channel_id=1, source_target_pairs={{0,16},{2,18},{4,20},{6,22},{8,24},{10,26},{12,28},{14,30},{16,0},... | collective-permute-start | bytes 208904 | tf_op jit(solution)/shard_map/ppermute | solution.py:408
  19.6 3.2 %collective-permute-start.5 = (bf16[272,128]{1,0:T(8,128)(2,1)S(1)}, bf16[272,128]{1,0:T(8,128)(2,1)S(1)}, u32[]{:S(2)}, u32[]{:S(2)}) collective-permute-start(bf16[272,128]{1,0:T(8,128)(2,1)S(1)} %shard_map.139.refs_4_), channel_id=1, source_target_pairs={{0,24},{2,26},{4,28},{6,30},{8,16},{10,18},{12,20},{14,22},{16,8},... | collective-permute-start | bytes 208904 | tf_op jit(solution)/shard_map/ppermute | solution.py:408
  23.1 2.7 %collective-permute-done.5.refs_7_ = bf16[272,128]{1,0:T(8,128)(2,1)S(1)} collective-permute-done((bf16[272,128]{1,0:T(8,128)(2,1)S(1)}, bf16[272,128]{1,0:T(8,128)(2,1)S(1)}, u32[]{:S(2)}, u32[]{:S(2)}) %collective-permute-start.5) | collective-permute-done | bytes 69664 | tf_op jit(solution)/shard_map/ppermute | solution.py:408
  25.9 1.6 %collective-permute-start.6 = (bf16[256,128]{1,0:T(8,128)(2,1)S(1)}, bf16[256,128]{1,0:T(8,128)(2,1)S(1)}, u32[]{:S(2)}, u32[]{:S(2)}) collective-permute-start(bf16[256,128]{1,0:T(8,128)(2,1)S(1)} %get-tuple-element.72), channel_id=1, source_target_pairs={{0,2},{2,0},{4,6},{6,4},{8,10},{10,8},{12,14},{14,12},{16,18},{18,... | collective-permute-start | bytes 196616 | tf_op jit(solution)/shard_map/ppermute | solution.py:408
  27.5 1.5 %collective-permute-start.7 = (bf16[256,128]{1,0:T(8,128)(2,1)S(1)}, bf16[256,128]{1,0:T(8,128)(2,1)S(1)}, u32[]{:S(2)}, u32[]{:S(2)}) collective-permute-start(bf16[256,128]{1,0:T(8,128)(2,1)S(1)} %get-tuple-element.73), channel_id=1, source_target_pairs={{0,4},{2,6},{4,0},{6,2},{8,12},{10,14},{12,8},{14,10},{16,20},{18,... | collective-permute-start | bytes 196616 | tf_op jit(solution)/shard_map/ppermute | solution.py:408
  29.0 1.9 %collective-permute-done.6.refs_1_ = bf16[256,128]{1,0:T(8,128)(2,1)S(1)} collective-permute-done((bf16[256,128]{1,0:T(8,128)(2,1)S(1)}, bf16[256,128]{1,0:T(8,128)(2,1)S(1)}, u32[]{:S(2)}, u32[]{:S(2)}) %collective-permute-start.6) | collective-permute-done | bytes 65568 | tf_op jit(solution)/shard_map/ppermute | solution.py:408
  30.9 1.8 %collective-permute-start.8 = (bf16[256,128]{1,0:T(8,128)(2,1)S(1)}, bf16[256,128]{1,0:T(8,128)(2,1)S(1)}, u32[]{:S(2)}, u32[]{:S(2)}) collective-permute-start(bf16[256,128]{1,0:T(8,128)(2,1)S(1)} %get-tuple-element.74), channel_id=1, source_target_pairs={{0,6},{2,4},{4,2},{6,0},{8,14},{10,12},{12,10},{14,8},{16,22},{18,... | collective-permute-start | bytes 196616 | tf_op jit(solution)/shard_map/ppermute | solution.py:408
  32.7 2.5 %shard_map.138 = (f32[4,128,256]{2,1,0:T(8,128)S(1)}, bf16[1024,2048]{1,0:T(8,128)(2,1)S(1)}) custom-call(s32[1]{0:T(128)} %bitcast.place_ref, bf16[128,1024]{1,0:T(8,128)(2,1)} %gate_hbm.1, f32[1,1024]{1,0:T(1,128)} %bitcast.19, bf16[2048,2048]{1,0:T(8,128)(2,1)} %w_hbm.3), custom_call_target="tpu_custom_call" | custom-call | tf_op jit(solution)/shard_map/pallas_call | solution.py:363
  35.2 2.7 %shard_map.137 = (f32[4,128,256]{2,1,0:T(8,128)S(1)}, bf16[4,128,256]{2,1,0:T(8,128)(2,1)S(1)}, bf16[1024,2048]{1,0:T(8,128)(2,1)S(1)}) custom-call(s32[1]{0:T(128)} %bitcast.place_ref, f32[4,128,256]{2,1,0:T(8,128)S(1)} %get-tuple-element.62.total_ref, f32[4,128,256]{2,1,0:T(8,128)S(1)} %get-tuple-element.63.key_ref, bf16[128,1024]{1,0:T(8,128)(2,1)} %q_hbm.1, ...), custom_call_target="tpu_custom_call" | custom-call | tf_op jit(solution)/shard_map/pallas_call | solution.py:363
  38.4 1.2 %shard_map.142.acc_ref = f32[64,2048]{1,0:T(8,128)S(1)} custom-call(s32[1]{0:T(128)} %bitcast.place_ref, f32[4,128,256]{2,1,0:T(8,128)S(1)} %get-tuple-element.64.intra_ref, bf16[4,128,256]{2,1,0:T(8,128)(2,1)S(1)} %get-tuple-element.65.qe_ref, f32[4,128,256]{2,1,0:T(8,128)S(1)} %get-tuple-element.66.gated_ref, ...), custom_call_target="tpu_custom_call" | custom-call | tf_op jit(solution)/shard_map/pallas_call | solution.py:363
  39.8 2.6 %shard_map.143 = (bf16[64,2048]{1,0:T(8,128)(2,1)S(1)}, bf16[256,64]{1,0:T(8,128)(2,1)S(1)}, bf16[256,64]{1,0:T(8,128)(2,1)S(1)}, bf16[512,2048]{1,0:T(8,128)(2,...) custom-call(s32[1]{0:T(128)} %bitcast.place_ref, ...), custom_call_target="tpu_custom_call" | custom-call | tf_op jit(solution)/shard_map/pallas_call | solution.py:363
  42.8 2.5 %collective-permute-start.28 = (bf16[16,2048]{1,0:T(8,128)(2,1)S(1)}, bf16[16,2048]{1,0:T(8,128)(2,1)S(1)}, u32[]{:S(2)}, u32[]{:S(2)}) collective-permute-start(bf16[16,2048]{1,0:T(8,128)(2,1)S(1)} %get-tuple-element.104), channel_id=1, source_target_pairs={{0,18},{2,16},{4,22},{6,20},{8,26},{10,24},{12,30},{14,28},{16,2},... | collective-permute-start | bytes 196616 | tf_op jit(solution)/shard_map/ppermute | solution.py:408
  46.2 3.9 %collective-permute-start.30 = (bf16[16,2048]{1,0:T(8,128)(2,1)S(1)}, bf16[16,2048]{1,0:T(8,128)(2,1)S(1)}, u32[]{:S(2)}, u32[]{:S(2)}) collective-permute-start(bf16[16,2048]{1,0:T(8,128)(2,1)S(1)} %get-tuple-element.106), channel_id=1, source_target_pairs={{0,22},{2,20},{4,18},{6,16},{8,30},{10,28},{12,26},{14,24},{16,6},... | collective-permute-start | bytes 196616 | tf_op jit(solution)/shard_map/ppermute | solution.py:408
  50.1 3.2 %collective-permute-start.31 = (bf16[16,2048]{1,0:T(8,128)(2,1)S(1)}, bf16[16,2048]{1,0:T(8,128)(2,1)S(1)}, u32[]{:S(2)}, u32[]{:S(2)}) collective-permute-start(bf16[16,2048]{1,0:T(8,128)(2,1)S(1)} %get-tuple-element.107), channel_id=1, source_target_pairs={{0,24},{2,26},{4,28},{6,30},{8,16},{10,18},{12,20},{14,22},{16,8},... | collective-permute-start | bytes 196616 | tf_op jit(solution)/shard_map/ppermute | solution.py:408
  53.3 1.5 %collective-permute-start.32 = (bf16[16,2048]{1,0:T(8,128)(2,1)S(1)}, bf16[16,2048]{1,0:T(8,128)(2,1)S(1)}, u32[]{:S(2)}, u32[]{:S(2)}) collective-permute-start(bf16[16,2048]{1,0:T(8,128)(2,1)S(1)} %get-tuple-element.108), channel_id=1, source_target_pairs={{0,26},{2,24},{4,30},{6,28},{8,18},{10,16},{12,22},{14,20},{16,10}... | collective-permute-start | bytes 196616 | tf_op jit(solution)/shard_map/ppermute | solution.py:408
  54.8 1.7 %collective-permute-done.28.refs_1_ = bf16[16,2048]{1,0:T(8,128)(2,1)S(1)} collective-permute-done((bf16[16,2048]{1,0:T(8,128)(2,1)S(1)}, bf16[16,2048]{1,0:T(8,128)(2,1)S(1)}, u32[]{:S(2)}, u32[]{:S(2)}) %collective-permute-start.28) | collective-permute-done | bytes 65568 | tf_op jit(solution)/shard_map/ppermute | solution.py:408
  56.5 1.2 %collective-permute-start.33 = (bf16[16,2048]{1,0:T(8,128)(2,1)S(1)}, bf16[16,2048]{1,0:T(8,128)(2,1)S(1)}, u32[]{:S(2)}, u32[]{:S(2)}) collective-permute-start(bf16[16,2048]{1,0:T(8,128)(2,1)S(1)} %get-tuple-element.109), channel_id=1, source_target_pairs={{0,28},{2,30},{4,24},{6,26},{8,20},{10,22},{12,16},{14,18},{16,12}... | collective-permute-start | bytes 196616 | tf_op jit(solution)/shard_map/ppermute | solution.py:408
  57.7 3.1 %collective-permute-done.29.refs_2_ = bf16[16,2048]{1,0:T(8,128)(2,1)S(1)} collective-permute-done((bf16[16,2048]{1,0:T(8,128)(2,1)S(1)}, bf16[16,2048]{1,0:T(8,128)(2,1)S(1)}, u32[]{:S(2)}, u32[]{:S(2)}) %collective-permute-start.29) | collective-permute-done | bytes 65568 | tf_op jit(solution)/shard_map/ppermute | solution.py:408
  60.8 2.2 %collective-permute-start.34 = (bf16[16,2048]{1,0:T(8,128)(2,1)S(1)}, bf16[16,2048]{1,0:T(8,128)(2,1)S(1)}, u32[]{:S(2)}, u32[]{:S(2)}) collective-permute-start(bf16[16,2048]{1,0:T(8,128)(2,1)S(1)} %get-tuple-element.110), channel_id=1, source_target_pairs={{0,30},{2,28},{4,26},{6,24},{8,22},{10,20},{12,18},{14,16},{16,14}... | collective-permute-start | bytes 196616 | tf_op jit(solution)/shard_map/ppermute | solution.py:408
  63.0 1.3 %collective-permute-start.13 = (bf16[16,2048]{1,0:T(8,128)(2,1)S(1)}, bf16[16,2048]{1,0:T(8,128)(2,1)S(1)}, u32[]{:S(2)}, u32[]{:S(2)}) collective-permute-start(bf16[16,2048]{1,0:T(8,128)(2,1)S(1)} %get-tuple-element.82), channel_id=1, source_target_pairs={{0,2},{2,0},{4,6},{6,4},{8,10},{10,8},{12,14},{14,12},{16,18},{18,... | collective-permute-start | bytes 196616 | tf_op jit(solution)/shard_map/ppermute | solution.py:408
  64.3 1.1 collective-permute-start.14
  65.4 1.1 collective-permute-start.15
  66.5 3.2 %collective-permute-start.16 = (bf16[16,2048]{1,0:T(8,128)(2,1)S(1)}, bf16[16,2048]{1,0:T(8,128)(2,1)S(1)}, u32[]{:S(2)}, u32[]{:S(2)}) collective-permute-start(bf16[16,2048]{1,0:T(8,128)(2,1)S(1)} %get-tuple-element.85), channel_id=1, source_target_pairs={{0,8},{2,10},{4,12},{6,14},{8,0},{10,2},{12,4},{14,6},{16,24},{18,... | collective-permute-start | bytes 196616 | tf_op jit(solution)/shard_map/ppermute | solution.py:408
  69.7 1.2 %collective-permute-start.17 = (bf16[16,2048]{1,0:T(8,128)(2,1)S(1)}, bf16[16,2048]{1,0:T(8,128)(2,1)S(1)}, u32[]{:S(2)}, u32[]{:S(2)}) collective-permute-start(bf16[16,2048]{1,0:T(8,128)(2,1)S(1)} %get-tuple-element.86), channel_id=1, source_target_pairs={{0,10},{2,8},{4,14},{6,12},{8,2},{10,0},{12,6},{14,4},{16,26},{18,... | collective-permute-start | bytes 196616 | tf_op jit(solution)/shard_map/ppermute | solution.py:408
  70.9 3.4 %collective-permute-start.19 = (bf16[16,2048]{1,0:T(8,128)(2,1)S(1)}, bf16[16,2048]{1,0:T(8,128)(2,1)S(1)}, u32[]{:S(2)}, u32[]{:S(2)}) collective-permute-start(bf16[16,2048]{1,0:T(8,128)(2,1)S(1)} %get-tuple-element.88), channel_id=1, source_target_pairs={{0,14},{2,12},{4,10},{6,8},{8,6},{10,4},{12,2},{14,0},{16,30},{18,... | collective-permute-start | bytes 196616 | tf_op jit(solution)/shard_map/ppermute | solution.py:408
  74.3 2.2 %shard_map.144 = (bf16[2048,512]{1,0:T(8,128)(2,1)S(1)}, bf16[2048,512]{1,0:T(8,128)(2,1)S(1)}) custom-call(bf16[2048,512]{1,0:T(8,128)(2,1)} %bitcast.14, bf16[2048,512]{1,0:T(8,128)(2,1)} %bitcast.16), custom_call_target="tpu_custom_call" | custom-call | tf_op jit(solution)/shard_map/pallas_call | solution.py:363
  76.6 4.1 %shard_map.147 = (bf16[16,2048]{1,0:T(8,128)(2,1)S(1)}, bf16[16,2048]{1,0:T(8,128)(2,1)S(1)}, bf16[16,2048]{1,0:T(8,128)(2,1)S(1)}, bf16[16,2048]{1,0:T(8,128)(2...) custom-call(bf16[16,2048]{1,0:T(8,128)(2,1)S(1)} %collective-permute, ...), custom_call_target="tpu_custom_call" | custom-call | tf_op jit(solution)/shard_map/pallas_call | solution.py:363
  81.3 2.8 %collective-permute-start.36 = (bf16[16,2048]{1,0:T(8,128)(2,1)S(1)}, bf16[16,2048]{1,0:T(8,128)(2,1)S(1)}, u32[]{:S(2)}, u32[]{:S(2)}) collective-permute-start(bf16[16,2048]{1,0:T(8,128)(2,1)S(1)} %get-tuple-element.112), channel_id=1, source_target_pairs={{0,18},{2,16},{4,22},{6,20},{8,26},{10,24},{12,30},{14,28},{16,2},... | collective-permute-start | bytes 196616 | tf_op jit(solution)/shard_map/ppermute | solution.py:408
  84.8 4.1 %shard_map.145 = (bf16[16,2048]{1,0:T(8,128)(2,1)S(1)}, bf16[16,2048]{1,0:T(8,128)(2,1)S(1)}, bf16[16,2048]{1,0:T(8,128)(2,1)S(1)}, bf16[16,2048]{1,0:T(8,128)(2...) custom-call(bf16[16,2048]{1,0:T(8,128)(2,1)S(1)} %get-tuple-element., ...), custom_call_target="tpu_custom_call" | custom-call | tf_op jit(solution)/shard_map/pallas_call | solution.py:363
  88.9 1.8 %collective-permute-start.20 = (bf16[16,2048]{1,0:T(8,128)(2,1)S(1)}, bf16[16,2048]{1,0:T(8,128)(2,1)S(1)}, u32[]{:S(2)}, u32[]{:S(2)}) collective-permute-start(bf16[16,2048]{1,0:T(8,128)(2,1)S(1)} %get-tuple-element.96), channel_id=1, source_target_pairs={{0,2},{2,0},{4,6},{6,4},{8,10},{10,8},{12,14},{14,12},{16,18},{18,... | collective-permute-start | bytes 196616 | tf_op jit(solution)/shard_map/ppermute | solution.py:408
  92.5 2.0 %collective-permute-start.23 = (bf16[16,2048]{1,0:T(8,128)(2,1)S(1)}, bf16[16,2048]{1,0:T(8,128)(2,1)S(1)}, u32[]{:S(2)}, u32[]{:S(2)}) collective-permute-start(bf16[16,2048]{1,0:T(8,128)(2,1)S(1)} %get-tuple-element.99), channel_id=1, source_target_pairs={{0,8},{2,10},{4,12},{6,14},{8,0},{10,2},{12,4},{14,6},{16,24},{18,... | collective-permute-start | bytes 196616 | tf_op jit(solution)/shard_map/ppermute | solution.py:408
  94.5 1.1 collective-permute-start.24
  95.7 1.5 %collective-permute-start.25 = (bf16[16,2048]{1,0:T(8,128)(2,1)S(1)}, bf16[16,2048]{1,0:T(8,128)(2,1)S(1)}, u32[]{:S(2)}, u32[]{:S(2)}) collective-permute-start(bf16[16,2048]{1,0:T(8,128)(2,1)S(1)} %get-tuple-element.101), channel_id=1, source_target_pairs={{0,12},{2,14},{4,8},{6,10},{8,4},{10,6},{12,0},{14,2},{16,28},{18,... | collective-permute-start | bytes 196616 | tf_op jit(solution)/shard_map/ppermute | solution.py:408
  97.2 1.3 %collective-permute-start.26 = (bf16[16,2048]{1,0:T(8,128)(2,1)S(1)}, bf16[16,2048]{1,0:T(8,128)(2,1)S(1)}, u32[]{:S(2)}, u32[]{:S(2)}) collective-permute-start(bf16[16,2048]{1,0:T(8,128)(2,1)S(1)} %get-tuple-element.102), channel_id=1, source_target_pairs={{0,14},{2,12},{4,10},{6,8},{8,6},{10,4},{12,2},{14,0},{16,30},{18,... | collective-permute-start | bytes 196616 | tf_op jit(solution)/shard_map/ppermute | solution.py:408
  98.4 3.6 %collective-permute-start.38 = (bf16[16,2048]{1,0:T(8,128)(2,1)S(1)}, bf16[16,2048]{1,0:T(8,128)(2,1)S(1)}, u32[]{:S(2)}, u32[]{:S(2)}) collective-permute-start(bf16[16,2048]{1,0:T(8,128)(2,1)S(1)} %get-tuple-element.114), channel_id=1, source_target_pairs={{0,22},{2,20},{4,18},{6,16},{8,30},{10,28},{12,26},{14,24},{16,6},... | collective-permute-start | bytes 196616 | tf_op jit(solution)/shard_map/ppermute | solution.py:408
  102.0 1.3 %collective-permute-start.39 = (bf16[16,2048]{1,0:T(8,128)(2,1)S(1)}, bf16[16,2048]{1,0:T(8,128)(2,1)S(1)}, u32[]{:S(2)}, u32[]{:S(2)}) collective-permute-start(bf16[16,2048]{1,0:T(8,128)(2,1)S(1)} %get-tuple-element.115), channel_id=1, source_target_pairs={{0,24},{2,26},{4,28},{6,30},{8,16},{10,18},{12,20},{14,22},{16,8},... | collective-permute-start | bytes 196616 | tf_op jit(solution)/shard_map/ppermute | solution.py:408
  103.4 2.9 %collective-permute-start.40 = (bf16[16,2048]{1,0:T(8,128)(2,1)S(1)}, bf16[16,2048]{1,0:T(8,128)(2,1)S(1)}, u32[]{:S(2)}, u32[]{:S(2)}) collective-permute-start(bf16[16,2048]{1,0:T(8,128)(2,1)S(1)} %get-tuple-element.116), channel_id=1, source_target_pairs={{0,26},{2,24},{4,30},{6,28},{8,18},{10,16},{12,22},{14,20},{16,10}... | collective-permute-start | bytes 196616 | tf_op jit(solution)/shard_map/ppermute | solution.py:408
  106.3 2.1 %collective-permute-start.41 = (bf16[16,2048]{1,0:T(8,128)(2,1)S(1)}, bf16[16,2048]{1,0:T(8,128)(2,1)S(1)}, u32[]{:S(2)}, u32[]{:S(2)}) collective-permute-start(bf16[16,2048]{1,0:T(8,128)(2,1)S(1)} %get-tuple-element.117), channel_id=1, source_target_pairs={{0,28},{2,30},{4,24},{6,26},{8,20},{10,22},{12,16},{14,18},{16,12}... | collective-permute-start | bytes 196616 | tf_op jit(solution)/shard_map/ppermute | solution.py:408
  108.4 3.1 %collective-permute-start.42 = (bf16[16,2048]{1,0:T(8,128)(2,1)S(1)}, bf16[16,2048]{1,0:T(8,128)(2,1)S(1)}, u32[]{:S(2)}, u32[]{:S(2)}) collective-permute-start(bf16[16,2048]{1,0:T(8,128)(2,1)S(1)} %get-tuple-element.118), channel_id=1, source_target_pairs={{0,30},{2,28},{4,26},{6,24},{8,22},{10,20},{12,18},{14,16},{16,14}... | collective-permute-start | bytes 196616 | tf_op jit(solution)/shard_map/ppermute | solution.py:408
  111.8 1.4 %collective-permute-done.41.refs_6_ = bf16[16,2048]{1,0:T(8,128)(2,1)S(1)} collective-permute-done((bf16[16,2048]{1,0:T(8,128)(2,1)S(1)}, bf16[16,2048]{1,0:T(8,128)(2,1)S(1)}, u32[]{:S(2)}, u32[]{:S(2)}) %collective-permute-start.41) | collective-permute-done | bytes 65568 | tf_op jit(solution)/shard_map/ppermute | solution.py:408
  113.2 3.0 %collective-permute-done.42.refs_7_ = bf16[16,2048]{1,0:T(8,128)(2,1)S(1)} collective-permute-done((bf16[16,2048]{1,0:T(8,128)(2,1)S(1)}, bf16[16,2048]{1,0:T(8,128)(2,1)S(1)}, u32[]{:S(2)}, u32[]{:S(2)}) %collective-permute-start.42) | collective-permute-done | bytes 65568 | tf_op jit(solution)/shard_map/ppermute | solution.py:408
  (55 shorter events, 8.4 us)
Async XLA Ops:
  0.0 39.8 %collective-permute-start.10 = (bf16[2048,512]{1,0:T(8,128)(2,1)}, bf16[2048,512]{1,0:T(8,128)(2,1)S(1)}, u32[]{:S(2)}, u32[]{:S(2)}) collective-permute-start(bf16[2048,512]{1,0:T(8,128)(2,1)} %bitcast.13), channel_id=1, source_target_pairs={{0,1},{1,0},{2,3},{3,2},{4,5},{5,4},{6,7},{7,6},{8,9},{9,8},{10,11... | collective-permute-start | bytes 6291464 | tf_op jit(solution)/shard_map/ppermute | solution.py:420
  0.5 39.3 %collective-permute-start.11 = (bf16[2048,512]{1,0:T(8,128)(2,1)}, bf16[2048,512]{1,0:T(8,128)(2,1)}, u32[]{:S(2)}, u32[]{:S(2)}) collective-permute-start(bf16[2048,512]{1,0:T(8,128)(2,1)} %bitcast.15), channel_id=1, source_target_pairs={{0,1},{1,0},{2,3},{3,2},{4,5},{5,4},{6,7},{7,6},{8,9},{9,8},{10,11... | collective-permute-start | bytes 6291464 | tf_op jit(solution)/shard_map/ppermute | solution.py:420
  0.5 39.3 %collective-permute-start.12 = (bf16[512,2048]{1,0:T(8,128)(2,1)}, bf16[512,2048]{1,0:T(8,128)(2,1)}, u32[]{:S(2)}, u32[]{:S(2)}) collective-permute-start(bf16[512,2048]{1,0:T(8,128)(2,1)} %bitcast.11), channel_id=1, source_target_pairs={{0,1},{1,0},{2,3},{3,2},{4,5},{5,4},{6,7},{7,6},{8,9},{9,8},{10,11... | collective-permute-start | bytes 6291464 | tf_op jit(solution)/shard_map/ppermute | solution.py:420
  3.9 5.4 %collective-permute-start = (bf16[272,128]{1,0:T(8,128)(2,1)S(1)}, bf16[272,128]{1,0:T(8,128)(2,1)S(1)}, u32[]{:S(2)}, u32[]{:S(2)}) collective-permute-start(bf16[272,128]{1,0:T(8,128)(2,1)S(1)} %get-tuple-element.68), channel_id=1, source_target_pairs={{0,2},{2,0},{4,6},{6,4},{8,10},{10,8},{12,14},{14,12},{16,18},{18,... | collective-permute-start | bytes 208904 | tf_op jit(solution)/shard_map/ppermute | solution.py:408
  6.4 5.5 %collective-permute-start.1 = (bf16[272,128]{1,0:T(8,128)(2,1)S(1)}, bf16[272,128]{1,0:T(8,128)(2,1)S(1)}, u32[]{:S(2)}, u32[]{:S(2)}) collective-permute-start(bf16[272,128]{1,0:T(8,128)(2,1)S(1)} %get-tuple-element.69), channel_id=1, source_target_pairs={{0,4},{2,6},{4,0},{6,2},{8,12},{10,14},{12,8},{14,10},{16,20},{18,... | collective-permute-start | bytes 208904 | tf_op jit(solution)/shard_map/ppermute | solution.py:408
  9.3 5.2 %collective-permute-start.2 = (bf16[272,128]{1,0:T(8,128)(2,1)S(1)}, bf16[272,128]{1,0:T(8,128)(2,1)S(1)}, u32[]{:S(2)}, u32[]{:S(2)}) collective-permute-start(bf16[272,128]{1,0:T(8,128)(2,1)S(1)} %get-tuple-element.70), channel_id=1, source_target_pairs={{0,6},{2,4},{4,2},{6,0},{8,14},{10,12},{12,10},{14,8},{16,22},{18,... | collective-permute-start | bytes 208904 | tf_op jit(solution)/shard_map/ppermute | solution.py:408
  14.5 5.0 %collective-permute-start.3 = (bf16[272,128]{1,0:T(8,128)(2,1)S(1)}, bf16[272,128]{1,0:T(8,128)(2,1)S(1)}, u32[]{:S(2)}, u32[]{:S(2)}) collective-permute-start(bf16[272,128]{1,0:T(8,128)(2,1)S(1)} %shard_map.139.refs_4_), channel_id=1, source_target_pairs={{0,8},{2,10},{4,12},{6,14},{8,0},{10,2},{12,4},{14,6},{16,24},{18,... | collective-permute-start | bytes 208904 | tf_op jit(solution)/shard_map/ppermute | solution.py:408
  16.4 6.7 %collective-permute-start.4 = (bf16[272,128]{1,0:T(8,128)(2,1)S(1)}, bf16[272,128]{1,0:T(8,128)(2,1)S(1)}, u32[]{:S(2)}, u32[]{:S(2)}) collective-permute-start(bf16[272,128]{1,0:T(8,128)(2,1)S(1)} %shard_map.139.refs_4_), channel_id=1, source_target_pairs={{0,16},{2,18},{4,20},{6,22},{8,24},{10,26},{12,28},{14,30},{16,0},... | collective-permute-start | bytes 208904 | tf_op jit(solution)/shard_map/ppermute | solution.py:408
  19.6 6.2 %collective-permute-start.5 = (bf16[272,128]{1,0:T(8,128)(2,1)S(1)}, bf16[272,128]{1,0:T(8,128)(2,1)S(1)}, u32[]{:S(2)}, u32[]{:S(2)}) collective-permute-start(bf16[272,128]{1,0:T(8,128)(2,1)S(1)} %shard_map.139.refs_4_), channel_id=1, source_target_pairs={{0,24},{2,26},{4,28},{6,30},{8,16},{10,18},{12,20},{14,22},{16,8},... | collective-permute-start | bytes 208904 | tf_op jit(solution)/shard_map/ppermute | solution.py:408
  25.9 5.0 %collective-permute-start.6 = (bf16[256,128]{1,0:T(8,128)(2,1)S(1)}, bf16[256,128]{1,0:T(8,128)(2,1)S(1)}, u32[]{:S(2)}, u32[]{:S(2)}) collective-permute-start(bf16[256,128]{1,0:T(8,128)(2,1)S(1)} %get-tuple-element.72), channel_id=1, source_target_pairs={{0,2},{2,0},{4,6},{6,4},{8,10},{10,8},{12,14},{14,12},{16,18},{18,... | collective-permute-start | bytes 196616 | tf_op jit(solution)/shard_map/ppermute | solution.py:408
  27.5 10.5 %collective-permute-start.7 = (bf16[256,128]{1,0:T(8,128)(2,1)S(1)}, bf16[256,128]{1,0:T(8,128)(2,1)S(1)}, u32[]{:S(2)}, u32[]{:S(2)}) collective-permute-start(bf16[256,128]{1,0:T(8,128)(2,1)S(1)} %get-tuple-element.73), channel_id=1, source_target_pairs={{0,4},{2,6},{4,0},{6,2},{8,12},{10,14},{12,8},{14,10},{16,20},{18,... | collective-permute-start | bytes 196616 | tf_op jit(solution)/shard_map/ppermute | solution.py:408
  30.9 7.1 %collective-permute-start.8 = (bf16[256,128]{1,0:T(8,128)(2,1)S(1)}, bf16[256,128]{1,0:T(8,128)(2,1)S(1)}, u32[]{:S(2)}, u32[]{:S(2)}) collective-permute-start(bf16[256,128]{1,0:T(8,128)(2,1)S(1)} %get-tuple-element.74), channel_id=1, source_target_pairs={{0,6},{2,4},{4,2},{6,0},{8,14},{10,12},{12,10},{14,8},{16,22},{18,... | collective-permute-start | bytes 196616 | tf_op jit(solution)/shard_map/ppermute | solution.py:408
  38.3 1.4 %collective-permute-start.9 = (bf16[64,1024]{1,0:T(8,128)(2,1)S(1)}, bf16[64,1024]{1,0:T(8,128)(2,1)S(1)}, u32[]{:S(2)}, u32[]{:S(2)}) collective-permute-start(bf16[64,1024]{1,0:T(8,128)(2,1)S(1)} %shard_map.141), channel_id=1, source_target_pairs={{0,1},{1,0},{2,3},{3,2},{4,5},{5,4},{6,7},{7,6},{8,9},{9,8},{10,11... | collective-permute-start | bytes 393224 | tf_op jit(solution)/shard_map/ppermute | solution.py:467
  38.4 1.4 %copy-start = (s32[64,2]{0,1:T(2,128)S(1)}, s32[64,2]{0,1:T(2,128)}, u32[]{:S(2)}) copy-start(s32[64,2]{0,1:T(2,128)} %param.23) | copy-start | bytes 1540
  38.4 1.3 %copy-start.1 = (f32[64,2]{0,1:T(2,128)S(1)}, f32[64,2]{0,1:T(2,128)}, u32[]{:S(2)}) copy-start(f32[64,2]{0,1:T(2,128)} %param.24) | copy-start | bytes 1540
  42.3 10.9 %collective-permute-start.27 = (bf16[16,2048]{1,0:T(8,128)(2,1)S(1)}, bf16[16,2048]{1,0:T(8,128)(2,1)S(1)}, u32[]{:S(2)}, u32[]{:S(2)}) collective-permute-start(bf16[16,2048]{1,0:T(8,128)(2,1)S(1)} %get-tuple-element.103), channel_id=1, source_target_pairs={{0,16},{2,18},{4,20},{6,22},{8,24},{10,26},{12,28},{14,30},{16,0},... | collective-permute-start | bytes 196616 | tf_op jit(solution)/shard_map/ppermute | solution.py:408
  42.8 13.7 %collective-permute-start.28 = (bf16[16,2048]{1,0:T(8,128)(2,1)S(1)}, bf16[16,2048]{1,0:T(8,128)(2,1)S(1)}, u32[]{:S(2)}, u32[]{:S(2)}) collective-permute-start(bf16[16,2048]{1,0:T(8,128)(2,1)S(1)} %get-tuple-element.104), channel_id=1, source_target_pairs={{0,18},{2,16},{4,22},{6,20},{8,26},{10,24},{12,30},{14,28},{16,2},... | collective-permute-start | bytes 196616 | tf_op jit(solution)/shard_map/ppermute | solution.py:408
  45.3 15.5 %collective-permute-start.29 = (bf16[16,2048]{1,0:T(8,128)(2,1)S(1)}, bf16[16,2048]{1,0:T(8,128)(2,1)S(1)}, u32[]{:S(2)}, u32[]{:S(2)}) collective-permute-start(bf16[16,2048]{1,0:T(8,128)(2,1)S(1)} %get-tuple-element.105), channel_id=1, source_target_pairs={{0,20},{2,22},{4,16},{6,18},{8,28},{10,30},{12,24},{14,26},{16,4},... | collective-permute-start | bytes 196616 | tf_op jit(solution)/shard_map/ppermute | solution.py:408
  46.2 16.9 %collective-permute-start.30 = (bf16[16,2048]{1,0:T(8,128)(2,1)S(1)}, bf16[16,2048]{1,0:T(8,128)(2,1)S(1)}, u32[]{:S(2)}, u32[]{:S(2)}) collective-permute-start(bf16[16,2048]{1,0:T(8,128)(2,1)S(1)} %get-tuple-element.106), channel_id=1, source_target_pairs={{0,22},{2,20},{4,18},{6,16},{8,30},{10,28},{12,26},{14,24},{16,6},... | collective-permute-start | bytes 196616 | tf_op jit(solution)/shard_map/ppermute | solution.py:408
  50.1 14.2 %collective-permute-start.31 = (bf16[16,2048]{1,0:T(8,128)(2,1)S(1)}, bf16[16,2048]{1,0:T(8,128)(2,1)S(1)}, u32[]{:S(2)}, u32[]{:S(2)}) collective-permute-start(bf16[16,2048]{1,0:T(8,128)(2,1)S(1)} %get-tuple-element.107), channel_id=1, source_target_pairs={{0,24},{2,26},{4,28},{6,30},{8,16},{10,18},{12,20},{14,22},{16,8},... | collective-permute-start | bytes 196616 | tf_op jit(solution)/shard_map/ppermute | solution.py:408
  53.3 12.1 %collective-permute-start.32 = (bf16[16,2048]{1,0:T(8,128)(2,1)S(1)}, bf16[16,2048]{1,0:T(8,128)(2,1)S(1)}, u32[]{:S(2)}, u32[]{:S(2)}) collective-permute-start(bf16[16,2048]{1,0:T(8,128)(2,1)S(1)} %get-tuple-element.108), channel_id=1, source_target_pairs={{0,26},{2,24},{4,30},{6,28},{8,18},{10,16},{12,22},{14,20},{16,10}... | collective-permute-start | bytes 196616 | tf_op jit(solution)/shard_map/ppermute | solution.py:408
  56.5 10.1 %collective-permute-start.33 = (bf16[16,2048]{1,0:T(8,128)(2,1)S(1)}, bf16[16,2048]{1,0:T(8,128)(2,1)S(1)}, u32[]{:S(2)}, u32[]{:S(2)}) collective-permute-start(bf16[16,2048]{1,0:T(8,128)(2,1)S(1)} %get-tuple-element.109), channel_id=1, source_target_pairs={{0,28},{2,30},{4,24},{6,26},{8,20},{10,22},{12,16},{14,18},{16,12}... | collective-permute-start | bytes 196616 | tf_op jit(solution)/shard_map/ppermute | solution.py:408
  60.8 8.9 %collective-permute-start.34 = (bf16[16,2048]{1,0:T(8,128)(2,1)S(1)}, bf16[16,2048]{1,0:T(8,128)(2,1)S(1)}, u32[]{:S(2)}, u32[]{:S(2)}) collective-permute-start(bf16[16,2048]{1,0:T(8,128)(2,1)S(1)} %get-tuple-element.110), channel_id=1, source_target_pairs={{0,30},{2,28},{4,26},{6,24},{8,22},{10,20},{12,18},{14,16},{16,14}... | collective-permute-start | bytes 196616 | tf_op jit(solution)/shard_map/ppermute | solution.py:408
  63.0 7.9 %collective-permute-start.13 = (bf16[16,2048]{1,0:T(8,128)(2,1)S(1)}, bf16[16,2048]{1,0:T(8,128)(2,1)S(1)}, u32[]{:S(2)}, u32[]{:S(2)}) collective-permute-start(bf16[16,2048]{1,0:T(8,128)(2,1)S(1)} %get-tuple-element.82), channel_id=1, source_target_pairs={{0,2},{2,0},{4,6},{6,4},{8,10},{10,8},{12,14},{14,12},{16,18},{18,... | collective-permute-start | bytes 196616 | tf_op jit(solution)/shard_map/ppermute | solution.py:408
  64.3 6.6 %collective-permute-start.14 = (bf16[16,2048]{1,0:T(8,128)(2,1)S(1)}, bf16[16,2048]{1,0:T(8,128)(2,1)S(1)}, u32[]{:S(2)}, u32[]{:S(2)}) collective-permute-start(bf16[16,2048]{1,0:T(8,128)(2,1)S(1)} %get-tuple-element.83), channel_id=1, source_target_pairs={{0,4},{2,6},{4,0},{6,2},{8,12},{10,14},{12,8},{14,10},{16,20},{18,... | collective-permute-start | bytes 196616 | tf_op jit(solution)/shard_map/ppermute | solution.py:408
  65.4 15.3 %collective-permute-start.15 = (bf16[16,2048]{1,0:T(8,128)(2,1)S(1)}, bf16[16,2048]{1,0:T(8,128)(2,1)S(1)}, u32[]{:S(2)}, u32[]{:S(2)}) collective-permute-start(bf16[16,2048]{1,0:T(8,128)(2,1)S(1)} %get-tuple-element.84), channel_id=1, source_target_pairs={{0,6},{2,4},{4,2},{6,0},{8,14},{10,12},{12,10},{14,8},{16,22},{18,... | collective-permute-start | bytes 196616 | tf_op jit(solution)/shard_map/ppermute | solution.py:408
  66.5 14.8 %collective-permute-start.16 = (bf16[16,2048]{1,0:T(8,128)(2,1)S(1)}, bf16[16,2048]{1,0:T(8,128)(2,1)S(1)}, u32[]{:S(2)}, u32[]{:S(2)}) collective-permute-start(bf16[16,2048]{1,0:T(8,128)(2,1)S(1)} %get-tuple-element.85), channel_id=1, source_target_pairs={{0,8},{2,10},{4,12},{6,14},{8,0},{10,2},{12,4},{14,6},{16,24},{18,... | collective-permute-start | bytes 196616 | tf_op jit(solution)/shard_map/ppermute | solution.py:408
  69.7 14.4 %collective-permute-start.17 = (bf16[16,2048]{1,0:T(8,128)(2,1)S(1)}, bf16[16,2048]{1,0:T(8,128)(2,1)S(1)}, u32[]{:S(2)}, u32[]{:S(2)}) collective-permute-start(bf16[16,2048]{1,0:T(8,128)(2,1)S(1)} %get-tuple-element.86), channel_id=1, source_target_pairs={{0,10},{2,8},{4,14},{6,12},{8,2},{10,0},{12,6},{14,4},{16,26},{18,... | collective-permute-start | bytes 196616 | tf_op jit(solution)/shard_map/ppermute | solution.py:408
  70.9 13.9 %collective-permute-start.18 = (bf16[16,2048]{1,0:T(8,128)(2,1)S(1)}, bf16[16,2048]{1,0:T(8,128)(2,1)S(1)}, u32[]{:S(2)}, u32[]{:S(2)}) collective-permute-start(bf16[16,2048]{1,0:T(8,128)(2,1)S(1)} %get-tuple-element.87), channel_id=1, source_target_pairs={{0,12},{2,14},{4,8},{6,10},{8,4},{10,6},{12,0},{14,2},{16,28},{18,... | collective-permute-start | bytes 196616 | tf_op jit(solution)/shard_map/ppermute | solution.py:408
  70.9 13.9 %collective-permute-start.19 = (bf16[16,2048]{1,0:T(8,128)(2,1)S(1)}, bf16[16,2048]{1,0:T(8,128)(2,1)S(1)}, u32[]{:S(2)}, u32[]{:S(2)}) collective-permute-start(bf16[16,2048]{1,0:T(8,128)(2,1)S(1)} %get-tuple-element.88), channel_id=1, source_target_pairs={{0,14},{2,12},{4,10},{6,8},{8,6},{10,4},{12,2},{14,0},{16,30},{18,... | collective-permute-start | bytes 196616 | tf_op jit(solution)/shard_map/ppermute | solution.py:408
  80.7 10.7 %collective-permute-start.35 = (bf16[16,2048]{1,0:T(8,128)(2,1)S(1)}, bf16[16,2048]{1,0:T(8,128)(2,1)S(1)}, u32[]{:S(2)}, u32[]{:S(2)}) collective-permute-start(bf16[16,2048]{1,0:T(8,128)(2,1)S(1)} %get-tuple-element.111), channel_id=1, source_target_pairs={{0,16},{2,18},{4,20},{6,22},{8,24},{10,26},{12,28},{14,30},{16,0},... | collective-permute-start | bytes 196616 | tf_op jit(solution)/shard_map/ppermute | solution.py:408
  81.3 11.2 %collective-permute-start.36 = (bf16[16,2048]{1,0:T(8,128)(2,1)S(1)}, bf16[16,2048]{1,0:T(8,128)(2,1)S(1)}, u32[]{:S(2)}, u32[]{:S(2)}) collective-permute-start(bf16[16,2048]{1,0:T(8,128)(2,1)S(1)} %get-tuple-element.112), channel_id=1, source_target_pairs={{0,18},{2,16},{4,22},{6,20},{8,26},{10,24},{12,30},{14,28},{16,2},... | collective-permute-start | bytes 196616 | tf_op jit(solution)/shard_map/ppermute | solution.py:408
  84.1 10.4 %collective-permute-start.37 = (bf16[16,2048]{1,0:T(8,128)(2,1)S(1)}, bf16[16,2048]{1,0:T(8,128)(2,1)S(1)}, u32[]{:S(2)}, u32[]{:S(2)}) collective-permute-start(bf16[16,2048]{1,0:T(8,128)(2,1)S(1)} %get-tuple-element.113), channel_id=1, source_target_pairs={{0,20},{2,22},{4,16},{6,18},{8,28},{10,30},{12,24},{14,26},{16,4},... | collective-permute-start | bytes 196616 | tf_op jit(solution)/shard_map/ppermute | solution.py:408
  88.9 6.7 %collective-permute-start.20 = (bf16[16,2048]{1,0:T(8,128)(2,1)S(1)}, bf16[16,2048]{1,0:T(8,128)(2,1)S(1)}, u32[]{:S(2)}, u32[]{:S(2)}) collective-permute-start(bf16[16,2048]{1,0:T(8,128)(2,1)S(1)} %get-tuple-element.96), channel_id=1, source_target_pairs={{0,2},{2,0},{4,6},{6,4},{8,10},{10,8},{12,14},{14,12},{16,18},{18,... | collective-permute-start | bytes 196616 | tf_op jit(solution)/shard_map/ppermute | solution.py:408
  90.7 6.5 %collective-permute-start.21 = (bf16[16,2048]{1,0:T(8,128)(2,1)S(1)}, bf16[16,2048]{1,0:T(8,128)(2,1)S(1)}, u32[]{:S(2)}, u32[]{:S(2)}) collective-permute-start(bf16[16,2048]{1,0:T(8,128)(2,1)S(1)} %get-tuple-element.97), channel_id=1, source_target_pairs={{0,4},{2,6},{4,0},{6,2},{8,12},{10,14},{12,8},{14,10},{16,20},{18,... | collective-permute-start | bytes 196616 | tf_op jit(solution)/shard_map/ppermute | solution.py:408
  91.4 7.0 %collective-permute-start.22 = (bf16[16,2048]{1,0:T(8,128)(2,1)S(1)}, bf16[16,2048]{1,0:T(8,128)(2,1)S(1)}, u32[]{:S(2)}, u32[]{:S(2)}) collective-permute-start(bf16[16,2048]{1,0:T(8,128)(2,1)S(1)} %get-tuple-element.98), channel_id=1, source_target_pairs={{0,6},{2,4},{4,2},{6,0},{8,14},{10,12},{12,10},{14,8},{16,22},{18,... | collective-permute-start | bytes 196616 | tf_op jit(solution)/shard_map/ppermute | solution.py:408
  92.5 9.5 %collective-permute-start.23 = (bf16[16,2048]{1,0:T(8,128)(2,1)S(1)}, bf16[16,2048]{1,0:T(8,128)(2,1)S(1)}, u32[]{:S(2)}, u32[]{:S(2)}) collective-permute-start(bf16[16,2048]{1,0:T(8,128)(2,1)S(1)} %get-tuple-element.99), channel_id=1, source_target_pairs={{0,8},{2,10},{4,12},{6,14},{8,0},{10,2},{12,4},{14,6},{16,24},{18,... | collective-permute-start | bytes 196616 | tf_op jit(solution)/shard_map/ppermute | solution.py:408
  94.5 8.8 %collective-permute-start.24 = (bf16[16,2048]{1,0:T(8,128)(2,1)S(1)}, bf16[16,2048]{1,0:T(8,128)(2,1)S(1)}, u32[]{:S(2)}, u32[]{:S(2)}) collective-permute-start(bf16[16,2048]{1,0:T(8,128)(2,1)S(1)} %get-tuple-element.100), channel_id=1, source_target_pairs={{0,10},{2,8},{4,14},{6,12},{8,2},{10,0},{12,6},{14,4},{16,26},{18,... | collective-permute-start | bytes 196616 | tf_op jit(solution)/shard_map/ppermute | solution.py:408
  95.7 10.6 %collective-permute-start.25 = (bf16[16,2048]{1,0:T(8,128)(2,1)S(1)}, bf16[16,2048]{1,0:T(8,128)(2,1)S(1)}, u32[]{:S(2)}, u32[]{:S(2)}) collective-permute-start(bf16[16,2048]{1,0:T(8,128)(2,1)S(1)} %get-tuple-element.101), channel_id=1, source_target_pairs={{0,12},{2,14},{4,8},{6,10},{8,4},{10,6},{12,0},{14,2},{16,28},{18,... | collective-permute-start | bytes 196616 | tf_op jit(solution)/shard_map/ppermute | solution.py:408
  97.2 11.2 %collective-permute-start.26 = (bf16[16,2048]{1,0:T(8,128)(2,1)S(1)}, bf16[16,2048]{1,0:T(8,128)(2,1)S(1)}, u32[]{:S(2)}, u32[]{:S(2)}) collective-permute-start(bf16[16,2048]{1,0:T(8,128)(2,1)S(1)} %get-tuple-element.102), channel_id=1, source_target_pairs={{0,14},{2,12},{4,10},{6,8},{8,6},{10,4},{12,2},{14,0},{16,30},{18,... | collective-permute-start | bytes 196616 | tf_op jit(solution)/shard_map/ppermute | solution.py:408
  98.4 13.4 %collective-permute-start.38 = (bf16[16,2048]{1,0:T(8,128)(2,1)S(1)}, bf16[16,2048]{1,0:T(8,128)(2,1)S(1)}, u32[]{:S(2)}, u32[]{:S(2)}) collective-permute-start(bf16[16,2048]{1,0:T(8,128)(2,1)S(1)} %get-tuple-element.114), channel_id=1, source_target_pairs={{0,22},{2,20},{4,18},{6,16},{8,30},{10,28},{12,26},{14,24},{16,6},... | collective-permute-start | bytes 196616 | tf_op jit(solution)/shard_map/ppermute | solution.py:408
  102.0 9.8 %collective-permute-start.39 = (bf16[16,2048]{1,0:T(8,128)(2,1)S(1)}, bf16[16,2048]{1,0:T(8,128)(2,1)S(1)}, u32[]{:S(2)}, u32[]{:S(2)}) collective-permute-start(bf16[16,2048]{1,0:T(8,128)(2,1)S(1)} %get-tuple-element.115), channel_id=1, source_target_pairs={{0,24},{2,26},{4,28},{6,30},{8,16},{10,18},{12,20},{14,22},{16,8},... | collective-permute-start | bytes 196616 | tf_op jit(solution)/shard_map/ppermute | solution.py:408
  103.4 8.5 %collective-permute-start.40 = (bf16[16,2048]{1,0:T(8,128)(2,1)S(1)}, bf16[16,2048]{1,0:T(8,128)(2,1)S(1)}, u32[]{:S(2)}, u32[]{:S(2)}) collective-permute-start(bf16[16,2048]{1,0:T(8,128)(2,1)S(1)} %get-tuple-element.116), channel_id=1, source_target_pairs={{0,26},{2,24},{4,30},{6,28},{8,18},{10,16},{12,22},{14,20},{16,10}... | collective-permute-start | bytes 196616 | tf_op jit(solution)/shard_map/ppermute | solution.py:408
  106.3 7.0 %collective-permute-start.41 = (bf16[16,2048]{1,0:T(8,128)(2,1)S(1)}, bf16[16,2048]{1,0:T(8,128)(2,1)S(1)}, u32[]{:S(2)}, u32[]{:S(2)}) collective-permute-start(bf16[16,2048]{1,0:T(8,128)(2,1)S(1)} %get-tuple-element.117), channel_id=1, source_target_pairs={{0,28},{2,30},{4,24},{6,26},{8,20},{10,22},{12,16},{14,18},{16,12}... | collective-permute-start | bytes 196616 | tf_op jit(solution)/shard_map/ppermute | solution.py:408
  108.4 7.9 %collective-permute-start.42 = (bf16[16,2048]{1,0:T(8,128)(2,1)S(1)}, bf16[16,2048]{1,0:T(8,128)(2,1)S(1)}, u32[]{:S(2)}, u32[]{:S(2)}) collective-permute-start(bf16[16,2048]{1,0:T(8,128)(2,1)S(1)} %get-tuple-element.118), channel_id=1, source_target_pairs={{0,30},{2,28},{4,26},{6,24},{8,22},{10,20},{12,18},{14,16},{16,14}... | collective-permute-start | bytes 196616 | tf_op jit(solution)/shard_map/ppermute | solution.py:408

commit v6 on v5

--- a/solution.py
+++ b/solution.py
@@ -265,10 +265,8 @@
 
 
 def project_kernel(
-    place_ref, recv_ref, acc_ref, route_ref, weight_ref, w_ref, res_hbm, gain_hbm, d_hbm,
-    upd_ref, hi_ref, lo_ref, d_ref, *refs, capacity,
+    recv_ref, acc_ref, w_ref, res_hbm, gain_hbm, d_hbm, upd_ref, norm_ref, d_ref, res_ref, gain_ref, sem
 ):
-    boxes, (res_ref, gain_ref, sem) = refs[:-3], refs[-3:]
     copies = fetch(
         [
             pltpu.make_async_copy(res_hbm, res_ref, sem.at[0]),
@@ -277,14 +275,6 @@
     )
     ahead = pltpu.make_async_copy(d_hbm, d_ref, sem.at[2])
     ahead.start()
-    place = lax.broadcasted_iota(jnp.int32, hi_ref.shape, 0)
-    chosen = jnp.zeros(place.shape, f32)
-    weighted = jnp.zeros(place.shape, f32)
-    for k, slot in enumerate(slots_of(route_ref[...] ^ (place_ref[0] >> 1), capacity)):
-        chosen = chosen + jnp.where(place == slot, 1.0, 0.0)
-        weighted = weighted + jnp.where(place == slot, weight_ref[k : k + 1], 0.0)
-    chosen = chosen.astype(bf16)
-    hi_ref[...], lo_ref[...] = split(weighted)
     partial = dot(recv_ref[...], w_ref[...])
     for copy in copies:
         copy.wait()
@@ -292,12 +282,49 @@
     upd_ref[...] = updated
     updated = updated.astype(f32)
     scale = lax.rsqrt(jnp.mean(updated * updated, axis=-1, keepdims=True) + epsilon)
-    normed = (updated * scale * gain_ref[...]).astype(bf16)
-    box = dot(chosen, normed).astype(bf16)
-    rows = box.shape[0] // len(boxes)
-    for i, ref in enumerate(boxes):
+    norm_ref[...] = (updated * scale * gain_ref[...]).astype(bf16)
+    ahead.wait()
+
+
+def placed_rows(slots, weights, target, valid):
+    chosen = jnp.zeros(target.shape, f32)
+    weighted = jnp.zeros(target.shape, f32)
+    for k, slot in enumerate(slots):
+        match = (target == slot) & valid
+        chosen = chosen + jnp.where(match, 1.0, 0.0)
+        weighted = weighted + jnp.where(match, weights[k : k + 1], 0.0)
+    return chosen.astype(bf16), *split(weighted)
+
+
+def own_kernel(place_ref, route_ref, weight_ref, norm_ref, box_ref, hi_ref, lo_ref, *, capacity):
+    slots = slots_of(route_ref[...] ^ (place_ref[0] >> 1), capacity)
+    row = lax.broadcasted_iota(jnp.int32, hi_ref.shape, 0)
+    chosen, hi_ref[...], lo_ref[...] = placed_rows(slots, weight_ref[...], row, row >= 0)
+    box_ref[...] = dot(chosen, norm_ref[...]).astype(bf16)
+
+
+def pair_kernel(
+    place_ref, route_ref, weight_ref, other_route_ref, other_weight_ref, norm_ref,
+    box_ref, chosen_ref, hi_ref, lo_ref, other_hi_ref, other_lo_ref, *, capacity,
+):
+    rank, side = place_ref[0] >> 1, side_of(place_ref)
+    row = lax.broadcasted_iota(jnp.int32, hi_ref.shape, 0)
+    core = (row // capacity) % 2
+    target = (row // (2 * capacity) * 2 + side) * capacity + row % capacity
+    slots = slots_of(route_ref[...] ^ rank, capacity)
+    chosen, hi_ref[...], lo_ref[...] = placed_rows(slots, weight_ref[...], target, core == side)
+    box_ref[...] = dot(chosen, norm_ref[...]).astype(bf16)
+    slots = slots_of(other_route_ref[...] ^ rank, capacity)
+    chosen_ref[...], other_hi_ref[...], other_lo_ref[...] = placed_rows(
+        slots, other_weight_ref[...], target, core != side
+    )
+
+
+def pack_kernel(box_ref, chosen_ref, norm_ref, *outs):
+    box = (box_ref[...].astype(f32) + dot(chosen_ref[...], norm_ref[...])).astype(bf16)
+    rows = box.shape[0] // len(outs)
+    for i, ref in enumerate(outs):
         ref[...] = box[i * rows : (i + 1) * rows]
-    ahead.wait()
 
 
 def expert_kernel(*refs):
@@ -326,15 +353,22 @@
             refs[blocks + 6 + i][:, lanes] = out[i * rows : (i + 1) * rows]
 
 
-def combine_kernel(base_ref, hi_ref, lo_ref, *refs, start):
-    blocks, (out_ref, back_ref) = refs[:-2], refs[-2:]
+def combine_kernel(*refs, start, count):
+    outs, back_ref = refs[-1 - count : -1], refs[-1]
+    blocks = refs[3 * count : -1 - count]
     rows = blocks[0].shape[0]
     for i, ref in enumerate(blocks):
         back_ref[i * rows : (i + 1) * rows] = ref[...]
     here = slice(start, start + back_ref.shape[0])
     back = back_ref[...]
-    total = dot(hi_ref[here], back, TN) + dot(lo_ref[here], back, TN)
-    out_ref[...] = (base_ref[...].astype(f32) + total).astype(out_ref.dtype)
+    for i, out_ref in enumerate(outs):
+        base_ref, hi_ref, lo_ref = refs[3 * i : 3 * i + 3]
+        total = dot(hi_ref[here], back, TN) + dot(lo_ref[here], back, TN)
+        out_ref[...] = (base_ref[...].astype(f32) + total).astype(out_ref.dtype)
+
+
+def add_kernel(a_ref, b_ref, out_ref):
+    out_ref[...] = (a_ref[...] + b_ref[...].astype(f32)).astype(out_ref.dtype)
 
 
 HBM = pl.BlockSpec(memory_space=pltpu.HBM)
@@ -418,6 +452,9 @@
     )(place, forget_logit, value, lower_bound.reshape(1, -1))
     states = states[:1] + [away(states[k], k) for k in range(1, GROUP)]
     others = tuple(lax.ppermute(w, "tp", swap) for w in weights)
+    route, weight = routing.T, route_weight.T
+    other_route = lax.ppermute(route, "tp", swap)
+    other_weight = lax.ppermute(weight, "tp", swap)
     intra, qe, w_own = call(
         intra_kernel,
         [SMEM] + [VMEM] * 2 + [HBM] * 3,
@@ -471,33 +508,18 @@
         [(VMEM, shape((half, width), f32))],
         [pltpu.VMEM((half, channels), bf16)],
     )(*mix_args, w_own)
-    recv, others = lax.optimization_barrier((recv, others))
-    direct = capacity % 16 == 0
-    blocks = ranks if direct else 1
-    block = shape((slots // blocks, width), bf16)
-    updated, hi, lo, down_kept, *boxes = call(
-        functools.partial(project_kernel, capacity=capacity),
-        [SMEM] + [VMEM] * 4 + [KEPT] + [HBM] * 3,
-        [
-            (VMEM, shape((half, width), bf16)),
-            (VMEM, shape((slots, half), bf16)),
-            (VMEM, shape((slots, half), bf16)),
-            (KEPT, shape((units, width), bf16)),
-        ]
-        + [(VMEM, block)] * blocks,
+    recv, others, other_route, other_weight = lax.optimization_barrier(
+        (recv, others, other_route, other_weight)
+    )
+    updated, normed, down_kept = call(
+        project_kernel,
+        [VMEM] * 2 + [KEPT] + [HBM] * 3,
+        [(VMEM, shape((half, width), bf16))] * 2 + [(KEPT, shape((units, width), bf16))],
         [pltpu.VMEM((half, width), bf16), pltpu.VMEM((1, width), f32), dma((3,))],
-    )(
-        place,
-        recv,
-        partial,
-        routing.T,
-        route_weight.T,
-        w_other,
-        residual_in,
-        ffn_gain.reshape(1, -1),
-        weights[2],
-    )
+    )(recv, partial, w_other, residual_in, ffn_gain.reshape(1, -1), weights[2])
     kept = (gate_kept, up_kept, down_kept, *others)
+    box = (VMEM, shape((slots, width), bf16))
+    table = (VMEM, shape((slots, half), bf16))
 
     def experts(arrays):
         rows = sum(x.shape[0] for x in arrays)
@@ -508,17 +530,16 @@
             [pltpu.VMEM((rows, width), bf16), pltpu.VMEM((rows, 2 * units), bf16)],
         )(*arrays, *kept)
 
-    def combine(base, arrays, start, kind):
+    def combine(sums, arrays, start, kind):
         rows = sum(x.shape[0] for x in arrays)
-        (out,) = call(
-            functools.partial(combine_kernel, start=start),
-            [VMEM] * (3 + len(arrays)),
-            [(VMEM, shape((half, width), kind))],
+        return call(
+            functools.partial(combine_kernel, start=start, count=len(sums)),
+            [VMEM] * (3 * len(sums) + len(arrays)),
+            [(VMEM, shape((half, width), kind))] * len(sums),
             [pltpu.VMEM((rows, width), bf16)],
-        )(base, hi, lo, *arrays)
-        return out
-
-    if not direct:
+        )(*(x for entry in sums for x in entry), *arrays)
+
+    if capacity % 16:
 
         def exchange(x):
             order = jnp.arange(ranks, dtype=jnp.int32) ^ rank
@@ -526,25 +547,50 @@
             x = lax.all_to_all(x, "sp", split_axis=0, concat_axis=0, tiled=True)
             return jnp.take(x, order, axis=0).reshape(slots, width)
 
-        (result,) = experts([exchange(boxes[0])])
-        return combine(updated, [exchange(result)], 0, bf16)
-
-    def moved(arrays, ks):
-        out = []
-        for k, x in zip(ks, arrays):
-            out.append(away(x, k) if k else x)
-        return out
-
-    middle = ranks // 2
-    near, far = range(middle), range(middle, ranks)
-    near_in = moved(boxes[:middle], near)
-    far_in = moved(boxes[middle:], far)
-    near_out = experts(near_in)
-    near_back = moved(near_out, near)
-    far_out = experts(far_in)
-    far_back = moved(far_out, far)
-    base = combine(updated, near_back, 0, f32)
-    return combine(base, far_back, middle * capacity, bf16)
+        outbox, hi, lo = call(
+            functools.partial(own_kernel, capacity=capacity),
+            [SMEM] + [VMEM] * 3,
+            [box, table, table],
+        )(place, route, weight, normed)
+        (result,) = experts([exchange(outbox)])
+        return combine([(updated, hi, lo)], [exchange(result)], 0, bf16)[0]
+
+    other_normed = lax.ppermute(normed, "tp", swap)
+    own_box, chosen, hi, lo, other_hi, other_lo = call(
+        functools.partial(pair_kernel, capacity=capacity), [SMEM] + [VMEM] * 5, [box] + [table] * 5
+    )(place, route, weight, other_route, other_weight, normed)
+    blocks = ranks // 2
+    boxes = call(
+        pack_kernel, [VMEM] * 3, [(VMEM, shape((2 * capacity, width), bf16))] * blocks
+    )(own_box, chosen, other_normed)
+
+    def paired(x, j):
+        pairs = [
+            (i * sides + side, (i ^ (2 * j + side)) * sides + side)
+            for i in range(ranks)
+            for side in range(sides)
+        ]
+        return lax.ppermute(x, ("sp", "tp"), pairs)
+
+    near = list(range(blocks // 2))
+    early = list(range(blocks // 2, blocks * 3 // 4))
+    late = list(range(blocks * 3 // 4, blocks))
+    arrived = [paired(x, j) for j, x in enumerate(boxes)]
+    back = [None] * blocks
+    for group in (early, near, late):
+        for j, x in zip(group, experts([arrived[j] for j in group])):
+            back[j] = paired(x, j)
+    zero = jnp.zeros((half, width), bf16)
+    own, other = combine(
+        [(updated, hi, lo), (zero, other_hi, other_lo)], [back[j] for j in near], 0, f32
+    )
+    start = len(near) * 2 * capacity
+    rest = [back[j] for j in early + late]
+    (other,) = combine([(other, other_hi, other_lo)], rest, start, bf16)
+    extra = lax.ppermute(other, "tp", swap)
+    (own,) = combine([(own, hi, lo)], rest, start, f32)
+    (layer_out,) = call(add_kernel, [VMEM] * 2, [(VMEM, shape((half, width), bf16))])(own, extra)
+    return layer_out
 
 
 def solution(mesh):

time: 118 us -> 107 us (0.907)
  starting transfers between devices: 74.1 us -> 49.8 us
  waiting for transfers between devices: 18.7 us -> 25.4 us
  Pallas kernels: 24.3 us -> 30.8 us
    ppermute x39 -> x9, starting transfers between devices: 73 us -> 19.4 us  [away(): return lax.ppermute(x, 'sp', [(i, i ^ k) for i in range(ranks)])]
    ppermute x0 -> x20, starting transfers between devices: none -> 29.4 us  [the longest x16 26.9 us: paired(): return lax.ppermute(x, ('sp', 'tp'), pairs)]
    ppermute x0 -> x20, waiting for transfers between devices: none -> 16.1 us  [the longest x16 13.8 us: paired(): return lax.ppermute(x, ('sp', 'tp'), pairs)]
    ppermute x39 -> x9, waiting for transfers between devices: 18.6 us -> 9.27 us  [away(): return lax.ppermute(x, 'sp', [(i, i ^ k) for i in range(ranks)])]
    pallas_call x13 -> x18, Pallas kernels: 24.3 us -> 30.8 us  [placed(): run(*(pltpu.with_memory_space_constraint(arg, fixed(spec)) if fixed(spec)...]
  transfers between devices with their start and end apart: 43 -> 33, of which waited for: 11 -> 12; matrix products, arithmetic and copies ran while one was open for 0% -> 0% of each run, Pallas kernels for 18% -> 25%
where the time goes in v6:
time: 107 us; the launch traced here: 106 us
  starting transfers between devices  49.8 us (47%)
  Pallas kernels  30.8 us (29%)
  waiting for transfers between devices  25.4 us (24%)
    pallas_call x18, Pallas kernels, placed(): run(*(pltpu.with_memory_space_constraint(arg, fixed(spec)) if fixed(spec)...  30.8 us
    ppermute x16, starting transfers between devices, paired(): return lax.ppermute(x, ('sp', 'tp'), pairs)  26.9 us
    ppermute x9, starting transfers between devices, away(): return lax.ppermute(x, 'sp', [(i, i ^ k) for i in range(ranks)])  19.4 us
    ppermute x16, waiting for transfers between devices, paired(): return lax.ppermute(x, ('sp', 'tp'), pairs)  13.8 us
    ppermute x9, waiting for transfers between devices, away(): return lax.ppermute(x, 'sp', [(i, i ^ k) for i in range(ranks)])  9.27 us
  transfers between devices with their start and end apart: 33, of which 12 were waited for; matrix products, arithmetic and copies ran while one was open for 0% of the time, Pallas kernels for 25%

profile of v6, /device:TPU:0, one launch (start us, length us, event | category | flops | bytes accessed | tf_op | source)
XLA Modules:
  0.0 106.4 jit_solution(423774789517544183)
XLA Ops:
  0.0 0.5 collective-permute-start.10
  0.5 0.5 collective-permute-start.12
  1.0 2.9 %shard_map.136 = (bf16[272,128]{1,0:T(8,128)(2,1)S(1)}, bf16[272,128]{1,0:T(8,128)(2,1)S(1)}, bf16[272,128]{1,0:T(8,128)(2,1)S(1)}, bf16[272,128]{1,0:T(8,128)(2...) custom-call(s32[1]{0:T(128)} %bitcast.place_ref, bf16[128,1024]{1,0:T(8,128)(2,1)} %f_hbm.1, ...), custom_call_target="tpu_custom_call" | custom-call | tf_op jit(solution)/shard_map/pallas_call | solution.py:397
  3.9 2.5 %collective-permute-start = (bf16[272,128]{1,0:T(8,128)(2,1)S(1)}, bf16[272,128]{1,0:T(8,128)(2,1)S(1)}, u32[]{:S(2)}, u32[]{:S(2)}) collective-permute-start(bf16[272,128]{1,0:T(8,128)(2,1)S(1)} %get-tuple-element.61), channel_id=1, source_target_pairs={{0,2},{2,0},{4,6},{6,4},{8,10},{10,8},{12,14},{14,12},{16,18},{18,... | collective-permute-start | bytes 208904 | tf_op jit(solution)/shard_map/ppermute | solution.py:442
  6.4 1.5 %collective-permute-start.1 = (bf16[272,128]{1,0:T(8,128)(2,1)S(1)}, bf16[272,128]{1,0:T(8,128)(2,1)S(1)}, u32[]{:S(2)}, u32[]{:S(2)}) collective-permute-start(bf16[272,128]{1,0:T(8,128)(2,1)S(1)} %get-tuple-element.62), channel_id=1, source_target_pairs={{0,4},{2,6},{4,0},{6,2},{8,12},{10,14},{12,8},{14,10},{16,20},{18,... | collective-permute-start | bytes 208904 | tf_op jit(solution)/shard_map/ppermute | solution.py:442
  7.9 1.3 %collective-permute-done.refs_1_ = bf16[272,128]{1,0:T(8,128)(2,1)S(1)} collective-permute-done((bf16[272,128]{1,0:T(8,128)(2,1)S(1)}, bf16[272,128]{1,0:T(8,128)(2,1)S(1)}, u32[]{:S(2)}, u32[]{:S(2)}) %collective-permute-start) | collective-permute-done | bytes 69664 | tf_op jit(solution)/shard_map/ppermute | solution.py:442
  9.3 2.7 %collective-permute-start.2 = (bf16[272,128]{1,0:T(8,128)(2,1)S(1)}, bf16[272,128]{1,0:T(8,128)(2,1)S(1)}, u32[]{:S(2)}, u32[]{:S(2)}) collective-permute-start(bf16[272,128]{1,0:T(8,128)(2,1)S(1)} %get-tuple-element.63), channel_id=1, source_target_pairs={{0,6},{2,4},{4,2},{6,0},{8,14},{10,12},{12,10},{14,8},{16,22},{18,... | collective-permute-start | bytes 208904 | tf_op jit(solution)/shard_map/ppermute | solution.py:442
  12.0 2.5 %collective-permute-done.2.refs_3_ = bf16[272,128]{1,0:T(8,128)(2,1)S(1)} collective-permute-done((bf16[272,128]{1,0:T(8,128)(2,1)S(1)}, bf16[272,128]{1,0:T(8,128)(2,1)S(1)}, u32[]{:S(2)}, u32[]{:S(2)}) %collective-permute-start.2) | collective-permute-done | bytes 69664 | tf_op jit(solution)/shard_map/ppermute | solution.py:442
  14.6 1.9 %collective-permute-start.3 = (bf16[272,128]{1,0:T(8,128)(2,1)S(1)}, bf16[272,128]{1,0:T(8,128)(2,1)S(1)}, u32[]{:S(2)}, u32[]{:S(2)}) collective-permute-start(bf16[272,128]{1,0:T(8,128)(2,1)S(1)} %shard_map.139.refs_4_), channel_id=1, source_target_pairs={{0,8},{2,10},{4,12},{6,14},{8,0},{10,2},{12,4},{14,6},{16,24},{18,... | collective-permute-start | bytes 208904 | tf_op jit(solution)/shard_map/ppermute | solution.py:442
  16.4 2.6 %collective-permute-start.4 = (bf16[272,128]{1,0:T(8,128)(2,1)S(1)}, bf16[272,128]{1,0:T(8,128)(2,1)S(1)}, u32[]{:S(2)}, u32[]{:S(2)}) collective-permute-start(bf16[272,128]{1,0:T(8,128)(2,1)S(1)} %shard_map.139.refs_4_), channel_id=1, source_target_pairs={{0,16},{2,18},{4,20},{6,22},{8,24},{10,26},{12,28},{14,30},{16,0},... | collective-permute-start | bytes 208904 | tf_op jit(solution)/shard_map/ppermute | solution.py:442
  19.0 0.5 collective-permute-done.3.refs_5_
  19.6 3.2 %collective-permute-start.5 = (bf16[272,128]{1,0:T(8,128)(2,1)S(1)}, bf16[272,128]{1,0:T(8,128)(2,1)S(1)}, u32[]{:S(2)}, u32[]{:S(2)}) collective-permute-start(bf16[272,128]{1,0:T(8,128)(2,1)S(1)} %shard_map.139.refs_4_), channel_id=1, source_target_pairs={{0,24},{2,26},{4,28},{6,30},{8,16},{10,18},{12,20},{14,22},{16,8},... | collective-permute-start | bytes 208904 | tf_op jit(solution)/shard_map/ppermute | solution.py:442
  23.1 2.6 %collective-permute-done.5.refs_7_ = bf16[272,128]{1,0:T(8,128)(2,1)S(1)} collective-permute-done((bf16[272,128]{1,0:T(8,128)(2,1)S(1)}, bf16[272,128]{1,0:T(8,128)(2,1)S(1)}, u32[]{:S(2)}, u32[]{:S(2)}) %collective-permute-start.5) | collective-permute-done | bytes 69664 | tf_op jit(solution)/shard_map/ppermute | solution.py:442
  25.9 1.6 %collective-permute-start.6 = (bf16[256,128]{1,0:T(8,128)(2,1)S(1)}, bf16[256,128]{1,0:T(8,128)(2,1)S(1)}, u32[]{:S(2)}, u32[]{:S(2)}) collective-permute-start(bf16[256,128]{1,0:T(8,128)(2,1)S(1)} %get-tuple-element.65), channel_id=1, source_target_pairs={{0,2},{2,0},{4,6},{6,4},{8,10},{10,8},{12,14},{14,12},{16,18},{18,... | collective-permute-start | bytes 196616 | tf_op jit(solution)/shard_map/ppermute | solution.py:442
  27.5 1.5 %collective-permute-start.7 = (bf16[256,128]{1,0:T(8,128)(2,1)S(1)}, bf16[256,128]{1,0:T(8,128)(2,1)S(1)}, u32[]{:S(2)}, u32[]{:S(2)}) collective-permute-start(bf16[256,128]{1,0:T(8,128)(2,1)S(1)} %get-tuple-element.66), channel_id=1, source_target_pairs={{0,4},{2,6},{4,0},{6,2},{8,12},{10,14},{12,8},{14,10},{16,20},{18,... | collective-permute-start | bytes 196616 | tf_op jit(solution)/shard_map/ppermute | solution.py:442
  29.0 1.9 %collective-permute-done.6.refs_1_ = bf16[256,128]{1,0:T(8,128)(2,1)S(1)} collective-permute-done((bf16[256,128]{1,0:T(8,128)(2,1)S(1)}, bf16[256,128]{1,0:T(8,128)(2,1)S(1)}, u32[]{:S(2)}, u32[]{:S(2)}) %collective-permute-start.6) | collective-permute-done | bytes 65568 | tf_op jit(solution)/shard_map/ppermute | solution.py:442
  30.9 1.8 %collective-permute-start.8 = (bf16[256,128]{1,0:T(8,128)(2,1)S(1)}, bf16[256,128]{1,0:T(8,128)(2,1)S(1)}, u32[]{:S(2)}, u32[]{:S(2)}) collective-permute-start(bf16[256,128]{1,0:T(8,128)(2,1)S(1)} %get-tuple-element.67), channel_id=1, source_target_pairs={{0,6},{2,4},{4,2},{6,0},{8,14},{10,12},{12,10},{14,8},{16,22},{18,... | collective-permute-start | bytes 196616 | tf_op jit(solution)/shard_map/ppermute | solution.py:442
  32.7 2.5 %shard_map.138 = (f32[4,128,256]{2,1,0:T(8,128)S(1)}, bf16[1024,2048]{1,0:T(8,128)(2,1)S(1)}) custom-call(s32[1]{0:T(128)} %bitcast.place_ref, bf16[128,1024]{1,0:T(8,128)(2,1)} %gate_hbm.1, f32[1,1024]{1,0:T(1,128)} %bitcast.21, bf16[2048,2048]{1,0:T(8,128)(2,1)} %w_hbm.3), custom_call_target="tpu_custom_call" | custom-call | tf_op jit(solution)/shard_map/pallas_call | solution.py:397
  35.2 2.7 %shard_map.137 = (f32[4,128,256]{2,1,0:T(8,128)S(1)}, bf16[4,128,256]{2,1,0:T(8,128)(2,1)S(1)}, bf16[1024,2048]{1,0:T(8,128)(2,1)S(1)}) custom-call(s32[1]{0:T(128)} %bitcast.place_ref, f32[4,128,256]{2,1,0:T(8,128)S(1)} %get-tuple-element.55.total_ref, f32[4,128,256]{2,1,0:T(8,128)S(1)} %get-tuple-element.56.key_ref, bf16[128,1024]{1,0:T(8,128)(2,1)} %q_hbm.1, ...), custom_call_target="tpu_custom_call" | custom-call | tf_op jit(solution)/shard_map/pallas_call | solution.py:397
  38.5 0.5 collective-permute-start.13
  39.0 0.8 collective-permute-done.13.other_route_ref
  40.1 1.2 %shard_map.142.acc_ref = f32[64,2048]{1,0:T(8,128)S(1)} custom-call(s32[1]{0:T(128)} %bitcast.place_ref, f32[4,128,256]{2,1,0:T(8,128)S(1)} %get-tuple-element.57.intra_ref, bf16[4,128,256]{2,1,0:T(8,128)(2,1)S(1)} %get-tuple-element.58.qe_ref, f32[4,128,256]{2,1,0:T(8,128)S(1)} %get-tuple-element.59.gated_ref, ...), custom_call_target="tpu_custom_call" | custom-call | tf_op jit(solution)/shard_map/pallas_call | solution.py:397
  41.4 2.4 %shard_map.143 = (bf16[64,2048]{1,0:T(8,128)(2,1)S(1)}, bf16[64,2048]{1,0:T(8,128)(2,1)S(1)}, bf16[512,2048]{1,0:T(8,128)(2,1)S(1)}) custom-call(bf16[64,1024]{1,0:T(8,128)(2,1)S(1)} %collective-permute-done.9.recv_ref, f32[64,2048]{1,0:T(8,128)S(1)} %shard_map.142.acc_ref, bf16[1024,2048]{1,0:T(8,128)(2,1)S(1)} %get-tuple-element.70.w_ref, ...), custom_call_target="tpu_custom_call" | custom-call | tf_op jit(solution)/shard_map/pallas_call | solution.py:397
  44.1 0.7 shard_map.144
  44.8 0.6 collective-permute-done.15.norm_ref
  45.9 0.7 collective-permute-start.16
  46.5 1.2 %collective-permute-start.17 = (bf16[32,2048]{1,0:T(8,128)(2,1)S(1)}, bf16[32,2048]{1,0:T(8,128)(2,1)S(1)}, u32[]{:S(2)}, u32[]{:S(2)}) collective-permute-start(bf16[32,2048]{1,0:T(8,128)(2,1)S(1)} %get-tuple-element.82), channel_id=1, source_target_pairs={{0,4},{1,7},{2,6},{3,5},{4,0},{5,3},{6,2},{7,1},{8,12},{9,15},{10,... | collective-permute-start | bytes 393224 | tf_op jit(solution)/shard_map/ppermute | solution.py:573
  47.7 2.3 %collective-permute-start.19 = (bf16[32,2048]{1,0:T(8,128)(2,1)S(1)}, bf16[32,2048]{1,0:T(8,128)(2,1)S(1)}, u32[]{:S(2)}, u32[]{:S(2)}) collective-permute-start(bf16[32,2048]{1,0:T(8,128)(2,1)S(1)} %get-tuple-element.84), channel_id=1, source_target_pairs={{0,12},{1,15},{2,14},{3,13},{4,8},{5,11},{6,10},{7,9},{8,4},{9,7},... | collective-permute-start | bytes 393224 | tf_op jit(solution)/shard_map/ppermute | solution.py:573
  50.1 3.2 %collective-permute-start.28 = (bf16[32,2048]{1,0:T(8,128)(2,1)S(1)}, bf16[32,2048]{1,0:T(8,128)(2,1)S(1)}, u32[]{:S(2)}, u32[]{:S(2)}) collective-permute-start(bf16[32,2048]{1,0:T(8,128)(2,1)S(1)} %get-tuple-element.100), channel_id=1, source_target_pairs={{0,24},{1,27},{2,26},{3,25},{4,28},{5,31},{6,30},{7,29},{8,16},{9,... | collective-permute-start | bytes 393224 | tf_op jit(solution)/shard_map/ppermute | solution.py:573
  53.3 1.2 %collective-permute-start.29 = (bf16[32,2048]{1,0:T(8,128)(2,1)S(1)}, bf16[32,2048]{1,0:T(8,128)(2,1)S(1)}, u32[]{:S(2)}, u32[]{:S(2)}) collective-permute-start(bf16[32,2048]{1,0:T(8,128)(2,1)S(1)} %get-tuple-element.101), channel_id=1, source_target_pairs={{0,28},{1,31},{2,30},{3,29},{4,24},{5,27},{6,26},{7,25},{8,20},{9,... | collective-permute-start | bytes 393224 | tf_op jit(solution)/shard_map/ppermute | solution.py:573
  54.5 2.2 %shard_map.146 = (bf16[2048,512]{1,0:T(8,128)(2,1)S(1)}, bf16[2048,512]{1,0:T(8,128)(2,1)S(1)}) custom-call(bf16[2048,512]{1,0:T(8,128)(2,1)} %bitcast.14, bf16[2048,512]{1,0:T(8,128)(2,1)} %bitcast.16), custom_call_target="tpu_custom_call" | custom-call | tf_op jit(solution)/shard_map/pallas_call | solution.py:397
  56.8 3.2 %collective-permute-start.25 = (bf16[32,2048]{1,0:T(8,128)(2,1)S(1)}, bf16[32,2048]{1,0:T(8,128)(2,1)S(1)}, u32[]{:S(2)}, u32[]{:S(2)}) collective-permute-start(bf16[32,2048]{1,0:T(8,128)(2,1)S(1)} %get-tuple-element.97), channel_id=1, source_target_pairs={{0,20},{1,23},{2,22},{3,21},{4,16},{5,19},{6,18},{7,17},{8,28},{9,... | collective-permute-start | bytes 393224 | tf_op jit(solution)/shard_map/ppermute | solution.py:573
  60.1 4.1 %shard_map.147 = (bf16[32,2048]{1,0:T(8,128)(2,1)S(1)}, bf16[32,2048]{1,0:T(8,128)(2,1)S(1)}, bf16[32,2048]{1,0:T(8,128)(2,1)S(1)}, bf16[32,2048]{1,0:T(8,128)(2,1)S(1)}) custom-call(bf16[32,2048]{1,0:T(8,128)(2,1)S(1)} %collective-permute-done.16.refs_0_, bf16[32,2048]{1,0:T(8,128)(2,1)S(1)} %collective-permute-done.17.refs_1_, ...), custom_call_target="tpu_custom_call" | custom-call | tf_op jit(solution)/shard_map/pallas_call | solution.py:397
  64.2 0.8 collective-permute-start.20
  65.1 1.2 %collective-permute-start.21 = (bf16[32,2048]{1,0:T(8,128)(2,1)S(1)}, bf16[32,2048]{1,0:T(8,128)(2,1)S(1)}, u32[]{:S(2)}, u32[]{:S(2)}) collective-permute-start(bf16[32,2048]{1,0:T(8,128)(2,1)S(1)} %get-tuple-element.92), channel_id=1, source_target_pairs={{0,4},{1,7},{2,6},{3,5},{4,0},{5,3},{6,2},{7,1},{8,12},{9,15},{10,... | collective-permute-start | bytes 393224 | tf_op jit(solution)/shard_map/ppermute | solution.py:573
  66.3 4.7 %collective-permute-start.22 = (bf16[32,2048]{1,0:T(8,128)(2,1)S(1)}, bf16[32,2048]{1,0:T(8,128)(2,1)S(1)}, u32[]{:S(2)}, u32[]{:S(2)}) collective-permute-start(bf16[32,2048]{1,0:T(8,128)(2,1)S(1)} %get-tuple-element.93), channel_id=1, source_target_pairs={{0,8},{1,11},{2,10},{3,9},{4,12},{5,15},{6,14},{7,13},{8,0},{9,3},... | collective-permute-start | bytes 393224 | tf_op jit(solution)/shard_map/ppermute | solution.py:573
  70.9 4.6 %shard_map.150 = (bf16[32,2048]{1,0:T(8,128)(2,1)S(1)}, bf16[32,2048]{1,0:T(8,128)(2,1)S(1)}) custom-call(bf16[32,2048]{1,0:T(8,128)(2,1)S(1)} %collective-permute-done.28.refs_0_, bf16[32,2048]{1,0:T(8,128)(2,1)S(1)} %collective-permute-done.29.refs_1_, bf16[2048,512]{1,0:T(8,128)(2,1)S(1)} %get-tuple-element.85.refs_4_.refs_2_, ...), custom_call_target="tpu_custom_call" | custom-call | tf_op jit(solution)/shard_map/pallas_call | solution.py:397
  75.5 0.6 collective-permute-start.23
  76.1 1.4 %collective-permute-start.30 = (bf16[32,2048]{1,0:T(8,128)(2,1)S(1)}, bf16[32,2048]{1,0:T(8,128)(2,1)S(1)}, u32[]{:S(2)}, u32[]{:S(2)}) collective-permute-start(bf16[32,2048]{1,0:T(8,128)(2,1)S(1)} %get-tuple-element.102), channel_id=1, source_target_pairs={{0,24},{1,27},{2,26},{3,25},{4,28},{5,31},{6,30},{7,29},{8,16},{9,... | collective-permute-start | bytes 393224 | tf_op jit(solution)/shard_map/ppermute | solution.py:573
  77.6 4.6 %shard_map.149 = (bf16[32,2048]{1,0:T(8,128)(2,1)S(1)}, bf16[32,2048]{1,0:T(8,128)(2,1)S(1)}) custom-call(bf16[32,2048]{1,0:T(8,128)(2,1)S(1)} %collective-permute-done.24.refs_0_, bf16[32,2048]{1,0:T(8,128)(2,1)S(1)} %collective-permute-done.25.refs_1_, bf16[2048,512]{1,0:T(8,128)(2,1)S(1)} %get-tuple-element.85.refs_4_.refs_2_, ...), custom_call_target="tpu_custom_call" | custom-call | tf_op jit(solution)/shard_map/pallas_call | solution.py:397
  82.1 2.9 %collective-permute-start.31 = (bf16[32,2048]{1,0:T(8,128)(2,1)S(1)}, bf16[32,2048]{1,0:T(8,128)(2,1)S(1)}, u32[]{:S(2)}, u32[]{:S(2)}) collective-permute-start(bf16[32,2048]{1,0:T(8,128)(2,1)S(1)} %get-tuple-element.103), channel_id=1, source_target_pairs={{0,28},{1,31},{2,30},{3,29},{4,24},{5,27},{6,26},{7,25},{8,20},{9,... | collective-permute-start | bytes 393224 | tf_op jit(solution)/shard_map/ppermute | solution.py:573
  85.3 3.1 %collective-permute-start.27 = (bf16[32,2048]{1,0:T(8,128)(2,1)S(1)}, bf16[32,2048]{1,0:T(8,128)(2,1)S(1)}, u32[]{:S(2)}, u32[]{:S(2)}) collective-permute-start(bf16[32,2048]{1,0:T(8,128)(2,1)S(1)} %get-tuple-element.99), channel_id=1, source_target_pairs={{0,20},{1,23},{2,22},{3,21},{4,16},{5,19},{6,18},{7,17},{8,28},{9,... | collective-permute-start | bytes 393224 | tf_op jit(solution)/shard_map/ppermute | solution.py:573
  88.9 1.0 collective-permute-done.31.refs_6_
  90.0 9.6 %collective-permute-done.26.refs_3_ = bf16[32,2048]{1,0:T(8,128)(2,1)S(1)} collective-permute-done((bf16[32,2048]{1,0:T(8,128)(2,1)S(1)}, bf16[32,2048]{1,0:T(8,128)(2,1)S(1)}, u32[]{:S(2)}, u32[]{:S(2)}) %collective-permute-start.26) | collective-permute-done | bytes 131104 | tf_op jit(solution)/shard_map/ppermute | solution.py:573
  99.6 3.2 %collective-permute-done.27.refs_4_ = bf16[32,2048]{1,0:T(8,128)(2,1)S(1)} collective-permute-done((bf16[32,2048]{1,0:T(8,128)(2,1)S(1)}, bf16[32,2048]{1,0:T(8,128)(2,1)S(1)}, u32[]{:S(2)}, u32[]{:S(2)}) %collective-permute-start.27) | collective-permute-done | bytes 131104 | tf_op jit(solution)/shard_map/ppermute | solution.py:573
  103.1 1.4 %collective-permute-start.32 = (bf16[64,2048]{1,0:T(8,128)(2,1)S(1)}, bf16[64,2048]{1,0:T(8,128)(2,1)S(1)}, u32[]{:S(2)}, u32[]{:S(2)}) collective-permute-start(bf16[64,2048]{1,0:T(8,128)(2,1)S(1)} %shard_map.152), channel_id=1, source_target_pairs={{0,1},{1,0},{2,3},{3,2},{4,5},{5,4},{6,7},{7,6},{8,9},{9,8},{10,11... | collective-permute-start | bytes 786440 | tf_op jit(solution)/shard_map/ppermute | solution.py:590
  104.8 0.8 collective-permute-done.32.b_ref
  105.6 0.7 shard_map.153
  (41 shorter events, 3.6 us)
Async XLA Ops:
  0.0 41.4 %collective-permute-start.10 = (bf16[2048,512]{1,0:T(8,128)(2,1)}, bf16[2048,512]{1,0:T(8,128)(2,1)S(1)}, u32[]{:S(2)}, u32[]{:S(2)}) collective-permute-start(bf16[2048,512]{1,0:T(8,128)(2,1)} %bitcast.13), channel_id=1, source_target_pairs={{0,1},{1,0},{2,3},{3,2},{4,5},{5,4},{6,7},{7,6},{8,9},{9,8},{10,11... | collective-permute-start | bytes 6291464 | tf_op jit(solution)/shard_map/ppermute | solution.py:454
  0.5 40.9 %collective-permute-start.11 = (bf16[2048,512]{1,0:T(8,128)(2,1)}, bf16[2048,512]{1,0:T(8,128)(2,1)}, u32[]{:S(2)}, u32[]{:S(2)}) collective-permute-start(bf16[2048,512]{1,0:T(8,128)(2,1)} %bitcast.15), channel_id=1, source_target_pairs={{0,1},{1,0},{2,3},{3,2},{4,5},{5,4},{6,7},{7,6},{8,9},{9,8},{10,11... | collective-permute-start | bytes 6291464 | tf_op jit(solution)/shard_map/ppermute | solution.py:454
  0.5 40.9 %collective-permute-start.12 = (bf16[512,2048]{1,0:T(8,128)(2,1)}, bf16[512,2048]{1,0:T(8,128)(2,1)}, u32[]{:S(2)}, u32[]{:S(2)}) collective-permute-start(bf16[512,2048]{1,0:T(8,128)(2,1)} %bitcast.17), channel_id=1, source_target_pairs={{0,1},{1,0},{2,3},{3,2},{4,5},{5,4},{6,7},{7,6},{8,9},{9,8},{10,11... | collective-permute-start | bytes 6291464 | tf_op jit(solution)/shard_map/ppermute | solution.py:454
  3.9 5.4 %collective-permute-start = (bf16[272,128]{1,0:T(8,128)(2,1)S(1)}, bf16[272,128]{1,0:T(8,128)(2,1)S(1)}, u32[]{:S(2)}, u32[]{:S(2)}) collective-permute-start(bf16[272,128]{1,0:T(8,128)(2,1)S(1)} %get-tuple-element.61), channel_id=1, source_target_pairs={{0,2},{2,0},{4,6},{6,4},{8,10},{10,8},{12,14},{14,12},{16,18},{18,... | collective-permute-start | bytes 208904 | tf_op jit(solution)/shard_map/ppermute | solution.py:442
  6.4 5.6 %collective-permute-start.1 = (bf16[272,128]{1,0:T(8,128)(2,1)S(1)}, bf16[272,128]{1,0:T(8,128)(2,1)S(1)}, u32[]{:S(2)}, u32[]{:S(2)}) collective-permute-start(bf16[272,128]{1,0:T(8,128)(2,1)S(1)} %get-tuple-element.62), channel_id=1, source_target_pairs={{0,4},{2,6},{4,0},{6,2},{8,12},{10,14},{12,8},{14,10},{16,20},{18,... | collective-permute-start | bytes 208904 | tf_op jit(solution)/shard_map/ppermute | solution.py:442
  9.3 5.2 %collective-permute-start.2 = (bf16[272,128]{1,0:T(8,128)(2,1)S(1)}, bf16[272,128]{1,0:T(8,128)(2,1)S(1)}, u32[]{:S(2)}, u32[]{:S(2)}) collective-permute-start(bf16[272,128]{1,0:T(8,128)(2,1)S(1)} %get-tuple-element.63), channel_id=1, source_target_pairs={{0,6},{2,4},{4,2},{6,0},{8,14},{10,12},{12,10},{14,8},{16,22},{18,... | collective-permute-start | bytes 208904 | tf_op jit(solution)/shard_map/ppermute | solution.py:442
  14.6 5.0 %collective-permute-start.3 = (bf16[272,128]{1,0:T(8,128)(2,1)S(1)}, bf16[272,128]{1,0:T(8,128)(2,1)S(1)}, u32[]{:S(2)}, u32[]{:S(2)}) collective-permute-start(bf16[272,128]{1,0:T(8,128)(2,1)S(1)} %shard_map.139.refs_4_), channel_id=1, source_target_pairs={{0,8},{2,10},{4,12},{6,14},{8,0},{10,2},{12,4},{14,6},{16,24},{18,... | collective-permute-start | bytes 208904 | tf_op jit(solution)/shard_map/ppermute | solution.py:442
  16.4 6.7 %collective-permute-start.4 = (bf16[272,128]{1,0:T(8,128)(2,1)S(1)}, bf16[272,128]{1,0:T(8,128)(2,1)S(1)}, u32[]{:S(2)}, u32[]{:S(2)}) collective-permute-start(bf16[272,128]{1,0:T(8,128)(2,1)S(1)} %shard_map.139.refs_4_), channel_id=1, source_target_pairs={{0,16},{2,18},{4,20},{6,22},{8,24},{10,26},{12,28},{14,30},{16,0},... | collective-permute-start | bytes 208904 | tf_op jit(solution)/shard_map/ppermute | solution.py:442
  19.6 6.2 %collective-permute-start.5 = (bf16[272,128]{1,0:T(8,128)(2,1)S(1)}, bf16[272,128]{1,0:T(8,128)(2,1)S(1)}, u32[]{:S(2)}, u32[]{:S(2)}) collective-permute-start(bf16[272,128]{1,0:T(8,128)(2,1)S(1)} %shard_map.139.refs_4_), channel_id=1, source_target_pairs={{0,24},{2,26},{4,28},{6,30},{8,16},{10,18},{12,20},{14,22},{16,8},... | collective-permute-start | bytes 208904 | tf_op jit(solution)/shard_map/ppermute | solution.py:442
  25.9 5.0 %collective-permute-start.6 = (bf16[256,128]{1,0:T(8,128)(2,1)S(1)}, bf16[256,128]{1,0:T(8,128)(2,1)S(1)}, u32[]{:S(2)}, u32[]{:S(2)}) collective-permute-start(bf16[256,128]{1,0:T(8,128)(2,1)S(1)} %get-tuple-element.65), channel_id=1, source_target_pairs={{0,2},{2,0},{4,6},{6,4},{8,10},{10,8},{12,14},{14,12},{16,18},{18,... | collective-permute-start | bytes 196616 | tf_op jit(solution)/shard_map/ppermute | solution.py:442
  27.5 10.5 %collective-permute-start.7 = (bf16[256,128]{1,0:T(8,128)(2,1)S(1)}, bf16[256,128]{1,0:T(8,128)(2,1)S(1)}, u32[]{:S(2)}, u32[]{:S(2)}) collective-permute-start(bf16[256,128]{1,0:T(8,128)(2,1)S(1)} %get-tuple-element.66), channel_id=1, source_target_pairs={{0,4},{2,6},{4,0},{6,2},{8,12},{10,14},{12,8},{14,10},{16,20},{18,... | collective-permute-start | bytes 196616 | tf_op jit(solution)/shard_map/ppermute | solution.py:442
  30.9 7.1 %collective-permute-start.8 = (bf16[256,128]{1,0:T(8,128)(2,1)S(1)}, bf16[256,128]{1,0:T(8,128)(2,1)S(1)}, u32[]{:S(2)}, u32[]{:S(2)}) collective-permute-start(bf16[256,128]{1,0:T(8,128)(2,1)S(1)} %get-tuple-element.67), channel_id=1, source_target_pairs={{0,6},{2,4},{4,2},{6,0},{8,14},{10,12},{12,10},{14,8},{16,22},{18,... | collective-permute-start | bytes 196616 | tf_op jit(solution)/shard_map/ppermute | solution.py:442
  35.2 3.3 %copy-start = (s32[64,2]{0,1:T(2,128)S(1)}, s32[64,2]{0,1:T(2,128)}, u32[]{:S(2)}) copy-start(s32[64,2]{0,1:T(2,128)} %param.23) | copy-start | bytes 1540
  35.2 4.6 %copy-start.1 = (f32[64,2]{0,1:T(2,128)S(1)}, f32[64,2]{0,1:T(2,128)}, u32[]{:S(2)}) copy-start(f32[64,2]{0,1:T(2,128)} %param.24) | copy-start | bytes 1540
  38.4 3.0 %collective-permute-start.9 = (bf16[64,1024]{1,0:T(8,128)(2,1)S(1)}, bf16[64,1024]{1,0:T(8,128)(2,1)S(1)}, u32[]{:S(2)}, u32[]{:S(2)}) collective-permute-start(bf16[64,1024]{1,0:T(8,128)(2,1)S(1)} %shard_map.141), channel_id=1, source_target_pairs={{0,1},{1,0},{2,3},{3,2},{4,5},{5,4},{6,7},{7,6},{8,9},{9,8},{10,11... | collective-permute-start | bytes 393224 | tf_op jit(solution)/shard_map/ppermute | solution.py:504
  38.5 1.3 %collective-permute-start.13 = (s32[2,64]{1,0:T(2,128)S(1)}, s32[2,64]{1,0:T(2,128)S(1)}, u32[]{:S(2)}, u32[]{:S(2)}) collective-permute-start(s32[2,64]{1,0:T(2,128)S(1)} %bitcast.9), channel_id=1, source_target_pairs={{0,1},{1,0},{2,3},{3,2},{4,5},{5,4},{6,7},{7,6},{8,9},{9,8},{10,11... | collective-permute-start | bytes 1544 | tf_op jit(solution)/shard_map/ppermute | solution.py:456
  39.8 1.5 %collective-permute-start.14 = (f32[2,64]{1,0:T(2,128)S(1)}, f32[2,64]{1,0:T(2,128)S(1)}, u32[]{:S(2)}, u32[]{:S(2)}) collective-permute-start(f32[2,64]{1,0:T(2,128)S(1)} %bitcast.11), channel_id=1, source_target_pairs={{0,1},{1,0},{2,3},{3,2},{4,5},{5,4},{6,7},{7,6},{8,9},{9,8},{10,11... | collective-permute-start | bytes 1544 | tf_op jit(solution)/shard_map/ppermute | solution.py:457
  43.8 1.6 %collective-permute-start.15 = (bf16[64,2048]{1,0:T(8,128)(2,1)S(1)}, bf16[64,2048]{1,0:T(8,128)(2,1)S(1)}, u32[]{:S(2)}, u32[]{:S(2)}) collective-permute-start(bf16[64,2048]{1,0:T(8,128)(2,1)S(1)} %get-tuple-element.74.norm_ref), channel_id=1, source_target_pairs={{0,1},{1,0},{2,3},{3,2},{4,5},{5,4},{6,7},{7,6},{8,9},{9,8},{10,11... | collective-permute-start | bytes 786440 | tf_op jit(solution)/shard_map/ppermute | solution.py:558
  45.9 7.4 %collective-permute-start.16 = (bf16[32,2048]{1,0:T(8,128)(2,1)S(1)}, bf16[32,2048]{1,0:T(8,128)(2,1)S(1)}, u32[]{:S(2)}, u32[]{:S(2)}) collective-permute-start(bf16[32,2048]{1,0:T(8,128)(2,1)S(1)} %get-tuple-element.81), channel_id=1, source_target_pairs={{0,0},{1,3},{2,2},{3,1},{4,4},{5,7},{6,6},{7,5},{8,8},{9,11},{10,1... | collective-permute-start | bytes 393224 | tf_op jit(solution)/shard_map/ppermute | solution.py:573
  46.5 10.2 %collective-permute-start.17 = (bf16[32,2048]{1,0:T(8,128)(2,1)S(1)}, bf16[32,2048]{1,0:T(8,128)(2,1)S(1)}, u32[]{:S(2)}, u32[]{:S(2)}) collective-permute-start(bf16[32,2048]{1,0:T(8,128)(2,1)S(1)} %get-tuple-element.82), channel_id=1, source_target_pairs={{0,4},{1,7},{2,6},{3,5},{4,0},{5,3},{6,2},{7,1},{8,12},{9,15},{10,... | collective-permute-start | bytes 393224 | tf_op jit(solution)/shard_map/ppermute | solution.py:573
  47.7 9.1 %collective-permute-start.18 = (bf16[32,2048]{1,0:T(8,128)(2,1)S(1)}, bf16[32,2048]{1,0:T(8,128)(2,1)S(1)}, u32[]{:S(2)}, u32[]{:S(2)}) collective-permute-start(bf16[32,2048]{1,0:T(8,128)(2,1)S(1)} %get-tuple-element.83), channel_id=1, source_target_pairs={{0,8},{1,11},{2,10},{3,9},{4,12},{5,15},{6,14},{7,13},{8,0},{9,3},... | collective-permute-start | bytes 393224 | tf_op jit(solution)/shard_map/ppermute | solution.py:573
  47.7 12.3 %collective-permute-start.19 = (bf16[32,2048]{1,0:T(8,128)(2,1)S(1)}, bf16[32,2048]{1,0:T(8,128)(2,1)S(1)}, u32[]{:S(2)}, u32[]{:S(2)}) collective-permute-start(bf16[32,2048]{1,0:T(8,128)(2,1)S(1)} %get-tuple-element.84), channel_id=1, source_target_pairs={{0,12},{1,15},{2,14},{3,13},{4,8},{5,11},{6,10},{7,9},{8,4},{9,7},... | collective-permute-start | bytes 393224 | tf_op jit(solution)/shard_map/ppermute | solution.py:573
  50.1 15.0 %collective-permute-start.28 = (bf16[32,2048]{1,0:T(8,128)(2,1)S(1)}, bf16[32,2048]{1,0:T(8,128)(2,1)S(1)}, u32[]{:S(2)}, u32[]{:S(2)}) collective-permute-start(bf16[32,2048]{1,0:T(8,128)(2,1)S(1)} %get-tuple-element.100), channel_id=1, source_target_pairs={{0,24},{1,27},{2,26},{3,25},{4,28},{5,31},{6,30},{7,29},{8,16},{9,... | collective-permute-start | bytes 393224 | tf_op jit(solution)/shard_map/ppermute | solution.py:573
  53.3 13.0 %collective-permute-start.29 = (bf16[32,2048]{1,0:T(8,128)(2,1)S(1)}, bf16[32,2048]{1,0:T(8,128)(2,1)S(1)}, u32[]{:S(2)}, u32[]{:S(2)}) collective-permute-start(bf16[32,2048]{1,0:T(8,128)(2,1)S(1)} %get-tuple-element.101), channel_id=1, source_target_pairs={{0,28},{1,31},{2,30},{3,29},{4,24},{5,27},{6,26},{7,25},{8,20},{9,... | collective-permute-start | bytes 393224 | tf_op jit(solution)/shard_map/ppermute | solution.py:573
  56.7 18.8 %collective-permute-start.24 = (bf16[32,2048]{1,0:T(8,128)(2,1)S(1)}, bf16[32,2048]{1,0:T(8,128)(2,1)S(1)}, u32[]{:S(2)}, u32[]{:S(2)}) collective-permute-start(bf16[32,2048]{1,0:T(8,128)(2,1)S(1)} %get-tuple-element.96), channel_id=1, source_target_pairs={{0,16},{1,19},{2,18},{3,17},{4,20},{5,23},{6,22},{7,21},{8,24},{9,... | collective-permute-start | bytes 393224 | tf_op jit(solution)/shard_map/ppermute | solution.py:573
  56.8 19.3 %collective-permute-start.25 = (bf16[32,2048]{1,0:T(8,128)(2,1)S(1)}, bf16[32,2048]{1,0:T(8,128)(2,1)S(1)}, u32[]{:S(2)}, u32[]{:S(2)}) collective-permute-start(bf16[32,2048]{1,0:T(8,128)(2,1)S(1)} %get-tuple-element.97), channel_id=1, source_target_pairs={{0,20},{1,23},{2,22},{3,21},{4,16},{5,19},{6,18},{7,17},{8,28},{9,... | collective-permute-start | bytes 393224 | tf_op jit(solution)/shard_map/ppermute | solution.py:573
  64.2 17.9 %collective-permute-start.20 = (bf16[32,2048]{1,0:T(8,128)(2,1)S(1)}, bf16[32,2048]{1,0:T(8,128)(2,1)S(1)}, u32[]{:S(2)}, u32[]{:S(2)}) collective-permute-start(bf16[32,2048]{1,0:T(8,128)(2,1)S(1)} %get-tuple-element.91), channel_id=1, source_target_pairs={{0,0},{1,3},{2,2},{3,1},{4,4},{5,7},{6,6},{7,5},{8,8},{9,11},{10,1... | collective-permute-start | bytes 393224 | tf_op jit(solution)/shard_map/ppermute | solution.py:573
  65.1 20.0 %collective-permute-start.21 = (bf16[32,2048]{1,0:T(8,128)(2,1)S(1)}, bf16[32,2048]{1,0:T(8,128)(2,1)S(1)}, u32[]{:S(2)}, u32[]{:S(2)}) collective-permute-start(bf16[32,2048]{1,0:T(8,128)(2,1)S(1)} %get-tuple-element.92), channel_id=1, source_target_pairs={{0,4},{1,7},{2,6},{3,5},{4,0},{5,3},{6,2},{7,1},{8,12},{9,15},{10,... | collective-permute-start | bytes 393224 | tf_op jit(solution)/shard_map/ppermute | solution.py:573
  66.3 19.1 %collective-permute-start.22 = (bf16[32,2048]{1,0:T(8,128)(2,1)S(1)}, bf16[32,2048]{1,0:T(8,128)(2,1)S(1)}, u32[]{:S(2)}, u32[]{:S(2)}) collective-permute-start(bf16[32,2048]{1,0:T(8,128)(2,1)S(1)} %get-tuple-element.93), channel_id=1, source_target_pairs={{0,8},{1,11},{2,10},{3,9},{4,12},{5,15},{6,14},{7,13},{8,0},{9,3},... | collective-permute-start | bytes 393224 | tf_op jit(solution)/shard_map/ppermute | solution.py:573
  75.5 12.9 %collective-permute-start.23 = (bf16[32,2048]{1,0:T(8,128)(2,1)S(1)}, bf16[32,2048]{1,0:T(8,128)(2,1)S(1)}, u32[]{:S(2)}, u32[]{:S(2)}) collective-permute-start(bf16[32,2048]{1,0:T(8,128)(2,1)S(1)} %get-tuple-element.94), channel_id=1, source_target_pairs={{0,12},{1,15},{2,14},{3,13},{4,8},{5,11},{6,10},{7,9},{8,4},{9,7},... | collective-permute-start | bytes 393224 | tf_op jit(solution)/shard_map/ppermute | solution.py:573
  76.1 12.8 %collective-permute-start.30 = (bf16[32,2048]{1,0:T(8,128)(2,1)S(1)}, bf16[32,2048]{1,0:T(8,128)(2,1)S(1)}, u32[]{:S(2)}, u32[]{:S(2)}) collective-permute-start(bf16[32,2048]{1,0:T(8,128)(2,1)S(1)} %get-tuple-element.102), channel_id=1, source_target_pairs={{0,24},{1,27},{2,26},{3,25},{4,28},{5,31},{6,30},{7,29},{8,16},{9,... | collective-permute-start | bytes 393224 | tf_op jit(solution)/shard_map/ppermute | solution.py:573
  82.1 7.8 %collective-permute-start.31 = (bf16[32,2048]{1,0:T(8,128)(2,1)S(1)}, bf16[32,2048]{1,0:T(8,128)(2,1)S(1)}, u32[]{:S(2)}, u32[]{:S(2)}) collective-permute-start(bf16[32,2048]{1,0:T(8,128)(2,1)S(1)} %get-tuple-element.103), channel_id=1, source_target_pairs={{0,28},{1,31},{2,30},{3,29},{4,24},{5,27},{6,26},{7,25},{8,20},{9,... | collective-permute-start | bytes 393224 | tf_op jit(solution)/shard_map/ppermute | solution.py:573
  85.1 14.5 %collective-permute-start.26 = (bf16[32,2048]{1,0:T(8,128)(2,1)S(1)}, bf16[32,2048]{1,0:T(8,128)(2,1)S(1)}, u32[]{:S(2)}, u32[]{:S(2)}) collective-permute-start(bf16[32,2048]{1,0:T(8,128)(2,1)S(1)} %get-tuple-element.98), channel_id=1, source_target_pairs={{0,16},{1,19},{2,18},{3,17},{4,20},{5,23},{6,22},{7,21},{8,24},{9,... | collective-permute-start | bytes 393224 | tf_op jit(solution)/shard_map/ppermute | solution.py:573
  85.3 17.4 %collective-permute-start.27 = (bf16[32,2048]{1,0:T(8,128)(2,1)S(1)}, bf16[32,2048]{1,0:T(8,128)(2,1)S(1)}, u32[]{:S(2)}, u32[]{:S(2)}) collective-permute-start(bf16[32,2048]{1,0:T(8,128)(2,1)S(1)} %get-tuple-element.99), channel_id=1, source_target_pairs={{0,20},{1,23},{2,22},{3,21},{4,16},{5,19},{6,18},{7,17},{8,28},{9,... | collective-permute-start | bytes 393224 | tf_op jit(solution)/shard_map/ppermute | solution.py:573
  103.1 2.5 %collective-permute-start.32 = (bf16[64,2048]{1,0:T(8,128)(2,1)S(1)}, bf16[64,2048]{1,0:T(8,128)(2,1)S(1)}, u32[]{:S(2)}, u32[]{:S(2)}) collective-permute-start(bf16[64,2048]{1,0:T(8,128)(2,1)S(1)} %shard_map.152), channel_id=1, source_target_pairs={{0,1},{1,0},{2,3},{3,2},{4,5},{5,4},{6,7},{7,6},{8,9},{9,8},{10,11... | collective-permute-start | bytes 786440 | tf_op jit(solution)/shard_map/ppermute | solution.py:590

commit v7 on v6

--- a/solution.py
+++ b/solution.py
@@ -85,24 +85,29 @@
     s = lax.broadcasted_iota(jnp.int32, (length, length), 1)
     tri = jnp.where(t >= s, 1.0, 0.0).astype(bf16)
     for k in range(GROUP):
-        for copy in copies[k]:
-            copy.wait()
+        copies[k][0].wait()
+        copies[k][1].wait()
+    weighted, last = [], []
+    for k in range(GROUP):
         key_gate = (1.0 - low_ref[k]) * sigmoid(-f_ref[k].astype(f32))
         hi, lo = split(jnp.log1p(-key_gate))
         total = dot(tri, hi) + dot(tri, lo)
-        last = total[length - 1 : length]
-        weighted = (key_gate * jnp.exp(last - total)).astype(bf16)
+        last.append(total[length - 1 : length])
+        weighted.append((key_gate * jnp.exp(last[k] - total)).astype(bf16))
         total_ref[k] = total
         key_ref[k] = key_gate
+    for k in range(GROUP):
+        copies[k][2].wait()
+    for k in range(GROUP):
         for h in range(heads):
             lanes = slice(h * HEAD_DIM, (h + 1) * HEAD_DIM)
-            outs[k][lanes] = dot(v_ref[k, :, lanes], weighted[:, lanes], TN).astype(bf16)
+            outs[k][lanes] = dot(v_ref[k, :, lanes], weighted[k][:, lanes], TN).astype(bf16)
             start = heads * HEAD_DIM + h * TAIL
-            outs[k][start : start + TAIL] = decay_tail(last[:, lanes])
+            outs[k][start : start + TAIL] = decay_tail(last[k][:, lanes])
 
 
 def intra_kernel(
-    place_ref, total_ref, key_ref, q_hbm, v_hbm, w_hbm, intra_ref, qe_ref, w_ref, q_ref, v_ref, sem
+    place_ref, total_ref, key_ref, q_hbm, v_hbm, w_hbm, intra_ref, qe_ref, own_ref, other_ref, q_ref, v_ref, sem
 ):
     length, block = q_ref.shape[1:]
     member = member_of(place_ref)
@@ -117,7 +122,11 @@
                 ]
             )
         )
-    ahead = side_rows(w_hbm, w_ref, side_of(place_ref), sem.at[2 * GROUP])
+    side = side_of(place_ref)
+    ahead = [
+        side_rows(w_hbm, own_ref, side, sem.at[2 * GROUP]),
+        side_rows(w_hbm, other_ref, 1 - side, sem.at[2 * GROUP + 1]),
+    ]
     t = lax.broadcasted_iota(jnp.int32, (length, length), 0)
     s = lax.broadcasted_iota(jnp.int32, (length, length), 1)
     for k in range(GROUP):
@@ -134,7 +143,8 @@
             scores = dot(scaled_query[:, lanes], scaled_key[:, lanes], NT)
             scores = jnp.where(t >= s, scores, 0.0).astype(bf16)
             intra_ref[k, :, lanes] = dot(scores, v_ref[k, :, lanes])
-    ahead.wait()
+    for copy in ahead:
+        copy.wait()
 
 
 def side_rows(hbm, ref, side, sem):
@@ -144,7 +154,10 @@
     return copy
 
 
-def gate_kernel(place_ref, gate_hbm, gain_hbm, w_hbm, gated_ref, w_ref, gate_ref, gain_ref, sem):
+def gate_kernel(
+    place_ref, gate_hbm, gain_hbm, res_hbm, norm_gain_hbm, d_hbm,
+    gated_ref, res_ref, norm_gain_ref, d_ref, gate_ref, gain_ref, sem,
+):
     block = gate_ref.shape[2]
     copies = []
     for k in range(GROUP):
@@ -157,13 +170,21 @@
                 ]
             )
         )
-    ahead = side_rows(w_hbm, w_ref, 1 - side_of(place_ref), sem.at[2 * GROUP])
+    ahead = fetch(
+        [
+            pltpu.make_async_copy(hbm, ref, sem.at[2 * GROUP + i])
+            for i, (hbm, ref) in enumerate(
+                ((res_hbm, res_ref), (norm_gain_hbm, norm_gain_ref), (d_hbm, d_ref))
+            )
+        ]
+    )
     for k in range(GROUP):
         for copy in copies[k]:
             copy.wait()
         gate = gate_ref[k].astype(f32)
         gated_ref[k] = gain_ref[k] * (gate * sigmoid(gate))
-    ahead.wait()
+    for copy in ahead:
+        copy.wait()
 
 
 def bring_kernel(*refs):
@@ -264,26 +285,13 @@
     return slots
 
 
-def project_kernel(
-    recv_ref, acc_ref, w_ref, res_hbm, gain_hbm, d_hbm, upd_ref, norm_ref, d_ref, res_ref, gain_ref, sem
-):
-    copies = fetch(
-        [
-            pltpu.make_async_copy(res_hbm, res_ref, sem.at[0]),
-            pltpu.make_async_copy(gain_hbm, gain_ref, sem.at[1]),
-        ]
-    )
-    ahead = pltpu.make_async_copy(d_hbm, d_ref, sem.at[2])
-    ahead.start()
+def project_kernel(recv_ref, acc_ref, w_ref, res_ref, gain_ref, upd_ref, norm_ref):
     partial = dot(recv_ref[...], w_ref[...])
-    for copy in copies:
-        copy.wait()
     updated = (res_ref[...].astype(f32) + (acc_ref[...] + partial)).astype(bf16)
     upd_ref[...] = updated
     updated = updated.astype(f32)
     scale = lax.rsqrt(jnp.mean(updated * updated, axis=-1, keepdims=True) + epsilon)
     norm_ref[...] = (updated * scale * gain_ref[...]).astype(bf16)
-    ahead.wait()
 
 
 def placed_rows(slots, weights, target, valid):
@@ -455,16 +463,21 @@
     route, weight = routing.T, route_weight.T
     other_route = lax.ppermute(route, "tp", swap)
     other_weight = lax.ppermute(weight, "tp", swap)
-    intra, qe, w_own = call(
-        intra_kernel,
-        [SMEM] + [VMEM] * 2 + [HBM] * 3,
+    gated, residual, norm_gain, down_kept = call(
+        gate_kernel,
+        [SMEM] + [HBM] * 5,
         [
             (VMEM, shape((GROUP, length, part), f32)),
-            (VMEM, shape((GROUP, length, part), bf16)),
-            (KEPT, shape((channels, width), bf16)),
+            (KEPT, shape((half, width), bf16)),
+            (KEPT, shape((1, width), f32)),
+            (KEPT, shape((units, width), bf16)),
         ],
-        [pltpu.VMEM((GROUP, length, part), bf16)] * 2 + [dma((2 * GROUP + 1,))],
-    )(place, total, key_gate, query, value, w_out)
+        [
+            pltpu.VMEM((GROUP, length, part), bf16),
+            pltpu.VMEM((GROUP, 1, part), f32),
+            dma((2 * GROUP + 3,)),
+        ],
+    )(place, out_gate, head_gain.reshape(1, -1), residual_in, ffn_gain.reshape(1, -1), weights[2])
     (totals,) = call(
         total_kernel,
         [SMEM] + [VMEM] * GROUP,
@@ -472,16 +485,17 @@
         [pltpu.VMEM((GROUP, carried, HEAD_DIM), bf16)],
     )(place, *states)
     totals = [totals] + [away(totals, GROUP * k) for k in range(1, groups)]
-    gated, w_other = call(
-        gate_kernel,
-        [SMEM] + [HBM] * 3,
-        [(VMEM, shape((GROUP, length, part), f32)), (KEPT, shape((channels, width), bf16))],
+    intra, qe, w_own, w_other = call(
+        intra_kernel,
+        [SMEM] + [VMEM] * 2 + [HBM] * 3,
         [
-            pltpu.VMEM((GROUP, length, part), bf16),
-            pltpu.VMEM((GROUP, 1, part), f32),
-            dma((2 * GROUP + 1,)),
+            (VMEM, shape((GROUP, length, part), f32)),
+            (VMEM, shape((GROUP, length, part), bf16)),
+            (KEPT, shape((channels, width), bf16)),
+            (KEPT, shape((channels, width), bf16)),
         ],
-    )(place, out_gate, head_gain.reshape(1, -1), w_out)
+        [pltpu.VMEM((GROUP, length, part), bf16)] * 2 + [dma((2 * GROUP + 2,))],
+    )(place, total, key_gate, query, value, w_out)
     priors = call(
         functools.partial(carry_kernel, groups=groups),
         [SMEM] + [VMEM] * (GROUP + groups),
@@ -511,12 +525,9 @@
     recv, others, other_route, other_weight = lax.optimization_barrier(
         (recv, others, other_route, other_weight)
     )
-    updated, normed, down_kept = call(
-        project_kernel,
-        [VMEM] * 2 + [KEPT] + [HBM] * 3,
-        [(VMEM, shape((half, width), bf16))] * 2 + [(KEPT, shape((units, width), bf16))],
-        [pltpu.VMEM((half, width), bf16), pltpu.VMEM((1, width), f32), dma((3,))],
-    )(recv, partial, w_other, residual_in, ffn_gain.reshape(1, -1), weights[2])
+    updated, normed = call(
+        project_kernel, [VMEM] * 2 + [KEPT] * 3, [(VMEM, shape((half, width), bf16))] * 2
+    )(recv, partial, w_other, residual, norm_gain)
     kept = (gate_kept, up_kept, down_kept, *others)
     box = (VMEM, shape((slots, width), bf16))
     table = (VMEM, shape((slots, half), bf16))

time: 107 us -> 105 us (0.981)
  Pallas kernels: 30.8 us -> 29.3 us
    pallas_call x18, Pallas kernels: 30.8 us -> 29.3 us  [placed(): run(*(pltpu.with_memory_space_constraint(arg, fixed(spec)) if fixed(spec)...]
  transfers between devices with their start and end apart: 33 -> 33, of which waited for: 12 -> 12; matrix products, arithmetic and copies ran while one was open for 0% -> 0% of each run, Pallas kernels for 25% -> 26%
where the time goes in v7:
time: 105 us
  starting transfers between devices  49.8 us (47%)
  Pallas kernels  29.3 us (28%)
  waiting for transfers between devices  25.4 us (24%)
    pallas_call x18, Pallas kernels, placed(): run(*(pltpu.with_memory_space_constraint(arg, fixed(spec)) if fixed(spec)...  29.3 us
    ppermute x16, starting transfers between devices, paired(): return lax.ppermute(x, ('sp', 'tp'), pairs)  27 us
    ppermute x9, starting transfers between devices, away(): return lax.ppermute(x, 'sp', [(i, i ^ k) for i in range(ranks)])  19.3 us
    ppermute x16, waiting for transfers between devices, paired(): return lax.ppermute(x, ('sp', 'tp'), pairs)  13.8 us
    ppermute x9, waiting for transfers between devices, away(): return lax.ppermute(x, 'sp', [(i, i ^ k) for i in range(ranks)])  9.29 us
  transfers between devices with their start and end apart: 33, of which 12 were waited for; matrix products, arithmetic and copies ran while one was open for 0% of the time, Pallas kernels for 26%

profile of v7, /device:TPU:0, one launch (start us, length us, event | category | flops | bytes accessed | tf_op | source)
XLA Modules:
  0.0 104.8 jit_solution(11750331661669326130)
XLA Ops:
  0.0 0.5 collective-permute-start.10
  0.5 0.5 collective-permute-start.12
  1.0 2.1 %shard_map.136 = (bf16[272,128]{1,0:T(8,128)(2,1)S(1)}, bf16[272,128]{1,0:T(8,128)(2,1)S(1)}, bf16[272,128]{1,0:T(8,128)(2,1)S(1)}, bf16[272,128]{1,0:T(8,128)(2...) custom-call(s32[1]{0:T(128)} %bitcast.place_ref, bf16[128,1024]{1,0:T(8,128)(2,1)} %f_hbm.1, ...), custom_call_target="tpu_custom_call" | custom-call | tf_op jit(solution)/shard_map/pallas_call | solution.py:405
  3.1 2.5 %collective-permute-start = (bf16[272,128]{1,0:T(8,128)(2,1)S(1)}, bf16[272,128]{1,0:T(8,128)(2,1)S(1)}, u32[]{:S(2)}, u32[]{:S(2)}) collective-permute-start(bf16[272,128]{1,0:T(8,128)(2,1)S(1)} %get-tuple-element.63), channel_id=1, source_target_pairs={{0,2},{2,0},{4,6},{6,4},{8,10},{10,8},{12,14},{14,12},{16,18},{18,... | collective-permute-start | bytes 208904 | tf_op jit(solution)/shard_map/ppermute | solution.py:450
  5.7 1.5 %collective-permute-start.1 = (bf16[272,128]{1,0:T(8,128)(2,1)S(1)}, bf16[272,128]{1,0:T(8,128)(2,1)S(1)}, u32[]{:S(2)}, u32[]{:S(2)}) collective-permute-start(bf16[272,128]{1,0:T(8,128)(2,1)S(1)} %get-tuple-element.64), channel_id=1, source_target_pairs={{0,4},{2,6},{4,0},{6,2},{8,12},{10,14},{12,8},{14,10},{16,20},{18,... | collective-permute-start | bytes 208904 | tf_op jit(solution)/shard_map/ppermute | solution.py:450
  7.2 1.3 %collective-permute-done.refs_1_ = bf16[272,128]{1,0:T(8,128)(2,1)S(1)} collective-permute-done((bf16[272,128]{1,0:T(8,128)(2,1)S(1)}, bf16[272,128]{1,0:T(8,128)(2,1)S(1)}, u32[]{:S(2)}, u32[]{:S(2)}) %collective-permute-start) | collective-permute-done | bytes 69664 | tf_op jit(solution)/shard_map/ppermute | solution.py:450
  8.5 2.7 %collective-permute-start.2 = (bf16[272,128]{1,0:T(8,128)(2,1)S(1)}, bf16[272,128]{1,0:T(8,128)(2,1)S(1)}, u32[]{:S(2)}, u32[]{:S(2)}) collective-permute-start(bf16[272,128]{1,0:T(8,128)(2,1)S(1)} %get-tuple-element.65), channel_id=1, source_target_pairs={{0,6},{2,4},{4,2},{6,0},{8,14},{10,12},{12,10},{14,8},{16,22},{18,... | collective-permute-start | bytes 208904 | tf_op jit(solution)/shard_map/ppermute | solution.py:450
  11.2 2.5 %collective-permute-done.2.refs_3_ = bf16[272,128]{1,0:T(8,128)(2,1)S(1)} collective-permute-done((bf16[272,128]{1,0:T(8,128)(2,1)S(1)}, bf16[272,128]{1,0:T(8,128)(2,1)S(1)}, u32[]{:S(2)}, u32[]{:S(2)}) %collective-permute-start.2) | collective-permute-done | bytes 69664 | tf_op jit(solution)/shard_map/ppermute | solution.py:450
  13.8 1.9 %collective-permute-start.3 = (bf16[272,128]{1,0:T(8,128)(2,1)S(1)}, bf16[272,128]{1,0:T(8,128)(2,1)S(1)}, u32[]{:S(2)}, u32[]{:S(2)}) collective-permute-start(bf16[272,128]{1,0:T(8,128)(2,1)S(1)} %shard_map.139.refs_4_), channel_id=1, source_target_pairs={{0,8},{2,10},{4,12},{6,14},{8,0},{10,2},{12,4},{14,6},{16,24},{18,... | collective-permute-start | bytes 208904 | tf_op jit(solution)/shard_map/ppermute | solution.py:450
  15.7 2.6 %collective-permute-start.4 = (bf16[272,128]{1,0:T(8,128)(2,1)S(1)}, bf16[272,128]{1,0:T(8,128)(2,1)S(1)}, u32[]{:S(2)}, u32[]{:S(2)}) collective-permute-start(bf16[272,128]{1,0:T(8,128)(2,1)S(1)} %shard_map.139.refs_4_), channel_id=1, source_target_pairs={{0,16},{2,18},{4,20},{6,22},{8,24},{10,26},{12,28},{14,30},{16,0},... | collective-permute-start | bytes 208904 | tf_op jit(solution)/shard_map/ppermute | solution.py:450
  18.3 0.6 collective-permute-done.3.refs_5_
  18.8 3.2 %collective-permute-start.5 = (bf16[272,128]{1,0:T(8,128)(2,1)S(1)}, bf16[272,128]{1,0:T(8,128)(2,1)S(1)}, u32[]{:S(2)}, u32[]{:S(2)}) collective-permute-start(bf16[272,128]{1,0:T(8,128)(2,1)S(1)} %shard_map.139.refs_4_), channel_id=1, source_target_pairs={{0,24},{2,26},{4,28},{6,30},{8,16},{10,18},{12,20},{14,22},{16,8},... | collective-permute-start | bytes 208904 | tf_op jit(solution)/shard_map/ppermute | solution.py:450
  22.4 2.6 %collective-permute-done.5.refs_7_ = bf16[272,128]{1,0:T(8,128)(2,1)S(1)} collective-permute-done((bf16[272,128]{1,0:T(8,128)(2,1)S(1)}, bf16[272,128]{1,0:T(8,128)(2,1)S(1)}, u32[]{:S(2)}, u32[]{:S(2)}) %collective-permute-start.5) | collective-permute-done | bytes 69664 | tf_op jit(solution)/shard_map/ppermute | solution.py:450
  25.2 1.5 %collective-permute-start.6 = (bf16[256,128]{1,0:T(8,128)(2,1)S(1)}, bf16[256,128]{1,0:T(8,128)(2,1)S(1)}, u32[]{:S(2)}, u32[]{:S(2)}) collective-permute-start(bf16[256,128]{1,0:T(8,128)(2,1)S(1)} %get-tuple-element.67), channel_id=1, source_target_pairs={{0,2},{2,0},{4,6},{6,4},{8,10},{10,8},{12,14},{14,12},{16,18},{18,... | collective-permute-start | bytes 196616 | tf_op jit(solution)/shard_map/ppermute | solution.py:450
  26.7 1.5 %collective-permute-start.7 = (bf16[256,128]{1,0:T(8,128)(2,1)S(1)}, bf16[256,128]{1,0:T(8,128)(2,1)S(1)}, u32[]{:S(2)}, u32[]{:S(2)}) collective-permute-start(bf16[256,128]{1,0:T(8,128)(2,1)S(1)} %get-tuple-element.68), channel_id=1, source_target_pairs={{0,4},{2,6},{4,0},{6,2},{8,12},{10,14},{12,8},{14,10},{16,20},{18,... | collective-permute-start | bytes 196616 | tf_op jit(solution)/shard_map/ppermute | solution.py:450
  28.3 1.9 %collective-permute-done.6.refs_1_ = bf16[256,128]{1,0:T(8,128)(2,1)S(1)} collective-permute-done((bf16[256,128]{1,0:T(8,128)(2,1)S(1)}, bf16[256,128]{1,0:T(8,128)(2,1)S(1)}, u32[]{:S(2)}, u32[]{:S(2)}) %collective-permute-start.6) | collective-permute-done | bytes 65568 | tf_op jit(solution)/shard_map/ppermute | solution.py:450
  30.1 1.8 %collective-permute-start.8 = (bf16[256,128]{1,0:T(8,128)(2,1)S(1)}, bf16[256,128]{1,0:T(8,128)(2,1)S(1)}, u32[]{:S(2)}, u32[]{:S(2)}) collective-permute-start(bf16[256,128]{1,0:T(8,128)(2,1)S(1)} %get-tuple-element.69), channel_id=1, source_target_pairs={{0,6},{2,4},{4,2},{6,0},{8,14},{10,12},{12,10},{14,8},{16,22},{18,... | collective-permute-start | bytes 196616 | tf_op jit(solution)/shard_map/ppermute | solution.py:450
  32.0 3.8 %shard_map.137 = (f32[4,128,256]{2,1,0:T(8,128)S(1)}, bf16[4,128,256]{2,1,0:T(8,128)(2,1)S(1)}, bf16[1024,2048]{1,0:T(8,128)(2,1)S(1)}, bf16[1024,2048]{1,0:T(8,128)(2,1)S(1)}) custom-call(s32[1]{0:T(128)} %bitcast.place_ref, f32[4,128,256]{2,1,0:T(8,128)S(1)} %get-tuple-element.57.total_ref, f32[4,128,256]{2,1,0:T(8,128)S(1)} %get-tuple-element.58.key_ref, ...), custom_call_target="tpu_custom_call" | custom-call | tf_op jit(solution)/shard_map/pallas_call | solution.py:405
  35.8 2.0 %shard_map.138 = (f32[4,128,256]{2,1,0:T(8,128)S(1)}, bf16[64,2048]{1,0:T(8,128)(2,1)S(1)}, f32[1,2048]{1,0:T(1,128)S(1)}, bf16[512,2048]{1,0:T(8,128)(2,1)S(1)}) custom-call(s32[1]{0:T(128)} %bitcast.place_ref, bf16[128,1024]{1,0:T(8,128)(2,1)} %gate_hbm.1, f32[1,1024]{1,0:T(1,128)} %bitcast.21, bf16[64,2048]{1,0:T(8,128)(2,1)} %res_hbm.1, ...), custom_call_target="tpu_custom_call" | custom-call | tf_op jit(solution)/shard_map/pallas_call | solution.py:405
  38.3 0.5 collective-permute-start.13
  38.8 0.8 collective-permute-done.13.other_route_ref
  40.0 1.2 %shard_map.142.acc_ref = f32[64,2048]{1,0:T(8,128)S(1)} custom-call(s32[1]{0:T(128)} %bitcast.place_ref, f32[4,128,256]{2,1,0:T(8,128)S(1)} %get-tuple-element.59.intra_ref, bf16[4,128,256]{2,1,0:T(8,128)(2,1)S(1)} %get-tuple-element.60.qe_ref, f32[4,128,256]{2,1,0:T(8,128)S(1)} %get-tuple-element.61.gated_ref, ...), custom_call_target="tpu_custom_call" | custom-call | tf_op jit(solution)/shard_map/pallas_call | solution.py:405
  41.3 1.0 shard_map.143
  42.5 0.7 shard_map.144
  43.3 0.6 collective-permute-done.15.norm_ref
  44.3 0.7 collective-permute-start.16
  45.0 1.2 %collective-permute-start.17 = (bf16[32,2048]{1,0:T(8,128)(2,1)S(1)}, bf16[32,2048]{1,0:T(8,128)(2,1)S(1)}, u32[]{:S(2)}, u32[]{:S(2)}) collective-permute-start(bf16[32,2048]{1,0:T(8,128)(2,1)S(1)} %get-tuple-element.86), channel_id=1, source_target_pairs={{0,4},{1,7},{2,6},{3,5},{4,0},{5,3},{6,2},{7,1},{8,12},{9,15},{10,... | collective-permute-start | bytes 393224 | tf_op jit(solution)/shard_map/ppermute | solution.py:584
  46.2 2.3 %collective-permute-start.19 = (bf16[32,2048]{1,0:T(8,128)(2,1)S(1)}, bf16[32,2048]{1,0:T(8,128)(2,1)S(1)}, u32[]{:S(2)}, u32[]{:S(2)}) collective-permute-start(bf16[32,2048]{1,0:T(8,128)(2,1)S(1)} %get-tuple-element.88), channel_id=1, source_target_pairs={{0,12},{1,15},{2,14},{3,13},{4,8},{5,11},{6,10},{7,9},{8,4},{9,7},... | collective-permute-start | bytes 393224 | tf_op jit(solution)/shard_map/ppermute | solution.py:584
  48.5 3.2 %collective-permute-start.28 = (bf16[32,2048]{1,0:T(8,128)(2,1)S(1)}, bf16[32,2048]{1,0:T(8,128)(2,1)S(1)}, u32[]{:S(2)}, u32[]{:S(2)}) collective-permute-start(bf16[32,2048]{1,0:T(8,128)(2,1)S(1)} %get-tuple-element.104), channel_id=1, source_target_pairs={{0,24},{1,27},{2,26},{3,25},{4,28},{5,31},{6,30},{7,29},{8,16},{9,... | collective-permute-start | bytes 393224 | tf_op jit(solution)/shard_map/ppermute | solution.py:584
  51.8 1.2 %collective-permute-start.29 = (bf16[32,2048]{1,0:T(8,128)(2,1)S(1)}, bf16[32,2048]{1,0:T(8,128)(2,1)S(1)}, u32[]{:S(2)}, u32[]{:S(2)}) collective-permute-start(bf16[32,2048]{1,0:T(8,128)(2,1)S(1)} %get-tuple-element.105), channel_id=1, source_target_pairs={{0,28},{1,31},{2,30},{3,29},{4,24},{5,27},{6,26},{7,25},{8,20},{9,... | collective-permute-start | bytes 393224 | tf_op jit(solution)/shard_map/ppermute | solution.py:584
  52.9 2.2 %shard_map.146 = (bf16[2048,512]{1,0:T(8,128)(2,1)S(1)}, bf16[2048,512]{1,0:T(8,128)(2,1)S(1)}) custom-call(bf16[2048,512]{1,0:T(8,128)(2,1)} %bitcast.16, bf16[2048,512]{1,0:T(8,128)(2,1)} %bitcast.18), custom_call_target="tpu_custom_call" | custom-call | tf_op jit(solution)/shard_map/pallas_call | solution.py:405
  55.3 3.2 %collective-permute-start.25 = (bf16[32,2048]{1,0:T(8,128)(2,1)S(1)}, bf16[32,2048]{1,0:T(8,128)(2,1)S(1)}, u32[]{:S(2)}, u32[]{:S(2)}) collective-permute-start(bf16[32,2048]{1,0:T(8,128)(2,1)S(1)} %get-tuple-element.101), channel_id=1, source_target_pairs={{0,20},{1,23},{2,22},{3,21},{4,16},{5,19},{6,18},{7,17},{8,28},{9,... | collective-permute-start | bytes 393224 | tf_op jit(solution)/shard_map/ppermute | solution.py:584
  58.5 4.1 %shard_map.147 = (bf16[32,2048]{1,0:T(8,128)(2,1)S(1)}, bf16[32,2048]{1,0:T(8,128)(2,1)S(1)}, bf16[32,2048]{1,0:T(8,128)(2,1)S(1)}, bf16[32,2048]{1,0:T(8,128)(2,1)S(1)}) custom-call(bf16[32,2048]{1,0:T(8,128)(2,1)S(1)} %collective-permute-done.16.refs_0_, bf16[32,2048]{1,0:T(8,128)(2,1)S(1)} %collective-permute-done.17.refs_1_, ...), custom_call_target="tpu_custom_call" | custom-call | tf_op jit(solution)/shard_map/pallas_call | solution.py:405
  62.7 0.8 collective-permute-start.20
  63.5 1.2 %collective-permute-start.21 = (bf16[32,2048]{1,0:T(8,128)(2,1)S(1)}, bf16[32,2048]{1,0:T(8,128)(2,1)S(1)}, u32[]{:S(2)}, u32[]{:S(2)}) collective-permute-start(bf16[32,2048]{1,0:T(8,128)(2,1)S(1)} %get-tuple-element.96), channel_id=1, source_target_pairs={{0,4},{1,7},{2,6},{3,5},{4,0},{5,3},{6,2},{7,1},{8,12},{9,15},{10,... | collective-permute-start | bytes 393224 | tf_op jit(solution)/shard_map/ppermute | solution.py:584
  64.7 4.6 %collective-permute-start.22 = (bf16[32,2048]{1,0:T(8,128)(2,1)S(1)}, bf16[32,2048]{1,0:T(8,128)(2,1)S(1)}, u32[]{:S(2)}, u32[]{:S(2)}) collective-permute-start(bf16[32,2048]{1,0:T(8,128)(2,1)S(1)} %get-tuple-element.97), channel_id=1, source_target_pairs={{0,8},{1,11},{2,10},{3,9},{4,12},{5,15},{6,14},{7,13},{8,0},{9,3},... | collective-permute-start | bytes 393224 | tf_op jit(solution)/shard_map/ppermute | solution.py:584
  69.4 4.6 %shard_map.150 = (bf16[32,2048]{1,0:T(8,128)(2,1)S(1)}, bf16[32,2048]{1,0:T(8,128)(2,1)S(1)}) custom-call(bf16[32,2048]{1,0:T(8,128)(2,1)S(1)} %collective-permute-done.28.refs_0_, bf16[32,2048]{1,0:T(8,128)(2,1)S(1)} %collective-permute-done.29.refs_1_, bf16[2048,512]{1,0:T(8,128)(2,1)S(1)} %get-tuple-element.89.refs_4_.refs_2_, ...), custom_call_target="tpu_custom_call" | custom-call | tf_op jit(solution)/shard_map/pallas_call | solution.py:405
  73.9 0.6 collective-permute-start.23
  74.6 1.5 %collective-permute-start.30 = (bf16[32,2048]{1,0:T(8,128)(2,1)S(1)}, bf16[32,2048]{1,0:T(8,128)(2,1)S(1)}, u32[]{:S(2)}, u32[]{:S(2)}) collective-permute-start(bf16[32,2048]{1,0:T(8,128)(2,1)S(1)} %get-tuple-element.106), channel_id=1, source_target_pairs={{0,24},{1,27},{2,26},{3,25},{4,28},{5,31},{6,30},{7,29},{8,16},{9,... | collective-permute-start | bytes 393224 | tf_op jit(solution)/shard_map/ppermute | solution.py:584
  76.0 4.6 %shard_map.149 = (bf16[32,2048]{1,0:T(8,128)(2,1)S(1)}, bf16[32,2048]{1,0:T(8,128)(2,1)S(1)}) custom-call(bf16[32,2048]{1,0:T(8,128)(2,1)S(1)} %collective-permute-done.24.refs_0_, bf16[32,2048]{1,0:T(8,128)(2,1)S(1)} %collective-permute-done.25.refs_1_, bf16[2048,512]{1,0:T(8,128)(2,1)S(1)} %get-tuple-element.89.refs_4_.refs_2_, ...), custom_call_target="tpu_custom_call" | custom-call | tf_op jit(solution)/shard_map/pallas_call | solution.py:405
  80.6 2.9 %collective-permute-start.31 = (bf16[32,2048]{1,0:T(8,128)(2,1)S(1)}, bf16[32,2048]{1,0:T(8,128)(2,1)S(1)}, u32[]{:S(2)}, u32[]{:S(2)}) collective-permute-start(bf16[32,2048]{1,0:T(8,128)(2,1)S(1)} %get-tuple-element.107), channel_id=1, source_target_pairs={{0,28},{1,31},{2,30},{3,29},{4,24},{5,27},{6,26},{7,25},{8,20},{9,... | collective-permute-start | bytes 393224 | tf_op jit(solution)/shard_map/ppermute | solution.py:584
  83.8 3.1 %collective-permute-start.27 = (bf16[32,2048]{1,0:T(8,128)(2,1)S(1)}, bf16[32,2048]{1,0:T(8,128)(2,1)S(1)}, u32[]{:S(2)}, u32[]{:S(2)}) collective-permute-start(bf16[32,2048]{1,0:T(8,128)(2,1)S(1)} %get-tuple-element.103), channel_id=1, source_target_pairs={{0,20},{1,23},{2,22},{3,21},{4,16},{5,19},{6,18},{7,17},{8,28},{9,... | collective-permute-start | bytes 393224 | tf_op jit(solution)/shard_map/ppermute | solution.py:584
  87.4 1.0 collective-permute-done.31.refs_6_
  88.4 9.6 %collective-permute-done.26.refs_3_ = bf16[32,2048]{1,0:T(8,128)(2,1)S(1)} collective-permute-done((bf16[32,2048]{1,0:T(8,128)(2,1)S(1)}, bf16[32,2048]{1,0:T(8,128)(2,1)S(1)}, u32[]{:S(2)}, u32[]{:S(2)}) %collective-permute-start.26) | collective-permute-done | bytes 131104 | tf_op jit(solution)/shard_map/ppermute | solution.py:584
  98.0 3.2 %collective-permute-done.27.refs_4_ = bf16[32,2048]{1,0:T(8,128)(2,1)S(1)} collective-permute-done((bf16[32,2048]{1,0:T(8,128)(2,1)S(1)}, bf16[32,2048]{1,0:T(8,128)(2,1)S(1)}, u32[]{:S(2)}, u32[]{:S(2)}) %collective-permute-start.27) | collective-permute-done | bytes 131104 | tf_op jit(solution)/shard_map/ppermute | solution.py:584
  101.6 1.4 %collective-permute-start.32 = (bf16[64,2048]{1,0:T(8,128)(2,1)S(1)}, bf16[64,2048]{1,0:T(8,128)(2,1)S(1)}, u32[]{:S(2)}, u32[]{:S(2)}) collective-permute-start(bf16[64,2048]{1,0:T(8,128)(2,1)S(1)} %shard_map.152), channel_id=1, source_target_pairs={{0,1},{1,0},{2,3},{3,2},{4,5},{5,4},{6,7},{7,6},{8,9},{9,8},{10,11... | collective-permute-start | bytes 786440 | tf_op jit(solution)/shard_map/ppermute | solution.py:601
  103.3 0.8 collective-permute-done.32.b_ref
  104.1 0.7 shard_map.153
  (41 shorter events, 3.6 us)
Async XLA Ops:
  0.0 41.2 %collective-permute-start.10 = (bf16[2048,512]{1,0:T(8,128)(2,1)}, bf16[2048,512]{1,0:T(8,128)(2,1)S(1)}, u32[]{:S(2)}, u32[]{:S(2)}) collective-permute-start(bf16[2048,512]{1,0:T(8,128)(2,1)} %bitcast.15), channel_id=1, source_target_pairs={{0,1},{1,0},{2,3},{3,2},{4,5},{5,4},{6,7},{7,6},{8,9},{9,8},{10,11... | collective-permute-start | bytes 6291464 | tf_op jit(solution)/shard_map/ppermute | solution.py:462
  0.5 40.8 %collective-permute-start.11 = (bf16[2048,512]{1,0:T(8,128)(2,1)}, bf16[2048,512]{1,0:T(8,128)(2,1)}, u32[]{:S(2)}, u32[]{:S(2)}) collective-permute-start(bf16[2048,512]{1,0:T(8,128)(2,1)} %bitcast.17), channel_id=1, source_target_pairs={{0,1},{1,0},{2,3},{3,2},{4,5},{5,4},{6,7},{7,6},{8,9},{9,8},{10,11... | collective-permute-start | bytes 6291464 | tf_op jit(solution)/shard_map/ppermute | solution.py:462
  0.5 40.7 %collective-permute-start.12 = (bf16[512,2048]{1,0:T(8,128)(2,1)}, bf16[512,2048]{1,0:T(8,128)(2,1)}, u32[]{:S(2)}, u32[]{:S(2)}) collective-permute-start(bf16[512,2048]{1,0:T(8,128)(2,1)} %bitcast.13), channel_id=1, source_target_pairs={{0,1},{1,0},{2,3},{3,2},{4,5},{5,4},{6,7},{7,6},{8,9},{9,8},{10,11... | collective-permute-start | bytes 6291464 | tf_op jit(solution)/shard_map/ppermute | solution.py:462
  3.1 5.4 %collective-permute-start = (bf16[272,128]{1,0:T(8,128)(2,1)S(1)}, bf16[272,128]{1,0:T(8,128)(2,1)S(1)}, u32[]{:S(2)}, u32[]{:S(2)}) collective-permute-start(bf16[272,128]{1,0:T(8,128)(2,1)S(1)} %get-tuple-element.63), channel_id=1, source_target_pairs={{0,2},{2,0},{4,6},{6,4},{8,10},{10,8},{12,14},{14,12},{16,18},{18,... | collective-permute-start | bytes 208904 | tf_op jit(solution)/shard_map/ppermute | solution.py:450
  5.7 5.6 %collective-permute-start.1 = (bf16[272,128]{1,0:T(8,128)(2,1)S(1)}, bf16[272,128]{1,0:T(8,128)(2,1)S(1)}, u32[]{:S(2)}, u32[]{:S(2)}) collective-permute-start(bf16[272,128]{1,0:T(8,128)(2,1)S(1)} %get-tuple-element.64), channel_id=1, source_target_pairs={{0,4},{2,6},{4,0},{6,2},{8,12},{10,14},{12,8},{14,10},{16,20},{18,... | collective-permute-start | bytes 208904 | tf_op jit(solution)/shard_map/ppermute | solution.py:450
  8.5 5.2 %collective-permute-start.2 = (bf16[272,128]{1,0:T(8,128)(2,1)S(1)}, bf16[272,128]{1,0:T(8,128)(2,1)S(1)}, u32[]{:S(2)}, u32[]{:S(2)}) collective-permute-start(bf16[272,128]{1,0:T(8,128)(2,1)S(1)} %get-tuple-element.65), channel_id=1, source_target_pairs={{0,6},{2,4},{4,2},{6,0},{8,14},{10,12},{12,10},{14,8},{16,22},{18,... | collective-permute-start | bytes 208904 | tf_op jit(solution)/shard_map/ppermute | solution.py:450
  13.8 5.0 %collective-permute-start.3 = (bf16[272,128]{1,0:T(8,128)(2,1)S(1)}, bf16[272,128]{1,0:T(8,128)(2,1)S(1)}, u32[]{:S(2)}, u32[]{:S(2)}) collective-permute-start(bf16[272,128]{1,0:T(8,128)(2,1)S(1)} %shard_map.139.refs_4_), channel_id=1, source_target_pairs={{0,8},{2,10},{4,12},{6,14},{8,0},{10,2},{12,4},{14,6},{16,24},{18,... | collective-permute-start | bytes 208904 | tf_op jit(solution)/shard_map/ppermute | solution.py:450
  15.7 6.7 %collective-permute-start.4 = (bf16[272,128]{1,0:T(8,128)(2,1)S(1)}, bf16[272,128]{1,0:T(8,128)(2,1)S(1)}, u32[]{:S(2)}, u32[]{:S(2)}) collective-permute-start(bf16[272,128]{1,0:T(8,128)(2,1)S(1)} %shard_map.139.refs_4_), channel_id=1, source_target_pairs={{0,16},{2,18},{4,20},{6,22},{8,24},{10,26},{12,28},{14,30},{16,0},... | collective-permute-start | bytes 208904 | tf_op jit(solution)/shard_map/ppermute | solution.py:450
  18.8 6.2 %collective-permute-start.5 = (bf16[272,128]{1,0:T(8,128)(2,1)S(1)}, bf16[272,128]{1,0:T(8,128)(2,1)S(1)}, u32[]{:S(2)}, u32[]{:S(2)}) collective-permute-start(bf16[272,128]{1,0:T(8,128)(2,1)S(1)} %shard_map.139.refs_4_), channel_id=1, source_target_pairs={{0,24},{2,26},{4,28},{6,30},{8,16},{10,18},{12,20},{14,22},{16,8},... | collective-permute-start | bytes 208904 | tf_op jit(solution)/shard_map/ppermute | solution.py:450
  25.2 5.0 %collective-permute-start.6 = (bf16[256,128]{1,0:T(8,128)(2,1)S(1)}, bf16[256,128]{1,0:T(8,128)(2,1)S(1)}, u32[]{:S(2)}, u32[]{:S(2)}) collective-permute-start(bf16[256,128]{1,0:T(8,128)(2,1)S(1)} %get-tuple-element.67), channel_id=1, source_target_pairs={{0,2},{2,0},{4,6},{6,4},{8,10},{10,8},{12,14},{14,12},{16,18},{18,... | collective-permute-start | bytes 196616 | tf_op jit(solution)/shard_map/ppermute | solution.py:450
  26.7 11.1 %collective-permute-start.7 = (bf16[256,128]{1,0:T(8,128)(2,1)S(1)}, bf16[256,128]{1,0:T(8,128)(2,1)S(1)}, u32[]{:S(2)}, u32[]{:S(2)}) collective-permute-start(bf16[256,128]{1,0:T(8,128)(2,1)S(1)} %get-tuple-element.68), channel_id=1, source_target_pairs={{0,4},{2,6},{4,0},{6,2},{8,12},{10,14},{12,8},{14,10},{16,20},{18,... | collective-permute-start | bytes 196616 | tf_op jit(solution)/shard_map/ppermute | solution.py:450
  30.1 7.7 %collective-permute-start.8 = (bf16[256,128]{1,0:T(8,128)(2,1)S(1)}, bf16[256,128]{1,0:T(8,128)(2,1)S(1)}, u32[]{:S(2)}, u32[]{:S(2)}) collective-permute-start(bf16[256,128]{1,0:T(8,128)(2,1)S(1)} %get-tuple-element.69), channel_id=1, source_target_pairs={{0,6},{2,4},{4,2},{6,0},{8,14},{10,12},{12,10},{14,8},{16,22},{18,... | collective-permute-start | bytes 196616 | tf_op jit(solution)/shard_map/ppermute | solution.py:450
  35.8 2.5 %copy-start = (s32[64,2]{0,1:T(2,128)S(1)}, s32[64,2]{0,1:T(2,128)}, u32[]{:S(2)}) copy-start(s32[64,2]{0,1:T(2,128)} %param.23) | copy-start | bytes 1540
  35.8 3.9 %copy-start.1 = (f32[64,2]{0,1:T(2,128)S(1)}, f32[64,2]{0,1:T(2,128)}, u32[]{:S(2)}) copy-start(f32[64,2]{0,1:T(2,128)} %param.24) | copy-start | bytes 1540
  38.3 3.0 %collective-permute-start.9 = (bf16[64,1024]{1,0:T(8,128)(2,1)S(1)}, bf16[64,1024]{1,0:T(8,128)(2,1)S(1)}, u32[]{:S(2)}, u32[]{:S(2)}) collective-permute-start(bf16[64,1024]{1,0:T(8,128)(2,1)S(1)} %shard_map.141), channel_id=1, source_target_pairs={{0,1},{1,0},{2,3},{3,2},{4,5},{5,4},{6,7},{7,6},{8,9},{9,8},{10,11... | collective-permute-start | bytes 393224 | tf_op jit(solution)/shard_map/ppermute | solution.py:518
  38.3 1.3 %collective-permute-start.13 = (s32[2,64]{1,0:T(2,128)S(1)}, s32[2,64]{1,0:T(2,128)S(1)}, u32[]{:S(2)}, u32[]{:S(2)}) collective-permute-start(s32[2,64]{1,0:T(2,128)S(1)} %bitcast.9), channel_id=1, source_target_pairs={{0,1},{1,0},{2,3},{3,2},{4,5},{5,4},{6,7},{7,6},{8,9},{9,8},{10,11... | collective-permute-start | bytes 1544 | tf_op jit(solution)/shard_map/ppermute | solution.py:464
  39.7 1.5 %collective-permute-start.14 = (f32[2,64]{1,0:T(2,128)S(1)}, f32[2,64]{1,0:T(2,128)S(1)}, u32[]{:S(2)}, u32[]{:S(2)}) collective-permute-start(f32[2,64]{1,0:T(2,128)S(1)} %bitcast.11), channel_id=1, source_target_pairs={{0,1},{1,0},{2,3},{3,2},{4,5},{5,4},{6,7},{7,6},{8,9},{9,8},{10,11... | collective-permute-start | bytes 1544 | tf_op jit(solution)/shard_map/ppermute | solution.py:465
  42.3 1.6 %collective-permute-start.15 = (bf16[64,2048]{1,0:T(8,128)(2,1)S(1)}, bf16[64,2048]{1,0:T(8,128)(2,1)S(1)}, u32[]{:S(2)}, u32[]{:S(2)}) collective-permute-start(bf16[64,2048]{1,0:T(8,128)(2,1)S(1)} %get-tuple-element.78.norm_ref), channel_id=1, source_target_pairs={{0,1},{1,0},{2,3},{3,2},{4,5},{5,4},{6,7},{7,6},{8,9},{9,8},{10,11... | collective-permute-start | bytes 786440 | tf_op jit(solution)/shard_map/ppermute | solution.py:569
  44.3 7.4 %collective-permute-start.16 = (bf16[32,2048]{1,0:T(8,128)(2,1)S(1)}, bf16[32,2048]{1,0:T(8,128)(2,1)S(1)}, u32[]{:S(2)}, u32[]{:S(2)}) collective-permute-start(bf16[32,2048]{1,0:T(8,128)(2,1)S(1)} %get-tuple-element.85), channel_id=1, source_target_pairs={{0,0},{1,3},{2,2},{3,1},{4,4},{5,7},{6,6},{7,5},{8,8},{9,11},{10,1... | collective-permute-start | bytes 393224 | tf_op jit(solution)/shard_map/ppermute | solution.py:584
  45.0 10.2 %collective-permute-start.17 = (bf16[32,2048]{1,0:T(8,128)(2,1)S(1)}, bf16[32,2048]{1,0:T(8,128)(2,1)S(1)}, u32[]{:S(2)}, u32[]{:S(2)}) collective-permute-start(bf16[32,2048]{1,0:T(8,128)(2,1)S(1)} %get-tuple-element.86), channel_id=1, source_target_pairs={{0,4},{1,7},{2,6},{3,5},{4,0},{5,3},{6,2},{7,1},{8,12},{9,15},{10,... | collective-permute-start | bytes 393224 | tf_op jit(solution)/shard_map/ppermute | solution.py:584
  46.2 9.1 %collective-permute-start.18 = (bf16[32,2048]{1,0:T(8,128)(2,1)S(1)}, bf16[32,2048]{1,0:T(8,128)(2,1)S(1)}, u32[]{:S(2)}, u32[]{:S(2)}) collective-permute-start(bf16[32,2048]{1,0:T(8,128)(2,1)S(1)} %get-tuple-element.87), channel_id=1, source_target_pairs={{0,8},{1,11},{2,10},{3,9},{4,12},{5,15},{6,14},{7,13},{8,0},{9,3},... | collective-permute-start | bytes 393224 | tf_op jit(solution)/shard_map/ppermute | solution.py:584
  46.2 12.3 %collective-permute-start.19 = (bf16[32,2048]{1,0:T(8,128)(2,1)S(1)}, bf16[32,2048]{1,0:T(8,128)(2,1)S(1)}, u32[]{:S(2)}, u32[]{:S(2)}) collective-permute-start(bf16[32,2048]{1,0:T(8,128)(2,1)S(1)} %get-tuple-element.88), channel_id=1, source_target_pairs={{0,12},{1,15},{2,14},{3,13},{4,8},{5,11},{6,10},{7,9},{8,4},{9,7},... | collective-permute-start | bytes 393224 | tf_op jit(solution)/shard_map/ppermute | solution.py:584
  48.5 15.0 %collective-permute-start.28 = (bf16[32,2048]{1,0:T(8,128)(2,1)S(1)}, bf16[32,2048]{1,0:T(8,128)(2,1)S(1)}, u32[]{:S(2)}, u32[]{:S(2)}) collective-permute-start(bf16[32,2048]{1,0:T(8,128)(2,1)S(1)} %get-tuple-element.104), channel_id=1, source_target_pairs={{0,24},{1,27},{2,26},{3,25},{4,28},{5,31},{6,30},{7,29},{8,16},{9,... | collective-permute-start | bytes 393224 | tf_op jit(solution)/shard_map/ppermute | solution.py:584
  51.8 13.0 %collective-permute-start.29 = (bf16[32,2048]{1,0:T(8,128)(2,1)S(1)}, bf16[32,2048]{1,0:T(8,128)(2,1)S(1)}, u32[]{:S(2)}, u32[]{:S(2)}) collective-permute-start(bf16[32,2048]{1,0:T(8,128)(2,1)S(1)} %get-tuple-element.105), channel_id=1, source_target_pairs={{0,28},{1,31},{2,30},{3,29},{4,24},{5,27},{6,26},{7,25},{8,20},{9,... | collective-permute-start | bytes 393224 | tf_op jit(solution)/shard_map/ppermute | solution.py:584
  55.2 18.7 %collective-permute-start.24 = (bf16[32,2048]{1,0:T(8,128)(2,1)S(1)}, bf16[32,2048]{1,0:T(8,128)(2,1)S(1)}, u32[]{:S(2)}, u32[]{:S(2)}) collective-permute-start(bf16[32,2048]{1,0:T(8,128)(2,1)S(1)} %get-tuple-element.100), channel_id=1, source_target_pairs={{0,16},{1,19},{2,18},{3,17},{4,20},{5,23},{6,22},{7,21},{8,24},{9,... | collective-permute-start | bytes 393224 | tf_op jit(solution)/shard_map/ppermute | solution.py:584
  55.3 19.3 %collective-permute-start.25 = (bf16[32,2048]{1,0:T(8,128)(2,1)S(1)}, bf16[32,2048]{1,0:T(8,128)(2,1)S(1)}, u32[]{:S(2)}, u32[]{:S(2)}) collective-permute-start(bf16[32,2048]{1,0:T(8,128)(2,1)S(1)} %get-tuple-element.101), channel_id=1, source_target_pairs={{0,20},{1,23},{2,22},{3,21},{4,16},{5,19},{6,18},{7,17},{8,28},{9,... | collective-permute-start | bytes 393224 | tf_op jit(solution)/shard_map/ppermute | solution.py:584
  62.7 18.0 %collective-permute-start.20 = (bf16[32,2048]{1,0:T(8,128)(2,1)S(1)}, bf16[32,2048]{1,0:T(8,128)(2,1)S(1)}, u32[]{:S(2)}, u32[]{:S(2)}) collective-permute-start(bf16[32,2048]{1,0:T(8,128)(2,1)S(1)} %get-tuple-element.95), channel_id=1, source_target_pairs={{0,0},{1,3},{2,2},{3,1},{4,4},{5,7},{6,6},{7,5},{8,8},{9,11},{10,1... | collective-permute-start | bytes 393224 | tf_op jit(solution)/shard_map/ppermute | solution.py:584
  63.5 20.0 %collective-permute-start.21 = (bf16[32,2048]{1,0:T(8,128)(2,1)S(1)}, bf16[32,2048]{1,0:T(8,128)(2,1)S(1)}, u32[]{:S(2)}, u32[]{:S(2)}) collective-permute-start(bf16[32,2048]{1,0:T(8,128)(2,1)S(1)} %get-tuple-element.96), channel_id=1, source_target_pairs={{0,4},{1,7},{2,6},{3,5},{4,0},{5,3},{6,2},{7,1},{8,12},{9,15},{10,... | collective-permute-start | bytes 393224 | tf_op jit(solution)/shard_map/ppermute | solution.py:584
  64.7 19.1 %collective-permute-start.22 = (bf16[32,2048]{1,0:T(8,128)(2,1)S(1)}, bf16[32,2048]{1,0:T(8,128)(2,1)S(1)}, u32[]{:S(2)}, u32[]{:S(2)}) collective-permute-start(bf16[32,2048]{1,0:T(8,128)(2,1)S(1)} %get-tuple-element.97), channel_id=1, source_target_pairs={{0,8},{1,11},{2,10},{3,9},{4,12},{5,15},{6,14},{7,13},{8,0},{9,3},... | collective-permute-start | bytes 393224 | tf_op jit(solution)/shard_map/ppermute | solution.py:584
  73.9 12.9 %collective-permute-start.23 = (bf16[32,2048]{1,0:T(8,128)(2,1)S(1)}, bf16[32,2048]{1,0:T(8,128)(2,1)S(1)}, u32[]{:S(2)}, u32[]{:S(2)}) collective-permute-start(bf16[32,2048]{1,0:T(8,128)(2,1)S(1)} %get-tuple-element.98), channel_id=1, source_target_pairs={{0,12},{1,15},{2,14},{3,13},{4,8},{5,11},{6,10},{7,9},{8,4},{9,7},... | collective-permute-start | bytes 393224 | tf_op jit(solution)/shard_map/ppermute | solution.py:584
  74.6 12.8 %collective-permute-start.30 = (bf16[32,2048]{1,0:T(8,128)(2,1)S(1)}, bf16[32,2048]{1,0:T(8,128)(2,1)S(1)}, u32[]{:S(2)}, u32[]{:S(2)}) collective-permute-start(bf16[32,2048]{1,0:T(8,128)(2,1)S(1)} %get-tuple-element.106), channel_id=1, source_target_pairs={{0,24},{1,27},{2,26},{3,25},{4,28},{5,31},{6,30},{7,29},{8,16},{9,... | collective-permute-start | bytes 393224 | tf_op jit(solution)/shard_map/ppermute | solution.py:584
  80.6 7.8 %collective-permute-start.31 = (bf16[32,2048]{1,0:T(8,128)(2,1)S(1)}, bf16[32,2048]{1,0:T(8,128)(2,1)S(1)}, u32[]{:S(2)}, u32[]{:S(2)}) collective-permute-start(bf16[32,2048]{1,0:T(8,128)(2,1)S(1)} %get-tuple-element.107), channel_id=1, source_target_pairs={{0,28},{1,31},{2,30},{3,29},{4,24},{5,27},{6,26},{7,25},{8,20},{9,... | collective-permute-start | bytes 393224 | tf_op jit(solution)/shard_map/ppermute | solution.py:584
  83.5 14.5 %collective-permute-start.26 = (bf16[32,2048]{1,0:T(8,128)(2,1)S(1)}, bf16[32,2048]{1,0:T(8,128)(2,1)S(1)}, u32[]{:S(2)}, u32[]{:S(2)}) collective-permute-start(bf16[32,2048]{1,0:T(8,128)(2,1)S(1)} %get-tuple-element.102), channel_id=1, source_target_pairs={{0,16},{1,19},{2,18},{3,17},{4,20},{5,23},{6,22},{7,21},{8,24},{9,... | collective-permute-start | bytes 393224 | tf_op jit(solution)/shard_map/ppermute | solution.py:584
  83.8 17.4 %collective-permute-start.27 = (bf16[32,2048]{1,0:T(8,128)(2,1)S(1)}, bf16[32,2048]{1,0:T(8,128)(2,1)S(1)}, u32[]{:S(2)}, u32[]{:S(2)}) collective-permute-start(bf16[32,2048]{1,0:T(8,128)(2,1)S(1)} %get-tuple-element.103), channel_id=1, source_target_pairs={{0,20},{1,23},{2,22},{3,21},{4,16},{5,19},{6,18},{7,17},{8,28},{9,... | collective-permute-start | bytes 393224 | tf_op jit(solution)/shard_map/ppermute | solution.py:584
  101.6 2.5 %collective-permute-start.32 = (bf16[64,2048]{1,0:T(8,128)(2,1)S(1)}, bf16[64,2048]{1,0:T(8,128)(2,1)S(1)}, u32[]{:S(2)}, u32[]{:S(2)}) collective-permute-start(bf16[64,2048]{1,0:T(8,128)(2,1)S(1)} %shard_map.152), channel_id=1, source_target_pairs={{0,1},{1,0},{2,3},{3,2},{4,5},{5,4},{6,7},{7,6},{8,9},{9,8},{10,11... | collective-permute-start | bytes 786440 | tf_op jit(solution)/shard_map/ppermute | solution.py:601

commit v8 on v7

--- a/solution.py
+++ b/solution.py
@@ -241,29 +241,22 @@
         outs[k][...] = state_ref[member ^ k]
 
 
-def mixed_rows(out_ref, side, member, intra_ref, qe_ref, gated_ref, states):
-    half = out_ref.shape[0]
+def mix_kernel(place_ref, intra_ref, qe_ref, gated_ref, *refs):
+    states, out_ref = refs[:GROUP], refs[GROUP]
     block = intra_ref.shape[2]
-    at = pl.ds(pl.multiple_of(side * half, half), half)
+    member = member_of(place_ref)
     for k in range(GROUP):
         mixed = []
         for h in range(block // HEAD_DIM):
             lanes = slice(h * HEAD_DIM, (h + 1) * HEAD_DIM)
-            out = intra_ref[k, at, lanes] + dot(qe_ref[k, at, lanes], states[k][lanes], NT)
+            out = intra_ref[k, :, lanes] + dot(qe_ref[k, :, lanes], states[k][lanes], NT)
             scale = lax.rsqrt(jnp.mean(out * out, axis=-1, keepdims=True) + epsilon)
-            mixed.append((out * scale * gated_ref[k, at, lanes]).astype(bf16))
+            mixed.append((out * scale * gated_ref[k, :, lanes]).astype(bf16))
         where = pl.ds(pl.multiple_of((member ^ k) * block, block), block)
         out_ref[:, where] = jnp.concatenate(mixed, axis=1)
 
 
-def send_kernel(place_ref, intra_ref, qe_ref, gated_ref, *refs):
-    mixed_rows(refs[GROUP], 1 - side_of(place_ref), member_of(place_ref), intra_ref, qe_ref, gated_ref, refs[:GROUP])
-
-
-def keep_kernel(place_ref, intra_ref, qe_ref, gated_ref, *refs):
-    states, (w_ref, acc_ref, mix_ref) = refs[:GROUP], refs[GROUP:]
-    side, member = side_of(place_ref), member_of(place_ref)
-    mixed_rows(mix_ref, side, member, intra_ref, qe_ref, gated_ref, states)
+def keep_kernel(mix_ref, w_ref, acc_ref):
     acc_ref[...] = dot(mix_ref[...], w_ref[...])
 
 
@@ -285,13 +278,30 @@
     return slots
 
 
-def project_kernel(recv_ref, acc_ref, w_ref, res_ref, gain_ref, upd_ref, norm_ref):
-    partial = dot(recv_ref[...], w_ref[...])
-    updated = (res_ref[...].astype(f32) + (acc_ref[...] + partial)).astype(bf16)
-    upd_ref[...] = updated
-    updated = updated.astype(f32)
-    scale = lax.rsqrt(jnp.mean(updated * updated, axis=-1, keepdims=True) + epsilon)
-    norm_ref[...] = (updated * scale * gain_ref[...]).astype(bf16)
+def project_kernel(
+    place_ref, recv_ref, acc_ref, w_ref, res_ref, other_res_ref, gain_ref, *refs, count
+):
+    chosen, upd_ref, outs, sum_ref = refs[:count], refs[count], refs[count + 1 : -1], refs[-1]
+    half, _ = upd_ref.shape
+    side = side_of(place_ref)
+    sum_ref[...] = acc_ref[...] + dot(recv_ref[...], w_ref[...])
+
+    def normed_rows(rows_ref, which):
+        at = pl.ds(pl.multiple_of(which * half, half), half)
+        updated = (rows_ref[...].astype(f32) + sum_ref[at]).astype(bf16)
+        wide = updated.astype(f32)
+        scale = lax.rsqrt(jnp.mean(wide * wide, axis=-1, keepdims=True) + epsilon)
+        return updated, (wide * scale * gain_ref[...]).astype(bf16)
+
+    upd_ref[...], own = normed_rows(res_ref, side)
+    if not count:
+        outs[0][...] = own
+    else:
+        _, other = normed_rows(other_res_ref, 1 - side)
+        box = (dot(chosen[0][...], own) + dot(chosen[1][...], other)).astype(bf16)
+        rows = box.shape[0] // len(outs)
+        for i, ref in enumerate(outs):
+            ref[...] = box[i * rows : (i + 1) * rows]
 
 
 def placed_rows(slots, weights, target, valid):
@@ -312,27 +322,19 @@
 
 
 def pair_kernel(
-    place_ref, route_ref, weight_ref, other_route_ref, other_weight_ref, norm_ref,
-    box_ref, chosen_ref, hi_ref, lo_ref, other_hi_ref, other_lo_ref, *, capacity,
+    place_ref, route_ref, weight_ref, other_route_ref, other_weight_ref,
+    chosen_ref, other_chosen_ref, hi_ref, lo_ref, other_hi_ref, other_lo_ref, *, capacity,
 ):
     rank, side = place_ref[0] >> 1, side_of(place_ref)
     row = lax.broadcasted_iota(jnp.int32, hi_ref.shape, 0)
     core = (row // capacity) % 2
     target = (row // (2 * capacity) * 2 + side) * capacity + row % capacity
     slots = slots_of(route_ref[...] ^ rank, capacity)
-    chosen, hi_ref[...], lo_ref[...] = placed_rows(slots, weight_ref[...], target, core == side)
-    box_ref[...] = dot(chosen, norm_ref[...]).astype(bf16)
+    chosen_ref[...], hi_ref[...], lo_ref[...] = placed_rows(slots, weight_ref[...], target, core == side)
     slots = slots_of(other_route_ref[...] ^ rank, capacity)
-    chosen_ref[...], other_hi_ref[...], other_lo_ref[...] = placed_rows(
+    other_chosen_ref[...], other_hi_ref[...], other_lo_ref[...] = placed_rows(
         slots, other_weight_ref[...], target, core != side
     )
-
-
-def pack_kernel(box_ref, chosen_ref, norm_ref, *outs):
-    box = (box_ref[...].astype(f32) + dot(chosen_ref[...], norm_ref[...])).astype(bf16)
-    rows = box.shape[0] // len(outs)
-    for i, ref in enumerate(outs):
-        ref[...] = box[i * rows : (i + 1) * rows]
 
 
 def expert_kernel(*refs):
@@ -463,6 +465,7 @@
     route, weight = routing.T, route_weight.T
     other_route = lax.ppermute(route, "tp", swap)
     other_weight = lax.ppermute(weight, "tp", swap)
+    other_residual = lax.ppermute(residual_in, "tp", swap)
     gated, residual, norm_gain, down_kept = call(
         gate_kernel,
         [SMEM] + [HBM] * 5,
@@ -512,25 +515,33 @@
         bring_kernel, [HBM] * 2, [(KEPT, shape((width, units), bf16))] * 2, [dma((2,))]
     )(*weights[:2])
 
-    mix_args = (place, intra, qe, gated, *priors)
-    mix_specs = [SMEM] + [VMEM] * (3 + GROUP)
-    (send,) = call(send_kernel, mix_specs, [(VMEM, shape((half, channels), bf16))])(*mix_args)
-    recv = lax.ppermute(send, "tp", swap)
-    (partial,) = call(
-        keep_kernel,
-        mix_specs + [KEPT],
-        [(VMEM, shape((half, width), f32))],
-        [pltpu.VMEM((half, channels), bf16)],
-    )(*mix_args, w_own)
-    recv, others, other_route, other_weight = lax.optimization_barrier(
-        (recv, others, other_route, other_weight)
-    )
-    updated, normed = call(
-        project_kernel, [VMEM] * 2 + [KEPT] * 3, [(VMEM, shape((half, width), bf16))] * 2
-    )(recv, partial, w_other, residual, norm_gain)
-    kept = (gate_kept, up_kept, down_kept, *others)
+    direct = capacity % 16 == 0
     box = (VMEM, shape((slots, width), bf16))
     table = (VMEM, shape((slots, half), bf16))
+    tables = []
+    if direct:
+        *tables, hi, lo, other_hi, other_lo = call(
+            functools.partial(pair_kernel, capacity=capacity), [SMEM] + [VMEM] * 4, [table] * 6
+        )(place, route, weight, other_route, other_weight)
+
+    (mixed,) = call(
+        mix_kernel, [SMEM] + [VMEM] * (3 + GROUP), [(VMEM, shape((length, channels), bf16))]
+    )(place, intra, qe, gated, *priors)
+    recv = lax.ppermute(mixed, "tp", swap)
+    (partial,) = call(
+        keep_kernel, [VMEM, KEPT], [(VMEM, shape((length, width), f32))]
+    )(mixed, w_own)
+    recv, others = lax.optimization_barrier((recv, others))
+    blocks = ranks // 2
+    normed = shape((half, width), bf16)
+    block = shape((2 * capacity, width), bf16)
+    updated, *boxes = call(
+        functools.partial(project_kernel, count=len(tables)),
+        [SMEM] + [VMEM] * 2 + [KEPT] * 2 + [VMEM, KEPT] + [VMEM] * len(tables),
+        [(VMEM, normed)] + ([(VMEM, block)] * blocks if direct else [(VMEM, normed)]),
+        [pltpu.VMEM((length, width), f32)],
+    )(place, recv, partial, w_other, residual, other_residual, norm_gain, *tables)
+    kept = (gate_kept, up_kept, down_kept, *others)
 
     def experts(arrays):
         rows = sum(x.shape[0] for x in arrays)
@@ -550,7 +561,7 @@
             [pltpu.VMEM((rows, width), bf16)],
         )(*(x for entry in sums for x in entry), *arrays)
 
-    if capacity % 16:
+    if not direct:
 
         def exchange(x):
             order = jnp.arange(ranks, dtype=jnp.int32) ^ rank
@@ -562,18 +573,9 @@
             functools.partial(own_kernel, capacity=capacity),
             [SMEM] + [VMEM] * 3,
             [box, table, table],
-        )(place, route, weight, normed)
+        )(place, route, weight, *boxes)
         (result,) = experts([exchange(outbox)])
         return combine([(updated, hi, lo)], [exchange(result)], 0, bf16)[0]
-
-    other_normed = lax.ppermute(normed, "tp", swap)
-    own_box, chosen, hi, lo, other_hi, other_lo = call(
-        functools.partial(pair_kernel, capacity=capacity), [SMEM] + [VMEM] * 5, [box] + [table] * 5
-    )(place, route, weight, other_route, other_weight, normed)
-    blocks = ranks // 2
-    boxes = call(
-        pack_kernel, [VMEM] * 3, [(VMEM, shape((2 * capacity, width), bf16))] * blocks
-    )(own_box, chosen, other_normed)
 
     def paired(x, j):
         pairs = [

time: 105 us -> 103 us (0.981)
  waiting for transfers between devices: 25.4 us -> 24.2 us
    pallas_call x18 -> x17, Pallas kernels: 29.3 us -> 28.9 us  [placed(): run(*(pltpu.with_memory_space_constraint(arg, fixed(spec)) if fixed(spec)...]
  transfers between devices with their start and end apart: 33 -> 33, of which waited for: 12 -> 11; matrix products, arithmetic and copies ran while one was open for 0% -> 0% of each run, Pallas kernels for 26% -> 25%
where the time goes in v8:
time: 103 us
  starting transfers between devices  49.7 us (48%)
  Pallas kernels  28.9 us (28%)
  waiting for transfers between devices  24.2 us (23%)
    pallas_call x17, Pallas kernels, placed(): run(*(pltpu.with_memory_space_constraint(arg, fixed(spec)) if fixed(spec)...  28.9 us
    ppermute x16, starting transfers between devices, paired(): return lax.ppermute(x, ('sp', 'tp'), pairs)  26.9 us
    ppermute x9, starting transfers between devices, away(): return lax.ppermute(x, 'sp', [(i, i ^ k) for i in range(ranks)])  19.3 us
    ppermute x16, waiting for transfers between devices, paired(): return lax.ppermute(x, ('sp', 'tp'), pairs)  13.8 us
    ppermute x9, waiting for transfers between devices, away(): return lax.ppermute(x, 'sp', [(i, i ^ k) for i in range(ranks)])  9.27 us
  transfers between devices with their start and end apart: 33, of which 11 were waited for; matrix products, arithmetic and copies ran while one was open for 0% of the time, Pallas kernels for 25%

profile of v8, /device:TPU:0, one launch (start us, length us, event | category | flops | bytes accessed | tf_op | source)
XLA Modules:
  0.0 103.1 jit_solution(14670617360062725980)
XLA Ops:
  0.0 0.5 collective-permute-start.10
  0.5 0.5 collective-permute-start.12
  1.0 2.1 %shard_map.136 = (bf16[272,128]{1,0:T(8,128)(2,1)S(1)}, bf16[272,128]{1,0:T(8,128)(2,1)S(1)}, bf16[272,128]{1,0:T(8,128)(2,1)S(1)}, bf16[272,128]{1,0:T(8,128)(2...) custom-call(s32[1]{0:T(128)} %bitcast.place_ref, bf16[128,1024]{1,0:T(8,128)(2,1)} %f_hbm.1, ...), custom_call_target="tpu_custom_call" | custom-call | tf_op jit(solution)/shard_map/pallas_call | solution.py:407
  3.1 2.5 %collective-permute-start = (bf16[272,128]{1,0:T(8,128)(2,1)S(1)}, bf16[272,128]{1,0:T(8,128)(2,1)S(1)}, u32[]{:S(2)}, u32[]{:S(2)}) collective-permute-start(bf16[272,128]{1,0:T(8,128)(2,1)S(1)} %get-tuple-element.60), channel_id=1, source_target_pairs={{0,2},{2,0},{4,6},{6,4},{8,10},{10,8},{12,14},{14,12},{16,18},{18,... | collective-permute-start | bytes 208904 | tf_op jit(solution)/shard_map/ppermute | solution.py:452
  5.7 1.5 %collective-permute-start.1 = (bf16[272,128]{1,0:T(8,128)(2,1)S(1)}, bf16[272,128]{1,0:T(8,128)(2,1)S(1)}, u32[]{:S(2)}, u32[]{:S(2)}) collective-permute-start(bf16[272,128]{1,0:T(8,128)(2,1)S(1)} %get-tuple-element.61), channel_id=1, source_target_pairs={{0,4},{2,6},{4,0},{6,2},{8,12},{10,14},{12,8},{14,10},{16,20},{18,... | collective-permute-start | bytes 208904 | tf_op jit(solution)/shard_map/ppermute | solution.py:452
  7.2 1.3 %collective-permute-done.refs_1_ = bf16[272,128]{1,0:T(8,128)(2,1)S(1)} collective-permute-done((bf16[272,128]{1,0:T(8,128)(2,1)S(1)}, bf16[272,128]{1,0:T(8,128)(2,1)S(1)}, u32[]{:S(2)}, u32[]{:S(2)}) %collective-permute-start) | collective-permute-done | bytes 69664 | tf_op jit(solution)/shard_map/ppermute | solution.py:452
  8.5 2.7 %collective-permute-start.2 = (bf16[272,128]{1,0:T(8,128)(2,1)S(1)}, bf16[272,128]{1,0:T(8,128)(2,1)S(1)}, u32[]{:S(2)}, u32[]{:S(2)}) collective-permute-start(bf16[272,128]{1,0:T(8,128)(2,1)S(1)} %get-tuple-element.62), channel_id=1, source_target_pairs={{0,6},{2,4},{4,2},{6,0},{8,14},{10,12},{12,10},{14,8},{16,22},{18,... | collective-permute-start | bytes 208904 | tf_op jit(solution)/shard_map/ppermute | solution.py:452
  11.2 2.5 %collective-permute-done.2.refs_3_ = bf16[272,128]{1,0:T(8,128)(2,1)S(1)} collective-permute-done((bf16[272,128]{1,0:T(8,128)(2,1)S(1)}, bf16[272,128]{1,0:T(8,128)(2,1)S(1)}, u32[]{:S(2)}, u32[]{:S(2)}) %collective-permute-start.2) | collective-permute-done | bytes 69664 | tf_op jit(solution)/shard_map/ppermute | solution.py:452
  13.8 1.9 %collective-permute-start.3 = (bf16[272,128]{1,0:T(8,128)(2,1)S(1)}, bf16[272,128]{1,0:T(8,128)(2,1)S(1)}, u32[]{:S(2)}, u32[]{:S(2)}) collective-permute-start(bf16[272,128]{1,0:T(8,128)(2,1)S(1)} %shard_map.139.refs_4_), channel_id=1, source_target_pairs={{0,8},{2,10},{4,12},{6,14},{8,0},{10,2},{12,4},{14,6},{16,24},{18,... | collective-permute-start | bytes 208904 | tf_op jit(solution)/shard_map/ppermute | solution.py:452
  15.7 2.6 %collective-permute-start.4 = (bf16[272,128]{1,0:T(8,128)(2,1)S(1)}, bf16[272,128]{1,0:T(8,128)(2,1)S(1)}, u32[]{:S(2)}, u32[]{:S(2)}) collective-permute-start(bf16[272,128]{1,0:T(8,128)(2,1)S(1)} %shard_map.139.refs_4_), channel_id=1, source_target_pairs={{0,16},{2,18},{4,20},{6,22},{8,24},{10,26},{12,28},{14,30},{16,0},... | collective-permute-start | bytes 208904 | tf_op jit(solution)/shard_map/ppermute | solution.py:452
  18.3 0.5 collective-permute-done.3.refs_5_
  18.8 3.2 %collective-permute-start.5 = (bf16[272,128]{1,0:T(8,128)(2,1)S(1)}, bf16[272,128]{1,0:T(8,128)(2,1)S(1)}, u32[]{:S(2)}, u32[]{:S(2)}) collective-permute-start(bf16[272,128]{1,0:T(8,128)(2,1)S(1)} %shard_map.139.refs_4_), channel_id=1, source_target_pairs={{0,24},{2,26},{4,28},{6,30},{8,16},{10,18},{12,20},{14,22},{16,8},... | collective-permute-start | bytes 208904 | tf_op jit(solution)/shard_map/ppermute | solution.py:452
  22.4 2.6 %collective-permute-done.5.refs_7_ = bf16[272,128]{1,0:T(8,128)(2,1)S(1)} collective-permute-done((bf16[272,128]{1,0:T(8,128)(2,1)S(1)}, bf16[272,128]{1,0:T(8,128)(2,1)S(1)}, u32[]{:S(2)}, u32[]{:S(2)}) %collective-permute-start.5) | collective-permute-done | bytes 69664 | tf_op jit(solution)/shard_map/ppermute | solution.py:452
  25.2 1.6 %collective-permute-start.6 = (bf16[256,128]{1,0:T(8,128)(2,1)S(1)}, bf16[256,128]{1,0:T(8,128)(2,1)S(1)}, u32[]{:S(2)}, u32[]{:S(2)}) collective-permute-start(bf16[256,128]{1,0:T(8,128)(2,1)S(1)} %get-tuple-element.64), channel_id=1, source_target_pairs={{0,2},{2,0},{4,6},{6,4},{8,10},{10,8},{12,14},{14,12},{16,18},{18,... | collective-permute-start | bytes 196616 | tf_op jit(solution)/shard_map/ppermute | solution.py:452
  26.7 1.5 %collective-permute-start.7 = (bf16[256,128]{1,0:T(8,128)(2,1)S(1)}, bf16[256,128]{1,0:T(8,128)(2,1)S(1)}, u32[]{:S(2)}, u32[]{:S(2)}) collective-permute-start(bf16[256,128]{1,0:T(8,128)(2,1)S(1)} %get-tuple-element.65), channel_id=1, source_target_pairs={{0,4},{2,6},{4,0},{6,2},{8,12},{10,14},{12,8},{14,10},{16,20},{18,... | collective-permute-start | bytes 196616 | tf_op jit(solution)/shard_map/ppermute | solution.py:452
  28.2 1.9 %collective-permute-done.6.refs_1_ = bf16[256,128]{1,0:T(8,128)(2,1)S(1)} collective-permute-done((bf16[256,128]{1,0:T(8,128)(2,1)S(1)}, bf16[256,128]{1,0:T(8,128)(2,1)S(1)}, u32[]{:S(2)}, u32[]{:S(2)}) %collective-permute-start.6) | collective-permute-done | bytes 65568 | tf_op jit(solution)/shard_map/ppermute | solution.py:452
  30.1 1.8 %collective-permute-start.8 = (bf16[256,128]{1,0:T(8,128)(2,1)S(1)}, bf16[256,128]{1,0:T(8,128)(2,1)S(1)}, u32[]{:S(2)}, u32[]{:S(2)}) collective-permute-start(bf16[256,128]{1,0:T(8,128)(2,1)S(1)} %get-tuple-element.66), channel_id=1, source_target_pairs={{0,6},{2,4},{4,2},{6,0},{8,14},{10,12},{12,10},{14,8},{16,22},{18,... | collective-permute-start | bytes 196616 | tf_op jit(solution)/shard_map/ppermute | solution.py:452
  32.0 3.9 %shard_map.137 = (f32[4,128,256]{2,1,0:T(8,128)S(1)}, bf16[4,128,256]{2,1,0:T(8,128)(2,1)S(1)}, bf16[1024,2048]{1,0:T(8,128)(2,1)S(1)}, bf16[1024,2048]{1,0:T(8,128)(2,1)S(1)}) custom-call(s32[1]{0:T(128)} %bitcast.place_ref, f32[4,128,256]{2,1,0:T(8,128)S(1)} %get-tuple-element.54.total_ref, f32[4,128,256]{2,1,0:T(8,128)S(1)} %get-tuple-element.55.key_ref, ...), custom_call_target="tpu_custom_call" | custom-call | tf_op jit(solution)/shard_map/pallas_call | solution.py:407
  35.9 2.0 %shard_map.138 = (f32[4,128,256]{2,1,0:T(8,128)S(1)}, bf16[64,2048]{1,0:T(8,128)(2,1)S(1)}, f32[1,2048]{1,0:T(1,128)S(1)}, bf16[512,2048]{1,0:T(8,128)(2,1)S(1)}) custom-call(s32[1]{0:T(128)} %bitcast.place_ref, bf16[128,1024]{1,0:T(8,128)(2,1)} %gate_hbm.1, f32[1,1024]{1,0:T(1,128)} %bitcast.21, bf16[64,2048]{1,0:T(8,128)(2,1)} %res_hbm.1, ...), custom_call_target="tpu_custom_call" | custom-call | tf_op jit(solution)/shard_map/pallas_call | solution.py:407
  38.0 0.5 collective-permute-start.15
  38.5 0.4 shard_map.141.mix_ref
  39.7 0.4 shard_map.143
  40.1 0.7 shard_map.142.acc_ref
  40.9 1.8 %shard_map.144 = (bf16[64,2048]{1,0:T(8,128)(2,1)S(1)}, bf16[32,2048]{1,0:T(8,128)(2,1)S(1)}, bf16[32,2048]{1,0:T(8,128)(2,1)S(1)}, bf16[32,2048]{1,0:T(8,128)(2...) custom-call(s32[1]{0:T(128)} %bitcast.place_ref, ...), custom_call_target="tpu_custom_call" | custom-call | tf_op jit(solution)/shard_map/pallas_call | solution.py:407
  42.7 0.7 collective-permute-start.16
  43.4 1.2 %collective-permute-start.17 = (bf16[32,2048]{1,0:T(8,128)(2,1)S(1)}, bf16[32,2048]{1,0:T(8,128)(2,1)S(1)}, u32[]{:S(2)}, u32[]{:S(2)}) collective-permute-start(bf16[32,2048]{1,0:T(8,128)(2,1)S(1)} %get-tuple-element.80), channel_id=1, source_target_pairs={{0,4},{1,7},{2,6},{3,5},{4,0},{5,3},{6,2},{7,1},{8,12},{9,15},{10,... | collective-permute-start | bytes 393224 | tf_op jit(solution)/shard_map/ppermute | solution.py:586
  44.6 2.3 %collective-permute-start.19 = (bf16[32,2048]{1,0:T(8,128)(2,1)S(1)}, bf16[32,2048]{1,0:T(8,128)(2,1)S(1)}, u32[]{:S(2)}, u32[]{:S(2)}) collective-permute-start(bf16[32,2048]{1,0:T(8,128)(2,1)S(1)} %get-tuple-element.82), channel_id=1, source_target_pairs={{0,12},{1,15},{2,14},{3,13},{4,8},{5,11},{6,10},{7,9},{8,4},{9,7},... | collective-permute-start | bytes 393224 | tf_op jit(solution)/shard_map/ppermute | solution.py:586
  46.9 3.2 %collective-permute-start.28 = (bf16[32,2048]{1,0:T(8,128)(2,1)S(1)}, bf16[32,2048]{1,0:T(8,128)(2,1)S(1)}, u32[]{:S(2)}, u32[]{:S(2)}) collective-permute-start(bf16[32,2048]{1,0:T(8,128)(2,1)S(1)} %get-tuple-element.98), channel_id=1, source_target_pairs={{0,24},{1,27},{2,26},{3,25},{4,28},{5,31},{6,30},{7,29},{8,16},{9,... | collective-permute-start | bytes 393224 | tf_op jit(solution)/shard_map/ppermute | solution.py:586
  50.2 1.2 %collective-permute-start.29 = (bf16[32,2048]{1,0:T(8,128)(2,1)S(1)}, bf16[32,2048]{1,0:T(8,128)(2,1)S(1)}, u32[]{:S(2)}, u32[]{:S(2)}) collective-permute-start(bf16[32,2048]{1,0:T(8,128)(2,1)S(1)} %get-tuple-element.99), channel_id=1, source_target_pairs={{0,28},{1,31},{2,30},{3,29},{4,24},{5,27},{6,26},{7,25},{8,20},{9,... | collective-permute-start | bytes 393224 | tf_op jit(solution)/shard_map/ppermute | solution.py:586
  51.3 2.2 %shard_map.145 = (bf16[2048,512]{1,0:T(8,128)(2,1)S(1)}, bf16[2048,512]{1,0:T(8,128)(2,1)S(1)}) custom-call(bf16[2048,512]{1,0:T(8,128)(2,1)} %bitcast.16, bf16[2048,512]{1,0:T(8,128)(2,1)} %bitcast.18), custom_call_target="tpu_custom_call" | custom-call | tf_op jit(solution)/shard_map/pallas_call | solution.py:407
  53.7 3.2 %collective-permute-start.25 = (bf16[32,2048]{1,0:T(8,128)(2,1)S(1)}, bf16[32,2048]{1,0:T(8,128)(2,1)S(1)}, u32[]{:S(2)}, u32[]{:S(2)}) collective-permute-start(bf16[32,2048]{1,0:T(8,128)(2,1)S(1)} %get-tuple-element.95), channel_id=1, source_target_pairs={{0,20},{1,23},{2,22},{3,21},{4,16},{5,19},{6,18},{7,17},{8,28},{9,... | collective-permute-start | bytes 393224 | tf_op jit(solution)/shard_map/ppermute | solution.py:586
  56.9 4.1 %shard_map.146 = (bf16[32,2048]{1,0:T(8,128)(2,1)S(1)}, bf16[32,2048]{1,0:T(8,128)(2,1)S(1)}, bf16[32,2048]{1,0:T(8,128)(2,1)S(1)}, bf16[32,2048]{1,0:T(8,128)(2,1)S(1)}) custom-call(bf16[32,2048]{1,0:T(8,128)(2,1)S(1)} %collective-permute-done.16.refs_0_, bf16[32,2048]{1,0:T(8,128)(2,1)S(1)} %collective-permute-done.17.refs_1_, ...), custom_call_target="tpu_custom_call" | custom-call | tf_op jit(solution)/shard_map/pallas_call | solution.py:407
  61.1 0.8 collective-permute-start.20
  61.9 1.2 %collective-permute-start.21 = (bf16[32,2048]{1,0:T(8,128)(2,1)S(1)}, bf16[32,2048]{1,0:T(8,128)(2,1)S(1)}, u32[]{:S(2)}, u32[]{:S(2)}) collective-permute-start(bf16[32,2048]{1,0:T(8,128)(2,1)S(1)} %get-tuple-element.90), channel_id=1, source_target_pairs={{0,4},{1,7},{2,6},{3,5},{4,0},{5,3},{6,2},{7,1},{8,12},{9,15},{10,... | collective-permute-start | bytes 393224 | tf_op jit(solution)/shard_map/ppermute | solution.py:586
  63.1 4.6 %collective-permute-start.22 = (bf16[32,2048]{1,0:T(8,128)(2,1)S(1)}, bf16[32,2048]{1,0:T(8,128)(2,1)S(1)}, u32[]{:S(2)}, u32[]{:S(2)}) collective-permute-start(bf16[32,2048]{1,0:T(8,128)(2,1)S(1)} %get-tuple-element.91), channel_id=1, source_target_pairs={{0,8},{1,11},{2,10},{3,9},{4,12},{5,15},{6,14},{7,13},{8,0},{9,3},... | collective-permute-start | bytes 393224 | tf_op jit(solution)/shard_map/ppermute | solution.py:586
  67.8 4.6 %shard_map.149 = (bf16[32,2048]{1,0:T(8,128)(2,1)S(1)}, bf16[32,2048]{1,0:T(8,128)(2,1)S(1)}) custom-call(bf16[32,2048]{1,0:T(8,128)(2,1)S(1)} %collective-permute-done.28.refs_0_, bf16[32,2048]{1,0:T(8,128)(2,1)S(1)} %collective-permute-done.29.refs_1_, bf16[2048,512]{1,0:T(8,128)(2,1)S(1)} %get-tuple-element.83.refs_4_.refs_2_, ...), custom_call_target="tpu_custom_call" | custom-call | tf_op jit(solution)/shard_map/pallas_call | solution.py:407
  72.3 0.6 collective-permute-start.23
  73.0 1.4 %collective-permute-start.30 = (bf16[32,2048]{1,0:T(8,128)(2,1)S(1)}, bf16[32,2048]{1,0:T(8,128)(2,1)S(1)}, u32[]{:S(2)}, u32[]{:S(2)}) collective-permute-start(bf16[32,2048]{1,0:T(8,128)(2,1)S(1)} %get-tuple-element.100), channel_id=1, source_target_pairs={{0,24},{1,27},{2,26},{3,25},{4,28},{5,31},{6,30},{7,29},{8,16},{9,... | collective-permute-start | bytes 393224 | tf_op jit(solution)/shard_map/ppermute | solution.py:586
  74.4 4.6 %shard_map.148 = (bf16[32,2048]{1,0:T(8,128)(2,1)S(1)}, bf16[32,2048]{1,0:T(8,128)(2,1)S(1)}) custom-call(bf16[32,2048]{1,0:T(8,128)(2,1)S(1)} %collective-permute-done.24.refs_0_, bf16[32,2048]{1,0:T(8,128)(2,1)S(1)} %collective-permute-done.25.refs_1_, bf16[2048,512]{1,0:T(8,128)(2,1)S(1)} %get-tuple-element.83.refs_4_.refs_2_, ...), custom_call_target="tpu_custom_call" | custom-call | tf_op jit(solution)/shard_map/pallas_call | solution.py:407
  79.0 3.0 %collective-permute-start.31 = (bf16[32,2048]{1,0:T(8,128)(2,1)S(1)}, bf16[32,2048]{1,0:T(8,128)(2,1)S(1)}, u32[]{:S(2)}, u32[]{:S(2)}) collective-permute-start(bf16[32,2048]{1,0:T(8,128)(2,1)S(1)} %get-tuple-element.101), channel_id=1, source_target_pairs={{0,28},{1,31},{2,30},{3,29},{4,24},{5,27},{6,26},{7,25},{8,20},{9,... | collective-permute-start | bytes 393224 | tf_op jit(solution)/shard_map/ppermute | solution.py:586
  82.1 3.2 %collective-permute-start.27 = (bf16[32,2048]{1,0:T(8,128)(2,1)S(1)}, bf16[32,2048]{1,0:T(8,128)(2,1)S(1)}, u32[]{:S(2)}, u32[]{:S(2)}) collective-permute-start(bf16[32,2048]{1,0:T(8,128)(2,1)S(1)} %get-tuple-element.97), channel_id=1, source_target_pairs={{0,20},{1,23},{2,22},{3,21},{4,16},{5,19},{6,18},{7,17},{8,28},{9,... | collective-permute-start | bytes 393224 | tf_op jit(solution)/shard_map/ppermute | solution.py:586
  85.3 0.5 shard_map.147
  85.8 1.0 collective-permute-done.31.refs_6_
  86.8 9.6 %collective-permute-done.26.refs_3_ = bf16[32,2048]{1,0:T(8,128)(2,1)S(1)} collective-permute-done((bf16[32,2048]{1,0:T(8,128)(2,1)S(1)}, bf16[32,2048]{1,0:T(8,128)(2,1)S(1)}, u32[]{:S(2)}, u32[]{:S(2)}) %collective-permute-start.26) | collective-permute-done | bytes 131104 | tf_op jit(solution)/shard_map/ppermute | solution.py:586
  96.4 3.2 %collective-permute-done.27.refs_4_ = bf16[32,2048]{1,0:T(8,128)(2,1)S(1)} collective-permute-done((bf16[32,2048]{1,0:T(8,128)(2,1)S(1)}, bf16[32,2048]{1,0:T(8,128)(2,1)S(1)}, u32[]{:S(2)}, u32[]{:S(2)}) %collective-permute-start.27) | collective-permute-done | bytes 131104 | tf_op jit(solution)/shard_map/ppermute | solution.py:586
  99.9 1.3 %collective-permute-start.32 = (bf16[64,2048]{1,0:T(8,128)(2,1)S(1)}, bf16[64,2048]{1,0:T(8,128)(2,1)S(1)}, u32[]{:S(2)}, u32[]{:S(2)}) collective-permute-start(bf16[64,2048]{1,0:T(8,128)(2,1)S(1)} %shard_map.151), channel_id=1, source_target_pairs={{0,1},{1,0},{2,3},{3,2},{4,5},{5,4},{6,7},{7,6},{8,9},{9,8},{10,11... | collective-permute-start | bytes 786440 | tf_op jit(solution)/shard_map/ppermute | solution.py:603
  101.5 0.8 collective-permute-done.32.b_ref
  102.4 0.7 shard_map.152
  (42 shorter events, 2.4 us)
Async XLA Ops:
  0.0 40.9 %collective-permute-start.10 = (bf16[2048,512]{1,0:T(8,128)(2,1)}, bf16[2048,512]{1,0:T(8,128)(2,1)S(1)}, u32[]{:S(2)}, u32[]{:S(2)}) collective-permute-start(bf16[2048,512]{1,0:T(8,128)(2,1)} %bitcast.15), channel_id=1, source_target_pairs={{0,1},{1,0},{2,3},{3,2},{4,5},{5,4},{6,7},{7,6},{8,9},{9,8},{10,11... | collective-permute-start | bytes 6291464 | tf_op jit(solution)/shard_map/ppermute | solution.py:464
  0.5 40.4 %collective-permute-start.11 = (bf16[2048,512]{1,0:T(8,128)(2,1)}, bf16[2048,512]{1,0:T(8,128)(2,1)}, u32[]{:S(2)}, u32[]{:S(2)}) collective-permute-start(bf16[2048,512]{1,0:T(8,128)(2,1)} %bitcast.17), channel_id=1, source_target_pairs={{0,1},{1,0},{2,3},{3,2},{4,5},{5,4},{6,7},{7,6},{8,9},{9,8},{10,11... | collective-permute-start | bytes 6291464 | tf_op jit(solution)/shard_map/ppermute | solution.py:464
  0.5 40.4 %collective-permute-start.12 = (bf16[512,2048]{1,0:T(8,128)(2,1)}, bf16[512,2048]{1,0:T(8,128)(2,1)}, u32[]{:S(2)}, u32[]{:S(2)}) collective-permute-start(bf16[512,2048]{1,0:T(8,128)(2,1)} %bitcast.13), channel_id=1, source_target_pairs={{0,1},{1,0},{2,3},{3,2},{4,5},{5,4},{6,7},{7,6},{8,9},{9,8},{10,11... | collective-permute-start | bytes 6291464 | tf_op jit(solution)/shard_map/ppermute | solution.py:464
  3.1 5.4 %collective-permute-start = (bf16[272,128]{1,0:T(8,128)(2,1)S(1)}, bf16[272,128]{1,0:T(8,128)(2,1)S(1)}, u32[]{:S(2)}, u32[]{:S(2)}) collective-permute-start(bf16[272,128]{1,0:T(8,128)(2,1)S(1)} %get-tuple-element.60), channel_id=1, source_target_pairs={{0,2},{2,0},{4,6},{6,4},{8,10},{10,8},{12,14},{14,12},{16,18},{18,... | collective-permute-start | bytes 208904 | tf_op jit(solution)/shard_map/ppermute | solution.py:452
  5.7 5.6 %collective-permute-start.1 = (bf16[272,128]{1,0:T(8,128)(2,1)S(1)}, bf16[272,128]{1,0:T(8,128)(2,1)S(1)}, u32[]{:S(2)}, u32[]{:S(2)}) collective-permute-start(bf16[272,128]{1,0:T(8,128)(2,1)S(1)} %get-tuple-element.61), channel_id=1, source_target_pairs={{0,4},{2,6},{4,0},{6,2},{8,12},{10,14},{12,8},{14,10},{16,20},{18,... | collective-permute-start | bytes 208904 | tf_op jit(solution)/shard_map/ppermute | solution.py:452
  8.5 5.2 %collective-permute-start.2 = (bf16[272,128]{1,0:T(8,128)(2,1)S(1)}, bf16[272,128]{1,0:T(8,128)(2,1)S(1)}, u32[]{:S(2)}, u32[]{:S(2)}) collective-permute-start(bf16[272,128]{1,0:T(8,128)(2,1)S(1)} %get-tuple-element.62), channel_id=1, source_target_pairs={{0,6},{2,4},{4,2},{6,0},{8,14},{10,12},{12,10},{14,8},{16,22},{18,... | collective-permute-start | bytes 208904 | tf_op jit(solution)/shard_map/ppermute | solution.py:452
  13.8 5.0 %collective-permute-start.3 = (bf16[272,128]{1,0:T(8,128)(2,1)S(1)}, bf16[272,128]{1,0:T(8,128)(2,1)S(1)}, u32[]{:S(2)}, u32[]{:S(2)}) collective-permute-start(bf16[272,128]{1,0:T(8,128)(2,1)S(1)} %shard_map.139.refs_4_), channel_id=1, source_target_pairs={{0,8},{2,10},{4,12},{6,14},{8,0},{10,2},{12,4},{14,6},{16,24},{18,... | collective-permute-start | bytes 208904 | tf_op jit(solution)/shard_map/ppermute | solution.py:452
  15.7 6.7 %collective-permute-start.4 = (bf16[272,128]{1,0:T(8,128)(2,1)S(1)}, bf16[272,128]{1,0:T(8,128)(2,1)S(1)}, u32[]{:S(2)}, u32[]{:S(2)}) collective-permute-start(bf16[272,128]{1,0:T(8,128)(2,1)S(1)} %shard_map.139.refs_4_), channel_id=1, source_target_pairs={{0,16},{2,18},{4,20},{6,22},{8,24},{10,26},{12,28},{14,30},{16,0},... | collective-permute-start | bytes 208904 | tf_op jit(solution)/shard_map/ppermute | solution.py:452
  18.8 6.2 %collective-permute-start.5 = (bf16[272,128]{1,0:T(8,128)(2,1)S(1)}, bf16[272,128]{1,0:T(8,128)(2,1)S(1)}, u32[]{:S(2)}, u32[]{:S(2)}) collective-permute-start(bf16[272,128]{1,0:T(8,128)(2,1)S(1)} %shard_map.139.refs_4_), channel_id=1, source_target_pairs={{0,24},{2,26},{4,28},{6,30},{8,16},{10,18},{12,20},{14,22},{16,8},... | collective-permute-start | bytes 208904 | tf_op jit(solution)/shard_map/ppermute | solution.py:452
  25.2 5.0 %collective-permute-start.6 = (bf16[256,128]{1,0:T(8,128)(2,1)S(1)}, bf16[256,128]{1,0:T(8,128)(2,1)S(1)}, u32[]{:S(2)}, u32[]{:S(2)}) collective-permute-start(bf16[256,128]{1,0:T(8,128)(2,1)S(1)} %get-tuple-element.64), channel_id=1, source_target_pairs={{0,2},{2,0},{4,6},{6,4},{8,10},{10,8},{12,14},{14,12},{16,18},{18,... | collective-permute-start | bytes 196616 | tf_op jit(solution)/shard_map/ppermute | solution.py:452
  26.7 9.1 %collective-permute-start.7 = (bf16[256,128]{1,0:T(8,128)(2,1)S(1)}, bf16[256,128]{1,0:T(8,128)(2,1)S(1)}, u32[]{:S(2)}, u32[]{:S(2)}) collective-permute-start(bf16[256,128]{1,0:T(8,128)(2,1)S(1)} %get-tuple-element.65), channel_id=1, source_target_pairs={{0,4},{2,6},{4,0},{6,2},{8,12},{10,14},{12,8},{14,10},{16,20},{18,... | collective-permute-start | bytes 196616 | tf_op jit(solution)/shard_map/ppermute | solution.py:452
  30.1 7.8 %collective-permute-start.8 = (bf16[256,128]{1,0:T(8,128)(2,1)S(1)}, bf16[256,128]{1,0:T(8,128)(2,1)S(1)}, u32[]{:S(2)}, u32[]{:S(2)}) collective-permute-start(bf16[256,128]{1,0:T(8,128)(2,1)S(1)} %get-tuple-element.66), channel_id=1, source_target_pairs={{0,6},{2,4},{4,2},{6,0},{8,14},{10,12},{12,10},{14,8},{16,22},{18,... | collective-permute-start | bytes 196616 | tf_op jit(solution)/shard_map/ppermute | solution.py:452
  32.0 3.9 %copy-start = (s32[64,2]{0,1:T(2,128)S(1)}, s32[64,2]{0,1:T(2,128)}, u32[]{:S(2)}) copy-start(s32[64,2]{0,1:T(2,128)} %param.23) | copy-start | bytes 1540
  35.8 2.2 %copy-start.1 = (f32[64,2]{0,1:T(2,128)S(1)}, f32[64,2]{0,1:T(2,128)}, u32[]{:S(2)}) copy-start(f32[64,2]{0,1:T(2,128)} %param.24) | copy-start | bytes 1540
  35.8 3.1 %collective-permute-start.14 = (s32[2,64]{1,0:T(2,128)S(1)}, s32[2,64]{1,0:T(2,128)S(1)}, u32[]{:S(2)}, u32[]{:S(2)}) collective-permute-start(s32[2,64]{1,0:T(2,128)S(1)} %bitcast.9), channel_id=1, source_target_pairs={{0,1},{1,0},{2,3},{3,2},{4,5},{5,4},{6,7},{7,6},{8,9},{9,8},{10,11... | collective-permute-start | bytes 1544 | tf_op jit(solution)/shard_map/ppermute | solution.py:466
  35.9 3.4 %copy-start.2 = (bf16[64,2048]{1,0:T(8,128)(2,1)S(1)}, bf16[64,2048]{1,0:T(8,128)(2,1)}, u32[]{:S(2)}) copy-start(bf16[64,2048]{1,0:T(8,128)(2,1)} %res_hbm.1) | copy-start | bytes 786436
  38.0 1.4 %collective-permute-start.15 = (f32[2,64]{1,0:T(2,128)S(1)}, f32[2,64]{1,0:T(2,128)S(1)}, u32[]{:S(2)}, u32[]{:S(2)}) collective-permute-start(f32[2,64]{1,0:T(2,128)S(1)} %bitcast.11), channel_id=1, source_target_pairs={{0,1},{1,0},{2,3},{3,2},{4,5},{5,4},{6,7},{7,6},{8,9},{9,8},{10,11... | collective-permute-start | bytes 1544 | tf_op jit(solution)/shard_map/ppermute | solution.py:467
  39.0 1.9 %collective-permute-start.9 = (bf16[128,1024]{1,0:T(8,128)(2,1)S(1)}, bf16[128,1024]{1,0:T(8,128)(2,1)S(1)}, u32[]{:S(2)}, u32[]{:S(2)}) collective-permute-start(bf16[128,1024]{1,0:T(8,128)(2,1)S(1)} %shard_map.141.mix_ref), channel_id=1, source_target_pairs={{0,1},{1,0},{2,3},{3,2},{4,5},{5,4},{6,7},{7,6},{8,9},{9,8},{10,11... | collective-permute-start | bytes 786440 | tf_op jit(solution)/shard_map/ppermute | solution.py:530
  39.4 1.6 %collective-permute-start.13 = (bf16[64,2048]{1,0:T(8,128)(2,1)S(1)}, bf16[64,2048]{1,0:T(8,128)(2,1)S(1)}, u32[]{:S(2)}, u32[]{:S(2)}) collective-permute-start(bf16[64,2048]{1,0:T(8,128)(2,1)S(1)} %copy-done.2), channel_id=1, source_target_pairs={{0,1},{1,0},{2,3},{3,2},{4,5},{5,4},{6,7},{7,6},{8,9},{9,8},{10,11... | collective-permute-start | bytes 786440 | tf_op jit(solution)/shard_map/ppermute | solution.py:468
  42.7 7.5 %collective-permute-start.16 = (bf16[32,2048]{1,0:T(8,128)(2,1)S(1)}, bf16[32,2048]{1,0:T(8,128)(2,1)S(1)}, u32[]{:S(2)}, u32[]{:S(2)}) collective-permute-start(bf16[32,2048]{1,0:T(8,128)(2,1)S(1)} %get-tuple-element.79), channel_id=1, source_target_pairs={{0,0},{1,3},{2,2},{3,1},{4,4},{5,7},{6,6},{7,5},{8,8},{9,11},{10,1... | collective-permute-start | bytes 393224 | tf_op jit(solution)/shard_map/ppermute | solution.py:586
  43.4 10.2 %collective-permute-start.17 = (bf16[32,2048]{1,0:T(8,128)(2,1)S(1)}, bf16[32,2048]{1,0:T(8,128)(2,1)S(1)}, u32[]{:S(2)}, u32[]{:S(2)}) collective-permute-start(bf16[32,2048]{1,0:T(8,128)(2,1)S(1)} %get-tuple-element.80), channel_id=1, source_target_pairs={{0,4},{1,7},{2,6},{3,5},{4,0},{5,3},{6,2},{7,1},{8,12},{9,15},{10,... | collective-permute-start | bytes 393224 | tf_op jit(solution)/shard_map/ppermute | solution.py:586
  44.6 9.1 %collective-permute-start.18 = (bf16[32,2048]{1,0:T(8,128)(2,1)S(1)}, bf16[32,2048]{1,0:T(8,128)(2,1)S(1)}, u32[]{:S(2)}, u32[]{:S(2)}) collective-permute-start(bf16[32,2048]{1,0:T(8,128)(2,1)S(1)} %get-tuple-element.81), channel_id=1, source_target_pairs={{0,8},{1,11},{2,10},{3,9},{4,12},{5,15},{6,14},{7,13},{8,0},{9,3},... | collective-permute-start | bytes 393224 | tf_op jit(solution)/shard_map/ppermute | solution.py:586
  44.6 12.3 %collective-permute-start.19 = (bf16[32,2048]{1,0:T(8,128)(2,1)S(1)}, bf16[32,2048]{1,0:T(8,128)(2,1)S(1)}, u32[]{:S(2)}, u32[]{:S(2)}) collective-permute-start(bf16[32,2048]{1,0:T(8,128)(2,1)S(1)} %get-tuple-element.82), channel_id=1, source_target_pairs={{0,12},{1,15},{2,14},{3,13},{4,8},{5,11},{6,10},{7,9},{8,4},{9,7},... | collective-permute-start | bytes 393224 | tf_op jit(solution)/shard_map/ppermute | solution.py:586
  46.9 15.0 %collective-permute-start.28 = (bf16[32,2048]{1,0:T(8,128)(2,1)S(1)}, bf16[32,2048]{1,0:T(8,128)(2,1)S(1)}, u32[]{:S(2)}, u32[]{:S(2)}) collective-permute-start(bf16[32,2048]{1,0:T(8,128)(2,1)S(1)} %get-tuple-element.98), channel_id=1, source_target_pairs={{0,24},{1,27},{2,26},{3,25},{4,28},{5,31},{6,30},{7,29},{8,16},{9,... | collective-permute-start | bytes 393224 | tf_op jit(solution)/shard_map/ppermute | solution.py:586
  50.2 13.0 %collective-permute-start.29 = (bf16[32,2048]{1,0:T(8,128)(2,1)S(1)}, bf16[32,2048]{1,0:T(8,128)(2,1)S(1)}, u32[]{:S(2)}, u32[]{:S(2)}) collective-permute-start(bf16[32,2048]{1,0:T(8,128)(2,1)S(1)} %get-tuple-element.99), channel_id=1, source_target_pairs={{0,28},{1,31},{2,30},{3,29},{4,24},{5,27},{6,26},{7,25},{8,20},{9,... | collective-permute-start | bytes 393224 | tf_op jit(solution)/shard_map/ppermute | solution.py:586
  53.6 18.7 %collective-permute-start.24 = (bf16[32,2048]{1,0:T(8,128)(2,1)S(1)}, bf16[32,2048]{1,0:T(8,128)(2,1)S(1)}, u32[]{:S(2)}, u32[]{:S(2)}) collective-permute-start(bf16[32,2048]{1,0:T(8,128)(2,1)S(1)} %get-tuple-element.94), channel_id=1, source_target_pairs={{0,16},{1,19},{2,18},{3,17},{4,20},{5,23},{6,22},{7,21},{8,24},{9,... | collective-permute-start | bytes 393224 | tf_op jit(solution)/shard_map/ppermute | solution.py:586
  53.7 19.3 %collective-permute-start.25 = (bf16[32,2048]{1,0:T(8,128)(2,1)S(1)}, bf16[32,2048]{1,0:T(8,128)(2,1)S(1)}, u32[]{:S(2)}, u32[]{:S(2)}) collective-permute-start(bf16[32,2048]{1,0:T(8,128)(2,1)S(1)} %get-tuple-element.95), channel_id=1, source_target_pairs={{0,20},{1,23},{2,22},{3,21},{4,16},{5,19},{6,18},{7,17},{8,28},{9,... | collective-permute-start | bytes 393224 | tf_op jit(solution)/shard_map/ppermute | solution.py:586
  61.1 17.9 %collective-permute-start.20 = (bf16[32,2048]{1,0:T(8,128)(2,1)S(1)}, bf16[32,2048]{1,0:T(8,128)(2,1)S(1)}, u32[]{:S(2)}, u32[]{:S(2)}) collective-permute-start(bf16[32,2048]{1,0:T(8,128)(2,1)S(1)} %get-tuple-element.89), channel_id=1, source_target_pairs={{0,0},{1,3},{2,2},{3,1},{4,4},{5,7},{6,6},{7,5},{8,8},{9,11},{10,1... | collective-permute-start | bytes 393224 | tf_op jit(solution)/shard_map/ppermute | solution.py:586
  61.9 20.0 %collective-permute-start.21 = (bf16[32,2048]{1,0:T(8,128)(2,1)S(1)}, bf16[32,2048]{1,0:T(8,128)(2,1)S(1)}, u32[]{:S(2)}, u32[]{:S(2)}) collective-permute-start(bf16[32,2048]{1,0:T(8,128)(2,1)S(1)} %get-tuple-element.90), channel_id=1, source_target_pairs={{0,4},{1,7},{2,6},{3,5},{4,0},{5,3},{6,2},{7,1},{8,12},{9,15},{10,... | collective-permute-start | bytes 393224 | tf_op jit(solution)/shard_map/ppermute | solution.py:586
  63.1 19.0 %collective-permute-start.22 = (bf16[32,2048]{1,0:T(8,128)(2,1)S(1)}, bf16[32,2048]{1,0:T(8,128)(2,1)S(1)}, u32[]{:S(2)}, u32[]{:S(2)}) collective-permute-start(bf16[32,2048]{1,0:T(8,128)(2,1)S(1)} %get-tuple-element.91), channel_id=1, source_target_pairs={{0,8},{1,11},{2,10},{3,9},{4,12},{5,15},{6,14},{7,13},{8,0},{9,3},... | collective-permute-start | bytes 393224 | tf_op jit(solution)/shard_map/ppermute | solution.py:586
  72.3 12.9 %collective-permute-start.23 = (bf16[32,2048]{1,0:T(8,128)(2,1)S(1)}, bf16[32,2048]{1,0:T(8,128)(2,1)S(1)}, u32[]{:S(2)}, u32[]{:S(2)}) collective-permute-start(bf16[32,2048]{1,0:T(8,128)(2,1)S(1)} %get-tuple-element.92), channel_id=1, source_target_pairs={{0,12},{1,15},{2,14},{3,13},{4,8},{5,11},{6,10},{7,9},{8,4},{9,7},... | collective-permute-start | bytes 393224 | tf_op jit(solution)/shard_map/ppermute | solution.py:586
  73.0 12.8 %collective-permute-start.30 = (bf16[32,2048]{1,0:T(8,128)(2,1)S(1)}, bf16[32,2048]{1,0:T(8,128)(2,1)S(1)}, u32[]{:S(2)}, u32[]{:S(2)}) collective-permute-start(bf16[32,2048]{1,0:T(8,128)(2,1)S(1)} %get-tuple-element.100), channel_id=1, source_target_pairs={{0,24},{1,27},{2,26},{3,25},{4,28},{5,31},{6,30},{7,29},{8,16},{9,... | collective-permute-start | bytes 393224 | tf_op jit(solution)/shard_map/ppermute | solution.py:586
  79.0 7.8 %collective-permute-start.31 = (bf16[32,2048]{1,0:T(8,128)(2,1)S(1)}, bf16[32,2048]{1,0:T(8,128)(2,1)S(1)}, u32[]{:S(2)}, u32[]{:S(2)}) collective-permute-start(bf16[32,2048]{1,0:T(8,128)(2,1)S(1)} %get-tuple-element.101), channel_id=1, source_target_pairs={{0,28},{1,31},{2,30},{3,29},{4,24},{5,27},{6,26},{7,25},{8,20},{9,... | collective-permute-start | bytes 393224 | tf_op jit(solution)/shard_map/ppermute | solution.py:586
  82.0 14.4 %collective-permute-start.26 = (bf16[32,2048]{1,0:T(8,128)(2,1)S(1)}, bf16[32,2048]{1,0:T(8,128)(2,1)S(1)}, u32[]{:S(2)}, u32[]{:S(2)}) collective-permute-start(bf16[32,2048]{1,0:T(8,128)(2,1)S(1)} %get-tuple-element.96), channel_id=1, source_target_pairs={{0,16},{1,19},{2,18},{3,17},{4,20},{5,23},{6,22},{7,21},{8,24},{9,... | collective-permute-start | bytes 393224 | tf_op jit(solution)/shard_map/ppermute | solution.py:586
  82.1 17.4 %collective-permute-start.27 = (bf16[32,2048]{1,0:T(8,128)(2,1)S(1)}, bf16[32,2048]{1,0:T(8,128)(2,1)S(1)}, u32[]{:S(2)}, u32[]{:S(2)}) collective-permute-start(bf16[32,2048]{1,0:T(8,128)(2,1)S(1)} %get-tuple-element.97), channel_id=1, source_target_pairs={{0,20},{1,23},{2,22},{3,21},{4,16},{5,19},{6,18},{7,17},{8,28},{9,... | collective-permute-start | bytes 393224 | tf_op jit(solution)/shard_map/ppermute | solution.py:586
  99.9 2.5 %collective-permute-start.32 = (bf16[64,2048]{1,0:T(8,128)(2,1)S(1)}, bf16[64,2048]{1,0:T(8,128)(2,1)S(1)}, u32[]{:S(2)}, u32[]{:S(2)}) collective-permute-start(bf16[64,2048]{1,0:T(8,128)(2,1)S(1)} %shard_map.151), channel_id=1, source_target_pairs={{0,1},{1,0},{2,3},{3,2},{4,5},{5,4},{6,7},{7,6},{8,9},{9,8},{10,11... | collective-permute-start | bytes 786440 | tf_op jit(solution)/shard_map/ppermute | solution.py:603
